TPU v7x, 256 devices: a whole 4x4x8 slice. The times are simulated.
256 devices in a mesh: fs: 32 (over z, y), rep: 4 (over x), tp: 2 (over core).
Axes of the slice: x: 4, y: 4, z: 8, core: 2. Of those that a mesh axis runs over, the one named last changes fastest.
Arguments:
- first_mix: bfloat16 [98304, 2048], P(('fs', 'rep'), 'tp'), may hold values from -6 to 6
- second_mix: bfloat16 [98304, 2048], P(('fs', 'rep'), 'tp'), may hold values from -6 to 6
- lambda_head: float32 [8], P('tp'), may hold values from 0.3 to 0.8
- head_gain: float32 [256], replicated, may hold values from 0.1 to 1.9
- out_cotangent: bfloat16 [98304, 2048], P(('fs', 'rep')), may hold values from -0.078125 to 0.078125
- basis: bfloat16 [2048, 256], P('tp'), may hold values from -0.125 to 0.125
- weight: float32 [2048, 2048], P('tp', 'fs'), may hold values from -3 to 3
- first_moment: float32 [2048, 256], P('fs', 'tp'), may hold values from -4.5 to 4.5
- second_moment: float32 [2048, 256], P('fs', 'tp'), may hold values from 0.05 to 0.5
Outputs:
- weight_new: float32 [2048, 2048], P('tp', 'fs')
- weight_copy: bfloat16 [2048, 2048], P('tp')
- step_out: float32 [2048, 2048], P('tp', 'fs')
- first_new: float32 [2048, 256], P('fs', 'tp')
- second_new: float32 [2048, 256], P('fs', 'tp')
All inputs are finite; a program needn't handle non-finite values.
Results may differ from a plain program's by a relative error of at most 0.0075.
Values may be sent and summed in bfloat16 or wider, within the bound.
No kernel may reach another device: no remote copies, remote signals or barrier semaphores. Data moves between devices by JAX's collectives and lax.ppermute only.
A program may use at most 64 MiB of HBM per device.

v0:
```python
import jax
import jax.numpy as jnp
from jax import lax
from jax.experimental import pallas as pl
from jax.experimental.pallas import tpu as pltpu
from jax.sharding import Mesh
from jax.sharding import PartitionSpec as P

OUT_SCALE = 0.8
BETA_FIRST = 0.9
BETA_SECOND = 0.95
FS = ("z", "y")
FS_REP = ("z", "y", "x")
SMEM = pl.BlockSpec(memory_space=pltpu.SMEM)
VMEM = pl.BlockSpec(memory_space=pltpu.VMEM)
MIB = 1024 * 1024


def shift(array, axis, hops):
    count = lax.axis_size(axis)
    return lax.ppermute(array, axis, [(i, (i + hops) % count) for i in range(count)])


def swap_cores(array):
    return lax.ppermute(array, "tp", [(0, 1), (1, 0)])


def dot(left, right, left_dim, right_dim):
    return lax.dot_general(
        left, right, (((left_dim,), (right_dim,)), ((), ())), preferred_element_type=jnp.float32
    )


def limit(mib):
    return pltpu.CompilerParams(vmem_limit_bytes=mib * MIB)


def heads_kernel(place_ref, lam_ref, first_ref, second_ref, gain_ref, basis_ref, own_ref, sent_ref):
    width = gain_ref.shape[1]
    gain = gain_ref[...] * OUT_SCALE
    total = None
    for head in range(first_ref.shape[1] // width):
        cols = slice(head * width, (head + 1) * width)
        mixture = first_ref[:, cols].astype(jnp.float32) - lam_ref[head] * second_ref[:, cols].astype(jnp.float32)
        inverse = lax.rsqrt(jnp.mean(mixture * mixture, axis=-1, keepdims=True) + 1e-06)
        normed = (mixture * inverse * gain).astype(jnp.bfloat16)
        term = jnp.dot(normed, basis_ref[cols, :], preferred_element_type=jnp.float32)
        total = term if total is None else total + term
    half = total.shape[1] // 2
    low, high = total[:, :half], total[:, half:]
    is_low = place_ref[3] == 0
    own_ref[...] = jnp.where(is_low, low, high)
    sent_ref[...] = jnp.where(is_low, high, low).astype(jnp.bfloat16)


def heads(place, lambda_head, first_mix, second_mix, head_gain, basis):
    tokens, values = first_mix.shape
    rank = basis.shape[1]
    tile = 256
    return pl.pallas_call(
        heads_kernel,
        grid=(tokens // tile,),
        in_specs=[
            SMEM,
            SMEM,
            pl.BlockSpec((tile, values), lambda i: (i, 0)),
            pl.BlockSpec((tile, values), lambda i: (i, 0)),
            pl.BlockSpec((1, head_gain.shape[0]), lambda i: (0, 0)),
            pl.BlockSpec((values, rank), lambda i: (0, 0)),
        ],
        out_specs=[pl.BlockSpec((tile, rank // 2), lambda i: (i, 0))] * 2,
        out_shape=[
            jax.ShapeDtypeStruct((tokens, rank // 2), jnp.float32),
            jax.ShapeDtypeStruct((tokens, rank // 2), jnp.bfloat16),
        ],
        compiler_params=limit(16),
        name="heads",
    )(place, lambda_head, first_mix, second_mix, head_gain[None, :], basis)


def widen_kernel(place_ref, own_ref, one_ref, two_ref, three_ref, out_ref, slots):
    y = place_ref[1]
    slots[y] = own_ref[...].astype(jnp.float32)
    slots[(y + 3) % 4] = one_ref[...].astype(jnp.float32)
    slots[(y + 2) % 4] = two_ref[...].astype(jnp.float32)
    slots[(y + 1) % 4] = three_ref[...].astype(jnp.float32)
    rows = slots.shape[0] * slots.shape[1]
    out_ref[...] = slots[...].reshape(rows, slots.shape[2]).T.astype(jnp.bfloat16)


def widen(place, blocks):
    rows, cols = blocks[0].shape
    return pl.pallas_call(
        widen_kernel,
        in_specs=[SMEM] + [VMEM] * 4,
        out_specs=VMEM,
        out_shape=jax.ShapeDtypeStruct((cols, 4 * rows), jnp.bfloat16),
        scratch_shapes=[pltpu.VMEM((4, rows, cols), jnp.float32)],
        compiler_params=limit(8),
        name="widen",
    )(place, *blocks)


def gradient_kernel(place_ref, own_ref, far_ref, cot_ref, out0, out1, out2, out3, parts):
    x = place_ref[2]
    reduced = (own_ref[...] + far_ref[...].astype(jnp.float32)).T.astype(jnp.bfloat16)
    wide = 512
    for at in range(cot_ref.shape[1] // wide):
        block = dot(reduced, cot_ref[:, at * wide : (at + 1) * wide], 1, 0).T.astype(jnp.bfloat16)
        parts[at * 8 : (at + 1) * 8] = block.reshape(8, 4, 16, block.shape[1])
    for hops, out in enumerate((out0, out1, out2, out3)):
        out[...] = parts[:, (x + hops) % 4]


def gradient(place, own, far, cot):
    rank = own.shape[1]
    return pl.pallas_call(
        gradient_kernel,
        in_specs=[SMEM] + [VMEM] * 3,
        out_specs=[VMEM] * 4,
        out_shape=[jax.ShapeDtypeStruct((32, 16, rank), jnp.bfloat16)] * 4,
        scratch_shapes=[pltpu.VMEM((32, 4, 16, rank), jnp.bfloat16)],
        compiler_params=limit(16),
        name="gradient",
    )(place, own, far, cot)


def moments(projected, first, second):
    first_new = BETA_FIRST * first + (1.0 - BETA_FIRST) * projected
    second_new = BETA_SECOND * second + (1.0 - BETA_SECOND) * projected * projected
    return first_new, second_new


def update_kernel(place_ref, pieces_ref, first_ref, second_ref, piece_ref, copies_ref):
    rows = pl.ds(pl.multiple_of(place_ref[2] * 16, 16), 16)
    piece = jnp.sum(pieces_ref[...].astype(jnp.float32), axis=0)
    piece_ref[...] = piece
    first_new, second_new = moments(piece, first_ref[rows, :], second_ref[rows, :])
    direction = (first_new / (jnp.sqrt(second_new) + 1e-08)).astype(jnp.bfloat16)
    copies_ref[...] = jnp.broadcast_to(direction[None], copies_ref.shape)


def update(place, pieces, first, second):
    return pl.pallas_call(
        update_kernel,
        in_specs=[SMEM] + [VMEM] * 3,
        out_specs=[VMEM] * 2,
        out_shape=[
            jax.ShapeDtypeStruct(pieces.shape[1:], jnp.float32),
            jax.ShapeDtypeStruct(pieces.shape, jnp.bfloat16),
        ],
        compiler_params=limit(4),
        name="update",
    )(place, pieces, first, second)


def finish_kernel(
    place_ref, basis_ref, weight_ref, first_ref, second_ref,
    p0, p1, p2, p3, n0, n1, n2, n3, m0, m1, m2, m3,
    w0, f1, f2, f3, b1, b2, b3, h1, h2,
    new_ref, step_ref, copy_ref, first_out, second_out,
    rows_ref, tiles, sems,
):
    z, y, x = place_ref[0], place_ref[1], place_ref[2]
    is_low = place_ref[3] == 0
    energy = jnp.float32(0.0)
    for hops, (piece, near_ref, far_ref) in enumerate(
        ((p0, n0, m0), (p1, n1, m1), (p2, n2, m2), (p3, n3, m3))
    ):
        source = (x + 4 - hops) % 4
        rows = pl.ds(pl.multiple_of(source * 16, 16), 16)
        first_new, second_new = moments(piece[...], first_ref[rows, :], second_ref[rows, :])
        first_out[rows, :] = first_new
        second_out[rows, :] = second_new
        near, far = near_ref[...], far_ref[...]
        rank = near.shape[2]
        rows_ref[:, source, :, :rank] = jnp.where(is_low, near, far)
        rows_ref[:, source, :, rank:] = jnp.where(is_low, far, near)
        wide_near, wide_far = near.astype(jnp.float32), far.astype(jnp.float32)
        energy += jnp.sum(wide_near * wide_near + wide_far * wide_far)
    count = rows_ref.shape[0] * rows_ref.shape[1] * rows_ref.shape[2] * rows_ref.shape[3]
    spread = jnp.sqrt(jnp.full((1, 128), energy / count, jnp.float32))
    scale = (-1.0 / (spread + 1e-06))[:, :1]
    basis = basis_ref[...]

    step = dot(rows_ref[z * 4 + y].reshape(64, basis.shape[1]), basis, 1, 1) * scale
    step_ref[...] = step
    new_ref[...] = weight_ref[...] + step
    copies = []
    for k, block in enumerate((w0, f1, f2, f3, b3, b2, b1, None)):
        at = (z + 8 - (k if k < 4 else k + 1 if block is not None else 4)) % 8
        part = rows_ref[pl.ds(at * 4, 4)].reshape(256, basis.shape[1])
        wide = dot(basis, part, 1, 1) * scale
        if block is None:
            lead = wide.shape[0] // 2
            tiles[k, :lead] = (h1[...].astype(jnp.float32) + wide[:lead]).astype(jnp.bfloat16)
            tiles[k, lead:] = (h2[...].astype(jnp.float32) + wide[lead:]).astype(jnp.bfloat16)
        else:
            tiles[k] = (block[...].astype(jnp.float32) + wide).astype(jnp.bfloat16)
        copy = pltpu.make_async_copy(
            tiles.at[k], copy_ref.at[:, pl.ds(pl.multiple_of(at * 256, 256), 256)], sems.at[k]
        )
        copy.start()
        copies.append(copy)
    for copy in copies:
        copy.wait()


def finish(place, basis, weight, first, second, pieces, near, far, blocks):
    values, rank = basis.shape
    like = lambda array: jax.ShapeDtypeStruct(array.shape, jnp.float32)
    return pl.pallas_call(
        finish_kernel,
        in_specs=[SMEM] + [VMEM] * (4 + 12 + len(blocks)),
        out_specs=[VMEM, VMEM, pl.BlockSpec(memory_space=pl.ANY), VMEM, VMEM],
        out_shape=[
            like(weight),
            like(weight),
            jax.ShapeDtypeStruct((values, 2048), jnp.bfloat16),
            like(first),
            like(second),
        ],
        scratch_shapes=[
            pltpu.VMEM((32, 4, 16, rank), jnp.bfloat16),
            pltpu.VMEM((8, values, 256), jnp.bfloat16),
            pltpu.SemaphoreType.DMA((8,)),
        ],
        compiler_params=limit(24),
        name="finish",
    )(place, basis, weight, first, second, *pieces, *near, *far, *blocks)


def to_all(array):
    return lax.all_to_all(array, FS, 0, 0, tiled=True)


def chain(first_mix, second_mix, lambda_head, head_gain, out_cotangent, basis, weight, first_moment, second_moment):
    place = jnp.stack([lax.axis_index(name).astype(jnp.int32) for name in ("z", "y", "x", "tp")])
    turned = weight.T
    lead = turned.shape[1] // 2

    narrow = turned.astype(jnp.bfloat16)
    w0 = widen(place, [narrow] + [shift(narrow, "y", hops) for hops in (1, 2, 3)])
    f1, b1 = shift(w0, "z", 1), shift(w0, "z", -1)
    f2, b2 = shift(f1, "z", 1), shift(b1, "z", -1)
    f3, b3 = shift(f2, "z", 1), shift(b2, "z", -1)
    h1, h2 = shift(f3[:lead], "z", 1), shift(b3[lead:], "z", -1)

    own, sent = heads(place, lambda_head, first_mix, second_mix, head_gain, basis)
    parts = gradient(place, own, swap_cores(sent), out_cotangent)
    arrived = [shift(parts[hops], "x", hops) for hops in (1, 2, 3)]
    summed = parts[0].astype(jnp.float32)
    for part in arrived:
        summed = summed + part.astype(jnp.float32)
    summed = summed.astype(jnp.bfloat16)
    piece, copies = update(place, to_all(summed), first_moment, second_moment)
    pieces = [piece] + [shift(piece, "x", hops) for hops in (1, 2, 3)]
    quarter = to_all(copies)
    near = [quarter] + [shift(quarter, "x", hops) for hops in (1, 2, 3)]
    far = [swap_cores(array) for array in near]
    weight_new, step_out, weight_copy, first_new, second_new = finish(
        place, basis, turned, first_moment, second_moment, pieces, near, far, (w0, f1, f2, f3, b1, b2, b3, h1, h2)
    )
    return (weight_new.T, weight_copy, step_out.T, first_new, second_new)


def solution(mesh):
    finer = Mesh(
        mesh.devices.reshape(8, 4, mesh.shape["rep"], mesh.shape["tp"]),
        ("z", "y", "x", "tp"),
    )
    return jax.shard_map(
        chain,
        mesh=finer,
        in_specs=(
            P(FS_REP, "tp"),
            P(FS_REP, "tp"),
            P("tp"),
            P(),
            P(FS_REP, None),
            P("tp", None),
            P("tp", FS),
            P(FS, "tp"),
            P(FS, "tp"),
        ),
        out_specs=(P("tp", FS), P("tp", None), P("tp", FS), P(FS, "tp"), P(FS, "tp")),
        check_vma=False,
    )
```

profile of v0, /device:TPU:1, one launch (start us, length us, event | category | flops | bytes accessed | tf_op | source)
XLA Modules:
  0.0 104.4 jit_solution(5849126466985384083)
XLA Ops:
  0.6 1.1 %bitcast_convert_fusion.own_ref = bf16[64,1024]{1,0:T(8,128)(2,1)S(1)} fusion(f32[1024,64]{0,1:T(8,128)} %param.15), kind=kLoop, calls=%fused_computation.2 | loop fusion | flops 65536 | bytes 393216 | tf_op jit(solution)/shard_map/convert_element_type | solution.py:242
  1.8 3.6 %collective-permute-start.16 = (bf16[64,1024]{1,0:T(8,128)(2,1)S(1)}, bf16[64,1024]{1,0:T(8,128)(2,1)S(1)}, u32[]{:S(2)}, u32[]{:S(2)}) collective-permute-start(bf16[64,1024]{1,0:T(8,128)(2,1)S(1)} %bitcast_convert_fusion.own_ref), channel_id=1, source_target_pairs={{0,24},{8,0},{16,8},{24,16},{1,25},{9,1},{17,9},{25,17},{2,26},{10... | collective-permute-start | bytes 393224 | tf_op jit(solution)/shard_map/ppermute | solution.py:21
  5.4 0.3 collective-permute-start.15
  5.7 0.7 collective-permute-start.14
  6.4 0.1 pad_add_fusion.place_ref
  6.5 2.6 %collective-permute-done.16.three_ref = bf16[64,1024]{1,0:T(8,128)(2,1)S(1)} collective-permute-done((bf16[64,1024]{1,0:T(8,128)(2,1)S(1)}, bf16[64,1024]{1,0:T(8,128)(2,1)S(1)}, u32[]{:S(2)}, u32[]{:S(2)}) %collective-permute-start.16) | collective-permute-done | bytes 131104 | tf_op jit(solution)/shard_map/ppermute | solution.py:21
  9.1 1.7 %collective-permute-done.15.two_ref = bf16[64,1024]{1,0:T(8,128)(2,1)S(1)} collective-permute-done((bf16[64,1024]{1,0:T(8,128)(2,1)S(1)}, bf16[64,1024]{1,0:T(8,128)(2,1)S(1)}, u32[]{:S(2)}, u32[]{:S(2)}) %collective-permute-start.15) | collective-permute-done | bytes 131104 | tf_op jit(solution)/shard_map/ppermute | solution.py:21
  10.8 4.3 %collective-permute-done.14.one_ref = bf16[64,1024]{1,0:T(8,128)(2,1)} collective-permute-done((bf16[64,1024]{1,0:T(8,128)(2,1)S(1)}, bf16[64,1024]{1,0:T(8,128)(2,1)}, u32[]{:S(2)}, u32[]{:S(2)}) %collective-permute-start.14) | collective-permute-done | bytes 131104 | tf_op jit(solution)/shard_map/ppermute | solution.py:21
  15.1 1.2 %widen.1.w0 = bf16[1024,256]{1,0:T(8,128)(2,1)S(1)} custom-call(s32[4]{0:T(128)S(1)} %pad_add_fusion.place_ref, bf16[64,1024]{1,0:T(8,128)(2,1)S(1)} %bitcast_convert_fusion.own_ref, bf16[64,1024]{1,0:T(8,128)(2,1)} %collective-permute-done.14.one_ref, bf16[64,1024]{1,0:T(8,128)(2,1)S(1)} %collective-permute-done.15.two_ref, ...), custom_call_target="tpu_custom_call" | custom-call | tf_op jit(solution)/shard_map/widen/pallas_call | solution.py:93
  16.4 5.7 %collective-permute-start.20 = (bf16[1024,256]{1,0:T(8,128)(2,1)S(1)}, bf16[1024,256]{1,0:T(8,128)(2,1)}, u32[]{:S(2)}, u32[]{:S(2)}) collective-permute-start(bf16[1024,256]{1,0:T(8,128)(2,1)S(1)} %widen.1.w0), channel_id=1, source_target_pairs={{0,224},{32,0},{64,32},{96,64},{128,96},{160,128},{192,160},{224,1... | collective-permute-start | bytes 1572872 | tf_op jit(solution)/shard_map/ppermute | solution.py:21
  22.0 1.0 copy-done.1
  23.1 1.4 %copy-done.5 = bf16[768,1024]{1,0:T(8,128)(2,1)S(1)} copy-done((bf16[768,1024]{1,0:T(8,128)(2,1)S(1)}, bf16[768,1024]{1,0:T(8,128)(2,1)}, u32[]{:S(2)}) %copy-start.5) | copy-done | bytes 1572888
  24.5 1.4 %copy-done.6 = bf16[768,1024]{1,0:T(8,128)(2,1)S(1)} copy-done((bf16[768,1024]{1,0:T(8,128)(2,1)S(1)}, bf16[768,1024]{1,0:T(8,128)(2,1)}, u32[]{:S(2)}) %copy-start.6) | copy-done | bytes 1572888
  25.9 0.7 copy-done.10
  26.5 0.7 copy-done.11
  27.2 2.0 %heads.1 = (f32[768,128]{1,0:T(8,128)S(1)}, bf16[768,128]{1,0:T(8,128)(2,1)S(1)}) custom-call(s32[4]{0:T(128)S(1)} %pad_add_fusion.place_ref, f32[4]{0:T(128)S(1)} %copy-done.11, bf16[768,1024]{1,0:T(8,128)(2,1)S(1)} %copy-done.5, bf16[768,1024]{1,0:T(8,128)(2,1)S(1)} %copy-done.6, f32[1,256]{1,0:T(1,128)S(1)} %bitcast.10, bf16[1024,256]{1,0:T(8,128)(2,1)S(1)} %copy-done.1), custom_call_target="tpu_custom_call" | custom-call | tf_op jit(solution)/shard_map/heads/pallas_call | solution.py:60
  29.2 0.9 collective-permute-start
  30.2 2.5 %collective-permute-done.20.b1 = bf16[1024,256]{1,0:T(8,128)(2,1)} collective-permute-done((bf16[1024,256]{1,0:T(8,128)(2,1)S(1)}, bf16[1024,256]{1,0:T(8,128)(2,1)}, u32[]{:S(2)}, u32[]{:S(2)}) %collective-permute-start.20) | collective-permute-done | bytes 524320 | tf_op jit(solution)/shard_map/ppermute | solution.py:21
  32.7 3.5 %collective-permute-start.21 = (bf16[1024,256]{1,0:T(8,128)(2,1)}, bf16[1024,256]{1,0:T(8,128)(2,1)}, u32[]{:S(2)}, u32[]{:S(2)}) collective-permute-start(bf16[1024,256]{1,0:T(8,128)(2,1)} %collective-permute-done.20.b1), channel_id=1, source_target_pairs={{0,224},{32,0},{64,32},{96,64},{128,96},{160,128},{192,160},{224,1... | collective-permute-start | bytes 1572872 | tf_op jit(solution)/shard_map/ppermute | solution.py:21
  36.2 1.3 %gradient.1 = (bf16[32,16,128]{2,1,0:T(8,128)(2,1)S(1)}, bf16[32,16,128]{2,1,0:T(8,128)(2,1)S(1)}, bf16[32,16,128]{2,1,0:T(8,128)(2,1)S(1)}, bf16[32,16,128]{2,1,0:T(8,128)(2,1)S(1)}) custom-call(s32[4]{0:T(128)S(1)} %pad_add_fusion.place_ref, f32[768,128]{1,0:T(8,128)S(1)} %get-tuple-element.18.own_ref, bf16[768,128]{1,0:T(8,128)(2,1)S(1)} %collective-permute-done.far_ref, ...), custom_call_target="tpu_custom_call" | custom-call | tf_op jit(solution)/shard_map/gradient/pallas_call | solution.py:117
  37.6 1.3 %collective-permute-start.1 = (bf16[32,16,128]{2,1,0:T(8,128)(2,1)S(1)}, bf16[32,16,128]{2,1,0:T(8,128)(2,1)S(1)}, u32[]{:S(2)}, u32[]{:S(2)}) collective-permute-start(bf16[32,16,128]{2,1,0:T(8,128)(2,1)S(1)} %get-tuple-element.21), channel_id=1, source_target_pairs={{0,2},{2,4},{4,6},{6,0},{1,3},{3,5},{5,7},{7,1},{8,10},{10,12},{12... | collective-permute-start | bytes 393224 | tf_op jit(solution)/shard_map/ppermute | solution.py:21
  38.9 2.4 %collective-permute-start.2 = (bf16[32,16,128]{2,1,0:T(8,128)(2,1)S(1)}, bf16[32,16,128]{2,1,0:T(8,128)(2,1)S(1)}, u32[]{:S(2)}, u32[]{:S(2)}) collective-permute-start(bf16[32,16,128]{2,1,0:T(8,128)(2,1)S(1)} %get-tuple-element.22), channel_id=1, source_target_pairs={{0,4},{2,6},{4,0},{6,2},{1,5},{3,7},{5,1},{7,3},{8,12},{10,14},{12... | collective-permute-start | bytes 393224 | tf_op jit(solution)/shard_map/ppermute | solution.py:21
  41.3 1.2 %collective-permute-start.3 = (bf16[32,16,128]{2,1,0:T(8,128)(2,1)S(1)}, bf16[32,16,128]{2,1,0:T(8,128)(2,1)S(1)}, u32[]{:S(2)}, u32[]{:S(2)}) collective-permute-start(bf16[32,16,128]{2,1,0:T(8,128)(2,1)S(1)} %get-tuple-element.23), channel_id=1, source_target_pairs={{0,6},{2,0},{4,2},{6,4},{1,7},{3,1},{5,3},{7,5},{8,14},{10,8},{12,... | collective-permute-start | bytes 393224 | tf_op jit(solution)/shard_map/ppermute | solution.py:21
  42.5 0.6 collective-permute-done.1
  43.1 2.6 %collective-permute-done.2 = bf16[32,16,128]{2,1,0:T(8,128)(2,1)S(1)} collective-permute-done((bf16[32,16,128]{2,1,0:T(8,128)(2,1)S(1)}, bf16[32,16,128]{2,1,0:T(8,128)(2,1)S(1)}, u32[]{:S(2)}, u32[]{:S(2)}) %collective-permute-start.2) | collective-permute-done | bytes 131104 | tf_op jit(solution)/shard_map/ppermute | solution.py:21
  45.7 0.6 collective-permute-done.3
  46.4 0.7 add_convert_fusion
  47.1 4.1 %all-to-all-start = ((bf16[32,16,128]{2,1,0:T(8,128)(2,1)}), bf16[32,16,128]{2,1,0:T(8,128)(2,1)S(1)}, u32[]{:S(2)}, u32[]{:S(2)}) async-start(bf16[32,16,128]{2,1,0:T(8,128)(2,1)} %add_convert_fusion), calls=%async_computation | async-start | bytes 262144 | tf_op jit(solution)/shard_map/all_to_all | solution.py:234
  51.2 2.6 %collective-permute-start.22 = (bf16[1024,256]{1,0:T(8,128)(2,1)}, bf16[1024,256]{1,0:T(8,128)(2,1)S(1)}, u32[]{:S(2)}, u32[]{:S(2)}) collective-permute-start(bf16[1024,256]{1,0:T(8,128)(2,1)} %collective-permute-done.21.b2), channel_id=1, source_target_pairs={{0,224},{32,0},{64,32},{96,64},{128,96},{160,128},{192,160},{224,1... | collective-permute-start | bytes 1572872 | tf_op jit(solution)/shard_map/ppermute | solution.py:21
  53.8 6.7 %all-to-all-done.pieces_ref = bf16[32,16,128]{2,1,0:T(8,128)(2,1)S(1)} async-done(((bf16[32,16,128]{2,1,0:T(8,128)(2,1)}), bf16[32,16,128]{2,1,0:T(8,128)(2,1)S(1)}, u32[]{:S(2)}, u32[]{:S(2)}) %all-to-all-start) | async-done | bytes 131104 | tf_op jit(solution)/shard_map/all_to_all | solution.py:234
  60.5 0.6 update.1
  61.1 13.3 %all_to_all.10.n0 = bf16[32,16,128]{2,1,0:T(8,128)(2,1)S(1)} all-to-all(bf16[32,16,128]{2,1,0:T(8,128)(2,1)S(1)} %get-tuple-element.25), channel_id=1, replica_groups=mesh['z'=8,'y'=4,'x'=4,'tp'=2] {'z','y'}, dimensions={0} | all-to-all | bytes 262144 | tf_op jit(solution)/shard_map/all_to_all | solution.py:234
  74.4 5.3 %collective-permute-start.10 = (bf16[32,16,128]{2,1,0:T(8,128)(2,1)S(1)}, bf16[32,16,128]{2,1,0:T(8,128)(2,1)S(1)}, u32[]{:S(2)}, u32[]{:S(2)}) collective-permute-start(bf16[32,16,128]{2,1,0:T(8,128)(2,1)S(1)} %all_to_all.10.n0), channel_id=1, source_target_pairs={{0,1},{1,0},{2,3},{3,2},{4,5},{5,4},{6,7},{7,6},{8,9},{9,8},{10,11... | collective-permute-start | bytes 393224 | tf_op jit(solution)/shard_map/ppermute | solution.py:25
  79.7 2.4 %collective-permute-start.6 = (f32[16,128]{1,0:T(8,128)S(1)}, f32[16,128]{1,0:T(8,128)S(1)}, u32[]{:S(2)}, u32[]{:S(2)}) collective-permute-start(f32[16,128]{1,0:T(8,128)S(1)} %get-tuple-element.24.p0), channel_id=1, source_target_pairs={{0,6},{2,0},{4,2},{6,4},{1,7},{3,1},{5,3},{7,5},{8,14},{10,8},{12,... | collective-permute-start | bytes 24584 | tf_op jit(solution)/shard_map/ppermute | solution.py:21
  82.0 0.4 collective-permute-start.5
  82.4 0.2 collective-permute-start.4
  82.7 2.5 %collective-permute-start.9 = (bf16[32,16,128]{2,1,0:T(8,128)(2,1)S(1)}, bf16[32,16,128]{2,1,0:T(8,128)(2,1)S(1)}, u32[]{:S(2)}, u32[]{:S(2)}) collective-permute-start(bf16[32,16,128]{2,1,0:T(8,128)(2,1)S(1)} %all_to_all.10.n0), channel_id=1, source_target_pairs={{0,6},{2,0},{4,2},{6,4},{1,7},{3,1},{5,3},{7,5},{8,14},{10,8},{12,... | collective-permute-start | bytes 393224 | tf_op jit(solution)/shard_map/ppermute | solution.py:21
  85.3 1.4 %collective-permute-start.8 = (bf16[32,16,128]{2,1,0:T(8,128)(2,1)S(1)}, bf16[32,16,128]{2,1,0:T(8,128)(2,1)S(1)}, u32[]{:S(2)}, u32[]{:S(2)}) collective-permute-start(bf16[32,16,128]{2,1,0:T(8,128)(2,1)S(1)} %all_to_all.10.n0), channel_id=1, source_target_pairs={{0,4},{2,6},{4,0},{6,2},{1,5},{3,7},{5,1},{7,3},{8,12},{10,14},{12... | collective-permute-start | bytes 393224 | tf_op jit(solution)/shard_map/ppermute | solution.py:21
  86.7 0.5 collective-permute-start.24
  87.2 1.1 %collective-permute-start.23 = (bf16[512,256]{1,0:T(8,128)(2,1)S(1)}, bf16[512,256]{1,0:T(8,128)(2,1)S(1)}, u32[]{:S(2)}, u32[]{:S(2)}) collective-permute-start(bf16[512,256]{1,0:T(8,128)(2,1)S(1)} %slice.8), channel_id=1, source_target_pairs={{0,32},{32,64},{64,96},{96,128},{128,160},{160,192},{192,224},{224... | collective-permute-start | bytes 786440 | tf_op jit(solution)/shard_map/ppermute | solution.py:21
  88.3 3.5 %collective-permute-start.13 = (bf16[32,16,128]{2,1,0:T(8,128)(2,1)S(1)}, bf16[32,16,128]{2,1,0:T(8,128)(2,1)S(1)}, u32[]{:S(2)}, u32[]{:S(2)}) collective-permute-start(bf16[32,16,128]{2,1,0:T(8,128)(2,1)S(1)} %collective-permute-done.9.n3), channel_id=1, source_target_pairs={{0,1},{1,0},{2,3},{3,2},{4,5},{5,4},{6,7},{7,6},{8,9},{9,8},{10,11... | collective-permute-start | bytes 393224 | tf_op jit(solution)/shard_map/ppermute | solution.py:25
  91.8 2.4 %collective-permute-start.12 = (bf16[32,16,128]{2,1,0:T(8,128)(2,1)S(1)}, bf16[32,16,128]{2,1,0:T(8,128)(2,1)S(1)}, u32[]{:S(2)}, u32[]{:S(2)}) collective-permute-start(bf16[32,16,128]{2,1,0:T(8,128)(2,1)S(1)} %collective-permute-done.8.n2), channel_id=1, source_target_pairs={{0,1},{1,0},{2,3},{3,2},{4,5},{5,4},{6,7},{7,6},{8,9},{9,8},{10,11... | collective-permute-start | bytes 393224 | tf_op jit(solution)/shard_map/ppermute | solution.py:25
  94.2 0.2 collective-permute-done.7.n1
  94.3 1.2 %collective-permute-start.11 = (bf16[32,16,128]{2,1,0:T(8,128)(2,1)S(1)}, bf16[32,16,128]{2,1,0:T(8,128)(2,1)S(1)}, u32[]{:S(2)}, u32[]{:S(2)}) collective-permute-start(bf16[32,16,128]{2,1,0:T(8,128)(2,1)S(1)} %collective-permute-done.7.n1), channel_id=1, source_target_pairs={{0,1},{1,0},{2,3},{3,2},{4,5},{5,4},{6,7},{7,6},{8,9},{9,8},{10,11... | collective-permute-start | bytes 393224 | tf_op jit(solution)/shard_map/ppermute | solution.py:25
  95.6 1.0 collective-permute-done.11.m1
  96.6 1.0 copy-done.2
  97.6 1.0 copy-done.4
  98.7 5.5 %finish.1 = (f32[64,1024]{1,0:T(8,128)}, f32[64,1024]{1,0:T(8,128)}, bf16[1024,2048]{1,0:T(8,128)(2,1)}, f32[64,128]{1,0:T(8,128)}, f32[64,128]{1,0:T(8,128)}) custom-call(s32[4]{0:T(128)S(1)} %pad_add_fusion.place_ref, bf16[1024,256]{1,0:T(8,128)(2,1)S(1)} %copy-done.2, f32[64,1024]{1,0:T(8,128)S(1)} %bitcast.9, f32[64,128]{1,0:T(8,128)S(1)} %copy-done.8, ...), custom_call_target="tpu_custom_call" | custom-call | tf_op jit(solution)/shard_map/finish/pallas_call | solution.py:212
  (39 shorter events, 0.1 us)
Async XLA Ops:
  0.6 35.6 %copy-start = (bf16[768,2048]{1,0:T(8,128)(2,1)S(1)}, bf16[768,2048]{1,0:T(8,128)(2,1)}, u32[]{:S(2)}) copy-start(bf16[768,2048]{1,0:T(8,128)(2,1)} %cot_ref.1) | copy-start | bytes 9437188
  1.8 7.3 %collective-permute-start.16 = (bf16[64,1024]{1,0:T(8,128)(2,1)S(1)}, bf16[64,1024]{1,0:T(8,128)(2,1)S(1)}, u32[]{:S(2)}, u32[]{:S(2)}) collective-permute-start(bf16[64,1024]{1,0:T(8,128)(2,1)S(1)} %bitcast_convert_fusion.own_ref), channel_id=1, source_target_pairs={{0,24},{8,0},{16,8},{24,16},{1,25},{9,1},{17,9},{25,17},{2,26},{10... | collective-permute-start | bytes 393224 | tf_op jit(solution)/shard_map/ppermute | solution.py:21
  5.4 5.4 %collective-permute-start.15 = (bf16[64,1024]{1,0:T(8,128)(2,1)S(1)}, bf16[64,1024]{1,0:T(8,128)(2,1)S(1)}, u32[]{:S(2)}, u32[]{:S(2)}) collective-permute-start(bf16[64,1024]{1,0:T(8,128)(2,1)S(1)} %bitcast_convert_fusion.own_ref), channel_id=1, source_target_pairs={{0,16},{8,24},{16,0},{24,8},{1,17},{9,25},{17,1},{25,9},{2,18},{10... | collective-permute-start | bytes 393224 | tf_op jit(solution)/shard_map/ppermute | solution.py:21
  5.7 9.4 %collective-permute-start.14 = (bf16[64,1024]{1,0:T(8,128)(2,1)S(1)}, bf16[64,1024]{1,0:T(8,128)(2,1)}, u32[]{:S(2)}, u32[]{:S(2)}) collective-permute-start(bf16[64,1024]{1,0:T(8,128)(2,1)S(1)} %bitcast_convert_fusion.own_ref), channel_id=1, source_target_pairs={{0,8},{8,16},{16,24},{24,0},{1,9},{9,17},{17,25},{25,1},{2,10},{10... | collective-permute-start | bytes 393224 | tf_op jit(solution)/shard_map/ppermute | solution.py:21
  16.3 21.3 %copy-start.3 = (bf16[1024,256]{1,0:T(8,128)(2,1)}, bf16[1024,256]{1,0:T(8,128)(2,1)S(1)}, u32[]{:S(2)}) copy-start(bf16[1024,256]{1,0:T(8,128)(2,1)S(1)} %widen.1.w0) | copy-start | bytes 1572868
  16.4 16.4 %collective-permute-start.20 = (bf16[1024,256]{1,0:T(8,128)(2,1)S(1)}, bf16[1024,256]{1,0:T(8,128)(2,1)}, u32[]{:S(2)}, u32[]{:S(2)}) collective-permute-start(bf16[1024,256]{1,0:T(8,128)(2,1)S(1)} %widen.1.w0), channel_id=1, source_target_pairs={{0,224},{32,0},{64,32},{96,64},{128,96},{160,128},{192,160},{224,1... | collective-permute-start | bytes 1572872 | tf_op jit(solution)/shard_map/ppermute | solution.py:21
  22.0 14.2 %collective-permute-start.17 = (bf16[1024,256]{1,0:T(8,128)(2,1)S(1)}, bf16[1024,256]{1,0:T(8,128)(2,1)}, u32[]{:S(2)}, u32[]{:S(2)}) collective-permute-start(bf16[1024,256]{1,0:T(8,128)(2,1)S(1)} %widen.1.w0), channel_id=1, source_target_pairs={{0,32},{32,64},{64,96},{96,128},{128,160},{160,192},{192,224},{224... | collective-permute-start | bytes 1572872 | tf_op jit(solution)/shard_map/ppermute | solution.py:21
  22.0 1.0 copy-start.1
  23.0 1.4 %copy-start.5 = (bf16[768,1024]{1,0:T(8,128)(2,1)S(1)}, bf16[768,1024]{1,0:T(8,128)(2,1)}, u32[]{:S(2)}) copy-start(bf16[768,1024]{1,0:T(8,128)(2,1)} %first_ref.3) | copy-start | bytes 4718596
  24.5 1.4 %copy-start.6 = (bf16[768,1024]{1,0:T(8,128)(2,1)S(1)}, bf16[768,1024]{1,0:T(8,128)(2,1)}, u32[]{:S(2)}) copy-start(bf16[768,1024]{1,0:T(8,128)(2,1)} %second_ref.3) | copy-start | bytes 4718596
  25.9 0.7 copy-start.10
  26.5 0.7 copy-start.11
  29.2 31.3 %copy-start.8 = (f32[64,128]{1,0:T(8,128)S(1)}, f32[64,128]{1,0:T(8,128)}, u32[]{:S(2)}) copy-start(f32[64,128]{1,0:T(8,128)} %first_ref.5) | copy-start | bytes 98308
  29.2 31.3 %copy-start.9 = (f32[64,128]{1,0:T(8,128)S(1)}, f32[64,128]{1,0:T(8,128)}, u32[]{:S(2)}) copy-start(f32[64,128]{1,0:T(8,128)} %second_ref.5) | copy-start | bytes 98308
  29.2 67.3 %copy-start.7 = (f32[1024,64]{0,1:T(8,128)S(1)}, f32[1024,64]{0,1:T(8,128)}, u32[]{:S(2)}) copy-start(f32[1024,64]{0,1:T(8,128)} %param.15) | copy-start | bytes 786436
  29.2 7.0 %collective-permute-start = (bf16[768,128]{1,0:T(8,128)(2,1)S(1)}, bf16[768,128]{1,0:T(8,128)(2,1)S(1)}, u32[]{:S(2)}, u32[]{:S(2)}) collective-permute-start(bf16[768,128]{1,0:T(8,128)(2,1)S(1)} %get-tuple-element.19), channel_id=1, source_target_pairs={{0,1},{1,0},{2,3},{3,2},{4,5},{5,4},{6,7},{7,6},{8,9},{9,8},{10,11... | collective-permute-start | bytes 589832 | tf_op jit(solution)/shard_map/ppermute | solution.py:25
  32.7 18.5 %collective-permute-start.21 = (bf16[1024,256]{1,0:T(8,128)(2,1)}, bf16[1024,256]{1,0:T(8,128)(2,1)}, u32[]{:S(2)}, u32[]{:S(2)}) collective-permute-start(bf16[1024,256]{1,0:T(8,128)(2,1)} %collective-permute-done.20.b1), channel_id=1, source_target_pairs={{0,224},{32,0},{64,32},{96,64},{128,96},{160,128},{192,160},{224,1... | collective-permute-start | bytes 1572872 | tf_op jit(solution)/shard_map/ppermute | solution.py:21
  36.2 17.5 %collective-permute-start.18 = (bf16[1024,256]{1,0:T(8,128)(2,1)}, bf16[1024,256]{1,0:T(8,128)(2,1)}, u32[]{:S(2)}, u32[]{:S(2)}) collective-permute-start(bf16[1024,256]{1,0:T(8,128)(2,1)} %collective-permute-done.17.f1), channel_id=1, source_target_pairs={{0,32},{32,64},{64,96},{96,128},{128,160},{160,192},{192,224},{224... | collective-permute-start | bytes 1572872 | tf_op jit(solution)/shard_map/ppermute | solution.py:21
  37.6 5.5 %collective-permute-start.1 = (bf16[32,16,128]{2,1,0:T(8,128)(2,1)S(1)}, bf16[32,16,128]{2,1,0:T(8,128)(2,1)S(1)}, u32[]{:S(2)}, u32[]{:S(2)}) collective-permute-start(bf16[32,16,128]{2,1,0:T(8,128)(2,1)S(1)} %get-tuple-element.21), channel_id=1, source_target_pairs={{0,2},{2,4},{4,6},{6,0},{1,3},{3,5},{5,7},{7,1},{8,10},{10,12},{12... | collective-permute-start | bytes 393224 | tf_op jit(solution)/shard_map/ppermute | solution.py:21
  38.9 6.8 %collective-permute-start.2 = (bf16[32,16,128]{2,1,0:T(8,128)(2,1)S(1)}, bf16[32,16,128]{2,1,0:T(8,128)(2,1)S(1)}, u32[]{:S(2)}, u32[]{:S(2)}) collective-permute-start(bf16[32,16,128]{2,1,0:T(8,128)(2,1)S(1)} %get-tuple-element.22), channel_id=1, source_target_pairs={{0,4},{2,6},{4,0},{6,2},{1,5},{3,7},{5,1},{7,3},{8,12},{10,14},{12... | collective-permute-start | bytes 393224 | tf_op jit(solution)/shard_map/ppermute | solution.py:21
  41.3 5.0 %collective-permute-start.3 = (bf16[32,16,128]{2,1,0:T(8,128)(2,1)S(1)}, bf16[32,16,128]{2,1,0:T(8,128)(2,1)S(1)}, u32[]{:S(2)}, u32[]{:S(2)}) collective-permute-start(bf16[32,16,128]{2,1,0:T(8,128)(2,1)S(1)} %get-tuple-element.23), channel_id=1, source_target_pairs={{0,6},{2,0},{4,2},{6,4},{1,7},{3,1},{5,3},{7,5},{8,14},{10,8},{12,... | collective-permute-start | bytes 393224 | tf_op jit(solution)/shard_map/ppermute | solution.py:21
  47.1 13.4 %all-to-all-start = ((bf16[32,16,128]{2,1,0:T(8,128)(2,1)}), bf16[32,16,128]{2,1,0:T(8,128)(2,1)S(1)}, u32[]{:S(2)}, u32[]{:S(2)}) async-start(bf16[32,16,128]{2,1,0:T(8,128)(2,1)} %add_convert_fusion), calls=%async_computation | async-start | bytes 262144 | tf_op jit(solution)/shard_map/all_to_all | solution.py:234
  51.2 31.3 %collective-permute-start.22 = (bf16[1024,256]{1,0:T(8,128)(2,1)}, bf16[1024,256]{1,0:T(8,128)(2,1)S(1)}, u32[]{:S(2)}, u32[]{:S(2)}) collective-permute-start(bf16[1024,256]{1,0:T(8,128)(2,1)} %collective-permute-done.21.b2), channel_id=1, source_target_pairs={{0,224},{32,0},{64,32},{96,64},{128,96},{160,128},{192,160},{224,1... | collective-permute-start | bytes 1572872 | tf_op jit(solution)/shard_map/ppermute | solution.py:21
  53.8 28.9 %collective-permute-start.19 = (bf16[1024,256]{1,0:T(8,128)(2,1)}, bf16[1024,256]{1,0:T(8,128)(2,1)S(1)}, u32[]{:S(2)}, u32[]{:S(2)}) collective-permute-start(bf16[1024,256]{1,0:T(8,128)(2,1)} %collective-permute-done.18.f2), channel_id=1, source_target_pairs={{0,32},{32,64},{64,96},{96,128},{128,160},{160,192},{192,224},{224... | collective-permute-start | bytes 1572872 | tf_op jit(solution)/shard_map/ppermute | solution.py:21
  74.4 12.8 %collective-permute-start.10 = (bf16[32,16,128]{2,1,0:T(8,128)(2,1)S(1)}, bf16[32,16,128]{2,1,0:T(8,128)(2,1)S(1)}, u32[]{:S(2)}, u32[]{:S(2)}) collective-permute-start(bf16[32,16,128]{2,1,0:T(8,128)(2,1)S(1)} %all_to_all.10.n0), channel_id=1, source_target_pairs={{0,1},{1,0},{2,3},{3,2},{4,5},{5,4},{6,7},{7,6},{8,9},{9,8},{10,11... | collective-permute-start | bytes 393224 | tf_op jit(solution)/shard_map/ppermute | solution.py:25
  79.7 5.6 %collective-permute-start.6 = (f32[16,128]{1,0:T(8,128)S(1)}, f32[16,128]{1,0:T(8,128)S(1)}, u32[]{:S(2)}, u32[]{:S(2)}) collective-permute-start(f32[16,128]{1,0:T(8,128)S(1)} %get-tuple-element.24.p0), channel_id=1, source_target_pairs={{0,6},{2,0},{4,2},{6,4},{1,7},{3,1},{5,3},{7,5},{8,14},{10,8},{12,... | collective-permute-start | bytes 24584 | tf_op jit(solution)/shard_map/ppermute | solution.py:21
  82.0 4.7 %collective-permute-start.5 = (f32[16,128]{1,0:T(8,128)S(1)}, f32[16,128]{1,0:T(8,128)S(1)}, u32[]{:S(2)}, u32[]{:S(2)}) collective-permute-start(f32[16,128]{1,0:T(8,128)S(1)} %get-tuple-element.24.p0), channel_id=1, source_target_pairs={{0,4},{2,6},{4,0},{6,2},{1,5},{3,7},{5,1},{7,3},{8,12},{10,14},{12... | collective-permute-start | bytes 24584 | tf_op jit(solution)/shard_map/ppermute | solution.py:21
  82.4 4.3 %collective-permute-start.4 = (f32[16,128]{1,0:T(8,128)S(1)}, f32[16,128]{1,0:T(8,128)S(1)}, u32[]{:S(2)}, u32[]{:S(2)}) collective-permute-start(f32[16,128]{1,0:T(8,128)S(1)} %get-tuple-element.24.p0), channel_id=1, source_target_pairs={{0,2},{2,4},{4,6},{6,0},{1,3},{3,5},{5,7},{7,1},{8,10},{10,12},{12... | collective-permute-start | bytes 24584 | tf_op jit(solution)/shard_map/ppermute | solution.py:21
  82.7 5.5 %collective-permute-start.9 = (bf16[32,16,128]{2,1,0:T(8,128)(2,1)S(1)}, bf16[32,16,128]{2,1,0:T(8,128)(2,1)S(1)}, u32[]{:S(2)}, u32[]{:S(2)}) collective-permute-start(bf16[32,16,128]{2,1,0:T(8,128)(2,1)S(1)} %all_to_all.10.n0), channel_id=1, source_target_pairs={{0,6},{2,0},{4,2},{6,4},{1,7},{3,1},{5,3},{7,5},{8,14},{10,8},{12,... | collective-permute-start | bytes 393224 | tf_op jit(solution)/shard_map/ppermute | solution.py:21
  85.3 6.5 %collective-permute-start.8 = (bf16[32,16,128]{2,1,0:T(8,128)(2,1)S(1)}, bf16[32,16,128]{2,1,0:T(8,128)(2,1)S(1)}, u32[]{:S(2)}, u32[]{:S(2)}) collective-permute-start(bf16[32,16,128]{2,1,0:T(8,128)(2,1)S(1)} %all_to_all.10.n0), channel_id=1, source_target_pairs={{0,4},{2,6},{4,0},{6,2},{1,5},{3,7},{5,1},{7,3},{8,12},{10,14},{12... | collective-permute-start | bytes 393224 | tf_op jit(solution)/shard_map/ppermute | solution.py:21
  86.7 7.6 %collective-permute-start.7 = (bf16[32,16,128]{2,1,0:T(8,128)(2,1)S(1)}, bf16[32,16,128]{2,1,0:T(8,128)(2,1)S(1)}, u32[]{:S(2)}, u32[]{:S(2)}) collective-permute-start(bf16[32,16,128]{2,1,0:T(8,128)(2,1)S(1)} %all_to_all.10.n0), channel_id=1, source_target_pairs={{0,2},{2,4},{4,6},{6,0},{1,3},{3,5},{5,7},{7,1},{8,10},{10,12},{12... | collective-permute-start | bytes 393224 | tf_op jit(solution)/shard_map/ppermute | solution.py:21
  86.7 9.9 %collective-permute-start.24 = (bf16[512,256]{1,0:T(8,128)(2,1)S(1)}, bf16[512,256]{1,0:T(8,128)(2,1)S(1)}, u32[]{:S(2)}, u32[]{:S(2)}) collective-permute-start(bf16[512,256]{1,0:T(8,128)(2,1)S(1)} %slice.9), channel_id=1, source_target_pairs={{0,224},{32,0},{64,32},{96,64},{128,96},{160,128},{192,160},{224,1... | collective-permute-start | bytes 786440 | tf_op jit(solution)/shard_map/ppermute | solution.py:21
  87.2 9.4 %collective-permute-start.23 = (bf16[512,256]{1,0:T(8,128)(2,1)S(1)}, bf16[512,256]{1,0:T(8,128)(2,1)S(1)}, u32[]{:S(2)}, u32[]{:S(2)}) collective-permute-start(bf16[512,256]{1,0:T(8,128)(2,1)S(1)} %slice.8), channel_id=1, source_target_pairs={{0,32},{32,64},{64,96},{96,128},{128,160},{160,192},{192,224},{224... | collective-permute-start | bytes 786440 | tf_op jit(solution)/shard_map/ppermute | solution.py:21
  88.3 7.3 %collective-permute-start.13 = (bf16[32,16,128]{2,1,0:T(8,128)(2,1)S(1)}, bf16[32,16,128]{2,1,0:T(8,128)(2,1)S(1)}, u32[]{:S(2)}, u32[]{:S(2)}) collective-permute-start(bf16[32,16,128]{2,1,0:T(8,128)(2,1)S(1)} %collective-permute-done.9.n3), channel_id=1, source_target_pairs={{0,1},{1,0},{2,3},{3,2},{4,5},{5,4},{6,7},{7,6},{8,9},{9,8},{10,11... | collective-permute-start | bytes 393224 | tf_op jit(solution)/shard_map/ppermute | solution.py:25
  91.8 3.8 %collective-permute-start.12 = (bf16[32,16,128]{2,1,0:T(8,128)(2,1)S(1)}, bf16[32,16,128]{2,1,0:T(8,128)(2,1)S(1)}, u32[]{:S(2)}, u32[]{:S(2)}) collective-permute-start(bf16[32,16,128]{2,1,0:T(8,128)(2,1)S(1)} %collective-permute-done.8.n2), channel_id=1, source_target_pairs={{0,1},{1,0},{2,3},{3,2},{4,5},{5,4},{6,7},{7,6},{8,9},{9,8},{10,11... | collective-permute-start | bytes 393224 | tf_op jit(solution)/shard_map/ppermute | solution.py:25
  94.3 2.2 %collective-permute-start.11 = (bf16[32,16,128]{2,1,0:T(8,128)(2,1)S(1)}, bf16[32,16,128]{2,1,0:T(8,128)(2,1)S(1)}, u32[]{:S(2)}, u32[]{:S(2)}) collective-permute-start(bf16[32,16,128]{2,1,0:T(8,128)(2,1)S(1)} %collective-permute-done.7.n1), channel_id=1, source_target_pairs={{0,1},{1,0},{2,3},{3,2},{4,5},{5,4},{6,7},{7,6},{8,9},{9,8},{10,11... | collective-permute-start | bytes 393224 | tf_op jit(solution)/shard_map/ppermute | solution.py:25
  96.6 1.0 %copy-start.2 = (bf16[1024,256]{1,0:T(8,128)(2,1)S(1)}, bf16[1024,256]{1,0:T(8,128)(2,1)}, u32[]{:S(2)}) copy-start(bf16[1024,256]{1,0:T(8,128)(2,1)} %basis_ref.3) | copy-start | bytes 1572868
  97.6 1.0 copy-start.4
where the time goes:
time: 105 us; the launch traced here: 104 us
  starting transfers between devices  47.3 us (45%)
  waiting for transfers between devices  23 us (22%)
  blocking collectives  13.3 us (13%)
  Pallas kernels  10.7 us (10%)
  local copies, waits for them, and re-layouts  7.33 us (7%)
  other arithmetic  1.92 us (2%)
    ppermute x20, starting transfers between devices, shift(): lax.ppermute(array, axis, [(i, (i + hops) % count) for i in range(count)])  29.8 us
    ppermute x20, waiting for transfers between devices, shift(): lax.ppermute(array, axis, [(i, (i + hops) % count) for i in range(count)])  15.2 us
    ppermute x5, starting transfers between devices, swap_cores(): return lax.ppermute(array, 'tp', [(0, 1), (1, 0)])  13.4 us
    all_to_all x1, blocking collectives, to_all(): return lax.all_to_all(array, FS, 0, 0, tiled=True)  13.3 us
    unnamed x24, local copies, waits for them, and re-layouts  7.3 us
    all_to_all x1, waiting for transfers between devices, to_all(): return lax.all_to_all(array, FS, 0, 0, tiled=True)  6.75 us
    pallas_call x1, Pallas kernels, finish(): pl.pallas_call(finish_kernel, in_specs=[SMEM] + [VMEM] * (4 + 12 + len(bl...  5.53 us
    all_to_all x1, starting transfers between devices, to_all(): return lax.all_to_all(array, FS, 0, 0, tiled=True)  4.06 us
  transfers between devices with their start and end apart: 26, of which 10 were waited for; matrix products, arithmetic and copies ran while one was open for 1% of the time, Pallas kernels for 4%

commit v1 on v0

v1 whole, which is shorter than its diff:
```python
import jax
import jax.numpy as jnp
from jax import lax
from jax.experimental import pallas as pl
from jax.experimental.pallas import tpu as pltpu
from jax.sharding import Mesh
from jax.sharding import PartitionSpec as P

OUT_SCALE = 0.8
BETA_FIRST = 0.9
BETA_SECOND = 0.95
FS = ("z", "y")
FS_REP = ("z", "y", "x")
SMEM = pl.BlockSpec(memory_space=pltpu.SMEM)
VMEM = pl.BlockSpec(memory_space=pltpu.VMEM)
HBM = pl.BlockSpec(memory_space=pltpu.HBM)
MIB = 1024 * 1024


def in_hbm(*arrays):
    return [pltpu.with_memory_space_constraint(array, pltpu.HBM) for array in arrays]


def in_vmem(*arrays):
    return [pltpu.with_memory_space_constraint(array, pltpu.VMEM) for array in arrays]


def shift(array, axis, hops):
    count = lax.axis_size(axis)
    return lax.ppermute(array, axis, [(i, (i + hops) % count) for i in range(count)])


def swap_cores(array):
    return lax.ppermute(array, "tp", [(0, 1), (1, 0)])


def dot(left, right, left_dim, right_dim):
    return lax.dot_general(
        left, right, (((left_dim,), (right_dim,)), ((), ())), preferred_element_type=jnp.float32
    )


def limit(mib):
    return pltpu.CompilerParams(vmem_limit_bytes=mib * MIB)


def heads_kernel(
    place_ref, lam_hbm, first_hbm, second_hbm, gain_hbm, basis_hbm, weight_hbm,
    own_ref, sent_ref, narrow_ref, first_ref, second_ref, basis_ref, lam_ref, gain_ref, weight_ref, sems,
):
    tokens, values = first_ref.shape
    width = gain_ref.shape[1]
    tile = tokens // 3

    def fetch(source, target, slot):
        copy = pltpu.make_async_copy(source, target, sems.at[slot])
        copy.start()
        return copy

    fixed = [fetch(lam_hbm, lam_ref, 0), fetch(gain_hbm, gain_ref, 1)]
    moving = []
    for step in range(3):
        rows = pl.ds(step * tile, tile)
        moving.append(
            [
                fetch(first_hbm.at[rows], first_ref.at[rows], 4 + 2 * step),
                fetch(second_hbm.at[rows], second_ref.at[rows], 5 + 2 * step),
            ]
        )
        if step == 0:
            fixed.append(fetch(basis_hbm, basis_ref, 2))
    last = fetch(weight_hbm, weight_ref, 3)
    for copy in fixed[:2]:
        copy.wait()
    gain = gain_ref[...] * OUT_SCALE
    is_low = place_ref[3] == 0
    for step in range(3):
        rows = pl.ds(step * tile, tile)
        for copy in moving[step]:
            copy.wait()
        if step == 0:
            fixed[2].wait()
        total = None
        for head in range(values // width):
            cols = slice(head * width, (head + 1) * width)
            first = first_ref[rows, cols].astype(jnp.float32)
            second = second_ref[rows, cols].astype(jnp.float32)
            mixture = first - lam_ref[:, head : head + 1] * second
            inverse = lax.rsqrt(jnp.mean(mixture * mixture, axis=-1, keepdims=True) + 1e-06)
            normed = (mixture * inverse * gain).astype(jnp.bfloat16)
            term = jnp.dot(normed, basis_ref[cols, :], preferred_element_type=jnp.float32)
            total = term if total is None else total + term
        half = total.shape[1] // 2
        low, high = total[:, :half], total[:, half:]
        own_ref[rows, :] = jnp.where(is_low, low, high)
        sent_ref[rows, :] = jnp.where(is_low, high, low).astype(jnp.bfloat16)
    last.wait()
    narrow_ref[...] = weight_ref[...].astype(jnp.bfloat16)


def heads(place, lambda_head, first_mix, second_mix, head_gain, basis, weight):
    tokens, values = first_mix.shape
    half = basis.shape[1] // 2
    lam, gain = lambda_head[None, :], head_gain[None, :]
    return pl.pallas_call(
        heads_kernel,
        in_specs=[SMEM] + [HBM] * 6,
        out_specs=[VMEM] * 3,
        out_shape=[
            jax.ShapeDtypeStruct((tokens, half), jnp.float32),
            jax.ShapeDtypeStruct((tokens, half), jnp.bfloat16),
            jax.ShapeDtypeStruct(weight.shape, jnp.bfloat16),
        ],
        scratch_shapes=[
            pltpu.VMEM((tokens, values), jnp.bfloat16),
            pltpu.VMEM((tokens, values), jnp.bfloat16),
            pltpu.VMEM(basis.shape, jnp.bfloat16),
            pltpu.VMEM(lam.shape, jnp.float32),
            pltpu.VMEM(gain.shape, jnp.float32),
            pltpu.VMEM(weight.shape, jnp.float32),
            pltpu.SemaphoreType.DMA((10,)),
        ],
        compiler_params=limit(12),
        name="heads",
    )(place, *in_hbm(lam, first_mix, second_mix, gain, basis, weight))


def widen_kernel(place_ref, own_ref, one_ref, two_ref, three_ref, out_ref, slots):
    y = place_ref[1]
    slots[y] = own_ref[...].astype(jnp.float32)
    slots[(y + 3) % 4] = one_ref[...].astype(jnp.float32)
    slots[(y + 2) % 4] = two_ref[...].astype(jnp.float32)
    slots[(y + 1) % 4] = three_ref[...].astype(jnp.float32)
    rows = slots.shape[0] * slots.shape[1]
    out_ref[...] = slots[...].reshape(rows, slots.shape[2]).T.astype(jnp.bfloat16)


def widen(place, blocks):
    rows, cols = blocks[0].shape
    return pl.pallas_call(
        widen_kernel,
        in_specs=[SMEM] + [VMEM] * 4,
        out_specs=VMEM,
        out_shape=jax.ShapeDtypeStruct((cols, 4 * rows), jnp.bfloat16),
        scratch_shapes=[pltpu.VMEM((4, rows, cols), jnp.float32)],
        compiler_params=limit(8),
        name="widen",
    )(place, *blocks)


def gradient_kernel(own_ref, far_ref, cot_ref, out_hbm, parts, sems):
    reduced = (own_ref[...] + far_ref[...].astype(jnp.float32)).T.astype(jnp.bfloat16)
    wide = 512
    copies = []
    for at in range(cot_ref.shape[1] // wide):
        block = dot(reduced, cot_ref[:, at * wide : (at + 1) * wide], 1, 0).T.astype(jnp.bfloat16)
        for z in range(2):
            rows = block[z * 256 : (z + 1) * 256]
            parts[:, at * 2 + z] = rows.reshape(16, 16, rows.shape[1])
        pair = pl.ds(at * 2, 2)
        copy = pltpu.make_async_copy(parts.at[:, pair], out_hbm.at[:, pair], sems.at[at])
        copy.start()
        copies.append(copy)
    for copy in copies:
        copy.wait()


def gradient(own, far, cot):
    shape = (16, 8, 16, own.shape[1])
    return pl.pallas_call(
        gradient_kernel,
        in_specs=[VMEM] * 3,
        out_specs=HBM,
        out_shape=pltpu.HBM(shape, jnp.bfloat16),
        scratch_shapes=[pltpu.VMEM(shape, jnp.bfloat16), pltpu.SemaphoreType.DMA((4,))],
        compiler_params=limit(8),
        name="gradient",
    )(own, far, cot)


def fold_kernel(parts_ref, out_hbm, sums, sem):
    sums[...] = jnp.sum(parts_ref[...].astype(jnp.float32), axis=0).astype(jnp.bfloat16)
    copy = pltpu.make_async_copy(sums, out_hbm, sem)
    copy.start()
    copy.wait()


def fold(parts):
    shape = parts.shape[1:]
    return pl.pallas_call(
        fold_kernel,
        in_specs=[VMEM],
        out_specs=HBM,
        out_shape=pltpu.HBM(shape, jnp.bfloat16),
        scratch_shapes=[pltpu.VMEM(shape, jnp.bfloat16), pltpu.SemaphoreType.DMA],
        compiler_params=limit(4),
        name="fold",
    )(parts)


def copy_to_all(source, target, sems):
    copies = []
    for slot in range(target.shape[0]):
        copy = pltpu.make_async_copy(source, target.at[slot], sems.at[slot])
        copy.start()
        copies.append(copy)
    for copy in copies:
        copy.wait()


def copies_of(array, count):
    return pl.pallas_call(
        copy_to_all,
        in_specs=[VMEM],
        out_specs=HBM,
        out_shape=pltpu.HBM((count, *array.shape), array.dtype),
        scratch_shapes=[pltpu.SemaphoreType.DMA((count,))],
        compiler_params=limit(4),
        name="copies",
    )(array)


def moments(projected, first, second):
    first_new = BETA_FIRST * first + (1.0 - BETA_FIRST) * projected
    second_new = BETA_SECOND * second + (1.0 - BETA_SECOND) * projected * projected
    return first_new, second_new


def update_kernel(place_ref, pieces_ref, first_ref, second_ref, piece_ref, copies_hbm, direction_ref, sems):
    rows = pl.ds(pl.multiple_of(place_ref[2] * 16, 16), 16)
    piece = jnp.sum(pieces_ref[...].astype(jnp.float32), axis=0)
    piece_ref[...] = piece
    first_new, second_new = moments(piece, first_ref[rows, :], second_ref[rows, :])
    direction_ref[...] = (first_new / (jnp.sqrt(second_new) + 1e-08)).astype(jnp.bfloat16)
    copy_to_all(direction_ref, copies_hbm, sems)


def update(place, pieces, first, second):
    count, rows, rank = pieces.shape
    return pl.pallas_call(
        update_kernel,
        in_specs=[SMEM] + [VMEM] * 3,
        out_specs=[VMEM, HBM],
        out_shape=[
            jax.ShapeDtypeStruct((rows, rank), jnp.float32),
            pltpu.HBM(pieces.shape, jnp.bfloat16),
        ],
        scratch_shapes=[pltpu.VMEM((rows, rank), jnp.bfloat16), pltpu.SemaphoreType.DMA((count,))],
        compiler_params=limit(4),
        name="update",
    )(place, pieces, first, second)


def finish_kernel(
    place_ref, basis_hbm, weight_hbm, first_hbm, second_hbm, p0, p1, p2, p3, near_ref, far_ref,
    w0, f1, f2, f3, b1, b2, b3, h1, h2,
    new_ref, step_ref, copy_ref, first_out, second_out,
    basis_ref, weight_ref, first_ref, second_ref, tiles, sems,
):
    fetched = []
    for slot, (source, target) in enumerate(
        ((basis_hbm, basis_ref), (weight_hbm, weight_ref), (first_hbm, first_ref), (second_hbm, second_ref))
    ):
        copy = pltpu.make_async_copy(source, target, sems.at[8 + slot])
        copy.start()
        fetched.append(copy)
    z, y, x = place_ref[0], place_ref[1], place_ref[2]
    is_low = place_ref[3] == 0
    near, far = near_ref[...].astype(jnp.float32), far_ref[...].astype(jnp.float32)
    energy = jnp.sum(near * near + far * far)
    count = 2 * near.shape[0] * near.shape[1] * near.shape[2] * near.shape[3]
    spread = jnp.sqrt(jnp.full((1, 128), energy / count, jnp.float32))
    scale = (-1.0 / (spread + 1e-06))[:, :1]
    for copy in fetched:
        copy.wait()
    basis = basis_ref[...]

    def rows_of(close, distant):
        close, distant = (array.reshape(-1, array.shape[-1]) for array in (close, distant))
        return jnp.concatenate(
            [jnp.where(is_low, close, distant), jnp.where(is_low, distant, close)], axis=1
        )

    copies = []
    for k, block in enumerate((w0, f1, f2, f3, b3, b2, b1, None)):
        at = (z + 8 - (k if k < 4 else k + 1 if block is not None else 4)) % 8
        wide = dot(basis, rows_of(near_ref[:, at], far_ref[:, at]), 1, 1) * scale
        if block is None:
            lead = wide.shape[0] // 2
            tiles[k, :lead] = (h1[...].astype(jnp.float32) + wide[:lead]).astype(jnp.bfloat16)
            tiles[k, lead:] = (h2[...].astype(jnp.float32) + wide[lead:]).astype(jnp.bfloat16)
        else:
            tiles[k] = (block[...].astype(jnp.float32) + wide).astype(jnp.bfloat16)
        copy = pltpu.make_async_copy(
            tiles.at[k], copy_ref.at[:, pl.ds(pl.multiple_of(at * 256, 256), 256)], sems.at[k]
        )
        copy.start()
        copies.append(copy)

    mine = pl.ds(y * 4, 4)
    step = dot(rows_of(near_ref[mine, z], far_ref[mine, z]), basis, 1, 1) * scale
    step_ref[...] = step
    new_ref[...] = weight_ref[...] + step
    for hops, piece in enumerate((p0, p1, p2, p3)):
        rows = pl.ds(pl.multiple_of((x + 4 - hops) % 4 * 16, 16), 16)
        first_new, second_new = moments(piece[...], first_ref[rows, :], second_ref[rows, :])
        first_out[rows, :] = first_new
        second_out[rows, :] = second_new
    for copy in copies:
        copy.wait()


def finish(place, basis, weight, first, second, pieces, near, far, blocks):
    values = basis.shape[0]
    like = lambda array: jax.ShapeDtypeStruct(array.shape, jnp.float32)
    return pl.pallas_call(
        finish_kernel,
        in_specs=[SMEM] + [HBM] * 4 + [VMEM] * (6 + len(blocks)),
        out_specs=[VMEM, VMEM, HBM, VMEM, VMEM],
        out_shape=[
            like(weight),
            like(weight),
            pltpu.HBM((values, 2048), jnp.bfloat16),
            like(first),
            like(second),
        ],
        scratch_shapes=[
            pltpu.VMEM(basis.shape, basis.dtype),
            pltpu.VMEM(weight.shape, weight.dtype),
            pltpu.VMEM(first.shape, first.dtype),
            pltpu.VMEM(second.shape, second.dtype),
            pltpu.VMEM((8, values, 256), jnp.bfloat16),
            pltpu.SemaphoreType.DMA((12,)),
        ],
        compiler_params=limit(16),
        name="finish",
    )(place, *in_hbm(basis, weight, first, second), *pieces, near, far, *in_vmem(*blocks))


def exchange(array, axes):
    return lax.all_to_all(array, axes, 0, 0, tiled=True)


def chain(first_mix, second_mix, lambda_head, head_gain, out_cotangent, basis, weight, first_moment, second_moment):
    place = jnp.stack([lax.axis_index(name).astype(jnp.int32) for name in ("z", "y", "x", "tp")])
    turned = weight.T
    own, sent, narrow = heads(place, lambda_head, first_mix, second_mix, head_gain, basis, turned)

    lead = turned.shape[1] // 2
    w0 = widen(place, [narrow] + [shift(narrow, "y", hops) for hops in (1, 2, 3)])
    f1, b1 = shift(w0, "z", 1), shift(w0, "z", -1)
    f2, b2 = shift(f1, "z", 1), shift(b1, "z", -1)
    f3, b3 = shift(f2, "z", 1), shift(b2, "z", -1)
    h1, h2 = shift(f3[:lead], "z", 1), shift(b3[lead:], "z", -1)

    parts = gradient(own, swap_cores(sent), out_cotangent)
    folded = fold(exchange(parts, ("y", "x")))
    piece, copies = update(place, exchange(folded, "z"), first_moment, second_moment)
    pieces = [piece] + [shift(piece, "x", hops) for hops in (1, 2, 3)]
    column = exchange(copies, "z")
    near = exchange(copies_of(column, 16), ("y", "x"))
    far = swap_cores(near)
    weight_new, step_out, weight_copy, first_new, second_new = finish(
        place, basis, turned, first_moment, second_moment, pieces, near, far, (w0, f1, f2, f3, b1, b2, b3, h1, h2)
    )
    return (weight_new.T, weight_copy, step_out.T, first_new, second_new)


def solution(mesh):
    finer = Mesh(
        mesh.devices.reshape(8, 4, mesh.shape["rep"], mesh.shape["tp"]),
        ("z", "y", "x", "tp"),
    )
    return jax.shard_map(
        chain,
        mesh=finer,
        in_specs=(
            P(FS_REP, "tp"),
            P(FS_REP, "tp"),
            P("tp"),
            P(),
            P(FS_REP, None),
            P("tp", None),
            P("tp", FS),
            P(FS, "tp"),
            P(FS, "tp"),
        ),
        out_specs=(P("tp", FS), P("tp", None), P("tp", FS), P(FS, "tp"), P(FS, "tp")),
        check_vma=False,
    )
```

time: 105 us -> 103 us (0.981)
  the two profiles are of different devices: /device:TPU:1 before, /device:TPU:16 now
where the time goes in v1:
time: 103 us; the launch traced here: 102 us
  starting transfers between devices  36.3 us (35%)
  waiting for transfers between devices  25.1 us (24%)
  blocking collectives  23.9 us (23%)
  Pallas kernels  16.1 us (16%)
    all_to_all x2, blocking collectives, exchange(): return lax.all_to_all(array, axes, 0, 0, tiled=True)  23.9 us
    ppermute x14, starting transfers between devices, shift(): lax.ppermute(array, axis, [(i, (i + hops) % count) for i in range(count)])  22.9 us
    ppermute x14, waiting for transfers between devices, shift(): lax.ppermute(array, axis, [(i, (i + hops) % count) for i in range(count)])  13.6 us
    all_to_all x2, starting transfers between devices, exchange(): return lax.all_to_all(array, axes, 0, 0, tiled=True)  13.4 us
    all_to_all x2, waiting for transfers between devices, exchange(): return lax.all_to_all(array, axes, 0, 0, tiled=True)  10.1 us
    pallas_call x1, Pallas kernels, finish(): pl.pallas_call(finish_kernel, in_specs=[SMEM] + [HBM] * 4 + [VMEM] * (6 +...  6.05 us
    pallas_call x1, Pallas kernels, heads(): pl.pallas_call(heads_kernel, in_specs=[SMEM] + [HBM] * 6, out_specs=[VMEM...  4.14 us
  transfers between devices with their start and end apart: 18, of which 11 were waited for; matrix products, arithmetic and copies ran while one was open for 0% of the time, Pallas kernels for 4%

profile of v1, /device:TPU:16, one launch (start us, length us, event | category | flops | bytes accessed | tf_op | source)
XLA Modules:
  0.0 102.5 jit_solution(5506549144181498905)
XLA Ops:
  0.6 0.0 copy-start
  0.6 0.1 pad_add_fusion.place_ref
  0.7 4.1 %heads.1 = (f32[768,128]{1,0:T(8,128)S(1)}, bf16[768,128]{1,0:T(8,128)(2,1)S(1)}, bf16[64,1024]{1,0:T(8,128)(2,1)S(1)}) custom-call(s32[4]{0:T(128)S(1)} %pad_add_fusion.place_ref, f32[1,4]{1,0:T(1,128)} %bitcast.12, bf16[768,1024]{1,0:T(8,128)(2,1)} %first_hbm.2, bf16[768,1024]{1,0:T(8,128)(2,1)} %second_hbm.2, f32[1,256]{1,0:T(1,128)} %bitcast.11, ...), custom_call_target="tpu_custom_call" | custom-call | tf_op jit(solution)/shard_map/heads/pallas_call | solution.py:105
  4.9 0.5 collective-permute-start.7
  5.4 2.9 %collective-permute-start.6 = (bf16[64,1024]{1,0:T(8,128)(2,1)S(1)}, bf16[64,1024]{1,0:T(8,128)(2,1)S(1)}, u32[]{:S(2)}, u32[]{:S(2)}) collective-permute-start(bf16[64,1024]{1,0:T(8,128)(2,1)S(1)} %get-tuple-element.19.own_ref), channel_id=1, source_target_pairs={{0,16},{8,24},{16,0},{24,8},{1,17},{9,25},{17,1},{25,9},{2,18},{10... | collective-permute-start | bytes 393224 | tf_op jit(solution)/shard_map/ppermute | solution.py:30
  8.3 1.3 %collective-permute-start.5 = (bf16[64,1024]{1,0:T(8,128)(2,1)S(1)}, bf16[64,1024]{1,0:T(8,128)(2,1)S(1)}, u32[]{:S(2)}, u32[]{:S(2)}) collective-permute-start(bf16[64,1024]{1,0:T(8,128)(2,1)S(1)} %get-tuple-element.19.own_ref), channel_id=1, source_target_pairs={{0,8},{8,16},{16,24},{24,0},{1,9},{9,17},{17,25},{25,1},{2,10},{10... | collective-permute-start | bytes 393224 | tf_op jit(solution)/shard_map/ppermute | solution.py:30
  9.6 1.7 %collective-permute-done.7.three_ref = bf16[64,1024]{1,0:T(8,128)(2,1)S(1)} collective-permute-done((bf16[64,1024]{1,0:T(8,128)(2,1)S(1)}, bf16[64,1024]{1,0:T(8,128)(2,1)S(1)}, u32[]{:S(2)}, u32[]{:S(2)}) %collective-permute-start.7) | collective-permute-done | bytes 131104 | tf_op jit(solution)/shard_map/ppermute | solution.py:30
  11.3 1.9 %collective-permute-done.6.two_ref = bf16[64,1024]{1,0:T(8,128)(2,1)S(1)} collective-permute-done((bf16[64,1024]{1,0:T(8,128)(2,1)S(1)}, bf16[64,1024]{1,0:T(8,128)(2,1)S(1)}, u32[]{:S(2)}, u32[]{:S(2)}) %collective-permute-start.6) | collective-permute-done | bytes 131104 | tf_op jit(solution)/shard_map/ppermute | solution.py:30
  13.3 1.4 %collective-permute-done.5.one_ref = bf16[64,1024]{1,0:T(8,128)(2,1)S(1)} collective-permute-done((bf16[64,1024]{1,0:T(8,128)(2,1)S(1)}, bf16[64,1024]{1,0:T(8,128)(2,1)S(1)}, u32[]{:S(2)}, u32[]{:S(2)}) %collective-permute-start.5) | collective-permute-done | bytes 131104 | tf_op jit(solution)/shard_map/ppermute | solution.py:30
  14.7 1.6 %widen.1.w0 = bf16[1024,256]{1,0:T(8,128)(2,1)} custom-call(s32[4]{0:T(128)S(1)} %pad_add_fusion.place_ref, bf16[64,1024]{1,0:T(8,128)(2,1)S(1)} %get-tuple-element.19.own_ref, bf16[64,1024]{1,0:T(8,128)(2,1)S(1)} %collective-permute-done.5.one_ref, bf16[64,1024]{1,0:T(8,128)(2,1)S(1)} %collective-permute-done.6.two_ref, ...), custom_call_target="tpu_custom_call" | custom-call | tf_op jit(solution)/shard_map/widen/pallas_call | solution.py:140
  16.3 5.9 %collective-permute-start.11 = (bf16[1024,256]{1,0:T(8,128)(2,1)}, bf16[1024,256]{1,0:T(8,128)(2,1)}, u32[]{:S(2)}, u32[]{:S(2)}) collective-permute-start(bf16[1024,256]{1,0:T(8,128)(2,1)} %widen.1.w0), channel_id=1, source_target_pairs={{0,224},{32,0},{64,32},{96,64},{128,96},{160,128},{192,160},{224,1... | collective-permute-start | bytes 1572872 | tf_op jit(solution)/shard_map/ppermute | solution.py:30
  22.2 0.0 collective-permute-start.8
  22.2 0.0 collective-permute-start
  22.2 1.4 %collective-permute-done.far_ref = bf16[768,128]{1,0:T(8,128)(2,1)S(1)} collective-permute-done((bf16[768,128]{1,0:T(8,128)(2,1)S(1)}, bf16[768,128]{1,0:T(8,128)(2,1)S(1)}, u32[]{:S(2)}, u32[]{:S(2)}) %collective-permute-start) | collective-permute-done | bytes 196640 | tf_op jit(solution)/shard_map/ppermute | solution.py:34
  23.6 1.4 %gradient.1 = bf16[16,8,16,128]{3,2,1,0:T(8,128)(2,1)} custom-call(f32[768,128]{1,0:T(8,128)S(1)} %get-tuple-element.15.own_ref, bf16[768,128]{1,0:T(8,128)(2,1)S(1)} %collective-permute-done.far_ref, bf16[768,2048]{1,0:T(8,128)(2,1)S(1)} %copy-done), custom_call_target="tpu_custom_call" | custom-call | tf_op jit(solution)/shard_map/gradient/pallas_call | solution.py:170
  25.0 7.3 %all-to-all-start = ((bf16[16,8,16,128]{3,2,1,0:T(8,128)(2,1)}), bf16[16,8,16,128]{3,2,1,0:T(8,128)(2,1)S(1)}, u32[]{:S(2)}, u32[]{:S(2)}) async-start(bf16[16,8,16,128]{3,2,1,0:T(8,128)(2,1)} %gradient.1), calls=%async_computation | async-start | bytes 1048576 | tf_op jit(solution)/shard_map/all_to_all | solution.py:341
  32.3 0.9 collective-permute-done.11.b1
  33.2 3.7 %collective-permute-start.12 = (bf16[1024,256]{1,0:T(8,128)(2,1)}, bf16[1024,256]{1,0:T(8,128)(2,1)S(1)}, u32[]{:S(2)}, u32[]{:S(2)}) collective-permute-start(bf16[1024,256]{1,0:T(8,128)(2,1)} %collective-permute-done.11.b1), channel_id=1, source_target_pairs={{0,224},{32,0},{64,32},{96,64},{128,96},{160,128},{192,160},{224,1... | collective-permute-start | bytes 1572872 | tf_op jit(solution)/shard_map/ppermute | solution.py:30
  36.9 0.0 collective-permute-done.8.f1
  36.9 0.0 collective-permute-start.9
  36.9 4.6 %all-to-all-done.parts_ref = bf16[16,8,16,128]{3,2,1,0:T(8,128)(2,1)S(1)} async-done(((bf16[16,8,16,128]{3,2,1,0:T(8,128)(2,1)}), bf16[16,8,16,128]{3,2,1,0:T(8,128)(2,1)S(1)}, u32[]{:S(2)}, u32[]{:S(2)}) %all-to-all-start) | async-done | bytes 524320 | tf_op jit(solution)/shard_map/all_to_all | solution.py:341
  41.6 0.7 fold.1
  42.3 12.7 %all_to_all.20.pieces_ref = bf16[8,16,128]{2,1,0:T(8,128)(2,1)S(1)} all-to-all(bf16[8,16,128]{2,1,0:T(8,128)(2,1)} %fold.1), channel_id=1, replica_groups=mesh['z'=8,'y'=4,'x'=4,'tp'=2] {'z'}, dimensions={0} | all-to-all | bytes 65536 | tf_op jit(solution)/shard_map/all_to_all | solution.py:341
  54.9 0.0 copy-done.1
  54.9 1.3 %update.1 = (f32[16,128]{1,0:T(8,128)S(1)}, bf16[8,16,128]{2,1,0:T(8,128)(2,1)}) custom-call(s32[4]{0:T(128)S(1)} %pad_add_fusion.place_ref, bf16[8,16,128]{2,1,0:T(8,128)(2,1)S(1)} %all_to_all.20.pieces_ref, f32[64,128]{1,0:T(8,128)S(1)} %copy-done.1, f32[64,128]{1,0:T(8,128)S(1)} %copy-done.2), custom_call_target="tpu_custom_call" | custom-call | tf_op jit(solution)/shard_map/update/pallas_call | solution.py:240
  56.2 11.3 %all_to_all.21.source = bf16[8,16,128]{2,1,0:T(8,128)(2,1)S(1)} all-to-all(bf16[8,16,128]{2,1,0:T(8,128)(2,1)} %get-tuple-element.18), channel_id=1, replica_groups=mesh['z'=8,'y'=4,'x'=4,'tp'=2] {'z'}, dimensions={0} | all-to-all | bytes 65536 | tf_op jit(solution)/shard_map/all_to_all | solution.py:341
  67.5 0.9 copies.1
  68.4 6.1 %all-to-all-start.3 = ((bf16[16,8,16,128]{3,2,1,0:T(8,128)(2,1)}), bf16[16,8,16,128]{3,2,1,0:T(8,128)(2,1)S(1)}, u32[]{:S(2)}, u32[]{:S(2)}) async-start(bf16[16,8,16,128]{3,2,1,0:T(8,128)(2,1)} %copies.1), calls=%async_computation.3 | async-start | bytes 1048576 | tf_op jit(solution)/shard_map/all_to_all | solution.py:341
  74.5 0.0 collective-permute-done.12.b2
  74.5 0.5 collective-permute-start.13
  75.0 0.0 collective-permute-done.9.f2
  75.0 1.6 %collective-permute-start.10 = (bf16[1024,256]{1,0:T(8,128)(2,1)S(1)}, bf16[1024,256]{1,0:T(8,128)(2,1)S(1)}, u32[]{:S(2)}, u32[]{:S(2)}) collective-permute-start(bf16[1024,256]{1,0:T(8,128)(2,1)S(1)} %collective-permute-done.9.f2), channel_id=1, source_target_pairs={{0,32},{32,64},{64,96},{96,128},{128,160},{160,192},{192,224},{224... | collective-permute-start | bytes 1572872 | tf_op jit(solution)/shard_map/ppermute | solution.py:30
  76.6 5.4 %all-to-all-done.3.near_ref = bf16[16,8,16,128]{3,2,1,0:T(8,128)(2,1)S(1)} async-done(((bf16[16,8,16,128]{3,2,1,0:T(8,128)(2,1)}), bf16[16,8,16,128]{3,2,1,0:T(8,128)(2,1)S(1)}, u32[]{:S(2)}, u32[]{:S(2)}) %all-to-all-start.3) | async-done | bytes 524320 | tf_op jit(solution)/shard_map/all_to_all | solution.py:341
  82.0 0.0 collective-permute-start.4
  82.0 2.2 %collective-permute-done.13.b3 = bf16[1024,256]{1,0:T(8,128)(2,1)S(1)} collective-permute-done((bf16[1024,256]{1,0:T(8,128)(2,1)S(1)}, bf16[1024,256]{1,0:T(8,128)(2,1)S(1)}, u32[]{:S(2)}, u32[]{:S(2)}) %collective-permute-start.13) | collective-permute-done | bytes 524320 | tf_op jit(solution)/shard_map/ppermute | solution.py:30
  84.3 1.7 %collective-permute-start.15 = (bf16[512,256]{1,0:T(8,128)(2,1)S(1)}, bf16[512,256]{1,0:T(8,128)(2,1)S(1)}, u32[]{:S(2)}, u32[]{:S(2)}) collective-permute-start(bf16[512,256]{1,0:T(8,128)(2,1)S(1)} %slice.9), channel_id=1, source_target_pairs={{0,224},{32,0},{64,32},{96,64},{128,96},{160,128},{192,160},{224,1... | collective-permute-start | bytes 786440 | tf_op jit(solution)/shard_map/ppermute | solution.py:30
  85.9 0.0 collective-permute-done.10.f3
  86.0 0.7 collective-permute-start.14
  86.7 3.1 %collective-permute-start.3 = (f32[16,128]{1,0:T(8,128)S(1)}, f32[16,128]{1,0:T(8,128)S(1)}, u32[]{:S(2)}, u32[]{:S(2)}) collective-permute-start(f32[16,128]{1,0:T(8,128)S(1)} %get-tuple-element.17.p0), channel_id=1, source_target_pairs={{0,6},{2,0},{4,2},{6,4},{1,7},{3,1},{5,3},{7,5},{8,14},{10,8},{12,... | collective-permute-start | bytes 24584 | tf_op jit(solution)/shard_map/ppermute | solution.py:30
  89.8 0.4 collective-permute-start.2
  90.2 0.9 collective-permute-done.3.p3
  91.1 0.6 collective-permute-start.1
  91.8 3.2 %collective-permute-done.2.p2 = f32[16,128]{1,0:T(8,128)S(1)} collective-permute-done((f32[16,128]{1,0:T(8,128)S(1)}, f32[16,128]{1,0:T(8,128)S(1)}, u32[]{:S(2)}, u32[]{:S(2)}) %collective-permute-start.2) | collective-permute-done | bytes 8224 | tf_op jit(solution)/shard_map/ppermute | solution.py:30
  94.9 1.3 %collective-permute-done.1.p1 = f32[16,128]{1,0:T(8,128)S(1)} collective-permute-done((f32[16,128]{1,0:T(8,128)S(1)}, f32[16,128]{1,0:T(8,128)S(1)}, u32[]{:S(2)}, u32[]{:S(2)}) %collective-permute-start.1) | collective-permute-done | bytes 8224 | tf_op jit(solution)/shard_map/ppermute | solution.py:30
  96.3 0.0 collective-permute-done.4.far_ref
  96.3 0.0 collective-permute-done.15.h2
  96.3 0.0 collective-permute-done.14.h1
  96.3 6.1 %finish.1 = (f32[64,1024]{1,0:T(8,128)}, f32[64,1024]{1,0:T(8,128)}, bf16[1024,2048]{1,0:T(8,128)(2,1)}, f32[64,128]{1,0:T(8,128)}, f32[64,128]{1,0:T(8,128)}) custom-call(s32[4]{0:T(128)S(1)} %pad_add_fusion.place_ref, bf16[1024,256]{1,0:T(8,128)(2,1)} %basis_hbm.3, f32[64,1024]{1,0:T(8,128)} %bitcast.10, f32[64,128]{1,0:T(8,128)} %first_hbm.3, ...), custom_call_target="tpu_custom_call" | custom-call | tf_op jit(solution)/shard_map/finish/pallas_call | solution.py:316
  (6 shorter events, 0.0 us)
Async XLA Ops:
  0.6 23.0 %copy-start = (bf16[768,2048]{1,0:T(8,128)(2,1)S(1)}, bf16[768,2048]{1,0:T(8,128)(2,1)}, u32[]{:S(2)}) copy-start(bf16[768,2048]{1,0:T(8,128)(2,1)} %cot_ref.1) | copy-start | bytes 9437188
  4.9 6.4 %collective-permute-start.7 = (bf16[64,1024]{1,0:T(8,128)(2,1)S(1)}, bf16[64,1024]{1,0:T(8,128)(2,1)S(1)}, u32[]{:S(2)}, u32[]{:S(2)}) collective-permute-start(bf16[64,1024]{1,0:T(8,128)(2,1)S(1)} %get-tuple-element.19.own_ref), channel_id=1, source_target_pairs={{0,24},{8,0},{16,8},{24,16},{1,25},{9,1},{17,9},{25,17},{2,26},{10... | collective-permute-start | bytes 393224 | tf_op jit(solution)/shard_map/ppermute | solution.py:30
  5.4 7.9 %collective-permute-start.6 = (bf16[64,1024]{1,0:T(8,128)(2,1)S(1)}, bf16[64,1024]{1,0:T(8,128)(2,1)S(1)}, u32[]{:S(2)}, u32[]{:S(2)}) collective-permute-start(bf16[64,1024]{1,0:T(8,128)(2,1)S(1)} %get-tuple-element.19.own_ref), channel_id=1, source_target_pairs={{0,16},{8,24},{16,0},{24,8},{1,17},{9,25},{17,1},{25,9},{2,18},{10... | collective-permute-start | bytes 393224 | tf_op jit(solution)/shard_map/ppermute | solution.py:30
  8.3 6.4 %collective-permute-start.5 = (bf16[64,1024]{1,0:T(8,128)(2,1)S(1)}, bf16[64,1024]{1,0:T(8,128)(2,1)S(1)}, u32[]{:S(2)}, u32[]{:S(2)}) collective-permute-start(bf16[64,1024]{1,0:T(8,128)(2,1)S(1)} %get-tuple-element.19.own_ref), channel_id=1, source_target_pairs={{0,8},{8,16},{16,24},{24,0},{1,9},{9,17},{17,25},{25,1},{2,10},{10... | collective-permute-start | bytes 393224 | tf_op jit(solution)/shard_map/ppermute | solution.py:30
  16.3 38.6 %copy-start.1 = (f32[64,128]{1,0:T(8,128)S(1)}, f32[64,128]{1,0:T(8,128)}, u32[]{:S(2)}) copy-start(f32[64,128]{1,0:T(8,128)} %first_hbm.3) | copy-start | bytes 98308
  16.3 38.6 %copy-start.2 = (f32[64,128]{1,0:T(8,128)S(1)}, f32[64,128]{1,0:T(8,128)}, u32[]{:S(2)}) copy-start(f32[64,128]{1,0:T(8,128)} %second_hbm.3) | copy-start | bytes 98308
  16.3 16.9 %collective-permute-start.11 = (bf16[1024,256]{1,0:T(8,128)(2,1)}, bf16[1024,256]{1,0:T(8,128)(2,1)}, u32[]{:S(2)}, u32[]{:S(2)}) collective-permute-start(bf16[1024,256]{1,0:T(8,128)(2,1)} %widen.1.w0), channel_id=1, source_target_pairs={{0,224},{32,0},{64,32},{96,64},{128,96},{160,128},{192,160},{224,1... | collective-permute-start | bytes 1572872 | tf_op jit(solution)/shard_map/ppermute | solution.py:30
  22.2 14.8 %collective-permute-start.8 = (bf16[1024,256]{1,0:T(8,128)(2,1)}, bf16[1024,256]{1,0:T(8,128)(2,1)}, u32[]{:S(2)}, u32[]{:S(2)}) collective-permute-start(bf16[1024,256]{1,0:T(8,128)(2,1)} %widen.1.w0), channel_id=1, source_target_pairs={{0,32},{32,64},{64,96},{96,128},{128,160},{160,192},{192,224},{224... | collective-permute-start | bytes 1572872 | tf_op jit(solution)/shard_map/ppermute | solution.py:30
  22.2 1.4 %collective-permute-start = (bf16[768,128]{1,0:T(8,128)(2,1)S(1)}, bf16[768,128]{1,0:T(8,128)(2,1)S(1)}, u32[]{:S(2)}, u32[]{:S(2)}) collective-permute-start(bf16[768,128]{1,0:T(8,128)(2,1)S(1)} %get-tuple-element.16), channel_id=1, source_target_pairs={{0,1},{1,0},{2,3},{3,2},{4,5},{5,4},{6,7},{7,6},{8,9},{9,8},{10,11... | collective-permute-start | bytes 589832 | tf_op jit(solution)/shard_map/ppermute | solution.py:34
  25.0 16.6 %all-to-all-start = ((bf16[16,8,16,128]{3,2,1,0:T(8,128)(2,1)}), bf16[16,8,16,128]{3,2,1,0:T(8,128)(2,1)S(1)}, u32[]{:S(2)}, u32[]{:S(2)}) async-start(bf16[16,8,16,128]{3,2,1,0:T(8,128)(2,1)} %gradient.1), calls=%async_computation | async-start | bytes 1048576 | tf_op jit(solution)/shard_map/all_to_all | solution.py:341
  33.2 41.3 %collective-permute-start.12 = (bf16[1024,256]{1,0:T(8,128)(2,1)}, bf16[1024,256]{1,0:T(8,128)(2,1)S(1)}, u32[]{:S(2)}, u32[]{:S(2)}) collective-permute-start(bf16[1024,256]{1,0:T(8,128)(2,1)} %collective-permute-done.11.b1), channel_id=1, source_target_pairs={{0,224},{32,0},{64,32},{96,64},{128,96},{160,128},{192,160},{224,1... | collective-permute-start | bytes 1572872 | tf_op jit(solution)/shard_map/ppermute | solution.py:30
  36.9 38.0 %collective-permute-start.9 = (bf16[1024,256]{1,0:T(8,128)(2,1)}, bf16[1024,256]{1,0:T(8,128)(2,1)S(1)}, u32[]{:S(2)}, u32[]{:S(2)}) collective-permute-start(bf16[1024,256]{1,0:T(8,128)(2,1)} %collective-permute-done.8.f1), channel_id=1, source_target_pairs={{0,32},{32,64},{64,96},{96,128},{128,160},{160,192},{192,224},{224... | collective-permute-start | bytes 1572872 | tf_op jit(solution)/shard_map/ppermute | solution.py:30
  68.4 13.6 %all-to-all-start.3 = ((bf16[16,8,16,128]{3,2,1,0:T(8,128)(2,1)}), bf16[16,8,16,128]{3,2,1,0:T(8,128)(2,1)S(1)}, u32[]{:S(2)}, u32[]{:S(2)}) async-start(bf16[16,8,16,128]{3,2,1,0:T(8,128)(2,1)} %copies.1), calls=%async_computation.3 | async-start | bytes 1048576 | tf_op jit(solution)/shard_map/all_to_all | solution.py:341
  74.5 9.7 %collective-permute-start.13 = (bf16[1024,256]{1,0:T(8,128)(2,1)S(1)}, bf16[1024,256]{1,0:T(8,128)(2,1)S(1)}, u32[]{:S(2)}, u32[]{:S(2)}) collective-permute-start(bf16[1024,256]{1,0:T(8,128)(2,1)S(1)} %collective-permute-done.12.b2), channel_id=1, source_target_pairs={{0,224},{32,0},{64,32},{96,64},{128,96},{160,128},{192,160},{224,1... | collective-permute-start | bytes 1572872 | tf_op jit(solution)/shard_map/ppermute | solution.py:30
  75.0 11.0 %collective-permute-start.10 = (bf16[1024,256]{1,0:T(8,128)(2,1)S(1)}, bf16[1024,256]{1,0:T(8,128)(2,1)S(1)}, u32[]{:S(2)}, u32[]{:S(2)}) collective-permute-start(bf16[1024,256]{1,0:T(8,128)(2,1)S(1)} %collective-permute-done.9.f2), channel_id=1, source_target_pairs={{0,32},{32,64},{64,96},{96,128},{128,160},{160,192},{192,224},{224... | collective-permute-start | bytes 1572872 | tf_op jit(solution)/shard_map/ppermute | solution.py:30
  82.0 14.2 %collective-permute-start.4 = (bf16[16,8,16,128]{3,2,1,0:T(8,128)(2,1)S(1)}, bf16[16,8,16,128]{3,2,1,0:T(8,128)(2,1)S(1)}, u32[]{:S(2)}, u32[]{:S(2)}) collective-permute-start(bf16[16,8,16,128]{3,2,1,0:T(8,128)(2,1)S(1)} %all-to-all-done.3.near_ref), channel_id=1, source_target_pairs={{0,1},{1,0},{2,3},{3,2},{4,5},{5,4},{6,7},{7,6},{8,9},{9,8},{10,11... | collective-permute-start | bytes 1572872 | tf_op jit(solution)/shard_map/ppermute | solution.py:34
  84.3 12.0 %collective-permute-start.15 = (bf16[512,256]{1,0:T(8,128)(2,1)S(1)}, bf16[512,256]{1,0:T(8,128)(2,1)S(1)}, u32[]{:S(2)}, u32[]{:S(2)}) collective-permute-start(bf16[512,256]{1,0:T(8,128)(2,1)S(1)} %slice.9), channel_id=1, source_target_pairs={{0,224},{32,0},{64,32},{96,64},{128,96},{160,128},{192,160},{224,1... | collective-permute-start | bytes 786440 | tf_op jit(solution)/shard_map/ppermute | solution.py:30
  86.0 10.3 %collective-permute-start.14 = (bf16[512,256]{1,0:T(8,128)(2,1)S(1)}, bf16[512,256]{1,0:T(8,128)(2,1)S(1)}, u32[]{:S(2)}, u32[]{:S(2)}) collective-permute-start(bf16[512,256]{1,0:T(8,128)(2,1)S(1)} %slice.8), channel_id=1, source_target_pairs={{0,32},{32,64},{64,96},{96,128},{128,160},{160,192},{192,224},{224... | collective-permute-start | bytes 786440 | tf_op jit(solution)/shard_map/ppermute | solution.py:30
  86.7 4.5 %collective-permute-start.3 = (f32[16,128]{1,0:T(8,128)S(1)}, f32[16,128]{1,0:T(8,128)S(1)}, u32[]{:S(2)}, u32[]{:S(2)}) collective-permute-start(f32[16,128]{1,0:T(8,128)S(1)} %get-tuple-element.17.p0), channel_id=1, source_target_pairs={{0,6},{2,0},{4,2},{6,4},{1,7},{3,1},{5,3},{7,5},{8,14},{10,8},{12,... | collective-permute-start | bytes 24584 | tf_op jit(solution)/shard_map/ppermute | solution.py:30
  89.8 5.2 %collective-permute-start.2 = (f32[16,128]{1,0:T(8,128)S(1)}, f32[16,128]{1,0:T(8,128)S(1)}, u32[]{:S(2)}, u32[]{:S(2)}) collective-permute-start(f32[16,128]{1,0:T(8,128)S(1)} %get-tuple-element.17.p0), channel_id=1, source_target_pairs={{0,4},{2,6},{4,0},{6,2},{1,5},{3,7},{5,1},{7,3},{8,12},{10,14},{12... | collective-permute-start | bytes 24584 | tf_op jit(solution)/shard_map/ppermute | solution.py:30
  91.1 5.1 %collective-permute-start.1 = (f32[16,128]{1,0:T(8,128)S(1)}, f32[16,128]{1,0:T(8,128)S(1)}, u32[]{:S(2)}, u32[]{:S(2)}) collective-permute-start(f32[16,128]{1,0:T(8,128)S(1)} %get-tuple-element.17.p0), channel_id=1, source_target_pairs={{0,2},{2,4},{4,6},{6,0},{1,3},{3,5},{5,7},{7,1},{8,10},{10,12},{12... | collective-permute-start | bytes 24584 | tf_op jit(solution)/shard_map/ppermute | solution.py:30

commit v2 on v1

--- a/solution.py
+++ b/solution.py
@@ -45,8 +45,8 @@
 
 
 def heads_kernel(
-    place_ref, lam_hbm, first_hbm, second_hbm, gain_hbm, basis_hbm, weight_hbm,
-    own_ref, sent_ref, narrow_ref, first_ref, second_ref, basis_ref, lam_ref, gain_ref, weight_ref, sems,
+    place_ref, lam_hbm, first_hbm, second_hbm, gain_hbm, basis_hbm,
+    own_ref, sent_ref, first_ref, second_ref, basis_ref, lam_ref, gain_ref, sems,
 ):
     tokens, values = first_ref.shape
     width = gain_ref.shape[1]
@@ -63,13 +63,12 @@
         rows = pl.ds(step * tile, tile)
         moving.append(
             [
-                fetch(first_hbm.at[rows], first_ref.at[rows], 4 + 2 * step),
-                fetch(second_hbm.at[rows], second_ref.at[rows], 5 + 2 * step),
+                fetch(first_hbm.at[rows], first_ref.at[rows], 3 + 2 * step),
+                fetch(second_hbm.at[rows], second_ref.at[rows], 4 + 2 * step),
             ]
         )
         if step == 0:
             fixed.append(fetch(basis_hbm, basis_ref, 2))
-    last = fetch(weight_hbm, weight_ref, 3)
     for copy in fixed[:2]:
         copy.wait()
     gain = gain_ref[...] * OUT_SCALE
@@ -94,22 +93,19 @@
         low, high = total[:, :half], total[:, half:]
         own_ref[rows, :] = jnp.where(is_low, low, high)
         sent_ref[rows, :] = jnp.where(is_low, high, low).astype(jnp.bfloat16)
-    last.wait()
-    narrow_ref[...] = weight_ref[...].astype(jnp.bfloat16)
-
-
-def heads(place, lambda_head, first_mix, second_mix, head_gain, basis, weight):
+
+
+def heads(place, lambda_head, first_mix, second_mix, head_gain, basis):
     tokens, values = first_mix.shape
     half = basis.shape[1] // 2
     lam, gain = lambda_head[None, :], head_gain[None, :]
     return pl.pallas_call(
         heads_kernel,
-        in_specs=[SMEM] + [HBM] * 6,
-        out_specs=[VMEM] * 3,
+        in_specs=[SMEM] + [HBM] * 5,
+        out_specs=[VMEM] * 2,
         out_shape=[
             jax.ShapeDtypeStruct((tokens, half), jnp.float32),
             jax.ShapeDtypeStruct((tokens, half), jnp.bfloat16),
-            jax.ShapeDtypeStruct(weight.shape, jnp.bfloat16),
         ],
         scratch_shapes=[
             pltpu.VMEM((tokens, values), jnp.bfloat16),
@@ -117,12 +113,11 @@
             pltpu.VMEM(basis.shape, jnp.bfloat16),
             pltpu.VMEM(lam.shape, jnp.float32),
             pltpu.VMEM(gain.shape, jnp.float32),
-            pltpu.VMEM(weight.shape, jnp.float32),
-            pltpu.SemaphoreType.DMA((10,)),
+            pltpu.SemaphoreType.DMA((9,)),
         ],
         compiler_params=limit(12),
         name="heads",
-    )(place, *in_hbm(lam, first_mix, second_mix, gain, basis, weight))
+    )(place, *in_hbm(lam, first_mix, second_mix, gain, basis))
 
 
 def widen_kernel(place_ref, own_ref, one_ref, two_ref, three_ref, out_ref, slots):
@@ -208,16 +203,29 @@
         copy.wait()
 
 
-def copies_of(array, count):
-    return pl.pallas_call(
-        copy_to_all,
-        in_specs=[VMEM],
+def letters_kernel(column_ref, extra_ref, out_hbm, sems):
+    rows = column_ref.shape[0]
+    copies = []
+    for slot in range(out_hbm.shape[0]):
+        for part, (source, target) in enumerate(((column_ref, pl.ds(0, rows)), (extra_ref, pl.ds(rows, 2)))):
+            copy = pltpu.make_async_copy(source, out_hbm.at[slot, target], sems.at[slot, part])
+            copy.start()
+            copies.append(copy)
+    for copy in copies:
+        copy.wait()
+
+
+def letters(column, extra, count):
+    blocks, rows, rank = column.shape
+    return pl.pallas_call(
+        letters_kernel,
+        in_specs=[VMEM] * 2,
         out_specs=HBM,
-        out_shape=pltpu.HBM((count, *array.shape), array.dtype),
-        scratch_shapes=[pltpu.SemaphoreType.DMA((count,))],
+        out_shape=pltpu.HBM((count, blocks + 2, rows, rank), column.dtype),
+        scratch_shapes=[pltpu.SemaphoreType.DMA((count, 2))],
         compiler_params=limit(4),
-        name="copies",
-    )(array)
+        name="letters",
+    )(column, extra)
 
 
 def moments(projected, first, second):
@@ -229,7 +237,9 @@
 def update_kernel(place_ref, pieces_ref, first_ref, second_ref, piece_ref, copies_hbm, direction_ref, sems):
     rows = pl.ds(pl.multiple_of(place_ref[2] * 16, 16), 16)
     piece = jnp.sum(pieces_ref[...].astype(jnp.float32), axis=0)
-    piece_ref[...] = piece
+    high = piece.astype(jnp.bfloat16)
+    piece_ref[0] = high
+    piece_ref[1] = (piece - high.astype(jnp.float32)).astype(jnp.bfloat16)
     first_new, second_new = moments(piece, first_ref[rows, :], second_ref[rows, :])
     direction_ref[...] = (first_new / (jnp.sqrt(second_new) + 1e-08)).astype(jnp.bfloat16)
     copy_to_all(direction_ref, copies_hbm, sems)
@@ -242,7 +252,7 @@
         in_specs=[SMEM] + [VMEM] * 3,
         out_specs=[VMEM, HBM],
         out_shape=[
-            jax.ShapeDtypeStruct((rows, rank), jnp.float32),
+            jax.ShapeDtypeStruct((2, rows, rank), jnp.bfloat16),
             pltpu.HBM(pieces.shape, jnp.bfloat16),
         ],
         scratch_shapes=[pltpu.VMEM((rows, rank), jnp.bfloat16), pltpu.SemaphoreType.DMA((count,))],
@@ -252,7 +262,7 @@
 
 
 def finish_kernel(
-    place_ref, basis_hbm, weight_hbm, first_hbm, second_hbm, p0, p1, p2, p3, near_ref, far_ref,
+    place_ref, basis_hbm, weight_hbm, first_hbm, second_hbm, near_ref, far_ref,
     w0, f1, f2, f3, b1, b2, b3, h1, h2,
     new_ref, step_ref, copy_ref, first_out, second_out,
     basis_ref, weight_ref, first_ref, second_ref, tiles, sems,
@@ -264,9 +274,9 @@
         copy = pltpu.make_async_copy(source, target, sems.at[8 + slot])
         copy.start()
         fetched.append(copy)
-    z, y, x = place_ref[0], place_ref[1], place_ref[2]
+    z, y = place_ref[0], place_ref[1]
     is_low = place_ref[3] == 0
-    near, far = near_ref[...].astype(jnp.float32), far_ref[...].astype(jnp.float32)
+    near, far = near_ref[:, :8].astype(jnp.float32), far_ref[:, :8].astype(jnp.float32)
     energy = jnp.sum(near * near + far * far)
     count = 2 * near.shape[0] * near.shape[1] * near.shape[2] * near.shape[3]
     spread = jnp.sqrt(jnp.full((1, 128), energy / count, jnp.float32))
@@ -301,21 +311,23 @@
     step = dot(rows_of(near_ref[mine, z], far_ref[mine, z]), basis, 1, 1) * scale
     step_ref[...] = step
     new_ref[...] = weight_ref[...] + step
-    for hops, piece in enumerate((p0, p1, p2, p3)):
-        rows = pl.ds(pl.multiple_of((x + 4 - hops) % 4 * 16, 16), 16)
-        first_new, second_new = moments(piece[...], first_ref[rows, :], second_ref[rows, :])
+    for source in range(4):
+        rows = pl.ds(source * 16, 16)
+        letter = y * 4 + source
+        piece = near_ref[letter, 8].astype(jnp.float32) + near_ref[letter, 9].astype(jnp.float32)
+        first_new, second_new = moments(piece, first_ref[rows, :], second_ref[rows, :])
         first_out[rows, :] = first_new
         second_out[rows, :] = second_new
     for copy in copies:
         copy.wait()
 
 
-def finish(place, basis, weight, first, second, pieces, near, far, blocks):
+def finish(place, basis, weight, first, second, near, far, blocks):
     values = basis.shape[0]
     like = lambda array: jax.ShapeDtypeStruct(array.shape, jnp.float32)
     return pl.pallas_call(
         finish_kernel,
-        in_specs=[SMEM] + [HBM] * 4 + [VMEM] * (6 + len(blocks)),
+        in_specs=[SMEM] + [HBM] * 4 + [VMEM] * (2 + len(blocks)),
         out_specs=[VMEM, VMEM, HBM, VMEM, VMEM],
         out_shape=[
             like(weight),
@@ -334,7 +346,7 @@
         ],
         compiler_params=limit(16),
         name="finish",
-    )(place, *in_hbm(basis, weight, first, second), *pieces, near, far, *in_vmem(*blocks))
+    )(place, *in_hbm(basis, weight, first, second), near, far, *in_vmem(*blocks))
 
 
 def exchange(array, axes):
@@ -344,7 +356,7 @@
 def chain(first_mix, second_mix, lambda_head, head_gain, out_cotangent, basis, weight, first_moment, second_moment):
     place = jnp.stack([lax.axis_index(name).astype(jnp.int32) for name in ("z", "y", "x", "tp")])
     turned = weight.T
-    own, sent, narrow = heads(place, lambda_head, first_mix, second_mix, head_gain, basis, turned)
+    narrow = turned.astype(jnp.bfloat16)
 
     lead = turned.shape[1] // 2
     w0 = widen(place, [narrow] + [shift(narrow, "y", hops) for hops in (1, 2, 3)])
@@ -353,15 +365,14 @@
     f3, b3 = shift(f2, "z", 1), shift(b2, "z", -1)
     h1, h2 = shift(f3[:lead], "z", 1), shift(b3[lead:], "z", -1)
 
+    own, sent = heads(place, lambda_head, first_mix, second_mix, head_gain, basis)
     parts = gradient(own, swap_cores(sent), out_cotangent)
     folded = fold(exchange(parts, ("y", "x")))
-    piece, copies = update(place, exchange(folded, "z"), first_moment, second_moment)
-    pieces = [piece] + [shift(piece, "x", hops) for hops in (1, 2, 3)]
-    column = exchange(copies, "z")
-    near = exchange(copies_of(column, 16), ("y", "x"))
+    extra, copies = update(place, exchange(folded, "z"), first_moment, second_moment)
+    near = exchange(letters(exchange(copies, "z"), extra, 16), ("y", "x"))
     far = swap_cores(near)
     weight_new, step_out, weight_copy, first_new, second_new = finish(
-        place, basis, turned, first_moment, second_moment, pieces, near, far, (w0, f1, f2, f3, b1, b2, b3, h1, h2)
+        place, basis, turned, first_moment, second_moment, near, far, (w0, f1, f2, f3, b1, b2, b3, h1, h2)
     )
     return (weight_new.T, weight_copy, step_out.T, first_new, second_new)
 

time: 103 us -> 91.1 us (0.88)
  the two profiles are of different devices: /device:TPU:16 before, /device:TPU:1 now
where the time goes in v2:
time: 91.1 us; the launch traced here: 89.8 us
  starting transfers between devices  36.8 us (40%)
  waiting for transfers between devices  21.1 us (23%)
  Pallas kernels  15.7 us (17%)
  blocking collectives  15.1 us (17%)
  between operations  0.95 us (1%)
    all_to_all x1, blocking collectives, exchange(): return lax.all_to_all(array, axes, 0, 0, tiled=True)  15.1 us
    ppermute x11, starting transfers between devices, shift(): lax.ppermute(array, axis, [(i, (i + hops) % count) for i in range(count)])  15.1 us
    all_to_all x3, waiting for transfers between devices, exchange(): return lax.all_to_all(array, axes, 0, 0, tiled=True)  13.3 us
    all_to_all x3, starting transfers between devices, exchange(): return lax.all_to_all(array, axes, 0, 0, tiled=True)  12.8 us
    ppermute x2, starting transfers between devices, swap_cores(): return lax.ppermute(array, 'tp', [(0, 1), (1, 0)])  8.89 us
    ppermute x11, waiting for transfers between devices, shift(): lax.ppermute(array, axis, [(i, (i + hops) % count) for i in range(count)])  7.8 us
    pallas_call x1, Pallas kernels, finish(): pl.pallas_call(finish_kernel, in_specs=[SMEM] + [HBM] * 4 + [VMEM] * (2 +...  5.86 us
    pallas_call x1, Pallas kernels, heads(): pl.pallas_call(heads_kernel, in_specs=[SMEM] + [HBM] * 5, out_specs=[VMEM...  4.13 us
  transfers between devices with their start and end apart: 16, of which 5 were waited for; matrix products, arithmetic and copies ran while one was open for 0% of the time, Pallas kernels for 6%

profile of v2, /device:TPU:1, one launch (start us, length us, event | category | flops | bytes accessed | tf_op | source)
XLA Modules:
  0.0 89.8 jit_solution(4521837720397932632)
XLA Ops:
  0.6 0.0 copy-start.3
  0.6 0.0 copy-start
  0.7 0.1 pad_add_fusion.place_ref
  0.7 4.1 %heads.1 = (f32[768,128]{1,0:T(8,128)S(1)}, bf16[768,128]{1,0:T(8,128)(2,1)S(1)}) custom-call(s32[4]{0:T(128)S(1)} %pad_add_fusion.place_ref, f32[1,4]{1,0:T(1,128)} %bitcast.12, bf16[768,1024]{1,0:T(8,128)(2,1)} %first_hbm.2, bf16[768,1024]{1,0:T(8,128)(2,1)} %second_hbm.2, f32[1,256]{1,0:T(1,128)} %bitcast.11, bf16[1024,256]{1,0:T(8,128)(2,1)} %basis_hbm.3), custom_call_target="tpu_custom_call" | custom-call | tf_op jit(solution)/shard_map/heads/pallas_call | solution.py:102
  4.9 3.3 %collective-permute-start = (bf16[768,128]{1,0:T(8,128)(2,1)S(1)}, bf16[768,128]{1,0:T(8,128)(2,1)S(1)}, u32[]{:S(2)}, u32[]{:S(2)}) collective-permute-start(bf16[768,128]{1,0:T(8,128)(2,1)S(1)} %get-tuple-element.15), channel_id=1, source_target_pairs={{0,1},{1,0},{2,3},{3,2},{4,5},{5,4},{6,7},{7,6},{8,9},{9,8},{10,11... | collective-permute-start | bytes 589832 | tf_op jit(solution)/shard_map/ppermute | solution.py:34
  8.2 0.0 copy-done.3
  8.2 1.1 %collective-permute-start.4 = (bf16[64,1024]{1,0:T(8,128)(2,1)S(1)}, bf16[64,1024]{1,0:T(8,128)(2,1)S(1)}, u32[]{:S(2)}, u32[]{:S(2)}) collective-permute-start(bf16[64,1024]{1,0:T(8,128)(2,1)S(1)} %bitcast_convert_fusion.own_ref), channel_id=1, source_target_pairs={{0,24},{8,0},{16,8},{24,16},{1,25},{9,1},{17,9},{25,17},{2,26},{10... | collective-permute-start | bytes 393224 | tf_op jit(solution)/shard_map/ppermute | solution.py:30
  9.3 0.3 collective-permute-start.3
  9.6 0.7 collective-permute-start.2
  10.3 0.0 collective-permute-done.far_ref
  10.3 0.0 copy-done
  10.3 0.0 copy-start.1
  10.3 1.4 %gradient.1 = bf16[16,8,16,128]{3,2,1,0:T(8,128)(2,1)} custom-call(f32[768,128]{1,0:T(8,128)S(1)} %get-tuple-element.14.own_ref, bf16[768,128]{1,0:T(8,128)(2,1)S(1)} %collective-permute-done.far_ref, bf16[768,2048]{1,0:T(8,128)(2,1)S(1)} %copy-done), custom_call_target="tpu_custom_call" | custom-call | tf_op jit(solution)/shard_map/gradient/pallas_call | solution.py:165
  11.8 5.8 %all-to-all-start = ((bf16[16,8,16,128]{3,2,1,0:T(8,128)(2,1)}), bf16[16,8,16,128]{3,2,1,0:T(8,128)(2,1)S(1)}, u32[]{:S(2)}, u32[]{:S(2)}) async-start(bf16[16,8,16,128]{3,2,1,0:T(8,128)(2,1)} %gradient.1), calls=%async_computation | async-start | bytes 1048576 | tf_op jit(solution)/shard_map/all_to_all | solution.py:353
  17.6 0.0 collective-permute-done.4.three_ref
  17.6 0.0 collective-permute-done.3.two_ref
  17.6 1.5 %collective-permute-done.2.one_ref = bf16[64,1024]{1,0:T(8,128)(2,1)} collective-permute-done((bf16[64,1024]{1,0:T(8,128)(2,1)S(1)}, bf16[64,1024]{1,0:T(8,128)(2,1)}, u32[]{:S(2)}, u32[]{:S(2)}) %collective-permute-start.2) | collective-permute-done | bytes 131104 | tf_op jit(solution)/shard_map/ppermute | solution.py:30
  19.1 1.2 %widen.1.w0 = bf16[1024,256]{1,0:T(8,128)(2,1)S(1)} custom-call(s32[4]{0:T(128)S(1)} %pad_add_fusion.place_ref, bf16[64,1024]{1,0:T(8,128)(2,1)S(1)} %bitcast_convert_fusion.own_ref, bf16[64,1024]{1,0:T(8,128)(2,1)} %collective-permute-done.2.one_ref, bf16[64,1024]{1,0:T(8,128)(2,1)} %collective-permute-done.3.two_ref, ...), custom_call_target="tpu_custom_call" | custom-call | tf_op jit(solution)/shard_map/widen/pallas_call | solution.py:135
  20.4 5.7 %collective-permute-start.8 = (bf16[1024,256]{1,0:T(8,128)(2,1)S(1)}, bf16[1024,256]{1,0:T(8,128)(2,1)S(1)}, u32[]{:S(2)}, u32[]{:S(2)}) collective-permute-start(bf16[1024,256]{1,0:T(8,128)(2,1)S(1)} %widen.1.w0), channel_id=1, source_target_pairs={{0,224},{32,0},{64,32},{96,64},{128,96},{160,128},{192,160},{224,1... | collective-permute-start | bytes 1572872 | tf_op jit(solution)/shard_map/ppermute | solution.py:30
  26.0 0.0 collective-permute-start.5
  26.0 2.1 %all-to-all-done.parts_ref = bf16[16,8,16,128]{3,2,1,0:T(8,128)(2,1)S(1)} async-done(((bf16[16,8,16,128]{3,2,1,0:T(8,128)(2,1)}), bf16[16,8,16,128]{3,2,1,0:T(8,128)(2,1)S(1)}, u32[]{:S(2)}, u32[]{:S(2)}) %all-to-all-start) | async-done | bytes 524320 | tf_op jit(solution)/shard_map/all_to_all | solution.py:353
  28.1 0.7 fold.1
  28.9 15.1 %all_to_all.20.pieces_ref = bf16[8,16,128]{2,1,0:T(8,128)(2,1)S(1)} all-to-all(bf16[8,16,128]{2,1,0:T(8,128)(2,1)} %fold.1), channel_id=1, replica_groups=mesh['z'=8,'y'=4,'x'=4,'tp'=2] {'z'}, dimensions={0} | all-to-all | bytes 65536 | tf_op jit(solution)/shard_map/all_to_all | solution.py:353
  43.9 0.0 copy-done.1
  43.9 0.0 copy-done.2
  43.9 1.3 %update.1 = (bf16[2,16,128]{2,1,0:T(8,128)(2,1)S(1)}, bf16[8,16,128]{2,1,0:T(8,128)(2,1)}) custom-call(s32[4]{0:T(128)S(1)} %pad_add_fusion.place_ref, bf16[8,16,128]{2,1,0:T(8,128)(2,1)S(1)} %all_to_all.20.pieces_ref, f32[64,128]{1,0:T(8,128)S(1)} %copy-done.1, f32[64,128]{1,0:T(8,128)S(1)} %copy-done.2), custom_call_target="tpu_custom_call" | custom-call | tf_op jit(solution)/shard_map/update/pallas_call | solution.py:250
  45.2 3.4 %all-to-all-start.2 = ((bf16[8,16,128]{2,1,0:T(8,128)(2,1)}), bf16[8,16,128]{2,1,0:T(8,128)(2,1)S(1)}, u32[]{:S(2)}, u32[]{:S(2)}) async-start(bf16[8,16,128]{2,1,0:T(8,128)(2,1)} %get-tuple-element.16), calls=%async_computation.2 | async-start | bytes 65536 | tf_op jit(solution)/shard_map/all_to_all | solution.py:353
  48.6 0.0 collective-permute-done.8.b1
  48.6 2.6 %collective-permute-start.9 = (bf16[1024,256]{1,0:T(8,128)(2,1)S(1)}, bf16[1024,256]{1,0:T(8,128)(2,1)}, u32[]{:S(2)}, u32[]{:S(2)}) collective-permute-start(bf16[1024,256]{1,0:T(8,128)(2,1)S(1)} %collective-permute-done.8.b1), channel_id=1, source_target_pairs={{0,224},{32,0},{64,32},{96,64},{128,96},{160,128},{192,160},{224,1... | collective-permute-start | bytes 1572872 | tf_op jit(solution)/shard_map/ppermute | solution.py:30
  51.2 0.0 collective-permute-done.5.f1
  51.2 0.0 collective-permute-start.6
  51.2 4.3 %all-to-all-done.2.column_ref = bf16[8,16,128]{2,1,0:T(8,128)(2,1)S(1)} async-done(((bf16[8,16,128]{2,1,0:T(8,128)(2,1)}), bf16[8,16,128]{2,1,0:T(8,128)(2,1)S(1)}, u32[]{:S(2)}, u32[]{:S(2)}) %all-to-all-start.2) | async-done | bytes 32800 | tf_op jit(solution)/shard_map/all_to_all | solution.py:353
  55.5 1.1 %letters.1 = bf16[16,10,16,128]{3,2,1,0:T(8,128)(2,1)} custom-call(bf16[8,16,128]{2,1,0:T(8,128)(2,1)S(1)} %all-to-all-done.2.column_ref, bf16[2,16,128]{2,1,0:T(8,128)(2,1)S(1)} %get-tuple-element.17.extra_ref), custom_call_target="tpu_custom_call" | custom-call | tf_op jit(solution)/shard_map/letters/pallas_call | solution.py:220
  56.6 3.6 %all-to-all-start.3 = ((bf16[16,10,16,128]{3,2,1,0:T(8,128)(2,1)}), bf16[16,10,16,128]{3,2,1,0:T(8,128)(2,1)S(1)}, u32[]{:S(2)}, u32[]{:S(2)}) async-start(bf16[16,10,16,128]{3,2,1,0:T(8,128)(2,1)} %letters.1), calls=%async_computation.3 | async-start | bytes 1310720 | tf_op jit(solution)/shard_map/all_to_all | solution.py:353
  60.2 0.0 collective-permute-done.9.b2
  60.2 2.9 %collective-permute-start.10 = (bf16[1024,256]{1,0:T(8,128)(2,1)}, bf16[1024,256]{1,0:T(8,128)(2,1)S(1)}, u32[]{:S(2)}, u32[]{:S(2)}) collective-permute-start(bf16[1024,256]{1,0:T(8,128)(2,1)} %collective-permute-done.9.b2), channel_id=1, source_target_pairs={{0,224},{32,0},{64,32},{96,64},{128,96},{160,128},{192,160},{224,1... | collective-permute-start | bytes 1572872 | tf_op jit(solution)/shard_map/ppermute | solution.py:30
  63.1 0.0 collective-permute-done.6.f2
  63.1 0.0 collective-permute-start.7
  63.1 6.9 %all-to-all-done.3.near_ref = bf16[16,10,16,128]{3,2,1,0:T(8,128)(2,1)S(1)} async-done(((bf16[16,10,16,128]{3,2,1,0:T(8,128)(2,1)}), bf16[16,10,16,128]{3,2,1,0:T(8,128)(2,1)S(1)}, u32[]{:S(2)}, u32[]{:S(2)}) %all-to-all-start.3) | async-done | bytes 655392 | tf_op jit(solution)/shard_map/all_to_all | solution.py:353
  70.0 5.6 %collective-permute-start.1 = (bf16[16,10,16,128]{3,2,1,0:T(8,128)(2,1)S(1)}, bf16[16,10,16,128]{3,2,1,0:T(8,128)(2,1)S(1)}, u32[]{:S(2)}, u32[]{:S(2)}) collective-permute-start(bf16[16,10,16,128]{3,2,1,0:T(8,128)(2,1)S(1)} %all-to-all-done.3.near_ref), channel_id=1, source_target_pairs={{0,1},{1,0},{2,3},{3,2},{4,5},{5,4},{6,7},{7,6},{8,9},{9,8},{10,11... | collective-permute-start | bytes 1966088 | tf_op jit(solution)/shard_map/ppermute | solution.py:34
  75.6 0.0 collective-permute-done.10.b3
  75.6 0.4 collective-permute-start.12
  76.0 0.0 collective-permute-done.7.f3
  76.0 1.4 %collective-permute-start.11 = (bf16[512,256]{1,0:T(8,128)(2,1)S(1)}, bf16[512,256]{1,0:T(8,128)(2,1)S(1)}, u32[]{:S(2)}, u32[]{:S(2)}) collective-permute-start(bf16[512,256]{1,0:T(8,128)(2,1)S(1)} %slice.8), channel_id=1, source_target_pairs={{0,32},{32,64},{64,96},{96,128},{128,160},{160,192},{192,224},{224... | collective-permute-start | bytes 786440 | tf_op jit(solution)/shard_map/ppermute | solution.py:30
  77.5 6.3 %collective-permute-done.12.h2 = bf16[512,256]{1,0:T(8,128)(2,1)S(1)} collective-permute-done((bf16[512,256]{1,0:T(8,128)(2,1)S(1)}, bf16[512,256]{1,0:T(8,128)(2,1)S(1)}, u32[]{:S(2)}, u32[]{:S(2)}) %collective-permute-start.12) | collective-permute-done | bytes 262176 | tf_op jit(solution)/shard_map/ppermute | solution.py:30
  83.7 0.0 collective-permute-done.11.h1
  83.8 0.0 collective-permute-done.1.far_ref
  83.8 5.9 %finish.1 = (f32[64,1024]{1,0:T(8,128)}, f32[64,1024]{1,0:T(8,128)}, bf16[1024,2048]{1,0:T(8,128)(2,1)}, f32[64,128]{1,0:T(8,128)}, f32[64,128]{1,0:T(8,128)}) custom-call(s32[4]{0:T(128)S(1)} %pad_add_fusion.place_ref, bf16[1024,256]{1,0:T(8,128)(2,1)} %basis_hbm.3, f32[64,1024]{1,0:T(8,128)} %bitcast.10, f32[64,128]{1,0:T(8,128)} %first_hbm.3, ...), custom_call_target="tpu_custom_call" | custom-call | tf_op jit(solution)/shard_map/finish/pallas_call | solution.py:328
  (4 shorter events, 0.1 us)
Async XLA Ops:
  0.6 7.5 %copy-start.3 = (f32[1024,64]{0,1:T(8,128)S(1)}, f32[1024,64]{0,1:T(8,128)}, u32[]{:S(2)}) copy-start(f32[1024,64]{0,1:T(8,128)} %param.15) | copy-start | bytes 786436
  0.6 9.7 %copy-start = (bf16[768,2048]{1,0:T(8,128)(2,1)S(1)}, bf16[768,2048]{1,0:T(8,128)(2,1)}, u32[]{:S(2)}) copy-start(bf16[768,2048]{1,0:T(8,128)(2,1)} %cot_ref.1) | copy-start | bytes 9437188
  4.9 5.5 %collective-permute-start = (bf16[768,128]{1,0:T(8,128)(2,1)S(1)}, bf16[768,128]{1,0:T(8,128)(2,1)S(1)}, u32[]{:S(2)}, u32[]{:S(2)}) collective-permute-start(bf16[768,128]{1,0:T(8,128)(2,1)S(1)} %get-tuple-element.15), channel_id=1, source_target_pairs={{0,1},{1,0},{2,3},{3,2},{4,5},{5,4},{6,7},{7,6},{8,9},{9,8},{10,11... | collective-permute-start | bytes 589832 | tf_op jit(solution)/shard_map/ppermute | solution.py:34
  8.2 9.4 %collective-permute-start.4 = (bf16[64,1024]{1,0:T(8,128)(2,1)S(1)}, bf16[64,1024]{1,0:T(8,128)(2,1)S(1)}, u32[]{:S(2)}, u32[]{:S(2)}) collective-permute-start(bf16[64,1024]{1,0:T(8,128)(2,1)S(1)} %bitcast_convert_fusion.own_ref), channel_id=1, source_target_pairs={{0,24},{8,0},{16,8},{24,16},{1,25},{9,1},{17,9},{25,17},{2,26},{10... | collective-permute-start | bytes 393224 | tf_op jit(solution)/shard_map/ppermute | solution.py:30
  9.3 8.3 %collective-permute-start.3 = (bf16[64,1024]{1,0:T(8,128)(2,1)S(1)}, bf16[64,1024]{1,0:T(8,128)(2,1)}, u32[]{:S(2)}, u32[]{:S(2)}) collective-permute-start(bf16[64,1024]{1,0:T(8,128)(2,1)S(1)} %bitcast_convert_fusion.own_ref), channel_id=1, source_target_pairs={{0,16},{8,24},{16,0},{24,8},{1,17},{9,25},{17,1},{25,9},{2,18},{10... | collective-permute-start | bytes 393224 | tf_op jit(solution)/shard_map/ppermute | solution.py:30
  9.6 9.5 %collective-permute-start.2 = (bf16[64,1024]{1,0:T(8,128)(2,1)S(1)}, bf16[64,1024]{1,0:T(8,128)(2,1)}, u32[]{:S(2)}, u32[]{:S(2)}) collective-permute-start(bf16[64,1024]{1,0:T(8,128)(2,1)S(1)} %bitcast_convert_fusion.own_ref), channel_id=1, source_target_pairs={{0,8},{8,16},{16,24},{24,0},{1,9},{9,17},{17,25},{25,1},{2,10},{10... | collective-permute-start | bytes 393224 | tf_op jit(solution)/shard_map/ppermute | solution.py:30
  10.3 33.6 %copy-start.1 = (f32[64,128]{1,0:T(8,128)S(1)}, f32[64,128]{1,0:T(8,128)}, u32[]{:S(2)}) copy-start(f32[64,128]{1,0:T(8,128)} %first_hbm.3) | copy-start | bytes 98308
  10.3 33.6 %copy-start.2 = (f32[64,128]{1,0:T(8,128)S(1)}, f32[64,128]{1,0:T(8,128)}, u32[]{:S(2)}) copy-start(f32[64,128]{1,0:T(8,128)} %second_hbm.3) | copy-start | bytes 98308
  11.8 16.4 %all-to-all-start = ((bf16[16,8,16,128]{3,2,1,0:T(8,128)(2,1)}), bf16[16,8,16,128]{3,2,1,0:T(8,128)(2,1)S(1)}, u32[]{:S(2)}, u32[]{:S(2)}) async-start(bf16[16,8,16,128]{3,2,1,0:T(8,128)(2,1)} %gradient.1), calls=%async_computation | async-start | bytes 1048576 | tf_op jit(solution)/shard_map/all_to_all | solution.py:353
  20.4 28.2 %collective-permute-start.8 = (bf16[1024,256]{1,0:T(8,128)(2,1)S(1)}, bf16[1024,256]{1,0:T(8,128)(2,1)S(1)}, u32[]{:S(2)}, u32[]{:S(2)}) collective-permute-start(bf16[1024,256]{1,0:T(8,128)(2,1)S(1)} %widen.1.w0), channel_id=1, source_target_pairs={{0,224},{32,0},{64,32},{96,64},{128,96},{160,128},{192,160},{224,1... | collective-permute-start | bytes 1572872 | tf_op jit(solution)/shard_map/ppermute | solution.py:30
  26.0 25.2 %collective-permute-start.5 = (bf16[1024,256]{1,0:T(8,128)(2,1)S(1)}, bf16[1024,256]{1,0:T(8,128)(2,1)S(1)}, u32[]{:S(2)}, u32[]{:S(2)}) collective-permute-start(bf16[1024,256]{1,0:T(8,128)(2,1)S(1)} %widen.1.w0), channel_id=1, source_target_pairs={{0,32},{32,64},{64,96},{96,128},{128,160},{160,192},{192,224},{224... | collective-permute-start | bytes 1572872 | tf_op jit(solution)/shard_map/ppermute | solution.py:30
  45.2 10.3 %all-to-all-start.2 = ((bf16[8,16,128]{2,1,0:T(8,128)(2,1)}), bf16[8,16,128]{2,1,0:T(8,128)(2,1)S(1)}, u32[]{:S(2)}, u32[]{:S(2)}) async-start(bf16[8,16,128]{2,1,0:T(8,128)(2,1)} %get-tuple-element.16), calls=%async_computation.2 | async-start | bytes 65536 | tf_op jit(solution)/shard_map/all_to_all | solution.py:353
  48.6 11.6 %collective-permute-start.9 = (bf16[1024,256]{1,0:T(8,128)(2,1)S(1)}, bf16[1024,256]{1,0:T(8,128)(2,1)}, u32[]{:S(2)}, u32[]{:S(2)}) collective-permute-start(bf16[1024,256]{1,0:T(8,128)(2,1)S(1)} %collective-permute-done.8.b1), channel_id=1, source_target_pairs={{0,224},{32,0},{64,32},{96,64},{128,96},{160,128},{192,160},{224,1... | collective-permute-start | bytes 1572872 | tf_op jit(solution)/shard_map/ppermute | solution.py:30
  51.2 11.9 %collective-permute-start.6 = (bf16[1024,256]{1,0:T(8,128)(2,1)S(1)}, bf16[1024,256]{1,0:T(8,128)(2,1)}, u32[]{:S(2)}, u32[]{:S(2)}) collective-permute-start(bf16[1024,256]{1,0:T(8,128)(2,1)S(1)} %collective-permute-done.5.f1), channel_id=1, source_target_pairs={{0,32},{32,64},{64,96},{96,128},{128,160},{160,192},{192,224},{224... | collective-permute-start | bytes 1572872 | tf_op jit(solution)/shard_map/ppermute | solution.py:30
  56.6 13.4 %all-to-all-start.3 = ((bf16[16,10,16,128]{3,2,1,0:T(8,128)(2,1)}), bf16[16,10,16,128]{3,2,1,0:T(8,128)(2,1)S(1)}, u32[]{:S(2)}, u32[]{:S(2)}) async-start(bf16[16,10,16,128]{3,2,1,0:T(8,128)(2,1)} %letters.1), calls=%async_computation.3 | async-start | bytes 1310720 | tf_op jit(solution)/shard_map/all_to_all | solution.py:353
  60.2 15.4 %collective-permute-start.10 = (bf16[1024,256]{1,0:T(8,128)(2,1)}, bf16[1024,256]{1,0:T(8,128)(2,1)S(1)}, u32[]{:S(2)}, u32[]{:S(2)}) collective-permute-start(bf16[1024,256]{1,0:T(8,128)(2,1)} %collective-permute-done.9.b2), channel_id=1, source_target_pairs={{0,224},{32,0},{64,32},{96,64},{128,96},{160,128},{192,160},{224,1... | collective-permute-start | bytes 1572872 | tf_op jit(solution)/shard_map/ppermute | solution.py:30
  63.1 12.9 %collective-permute-start.7 = (bf16[1024,256]{1,0:T(8,128)(2,1)}, bf16[1024,256]{1,0:T(8,128)(2,1)S(1)}, u32[]{:S(2)}, u32[]{:S(2)}) collective-permute-start(bf16[1024,256]{1,0:T(8,128)(2,1)} %collective-permute-done.6.f2), channel_id=1, source_target_pairs={{0,32},{32,64},{64,96},{96,128},{128,160},{160,192},{192,224},{224... | collective-permute-start | bytes 1572872 | tf_op jit(solution)/shard_map/ppermute | solution.py:30
  70.0 13.8 %collective-permute-start.1 = (bf16[16,10,16,128]{3,2,1,0:T(8,128)(2,1)S(1)}, bf16[16,10,16,128]{3,2,1,0:T(8,128)(2,1)S(1)}, u32[]{:S(2)}, u32[]{:S(2)}) collective-permute-start(bf16[16,10,16,128]{3,2,1,0:T(8,128)(2,1)S(1)} %all-to-all-done.3.near_ref), channel_id=1, source_target_pairs={{0,1},{1,0},{2,3},{3,2},{4,5},{5,4},{6,7},{7,6},{8,9},{9,8},{10,11... | collective-permute-start | bytes 1966088 | tf_op jit(solution)/shard_map/ppermute | solution.py:34
  75.6 8.1 %collective-permute-start.12 = (bf16[512,256]{1,0:T(8,128)(2,1)S(1)}, bf16[512,256]{1,0:T(8,128)(2,1)S(1)}, u32[]{:S(2)}, u32[]{:S(2)}) collective-permute-start(bf16[512,256]{1,0:T(8,128)(2,1)S(1)} %slice.9), channel_id=1, source_target_pairs={{0,224},{32,0},{64,32},{96,64},{128,96},{160,128},{192,160},{224,1... | collective-permute-start | bytes 786440 | tf_op jit(solution)/shard_map/ppermute | solution.py:30
  76.0 7.7 %collective-permute-start.11 = (bf16[512,256]{1,0:T(8,128)(2,1)S(1)}, bf16[512,256]{1,0:T(8,128)(2,1)S(1)}, u32[]{:S(2)}, u32[]{:S(2)}) collective-permute-start(bf16[512,256]{1,0:T(8,128)(2,1)S(1)} %slice.8), channel_id=1, source_target_pairs={{0,32},{32,64},{64,96},{96,128},{128,160},{160,192},{192,224},{224... | collective-permute-start | bytes 786440 | tf_op jit(solution)/shard_map/ppermute | solution.py:30

commit v3 on v1

--- a/solution.py
+++ b/solution.py
@@ -178,46 +178,35 @@
     )(own, far, cot)
 
 
-def fold_kernel(parts_ref, out_hbm, sums, sem):
-    sums[...] = jnp.sum(parts_ref[...].astype(jnp.float32), axis=0).astype(jnp.bfloat16)
-    copy = pltpu.make_async_copy(sums, out_hbm, sem)
-    copy.start()
-    copy.wait()
-
-
-def fold(parts):
-    shape = parts.shape[1:]
-    return pl.pallas_call(
-        fold_kernel,
-        in_specs=[VMEM],
-        out_specs=HBM,
-        out_shape=pltpu.HBM(shape, jnp.bfloat16),
-        scratch_shapes=[pltpu.VMEM(shape, jnp.bfloat16), pltpu.SemaphoreType.DMA],
-        compiler_params=limit(4),
-        name="fold",
-    )(parts)
-
-
-def copy_to_all(source, target, sems):
+def send(pairs, sems):
     copies = []
-    for slot in range(target.shape[0]):
-        copy = pltpu.make_async_copy(source, target.at[slot], sems.at[slot])
+    for slot, (source, target) in enumerate(pairs):
+        copy = pltpu.make_async_copy(source, target, sems.at[slot])
         copy.start()
         copies.append(copy)
     for copy in copies:
         copy.wait()
 
 
-def copies_of(array, count):
-    return pl.pallas_call(
-        copy_to_all,
-        in_specs=[VMEM],
+def fold_kernel(place_ref, parts_ref, first_ref, second_ref, out_hbm, letter_ref, sems):
+    rows = pl.ds(pl.multiple_of(place_ref[2] * 16, 16), 16)
+    letter_ref[:8] = jnp.sum(parts_ref[...].astype(jnp.float32), axis=0).astype(jnp.bfloat16)
+    letter_ref[8] = first_ref[rows, :].astype(jnp.bfloat16)
+    letter_ref[9] = second_ref[rows, :].astype(jnp.bfloat16)
+    send([(letter_ref, out_hbm.at[z]) for z in range(8)], sems)
+
+
+def fold(place, parts, first, second):
+    shape = (10, *parts.shape[2:])
+    return pl.pallas_call(
+        fold_kernel,
+        in_specs=[SMEM] + [VMEM] * 3,
         out_specs=HBM,
-        out_shape=pltpu.HBM((count, *array.shape), array.dtype),
-        scratch_shapes=[pltpu.SemaphoreType.DMA((count,))],
-        compiler_params=limit(4),
-        name="copies",
-    )(array)
+        out_shape=pltpu.HBM((8, *shape), jnp.bfloat16),
+        scratch_shapes=[pltpu.VMEM(shape, jnp.bfloat16), pltpu.SemaphoreType.DMA((8,))],
+        compiler_params=limit(8),
+        name="fold",
+    )(place, parts, first, second)
 
 
 def moments(projected, first, second):
@@ -226,33 +215,37 @@
     return first_new, second_new
 
 
-def update_kernel(place_ref, pieces_ref, first_ref, second_ref, piece_ref, copies_hbm, direction_ref, sems):
-    rows = pl.ds(pl.multiple_of(place_ref[2] * 16, 16), 16)
-    piece = jnp.sum(pieces_ref[...].astype(jnp.float32), axis=0)
-    piece_ref[...] = piece
-    first_new, second_new = moments(piece, first_ref[rows, :], second_ref[rows, :])
-    direction_ref[...] = (first_new / (jnp.sqrt(second_new) + 1e-08)).astype(jnp.bfloat16)
-    copy_to_all(direction_ref, copies_hbm, sems)
-
-
-def update(place, pieces, first, second):
-    count, rows, rank = pieces.shape
+def update_kernel(place_ref, letters_ref, out_hbm, letter_ref, projected_ref, sems):
+    projected_ref[...] = jnp.sum(letters_ref[:, :8].astype(jnp.float32), axis=0)
+    first, second = letters_ref[:, 8].astype(jnp.float32), letters_ref[:, 9].astype(jnp.float32)
+    first_new, second_new = moments(projected_ref[...], first, second)
+    letter_ref[:8] = (first_new / (jnp.sqrt(second_new) + 1e-08)).astype(jnp.bfloat16)
+    mine = projected_ref[place_ref[0]]
+    high = mine.astype(jnp.bfloat16)
+    letter_ref[8] = high
+    letter_ref[9] = (mine - high.astype(jnp.float32)).astype(jnp.bfloat16)
+    send([(letter_ref, out_hbm.at[peer]) for peer in range(16)], sems)
+
+
+def update(place, letters):
+    shape = letters.shape[1:]
     return pl.pallas_call(
         update_kernel,
-        in_specs=[SMEM] + [VMEM] * 3,
-        out_specs=[VMEM, HBM],
-        out_shape=[
-            jax.ShapeDtypeStruct((rows, rank), jnp.float32),
-            pltpu.HBM(pieces.shape, jnp.bfloat16),
-        ],
-        scratch_shapes=[pltpu.VMEM((rows, rank), jnp.bfloat16), pltpu.SemaphoreType.DMA((count,))],
-        compiler_params=limit(4),
+        in_specs=[SMEM, VMEM],
+        out_specs=HBM,
+        out_shape=pltpu.HBM((16, *shape), jnp.bfloat16),
+        scratch_shapes=[
+            pltpu.VMEM(shape, jnp.bfloat16),
+            pltpu.VMEM((8, *shape[1:]), jnp.float32),
+            pltpu.SemaphoreType.DMA((16,)),
+        ],
+        compiler_params=limit(8),
         name="update",
-    )(place, pieces, first, second)
+    )(place, letters)
 
 
 def finish_kernel(
-    place_ref, basis_hbm, weight_hbm, first_hbm, second_hbm, p0, p1, p2, p3, near_ref, far_ref,
+    place_ref, basis_hbm, weight_hbm, first_hbm, second_hbm, near_ref, far_ref,
     w0, f1, f2, f3, b1, b2, b3, h1, h2,
     new_ref, step_ref, copy_ref, first_out, second_out,
     basis_ref, weight_ref, first_ref, second_ref, tiles, sems,
@@ -264,9 +257,9 @@
         copy = pltpu.make_async_copy(source, target, sems.at[8 + slot])
         copy.start()
         fetched.append(copy)
-    z, y, x = place_ref[0], place_ref[1], place_ref[2]
+    z, y = place_ref[0], place_ref[1]
     is_low = place_ref[3] == 0
-    near, far = near_ref[...].astype(jnp.float32), far_ref[...].astype(jnp.float32)
+    near, far = near_ref[:, :8].astype(jnp.float32), far_ref[:, :8].astype(jnp.float32)
     energy = jnp.sum(near * near + far * far)
     count = 2 * near.shape[0] * near.shape[1] * near.shape[2] * near.shape[3]
     spread = jnp.sqrt(jnp.full((1, 128), energy / count, jnp.float32))
@@ -301,21 +294,23 @@
     step = dot(rows_of(near_ref[mine, z], far_ref[mine, z]), basis, 1, 1) * scale
     step_ref[...] = step
     new_ref[...] = weight_ref[...] + step
-    for hops, piece in enumerate((p0, p1, p2, p3)):
-        rows = pl.ds(pl.multiple_of((x + 4 - hops) % 4 * 16, 16), 16)
-        first_new, second_new = moments(piece[...], first_ref[rows, :], second_ref[rows, :])
+    for source in range(4):
+        rows = pl.ds(source * 16, 16)
+        letter = y * 4 + source
+        piece = near_ref[letter, 8].astype(jnp.float32) + near_ref[letter, 9].astype(jnp.float32)
+        first_new, second_new = moments(piece, first_ref[rows, :], second_ref[rows, :])
         first_out[rows, :] = first_new
         second_out[rows, :] = second_new
     for copy in copies:
         copy.wait()
 
 
-def finish(place, basis, weight, first, second, pieces, near, far, blocks):
+def finish(place, basis, weight, first, second, near, far, blocks):
     values = basis.shape[0]
     like = lambda array: jax.ShapeDtypeStruct(array.shape, jnp.float32)
     return pl.pallas_call(
         finish_kernel,
-        in_specs=[SMEM] + [HBM] * 4 + [VMEM] * (6 + len(blocks)),
+        in_specs=[SMEM] + [HBM] * 4 + [VMEM] * (2 + len(blocks)),
         out_specs=[VMEM, VMEM, HBM, VMEM, VMEM],
         out_shape=[
             like(weight),
@@ -334,7 +329,7 @@
         ],
         compiler_params=limit(16),
         name="finish",
-    )(place, *in_hbm(basis, weight, first, second), *pieces, near, far, *in_vmem(*blocks))
+    )(place, *in_hbm(basis, weight, first, second), near, far, *in_vmem(*blocks))
 
 
 def exchange(array, axes):
@@ -354,14 +349,11 @@
     h1, h2 = shift(f3[:lead], "z", 1), shift(b3[lead:], "z", -1)
 
     parts = gradient(own, swap_cores(sent), out_cotangent)
-    folded = fold(exchange(parts, ("y", "x")))
-    piece, copies = update(place, exchange(folded, "z"), first_moment, second_moment)
-    pieces = [piece] + [shift(piece, "x", hops) for hops in (1, 2, 3)]
-    column = exchange(copies, "z")
-    near = exchange(copies_of(column, 16), ("y", "x"))
+    sums = fold(place, exchange(parts, ("y", "x")), first_moment, second_moment)
+    near = exchange(update(place, exchange(sums, "z")), ("y", "x"))
     far = swap_cores(near)
     weight_new, step_out, weight_copy, first_new, second_new = finish(
-        place, basis, turned, first_moment, second_moment, pieces, near, far, (w0, f1, f2, f3, b1, b2, b3, h1, h2)
+        place, basis, turned, first_moment, second_moment, near, far, (w0, f1, f2, f3, b1, b2, b3, h1, h2)
     )
     return (weight_new.T, weight_copy, step_out.T, first_new, second_new)
 

time: 103 us -> 99 us (0.961)
  the two profiles are of different devices: /device:TPU:16 before, /device:TPU:2 now
where the time goes in v3:
time: 99 us; the launch traced here: 98.5 us
  waiting for transfers between devices  44 us (44%)
  starting transfers between devices  38.4 us (39%)
  Pallas kernels  15.2 us (15%)
    ppermute x11, waiting for transfers between devices, shift(): lax.ppermute(array, axis, [(i, (i + hops) % count) for i in range(count)])  33 us
    all_to_all x3, starting transfers between devices, exchange(): return lax.all_to_all(array, axes, 0, 0, tiled=True)  21.2 us
    ppermute x11, starting transfers between devices, shift(): lax.ppermute(array, axis, [(i, (i + hops) % count) for i in range(count)])  17.2 us
    all_to_all x3, waiting for transfers between devices, exchange(): return lax.all_to_all(array, axes, 0, 0, tiled=True)  9.59 us
    pallas_call x1, Pallas kernels, finish(): pl.pallas_call(finish_kernel, in_specs=[SMEM] + [HBM] * 4 + [VMEM] * (2 +...  5.86 us
    pallas_call x1, Pallas kernels, heads(): pl.pallas_call(heads_kernel, in_specs=[SMEM] + [HBM] * 6, out_specs=[VMEM...  4.14 us
  transfers between devices with their start and end apart: 16, of which 8 were waited for; matrix products, arithmetic and copies ran while one was open for 0% of the time, Pallas kernels for 4%

profile of v3, /device:TPU:2, one launch (start us, length us, event | category | flops | bytes accessed | tf_op | source)
XLA Modules:
  0.0 98.5 jit_solution(12730013641192128103)
XLA Ops:
  0.6 0.0 copy-start
  0.6 0.1 pad_add_fusion.place_ref
  0.7 4.1 %heads.1 = (f32[768,128]{1,0:T(8,128)S(1)}, bf16[768,128]{1,0:T(8,128)(2,1)S(1)}, bf16[64,1024]{1,0:T(8,128)(2,1)S(1)}) custom-call(s32[4]{0:T(128)S(1)} %pad_add_fusion.place_ref, f32[1,4]{1,0:T(1,128)} %bitcast.12, bf16[768,1024]{1,0:T(8,128)(2,1)} %first_hbm.2, bf16[768,1024]{1,0:T(8,128)(2,1)} %second_hbm.2, f32[1,256]{1,0:T(1,128)} %bitcast.11, ...), custom_call_target="tpu_custom_call" | custom-call | tf_op jit(solution)/shard_map/heads/pallas_call | solution.py:105
  4.9 0.0 copy-start.1
  4.9 0.0 copy-start.2
  4.9 0.1 collective-permute-start
  5.0 1.4 %collective-permute-done.far_ref = bf16[768,128]{1,0:T(8,128)(2,1)S(1)} collective-permute-done((bf16[768,128]{1,0:T(8,128)(2,1)S(1)}, bf16[768,128]{1,0:T(8,128)(2,1)S(1)}, u32[]{:S(2)}, u32[]{:S(2)}) %collective-permute-start) | collective-permute-done | bytes 196640 | tf_op jit(solution)/shard_map/ppermute | solution.py:34
  6.4 0.0 copy-done
  6.4 1.4 %gradient.1 = bf16[16,8,16,128]{3,2,1,0:T(8,128)(2,1)} custom-call(f32[768,128]{1,0:T(8,128)S(1)} %get-tuple-element.13.own_ref, bf16[768,128]{1,0:T(8,128)(2,1)S(1)} %collective-permute-done.far_ref, bf16[768,2048]{1,0:T(8,128)(2,1)S(1)} %copy-done), custom_call_target="tpu_custom_call" | custom-call | tf_op jit(solution)/shard_map/gradient/pallas_call | solution.py:170
  7.8 7.5 %all-to-all-start = ((bf16[16,8,16,128]{3,2,1,0:T(8,128)(2,1)}), bf16[16,8,16,128]{3,2,1,0:T(8,128)(2,1)S(1)}, u32[]{:S(2)}, u32[]{:S(2)}) async-start(bf16[16,8,16,128]{3,2,1,0:T(8,128)(2,1)} %gradient.1), calls=%async_computation | async-start | bytes 1048576 | tf_op jit(solution)/shard_map/all_to_all | solution.py:336
  15.3 2.7 %collective-permute-start.4 = (bf16[64,1024]{1,0:T(8,128)(2,1)S(1)}, bf16[64,1024]{1,0:T(8,128)(2,1)S(1)}, u32[]{:S(2)}, u32[]{:S(2)}) collective-permute-start(bf16[64,1024]{1,0:T(8,128)(2,1)S(1)} %get-tuple-element.15.own_ref), channel_id=1, source_target_pairs={{0,24},{8,0},{16,8},{24,16},{1,25},{9,1},{17,9},{25,17},{2,26},{10... | collective-permute-start | bytes 393224 | tf_op jit(solution)/shard_map/ppermute | solution.py:30
  18.0 0.9 collective-permute-start.3
  18.9 0.9 collective-permute-start.2
  19.7 6.4 %all-to-all-done.parts_ref = bf16[16,8,16,128]{3,2,1,0:T(8,128)(2,1)S(1)} async-done(((bf16[16,8,16,128]{3,2,1,0:T(8,128)(2,1)}), bf16[16,8,16,128]{3,2,1,0:T(8,128)(2,1)S(1)}, u32[]{:S(2)}, u32[]{:S(2)}) %all-to-all-start) | async-done | bytes 524320 | tf_op jit(solution)/shard_map/all_to_all | solution.py:336
  26.1 0.0 copy-done.1
  26.1 0.0 copy-done.2
  26.1 1.4 %fold.1 = bf16[8,10,16,128]{3,2,1,0:T(8,128)(2,1)} custom-call(s32[4]{0:T(128)S(1)} %pad_add_fusion.place_ref, bf16[16,8,16,128]{3,2,1,0:T(8,128)(2,1)S(1)} %all-to-all-done.parts_ref, f32[64,128]{1,0:T(8,128)S(1)} %copy-done.1, f32[64,128]{1,0:T(8,128)S(1)} %copy-done.2), custom_call_target="tpu_custom_call" | custom-call | tf_op jit(solution)/shard_map/fold/pallas_call | solution.py:201
  27.5 8.5 %all-to-all-start.1 = ((bf16[8,10,16,128]{3,2,1,0:T(8,128)(2,1)}), bf16[8,10,16,128]{3,2,1,0:T(8,128)(2,1)S(1)}, u32[]{:S(2)}, u32[]{:S(2)}) async-start(bf16[8,10,16,128]{3,2,1,0:T(8,128)(2,1)} %fold.1), calls=%async_computation.1 | async-start | bytes 655360 | tf_op jit(solution)/shard_map/all_to_all | solution.py:336
  36.0 0.0 collective-permute-done.4.three_ref
  36.0 0.0 collective-permute-done.3.two_ref
  36.0 0.0 collective-permute-done.2.one_ref
  36.1 0.8 widen.1.w0
  36.9 3.3 %collective-permute-start.8 = (bf16[1024,256]{1,0:T(8,128)(2,1)S(1)}, bf16[1024,256]{1,0:T(8,128)(2,1)S(1)}, u32[]{:S(2)}, u32[]{:S(2)}) collective-permute-start(bf16[1024,256]{1,0:T(8,128)(2,1)S(1)} %widen.1.w0), channel_id=1, source_target_pairs={{0,224},{32,0},{64,32},{96,64},{128,96},{160,128},{192,160},{224,1... | collective-permute-start | bytes 1572872 | tf_op jit(solution)/shard_map/ppermute | solution.py:30
  40.2 0.0 collective-permute-start.5
  40.2 15.2 %collective-permute-done.8.b1 = bf16[1024,256]{1,0:T(8,128)(2,1)S(1)} collective-permute-done((bf16[1024,256]{1,0:T(8,128)(2,1)S(1)}, bf16[1024,256]{1,0:T(8,128)(2,1)S(1)}, u32[]{:S(2)}, u32[]{:S(2)}) %collective-permute-start.8) | collective-permute-done | bytes 524320 | tf_op jit(solution)/shard_map/ppermute | solution.py:30
  55.4 1.8 %collective-permute-start.9 = (bf16[1024,256]{1,0:T(8,128)(2,1)S(1)}, bf16[1024,256]{1,0:T(8,128)(2,1)}, u32[]{:S(2)}, u32[]{:S(2)}) collective-permute-start(bf16[1024,256]{1,0:T(8,128)(2,1)S(1)} %collective-permute-done.8.b1), channel_id=1, source_target_pairs={{0,224},{32,0},{64,32},{96,64},{128,96},{160,128},{192,160},{224,1... | collective-permute-start | bytes 1572872 | tf_op jit(solution)/shard_map/ppermute | solution.py:30
  57.2 0.0 collective-permute-done.5.f1
  57.2 0.2 collective-permute-start.6
  57.4 0.0 all-to-all-done.1.letters_ref
  57.4 1.6 %update.1 = bf16[16,10,16,128]{3,2,1,0:T(8,128)(2,1)} custom-call(s32[4]{0:T(128)S(1)} %pad_add_fusion.place_ref, bf16[8,10,16,128]{3,2,1,0:T(8,128)(2,1)S(1)} %all-to-all-done.1.letters_ref), custom_call_target="tpu_custom_call" | custom-call | tf_op jit(solution)/shard_map/update/pallas_call | solution.py:232
  59.0 5.2 %all-to-all-start.2 = ((bf16[16,10,16,128]{3,2,1,0:T(8,128)(2,1)}), bf16[16,10,16,128]{3,2,1,0:T(8,128)(2,1)S(1)}, u32[]{:S(2)}, u32[]{:S(2)}) async-start(bf16[16,10,16,128]{3,2,1,0:T(8,128)(2,1)} %update.1), calls=%async_computation.2 | async-start | bytes 1310720 | tf_op jit(solution)/shard_map/all_to_all | solution.py:336
  64.2 3.5 %collective-permute-done.9.b2 = bf16[1024,256]{1,0:T(8,128)(2,1)} collective-permute-done((bf16[1024,256]{1,0:T(8,128)(2,1)S(1)}, bf16[1024,256]{1,0:T(8,128)(2,1)}, u32[]{:S(2)}, u32[]{:S(2)}) %collective-permute-start.9) | collective-permute-done | bytes 524320 | tf_op jit(solution)/shard_map/ppermute | solution.py:30
  67.7 3.7 %collective-permute-start.10 = (bf16[1024,256]{1,0:T(8,128)(2,1)}, bf16[1024,256]{1,0:T(8,128)(2,1)S(1)}, u32[]{:S(2)}, u32[]{:S(2)}) collective-permute-start(bf16[1024,256]{1,0:T(8,128)(2,1)} %collective-permute-done.9.b2), channel_id=1, source_target_pairs={{0,224},{32,0},{64,32},{96,64},{128,96},{160,128},{192,160},{224,1... | collective-permute-start | bytes 1572872 | tf_op jit(solution)/shard_map/ppermute | solution.py:30
  71.4 0.0 collective-permute-done.6.f2
  71.4 0.0 collective-permute-start.7
  71.4 3.2 %all-to-all-done.2.near_ref = bf16[16,10,16,128]{3,2,1,0:T(8,128)(2,1)S(1)} async-done(((bf16[16,10,16,128]{3,2,1,0:T(8,128)(2,1)}), bf16[16,10,16,128]{3,2,1,0:T(8,128)(2,1)S(1)}, u32[]{:S(2)}, u32[]{:S(2)}) %all-to-all-start.2) | async-done | bytes 655392 | tf_op jit(solution)/shard_map/all_to_all | solution.py:336
  74.6 0.0 collective-permute-start.1
  74.6 6.7 %collective-permute-done.10.b3 = bf16[1024,256]{1,0:T(8,128)(2,1)S(1)} collective-permute-done((bf16[1024,256]{1,0:T(8,128)(2,1)}, bf16[1024,256]{1,0:T(8,128)(2,1)S(1)}, u32[]{:S(2)}, u32[]{:S(2)}) %collective-permute-start.10) | collective-permute-done | bytes 524320 | tf_op jit(solution)/shard_map/ppermute | solution.py:30
  81.3 3.7 %collective-permute-start.12 = (bf16[512,256]{1,0:T(8,128)(2,1)S(1)}, bf16[512,256]{1,0:T(8,128)(2,1)S(1)}, u32[]{:S(2)}, u32[]{:S(2)}) collective-permute-start(bf16[512,256]{1,0:T(8,128)(2,1)S(1)} %slice.9), channel_id=1, source_target_pairs={{0,224},{32,0},{64,32},{96,64},{128,96},{160,128},{192,160},{224,1... | collective-permute-start | bytes 786440 | tf_op jit(solution)/shard_map/ppermute | solution.py:30
  85.0 0.0 collective-permute-done.7.f3
  85.0 0.1 collective-permute-start.11
  85.1 3.8 %collective-permute-done.12.h2 = bf16[512,256]{1,0:T(8,128)(2,1)S(1)} collective-permute-done((bf16[512,256]{1,0:T(8,128)(2,1)S(1)}, bf16[512,256]{1,0:T(8,128)(2,1)S(1)}, u32[]{:S(2)}, u32[]{:S(2)}) %collective-permute-start.12) | collective-permute-done | bytes 262176 | tf_op jit(solution)/shard_map/ppermute | solution.py:30
  88.9 3.8 %collective-permute-done.11.h1 = bf16[512,256]{1,0:T(8,128)(2,1)S(1)} collective-permute-done((bf16[512,256]{1,0:T(8,128)(2,1)S(1)}, bf16[512,256]{1,0:T(8,128)(2,1)S(1)}, u32[]{:S(2)}, u32[]{:S(2)}) %collective-permute-start.11) | collective-permute-done | bytes 262176 | tf_op jit(solution)/shard_map/ppermute | solution.py:30
  92.7 0.0 collective-permute-done.1.far_ref
  92.7 5.9 %finish.1 = (f32[64,1024]{1,0:T(8,128)}, f32[64,1024]{1,0:T(8,128)}, bf16[1024,2048]{1,0:T(8,128)(2,1)}, f32[64,128]{1,0:T(8,128)}, f32[64,128]{1,0:T(8,128)}) custom-call(s32[4]{0:T(128)S(1)} %pad_add_fusion.place_ref, bf16[1024,256]{1,0:T(8,128)(2,1)} %basis_hbm.3, f32[64,1024]{1,0:T(8,128)} %bitcast.10, f32[64,128]{1,0:T(8,128)} %first_hbm.3, ...), custom_call_target="tpu_custom_call" | custom-call | tf_op jit(solution)/shard_map/finish/pallas_call | solution.py:311
  (2 shorter events, 0.0 us)
Async XLA Ops:
  0.6 5.8 %copy-start = (bf16[768,2048]{1,0:T(8,128)(2,1)S(1)}, bf16[768,2048]{1,0:T(8,128)(2,1)}, u32[]{:S(2)}) copy-start(bf16[768,2048]{1,0:T(8,128)(2,1)} %cot_ref.1) | copy-start | bytes 9437188
  4.9 21.3 %copy-start.1 = (f32[64,128]{1,0:T(8,128)S(1)}, f32[64,128]{1,0:T(8,128)}, u32[]{:S(2)}) copy-start(f32[64,128]{1,0:T(8,128)} %first_hbm.3) | copy-start | bytes 98308
  4.9 21.3 %copy-start.2 = (f32[64,128]{1,0:T(8,128)S(1)}, f32[64,128]{1,0:T(8,128)}, u32[]{:S(2)}) copy-start(f32[64,128]{1,0:T(8,128)} %second_hbm.3) | copy-start | bytes 98308
  4.9 1.5 %collective-permute-start = (bf16[768,128]{1,0:T(8,128)(2,1)S(1)}, bf16[768,128]{1,0:T(8,128)(2,1)S(1)}, u32[]{:S(2)}, u32[]{:S(2)}) collective-permute-start(bf16[768,128]{1,0:T(8,128)(2,1)S(1)} %get-tuple-element.14), channel_id=1, source_target_pairs={{0,1},{1,0},{2,3},{3,2},{4,5},{5,4},{6,7},{7,6},{8,9},{9,8},{10,11... | collective-permute-start | bytes 589832 | tf_op jit(solution)/shard_map/ppermute | solution.py:34
  7.8 18.3 %all-to-all-start = ((bf16[16,8,16,128]{3,2,1,0:T(8,128)(2,1)}), bf16[16,8,16,128]{3,2,1,0:T(8,128)(2,1)S(1)}, u32[]{:S(2)}, u32[]{:S(2)}) async-start(bf16[16,8,16,128]{3,2,1,0:T(8,128)(2,1)} %gradient.1), calls=%async_computation | async-start | bytes 1048576 | tf_op jit(solution)/shard_map/all_to_all | solution.py:336
  15.3 20.7 %collective-permute-start.4 = (bf16[64,1024]{1,0:T(8,128)(2,1)S(1)}, bf16[64,1024]{1,0:T(8,128)(2,1)S(1)}, u32[]{:S(2)}, u32[]{:S(2)}) collective-permute-start(bf16[64,1024]{1,0:T(8,128)(2,1)S(1)} %get-tuple-element.15.own_ref), channel_id=1, source_target_pairs={{0,24},{8,0},{16,8},{24,16},{1,25},{9,1},{17,9},{25,17},{2,26},{10... | collective-permute-start | bytes 393224 | tf_op jit(solution)/shard_map/ppermute | solution.py:30
  18.0 18.0 %collective-permute-start.3 = (bf16[64,1024]{1,0:T(8,128)(2,1)S(1)}, bf16[64,1024]{1,0:T(8,128)(2,1)S(1)}, u32[]{:S(2)}, u32[]{:S(2)}) collective-permute-start(bf16[64,1024]{1,0:T(8,128)(2,1)S(1)} %get-tuple-element.15.own_ref), channel_id=1, source_target_pairs={{0,16},{8,24},{16,0},{24,8},{1,17},{9,25},{17,1},{25,9},{2,18},{10... | collective-permute-start | bytes 393224 | tf_op jit(solution)/shard_map/ppermute | solution.py:30
  18.9 17.2 %collective-permute-start.2 = (bf16[64,1024]{1,0:T(8,128)(2,1)S(1)}, bf16[64,1024]{1,0:T(8,128)(2,1)S(1)}, u32[]{:S(2)}, u32[]{:S(2)}) collective-permute-start(bf16[64,1024]{1,0:T(8,128)(2,1)S(1)} %get-tuple-element.15.own_ref), channel_id=1, source_target_pairs={{0,8},{8,16},{16,24},{24,0},{1,9},{9,17},{17,25},{25,1},{2,10},{10... | collective-permute-start | bytes 393224 | tf_op jit(solution)/shard_map/ppermute | solution.py:30
  27.5 29.9 %all-to-all-start.1 = ((bf16[8,10,16,128]{3,2,1,0:T(8,128)(2,1)}), bf16[8,10,16,128]{3,2,1,0:T(8,128)(2,1)S(1)}, u32[]{:S(2)}, u32[]{:S(2)}) async-start(bf16[8,10,16,128]{3,2,1,0:T(8,128)(2,1)} %fold.1), calls=%async_computation.1 | async-start | bytes 655360 | tf_op jit(solution)/shard_map/all_to_all | solution.py:336
  36.9 18.5 %collective-permute-start.8 = (bf16[1024,256]{1,0:T(8,128)(2,1)S(1)}, bf16[1024,256]{1,0:T(8,128)(2,1)S(1)}, u32[]{:S(2)}, u32[]{:S(2)}) collective-permute-start(bf16[1024,256]{1,0:T(8,128)(2,1)S(1)} %widen.1.w0), channel_id=1, source_target_pairs={{0,224},{32,0},{64,32},{96,64},{128,96},{160,128},{192,160},{224,1... | collective-permute-start | bytes 1572872 | tf_op jit(solution)/shard_map/ppermute | solution.py:30
  40.2 17.0 %collective-permute-start.5 = (bf16[1024,256]{1,0:T(8,128)(2,1)S(1)}, bf16[1024,256]{1,0:T(8,128)(2,1)S(1)}, u32[]{:S(2)}, u32[]{:S(2)}) collective-permute-start(bf16[1024,256]{1,0:T(8,128)(2,1)S(1)} %widen.1.w0), channel_id=1, source_target_pairs={{0,32},{32,64},{64,96},{96,128},{128,160},{160,192},{192,224},{224... | collective-permute-start | bytes 1572872 | tf_op jit(solution)/shard_map/ppermute | solution.py:30
  55.4 12.3 %collective-permute-start.9 = (bf16[1024,256]{1,0:T(8,128)(2,1)S(1)}, bf16[1024,256]{1,0:T(8,128)(2,1)}, u32[]{:S(2)}, u32[]{:S(2)}) collective-permute-start(bf16[1024,256]{1,0:T(8,128)(2,1)S(1)} %collective-permute-done.8.b1), channel_id=1, source_target_pairs={{0,224},{32,0},{64,32},{96,64},{128,96},{160,128},{192,160},{224,1... | collective-permute-start | bytes 1572872 | tf_op jit(solution)/shard_map/ppermute | solution.py:30
  57.2 14.2 %collective-permute-start.6 = (bf16[1024,256]{1,0:T(8,128)(2,1)S(1)}, bf16[1024,256]{1,0:T(8,128)(2,1)}, u32[]{:S(2)}, u32[]{:S(2)}) collective-permute-start(bf16[1024,256]{1,0:T(8,128)(2,1)S(1)} %collective-permute-done.5.f1), channel_id=1, source_target_pairs={{0,32},{32,64},{64,96},{96,128},{128,160},{160,192},{192,224},{224... | collective-permute-start | bytes 1572872 | tf_op jit(solution)/shard_map/ppermute | solution.py:30
  59.0 15.6 %all-to-all-start.2 = ((bf16[16,10,16,128]{3,2,1,0:T(8,128)(2,1)}), bf16[16,10,16,128]{3,2,1,0:T(8,128)(2,1)S(1)}, u32[]{:S(2)}, u32[]{:S(2)}) async-start(bf16[16,10,16,128]{3,2,1,0:T(8,128)(2,1)} %update.1), calls=%async_computation.2 | async-start | bytes 1310720 | tf_op jit(solution)/shard_map/all_to_all | solution.py:336
  67.7 13.6 %collective-permute-start.10 = (bf16[1024,256]{1,0:T(8,128)(2,1)}, bf16[1024,256]{1,0:T(8,128)(2,1)S(1)}, u32[]{:S(2)}, u32[]{:S(2)}) collective-permute-start(bf16[1024,256]{1,0:T(8,128)(2,1)} %collective-permute-done.9.b2), channel_id=1, source_target_pairs={{0,224},{32,0},{64,32},{96,64},{128,96},{160,128},{192,160},{224,1... | collective-permute-start | bytes 1572872 | tf_op jit(solution)/shard_map/ppermute | solution.py:30
  71.4 13.6 %collective-permute-start.7 = (bf16[1024,256]{1,0:T(8,128)(2,1)}, bf16[1024,256]{1,0:T(8,128)(2,1)S(1)}, u32[]{:S(2)}, u32[]{:S(2)}) collective-permute-start(bf16[1024,256]{1,0:T(8,128)(2,1)} %collective-permute-done.6.f2), channel_id=1, source_target_pairs={{0,32},{32,64},{64,96},{96,128},{128,160},{160,192},{192,224},{224... | collective-permute-start | bytes 1572872 | tf_op jit(solution)/shard_map/ppermute | solution.py:30
  74.6 18.1 %collective-permute-start.1 = (bf16[16,10,16,128]{3,2,1,0:T(8,128)(2,1)S(1)}, bf16[16,10,16,128]{3,2,1,0:T(8,128)(2,1)S(1)}, u32[]{:S(2)}, u32[]{:S(2)}) collective-permute-start(bf16[16,10,16,128]{3,2,1,0:T(8,128)(2,1)S(1)} %all-to-all-done.2.near_ref), channel_id=1, source_target_pairs={{0,1},{1,0},{2,3},{3,2},{4,5},{5,4},{6,7},{7,6},{8,9},{9,8},{10,11... | collective-permute-start | bytes 1966088 | tf_op jit(solution)/shard_map/ppermute | solution.py:34
  81.3 7.6 %collective-permute-start.12 = (bf16[512,256]{1,0:T(8,128)(2,1)S(1)}, bf16[512,256]{1,0:T(8,128)(2,1)S(1)}, u32[]{:S(2)}, u32[]{:S(2)}) collective-permute-start(bf16[512,256]{1,0:T(8,128)(2,1)S(1)} %slice.9), channel_id=1, source_target_pairs={{0,224},{32,0},{64,32},{96,64},{128,96},{160,128},{192,160},{224,1... | collective-permute-start | bytes 786440 | tf_op jit(solution)/shard_map/ppermute | solution.py:30
  85.0 7.7 %collective-permute-start.11 = (bf16[512,256]{1,0:T(8,128)(2,1)S(1)}, bf16[512,256]{1,0:T(8,128)(2,1)S(1)}, u32[]{:S(2)}, u32[]{:S(2)}) collective-permute-start(bf16[512,256]{1,0:T(8,128)(2,1)S(1)} %slice.8), channel_id=1, source_target_pairs={{0,32},{32,64},{64,96},{96,128},{128,160},{160,192},{192,224},{224... | collective-permute-start | bytes 786440 | tf_op jit(solution)/shard_map/ppermute | solution.py:30

commit v4 on v3

--- a/solution.py
+++ b/solution.py
@@ -244,17 +244,20 @@
     )(place, letters)
 
 
+def columns(block):
+    return pl.ds(pl.multiple_of(block % 8 * 256, 256), 256)
+
+
 def finish_kernel(
-    place_ref, basis_hbm, weight_hbm, first_hbm, second_hbm, near_ref, far_ref,
-    w0, f1, f2, f3, b1, b2, b3, h1, h2,
-    new_ref, step_ref, copy_ref, first_out, second_out,
+    place_ref, basis_hbm, weight_hbm, first_hbm, second_hbm, near_ref, far_ref, w0, f1, f2, w4, b2, b1,
+    new_ref, step_ref, copy_ref, first_out, second_out, later_ref,
     basis_ref, weight_ref, first_ref, second_ref, tiles, sems,
 ):
     fetched = []
     for slot, (source, target) in enumerate(
         ((basis_hbm, basis_ref), (weight_hbm, weight_ref), (first_hbm, first_ref), (second_hbm, second_ref))
     ):
-        copy = pltpu.make_async_copy(source, target, sems.at[8 + slot])
+        copy = pltpu.make_async_copy(source, target, sems.at[6 + slot])
         copy.start()
         fetched.append(copy)
     z, y = place_ref[0], place_ref[1]
@@ -274,21 +277,18 @@
             [jnp.where(is_low, close, distant), jnp.where(is_low, distant, close)], axis=1
         )
 
+    def step_of(block):
+        at = block % 8
+        return dot(basis, rows_of(near_ref[:, at], far_ref[:, at]), 1, 1) * scale
+
     copies = []
-    for k, block in enumerate((w0, f1, f2, f3, b3, b2, b1, None)):
-        at = (z + 8 - (k if k < 4 else k + 1 if block is not None else 4)) % 8
-        wide = dot(basis, rows_of(near_ref[:, at], far_ref[:, at]), 1, 1) * scale
-        if block is None:
-            lead = wide.shape[0] // 2
-            tiles[k, :lead] = (h1[...].astype(jnp.float32) + wide[:lead]).astype(jnp.bfloat16)
-            tiles[k, lead:] = (h2[...].astype(jnp.float32) + wide[lead:]).astype(jnp.bfloat16)
-        else:
-            tiles[k] = (block[...].astype(jnp.float32) + wide).astype(jnp.bfloat16)
-        copy = pltpu.make_async_copy(
-            tiles.at[k], copy_ref.at[:, pl.ds(pl.multiple_of(at * 256, 256), 256)], sems.at[k]
-        )
+    for slot, (block, hops) in enumerate(((w0, 0), (f1, 7), (b1, 1), (f2, 6), (b2, 2), (w4, 4))):
+        tiles[slot] = (block[...].astype(jnp.float32) + step_of(z + hops)).astype(jnp.bfloat16)
+        copy = pltpu.make_async_copy(tiles.at[slot], copy_ref.at[:, columns(z + hops)], sems.at[slot])
         copy.start()
         copies.append(copy)
+    for slot, hops in enumerate((5, 3)):
+        later_ref[slot] = step_of(z + hops)
 
     mine = pl.ds(y * 4, 4)
     step = dot(rows_of(near_ref[mine, z], far_ref[mine, z]), basis, 1, 1) * scale
@@ -311,27 +311,53 @@
     return pl.pallas_call(
         finish_kernel,
         in_specs=[SMEM] + [HBM] * 4 + [VMEM] * (2 + len(blocks)),
-        out_specs=[VMEM, VMEM, HBM, VMEM, VMEM],
+        out_specs=[VMEM, VMEM, HBM, VMEM, VMEM, VMEM],
         out_shape=[
             like(weight),
             like(weight),
             pltpu.HBM((values, 2048), jnp.bfloat16),
             like(first),
             like(second),
+            pltpu.VMEM((2, values, 256), jnp.float32),
         ],
         scratch_shapes=[
             pltpu.VMEM(basis.shape, basis.dtype),
             pltpu.VMEM(weight.shape, weight.dtype),
             pltpu.VMEM(first.shape, first.dtype),
             pltpu.VMEM(second.shape, second.dtype),
-            pltpu.VMEM((8, values, 256), jnp.bfloat16),
-            pltpu.SemaphoreType.DMA((12,)),
+            pltpu.VMEM((6, values, 256), jnp.bfloat16),
+            pltpu.SemaphoreType.DMA((10,)),
         ],
         compiler_params=limit(16),
         name="finish",
     )(place, *in_hbm(basis, weight, first, second), near, far, *in_vmem(*blocks))
 
 
+def last_kernel(place_ref, later_ref, f3, b3, copy_in, copy_ref, tiles, sems):
+    z = place_ref[0]
+    copies = []
+    for slot, (block, hops) in enumerate(((f3, 5), (b3, 3))):
+        tiles[slot] = (block[...].astype(jnp.float32) + later_ref[slot]).astype(jnp.bfloat16)
+        copy = pltpu.make_async_copy(tiles.at[slot], copy_ref.at[:, columns(z + hops)], sems.at[slot])
+        copy.start()
+        copies.append(copy)
+    for copy in copies:
+        copy.wait()
+
+
+def last(place, later, f3, b3, copy):
+    return pl.pallas_call(
+        last_kernel,
+        in_specs=[SMEM, VMEM, VMEM, VMEM, HBM],
+        out_specs=HBM,
+        out_shape=pltpu.HBM(copy.shape, copy.dtype),
+        input_output_aliases={4: 0},
+        scratch_shapes=[pltpu.VMEM((2, copy.shape[0], 256), copy.dtype), pltpu.SemaphoreType.DMA((2,))],
+        compiler_params=limit(8),
+        name="last",
+    )(place, *in_vmem(later, f3, b3), *in_hbm(copy))
+
+
 def exchange(array, axes):
     return lax.all_to_all(array, axes, 0, 0, tiled=True)
 
@@ -341,20 +367,21 @@
     turned = weight.T
     own, sent, narrow = heads(place, lambda_head, first_mix, second_mix, head_gain, basis, turned)
 
-    lead = turned.shape[1] // 2
     w0 = widen(place, [narrow] + [shift(narrow, "y", hops) for hops in (1, 2, 3)])
+    opposite = shift(narrow, "z", 4)
+    w4 = widen(place, [opposite] + [shift(opposite, "y", hops) for hops in (1, 2, 3)])
     f1, b1 = shift(w0, "z", 1), shift(w0, "z", -1)
     f2, b2 = shift(f1, "z", 1), shift(b1, "z", -1)
     f3, b3 = shift(f2, "z", 1), shift(b2, "z", -1)
-    h1, h2 = shift(f3[:lead], "z", 1), shift(b3[lead:], "z", -1)
 
     parts = gradient(own, swap_cores(sent), out_cotangent)
     sums = fold(place, exchange(parts, ("y", "x")), first_moment, second_moment)
     near = exchange(update(place, exchange(sums, "z")), ("y", "x"))
     far = swap_cores(near)
-    weight_new, step_out, weight_copy, first_new, second_new = finish(
-        place, basis, turned, first_moment, second_moment, near, far, (w0, f1, f2, f3, b1, b2, b3, h1, h2)
+    weight_new, step_out, most, first_new, second_new, later = finish(
+        place, basis, turned, first_moment, second_moment, near, far, (w0, f1, f2, w4, b2, b1)
     )
+    weight_copy = last(place, later, f3, b3, most)
     return (weight_new.T, weight_copy, step_out.T, first_new, second_new)
 
 

time: 99 us -> 114 us (1.15)
  the two profiles are of different devices: /device:TPU:2 before, /device:TPU:28 now
where the time goes in v4:
time: 114 us
  waiting for transfers between devices  43.9 us (39%)
  starting transfers between devices  37.3 us (33%)
  Pallas kernels  16.8 us (15%)
  blocking collectives  14.8 us (13%)
    ppermute x13, waiting for transfers between devices, shift(): lax.ppermute(array, axis, [(i, (i + hops) % count) for i in range(count)])  40.8 us
    ppermute x13, starting transfers between devices, shift(): lax.ppermute(array, axis, [(i, (i + hops) % count) for i in range(count)])  21.7 us
    all_to_all x2, starting transfers between devices, exchange(): return lax.all_to_all(array, axes, 0, 0, tiled=True)  15.4 us
    all_to_all x1, blocking collectives, exchange(): return lax.all_to_all(array, axes, 0, 0, tiled=True)  14.8 us
    pallas_call x1, Pallas kernels, finish(): pl.pallas_call(finish_kernel, in_specs=[SMEM] + [HBM] * 4 + [VMEM] * (2 +...  5.01 us
    pallas_call x1, Pallas kernels, heads(): pl.pallas_call(heads_kernel, in_specs=[SMEM] + [HBM] * 6, out_specs=[VMEM...  4.14 us
  transfers between devices with their start and end apart: 17, of which 10 were waited for; matrix products, arithmetic and copies ran while one was open for 0% of the time, Pallas kernels for 7%

profile of v4, /device:TPU:28, one launch (start us, length us, event | category | flops | bytes accessed | tf_op | source)
XLA Modules:
  0.0 113.7 jit_solution(17789607247939787353)
XLA Ops:
  0.6 0.1 pad_add_fusion.place_ref
  0.7 4.1 %heads.1 = (f32[768,128]{1,0:T(8,128)S(1)}, bf16[768,128]{1,0:T(8,128)(2,1)S(1)}, bf16[64,1024]{1,0:T(8,128)(2,1)S(1)}) custom-call(s32[4]{0:T(128)S(1)} %pad_add_fusion.place_ref, f32[1,4]{1,0:T(1,128)} %bitcast.12, bf16[768,1024]{1,0:T(8,128)(2,1)} %first_hbm.2, bf16[768,1024]{1,0:T(8,128)(2,1)} %second_hbm.2, f32[1,256]{1,0:T(1,128)} %bitcast.11, ...), custom_call_target="tpu_custom_call" | custom-call | tf_op jit(solution)/shard_map/heads/pallas_call | solution.py:105
  4.9 0.0 copy-start.1
  4.9 0.0 copy-start.2
  4.9 0.1 collective-permute-start
  5.0 1.4 %collective-permute-done.far_ref = bf16[768,128]{1,0:T(8,128)(2,1)S(1)} collective-permute-done((bf16[768,128]{1,0:T(8,128)(2,1)S(1)}, bf16[768,128]{1,0:T(8,128)(2,1)S(1)}, u32[]{:S(2)}, u32[]{:S(2)}) %collective-permute-start) | collective-permute-done | bytes 196640 | tf_op jit(solution)/shard_map/ppermute | solution.py:34
  6.4 0.0 copy-done
  6.4 1.4 %gradient.1 = bf16[16,8,16,128]{3,2,1,0:T(8,128)(2,1)} custom-call(f32[768,128]{1,0:T(8,128)S(1)} %get-tuple-element.14.own_ref, bf16[768,128]{1,0:T(8,128)(2,1)S(1)} %collective-permute-done.far_ref, bf16[768,2048]{1,0:T(8,128)(2,1)S(1)} %copy-done), custom_call_target="tpu_custom_call" | custom-call | tf_op jit(solution)/shard_map/gradient/pallas_call | solution.py:170
  7.8 14.8 %all_to_all.15.parts_ref = bf16[16,8,16,128]{3,2,1,0:T(8,128)(2,1)S(1)} all-to-all(bf16[16,8,16,128]{3,2,1,0:T(8,128)(2,1)} %gradient.1), channel_id=1, replica_groups=mesh['z'=8,'y'=4,'x'=4,'tp'=2] {'y','x'}, dimensions={0} | all-to-all | bytes 1048576 | tf_op jit(solution)/shard_map/all_to_all | solution.py:362
  22.6 0.0 copy-done.1
  22.6 1.4 %fold.1 = bf16[8,10,16,128]{3,2,1,0:T(8,128)(2,1)} custom-call(s32[4]{0:T(128)S(1)} %pad_add_fusion.place_ref, bf16[16,8,16,128]{3,2,1,0:T(8,128)(2,1)S(1)} %all_to_all.15.parts_ref, f32[64,128]{1,0:T(8,128)S(1)} %copy-done.1, f32[64,128]{1,0:T(8,128)S(1)} %copy-done.2), custom_call_target="tpu_custom_call" | custom-call | tf_op jit(solution)/shard_map/fold/pallas_call | solution.py:201
  24.0 8.5 %all-to-all-start.1 = ((bf16[8,10,16,128]{3,2,1,0:T(8,128)(2,1)}), bf16[8,10,16,128]{3,2,1,0:T(8,128)(2,1)S(1)}, u32[]{:S(2)}, u32[]{:S(2)}) async-start(bf16[8,10,16,128]{3,2,1,0:T(8,128)(2,1)} %fold.1), calls=%async_computation.1 | async-start | bytes 655360 | tf_op jit(solution)/shard_map/all_to_all | solution.py:362
  32.5 2.1 %collective-permute-start.2 = (bf16[64,1024]{1,0:T(8,128)(2,1)S(1)}, bf16[64,1024]{1,0:T(8,128)(2,1)S(1)}, u32[]{:S(2)}, u32[]{:S(2)}) collective-permute-start(bf16[64,1024]{1,0:T(8,128)(2,1)S(1)} %get-tuple-element.16.own_ref), channel_id=1, source_target_pairs={{0,8},{8,16},{16,24},{24,0},{1,9},{9,17},{17,25},{25,1},{2,10},{10... | collective-permute-start | bytes 393224 | tf_op jit(solution)/shard_map/ppermute | solution.py:30
  34.6 0.9 collective-permute-start.3
  35.5 0.6 collective-permute-start.4
  36.1 3.7 %collective-permute-done.2.one_ref = bf16[64,1024]{1,0:T(8,128)(2,1)S(1)} collective-permute-done((bf16[64,1024]{1,0:T(8,128)(2,1)S(1)}, bf16[64,1024]{1,0:T(8,128)(2,1)S(1)}, u32[]{:S(2)}, u32[]{:S(2)}) %collective-permute-start.2) | collective-permute-done | bytes 131104 | tf_op jit(solution)/shard_map/ppermute | solution.py:30
  39.8 2.3 %collective-permute-done.3.two_ref = bf16[64,1024]{1,0:T(8,128)(2,1)S(1)} collective-permute-done((bf16[64,1024]{1,0:T(8,128)(2,1)S(1)}, bf16[64,1024]{1,0:T(8,128)(2,1)S(1)}, u32[]{:S(2)}, u32[]{:S(2)}) %collective-permute-start.3) | collective-permute-done | bytes 131104 | tf_op jit(solution)/shard_map/ppermute | solution.py:30
  42.0 1.4 %collective-permute-done.4.three_ref = bf16[64,1024]{1,0:T(8,128)(2,1)S(1)} collective-permute-done((bf16[64,1024]{1,0:T(8,128)(2,1)S(1)}, bf16[64,1024]{1,0:T(8,128)(2,1)S(1)}, u32[]{:S(2)}, u32[]{:S(2)}) %collective-permute-start.4) | collective-permute-done | bytes 131104 | tf_op jit(solution)/shard_map/ppermute | solution.py:30
  43.4 0.8 widen.2.w0
  44.3 1.8 %collective-permute-start.5 = (bf16[1024,256]{1,0:T(8,128)(2,1)S(1)}, bf16[1024,256]{1,0:T(8,128)(2,1)S(1)}, u32[]{:S(2)}, u32[]{:S(2)}) collective-permute-start(bf16[1024,256]{1,0:T(8,128)(2,1)S(1)} %widen.2.w0), channel_id=1, source_target_pairs={{0,32},{32,64},{64,96},{96,128},{128,160},{160,192},{192,224},{224... | collective-permute-start | bytes 1572872 | tf_op jit(solution)/shard_map/ppermute | solution.py:30
  46.1 1.5 %collective-permute-start.11 = (bf16[1024,256]{1,0:T(8,128)(2,1)S(1)}, bf16[1024,256]{1,0:T(8,128)(2,1)S(1)}, u32[]{:S(2)}, u32[]{:S(2)}) collective-permute-start(bf16[1024,256]{1,0:T(8,128)(2,1)S(1)} %widen.2.w0), channel_id=1, source_target_pairs={{0,224},{32,0},{64,32},{96,64},{128,96},{160,128},{192,160},{224,1... | collective-permute-start | bytes 1572872 | tf_op jit(solution)/shard_map/ppermute | solution.py:30
  47.6 0.0 all-to-all-done.1.letters_ref
  47.6 1.6 %update.1 = bf16[16,10,16,128]{3,2,1,0:T(8,128)(2,1)} custom-call(s32[4]{0:T(128)S(1)} %pad_add_fusion.place_ref, bf16[8,10,16,128]{3,2,1,0:T(8,128)(2,1)S(1)} %all-to-all-done.1.letters_ref), custom_call_target="tpu_custom_call" | custom-call | tf_op jit(solution)/shard_map/update/pallas_call | solution.py:232
  49.2 6.9 %all-to-all-start.2 = ((bf16[16,10,16,128]{3,2,1,0:T(8,128)(2,1)}), bf16[16,10,16,128]{3,2,1,0:T(8,128)(2,1)S(1)}, u32[]{:S(2)}, u32[]{:S(2)}) async-start(bf16[16,10,16,128]{3,2,1,0:T(8,128)(2,1)} %update.1), calls=%async_computation.2 | async-start | bytes 1310720 | tf_op jit(solution)/shard_map/all_to_all | solution.py:362
  56.1 2.6 %collective-permute-done.5.f1 = bf16[1024,256]{1,0:T(8,128)(2,1)S(1)} collective-permute-done((bf16[1024,256]{1,0:T(8,128)(2,1)S(1)}, bf16[1024,256]{1,0:T(8,128)(2,1)S(1)}, u32[]{:S(2)}, u32[]{:S(2)}) %collective-permute-start.5) | collective-permute-done | bytes 524320 | tf_op jit(solution)/shard_map/ppermute | solution.py:30
  58.7 0.3 collective-permute-start.6
  59.0 0.0 collective-permute-done.11.b1
  59.0 3.0 %collective-permute-start.12 = (bf16[1024,256]{1,0:T(8,128)(2,1)S(1)}, bf16[1024,256]{1,0:T(8,128)(2,1)S(1)}, u32[]{:S(2)}, u32[]{:S(2)}) collective-permute-start(bf16[1024,256]{1,0:T(8,128)(2,1)S(1)} %collective-permute-done.11.b1), channel_id=1, source_target_pairs={{0,224},{32,0},{64,32},{96,64},{128,96},{160,128},{192,160},{224,1... | collective-permute-start | bytes 1572872 | tf_op jit(solution)/shard_map/ppermute | solution.py:30
  62.0 1.7 %all-to-all-done.2.near_ref = bf16[16,10,16,128]{3,2,1,0:T(8,128)(2,1)S(1)} async-done(((bf16[16,10,16,128]{3,2,1,0:T(8,128)(2,1)}), bf16[16,10,16,128]{3,2,1,0:T(8,128)(2,1)S(1)}, u32[]{:S(2)}, u32[]{:S(2)}) %all-to-all-start.2) | async-done | bytes 655392 | tf_op jit(solution)/shard_map/all_to_all | solution.py:362
  63.7 0.0 collective-permute-start.1
  63.7 8.6 %collective-permute-done.6.f2 = bf16[1024,256]{1,0:T(8,128)(2,1)S(1)} collective-permute-done((bf16[1024,256]{1,0:T(8,128)(2,1)S(1)}, bf16[1024,256]{1,0:T(8,128)(2,1)S(1)}, u32[]{:S(2)}, u32[]{:S(2)}) %collective-permute-start.6) | collective-permute-done | bytes 524320 | tf_op jit(solution)/shard_map/ppermute | solution.py:30
  72.3 0.0 collective-permute-start.13
  72.3 0.0 collective-permute-done.12.b2
  72.3 3.2 %collective-permute-start.14 = (bf16[1024,256]{1,0:T(8,128)(2,1)S(1)}, bf16[1024,256]{1,0:T(8,128)(2,1)S(1)}, u32[]{:S(2)}, u32[]{:S(2)}) collective-permute-start(bf16[1024,256]{1,0:T(8,128)(2,1)S(1)} %collective-permute-done.12.b2), channel_id=1, source_target_pairs={{0,224},{32,0},{64,32},{96,64},{128,96},{160,128},{192,160},{224,1... | collective-permute-start | bytes 1572872 | tf_op jit(solution)/shard_map/ppermute | solution.py:30
  75.5 5.1 %collective-permute-start.7 = (bf16[64,1024]{1,0:T(8,128)(2,1)S(1)}, bf16[64,1024]{1,0:T(8,128)(2,1)S(1)}, u32[]{:S(2)}, u32[]{:S(2)}) collective-permute-start(bf16[64,1024]{1,0:T(8,128)(2,1)S(1)} %get-tuple-element.16.own_ref), channel_id=1, source_target_pairs={{0,128},{32,160},{64,192},{96,224},{128,0},{160,32},{192,64},{224,... | collective-permute-start | bytes 393224 | tf_op jit(solution)/shard_map/ppermute | solution.py:30
  80.6 11.8 %collective-permute-done.7.own_ref = bf16[64,1024]{1,0:T(8,128)(2,1)S(1)} collective-permute-done((bf16[64,1024]{1,0:T(8,128)(2,1)S(1)}, bf16[64,1024]{1,0:T(8,128)(2,1)S(1)}, u32[]{:S(2)}, u32[]{:S(2)}) %collective-permute-start.7) | collective-permute-done | bytes 131104 | tf_op jit(solution)/shard_map/ppermute | solution.py:30
  92.4 0.0 collective-permute-start.10
  92.4 3.2 %collective-permute-start.8 = (bf16[64,1024]{1,0:T(8,128)(2,1)S(1)}, bf16[64,1024]{1,0:T(8,128)(2,1)S(1)}, u32[]{:S(2)}, u32[]{:S(2)}) collective-permute-start(bf16[64,1024]{1,0:T(8,128)(2,1)S(1)} %collective-permute-done.7.own_ref), channel_id=1, source_target_pairs={{0,8},{8,16},{16,24},{24,0},{1,9},{9,17},{17,25},{25,1},{2,10},{10... | collective-permute-start | bytes 393224 | tf_op jit(solution)/shard_map/ppermute | solution.py:30
  95.7 4.0 %collective-permute-done.10.three_ref = bf16[64,1024]{1,0:T(8,128)(2,1)S(1)} collective-permute-done((bf16[64,1024]{1,0:T(8,128)(2,1)S(1)}, bf16[64,1024]{1,0:T(8,128)(2,1)S(1)}, u32[]{:S(2)}, u32[]{:S(2)}) %collective-permute-start.10) | collective-permute-done | bytes 131104 | tf_op jit(solution)/shard_map/ppermute | solution.py:30
  99.6 0.0 collective-permute-start.9
  99.6 0.0 collective-permute-done.8.one_ref
  99.6 6.5 %collective-permute-done.9.two_ref = bf16[64,1024]{1,0:T(8,128)(2,1)S(1)} collective-permute-done((bf16[64,1024]{1,0:T(8,128)(2,1)S(1)}, bf16[64,1024]{1,0:T(8,128)(2,1)S(1)}, u32[]{:S(2)}, u32[]{:S(2)}) %collective-permute-start.9) | collective-permute-done | bytes 131104 | tf_op jit(solution)/shard_map/ppermute | solution.py:30
  106.1 0.8 widen.3.w4
  106.9 0.0 collective-permute-done.1.far_ref
  106.9 5.0 %finish.1 = (f32[64,1024]{1,0:T(8,128)}, f32[64,1024]{1,0:T(8,128)}, bf16[1024,2048]{1,0:T(8,128)(2,1)}, f32[64,128]{1,0:T(8,128)}, f32[64,128]{1,0:T(8,128)}, /*index=5*/f32[2,1024,256]{2,1,0:T(8,128)S(1)}) custom-call(s32[4]{0:T(128)S(1)} %pad_add_fusion.place_ref, bf16[1024,256]{1,0:T(8,128)(2,1)} %basis_hbm.3, f32[64,1024]{1,0:T(8,128)} %bitcast.10, ...), custom_call_target="tpu_custom_call" | custom-call | tf_op jit(solution)/shard_map/finish/pallas_call | solution.py:311
  111.9 0.0 collective-permute-done.13.f3
  111.9 0.0 collective-permute-done.14.b3
  112.0 1.6 %last.1 = bf16[1024,2048]{1,0:T(8,128)(2,1)} custom-call(s32[4]{0:T(128)S(1)} %pad_add_fusion.place_ref, f32[2,1024,256]{2,1,0:T(8,128)S(1)} %get-tuple-element.18.later_ref, bf16[1024,256]{1,0:T(8,128)(2,1)S(1)} %collective-permute-done.13.f3, bf16[1024,256]{1,0:T(8,128)(2,1)S(1)} %collective-permute-done.14.b3, ...), custom_call_target="tpu_custom_call", output_to_operand_aliasing={{}: (4, {})} | custom-call | tf_op jit(solution)/shard_map/last/pallas_call | solution.py:349
  (2 shorter events, 0.0 us)
Async XLA Ops:
  0.6 5.8 %copy-start = (bf16[768,2048]{1,0:T(8,128)(2,1)S(1)}, bf16[768,2048]{1,0:T(8,128)(2,1)}, u32[]{:S(2)}) copy-start(bf16[768,2048]{1,0:T(8,128)(2,1)} %cot_ref.1) | copy-start | bytes 9437188
  4.9 17.7 %copy-start.1 = (f32[64,128]{1,0:T(8,128)S(1)}, f32[64,128]{1,0:T(8,128)}, u32[]{:S(2)}) copy-start(f32[64,128]{1,0:T(8,128)} %first_hbm.3) | copy-start | bytes 98308
  4.9 17.7 %copy-start.2 = (f32[64,128]{1,0:T(8,128)S(1)}, f32[64,128]{1,0:T(8,128)}, u32[]{:S(2)}) copy-start(f32[64,128]{1,0:T(8,128)} %second_hbm.3) | copy-start | bytes 98308
  4.9 1.5 %collective-permute-start = (bf16[768,128]{1,0:T(8,128)(2,1)S(1)}, bf16[768,128]{1,0:T(8,128)(2,1)S(1)}, u32[]{:S(2)}, u32[]{:S(2)}) collective-permute-start(bf16[768,128]{1,0:T(8,128)(2,1)S(1)} %get-tuple-element.15), channel_id=1, source_target_pairs={{0,1},{1,0},{2,3},{3,2},{4,5},{5,4},{6,7},{7,6},{8,9},{9,8},{10,11... | collective-permute-start | bytes 589832 | tf_op jit(solution)/shard_map/ppermute | solution.py:34
  24.0 23.6 %all-to-all-start.1 = ((bf16[8,10,16,128]{3,2,1,0:T(8,128)(2,1)}), bf16[8,10,16,128]{3,2,1,0:T(8,128)(2,1)S(1)}, u32[]{:S(2)}, u32[]{:S(2)}) async-start(bf16[8,10,16,128]{3,2,1,0:T(8,128)(2,1)} %fold.1), calls=%async_computation.1 | async-start | bytes 655360 | tf_op jit(solution)/shard_map/all_to_all | solution.py:362
  32.5 7.3 %collective-permute-start.2 = (bf16[64,1024]{1,0:T(8,128)(2,1)S(1)}, bf16[64,1024]{1,0:T(8,128)(2,1)S(1)}, u32[]{:S(2)}, u32[]{:S(2)}) collective-permute-start(bf16[64,1024]{1,0:T(8,128)(2,1)S(1)} %get-tuple-element.16.own_ref), channel_id=1, source_target_pairs={{0,8},{8,16},{16,24},{24,0},{1,9},{9,17},{17,25},{25,1},{2,10},{10... | collective-permute-start | bytes 393224 | tf_op jit(solution)/shard_map/ppermute | solution.py:30
  34.6 7.4 %collective-permute-start.3 = (bf16[64,1024]{1,0:T(8,128)(2,1)S(1)}, bf16[64,1024]{1,0:T(8,128)(2,1)S(1)}, u32[]{:S(2)}, u32[]{:S(2)}) collective-permute-start(bf16[64,1024]{1,0:T(8,128)(2,1)S(1)} %get-tuple-element.16.own_ref), channel_id=1, source_target_pairs={{0,16},{8,24},{16,0},{24,8},{1,17},{9,25},{17,1},{25,9},{2,18},{10... | collective-permute-start | bytes 393224 | tf_op jit(solution)/shard_map/ppermute | solution.py:30
  35.5 7.9 %collective-permute-start.4 = (bf16[64,1024]{1,0:T(8,128)(2,1)S(1)}, bf16[64,1024]{1,0:T(8,128)(2,1)S(1)}, u32[]{:S(2)}, u32[]{:S(2)}) collective-permute-start(bf16[64,1024]{1,0:T(8,128)(2,1)S(1)} %get-tuple-element.16.own_ref), channel_id=1, source_target_pairs={{0,24},{8,0},{16,8},{24,16},{1,25},{9,1},{17,9},{25,17},{2,26},{10... | collective-permute-start | bytes 393224 | tf_op jit(solution)/shard_map/ppermute | solution.py:30
  44.3 14.5 %collective-permute-start.5 = (bf16[1024,256]{1,0:T(8,128)(2,1)S(1)}, bf16[1024,256]{1,0:T(8,128)(2,1)S(1)}, u32[]{:S(2)}, u32[]{:S(2)}) collective-permute-start(bf16[1024,256]{1,0:T(8,128)(2,1)S(1)} %widen.2.w0), channel_id=1, source_target_pairs={{0,32},{32,64},{64,96},{96,128},{128,160},{160,192},{192,224},{224... | collective-permute-start | bytes 1572872 | tf_op jit(solution)/shard_map/ppermute | solution.py:30
  46.1 12.9 %collective-permute-start.11 = (bf16[1024,256]{1,0:T(8,128)(2,1)S(1)}, bf16[1024,256]{1,0:T(8,128)(2,1)S(1)}, u32[]{:S(2)}, u32[]{:S(2)}) collective-permute-start(bf16[1024,256]{1,0:T(8,128)(2,1)S(1)} %widen.2.w0), channel_id=1, source_target_pairs={{0,224},{32,0},{64,32},{96,64},{128,96},{160,128},{192,160},{224,1... | collective-permute-start | bytes 1572872 | tf_op jit(solution)/shard_map/ppermute | solution.py:30
  49.2 14.5 %all-to-all-start.2 = ((bf16[16,10,16,128]{3,2,1,0:T(8,128)(2,1)}), bf16[16,10,16,128]{3,2,1,0:T(8,128)(2,1)S(1)}, u32[]{:S(2)}, u32[]{:S(2)}) async-start(bf16[16,10,16,128]{3,2,1,0:T(8,128)(2,1)} %update.1), calls=%async_computation.2 | async-start | bytes 1310720 | tf_op jit(solution)/shard_map/all_to_all | solution.py:362
  58.7 13.5 %collective-permute-start.6 = (bf16[1024,256]{1,0:T(8,128)(2,1)S(1)}, bf16[1024,256]{1,0:T(8,128)(2,1)S(1)}, u32[]{:S(2)}, u32[]{:S(2)}) collective-permute-start(bf16[1024,256]{1,0:T(8,128)(2,1)S(1)} %collective-permute-done.5.f1), channel_id=1, source_target_pairs={{0,32},{32,64},{64,96},{96,128},{128,160},{160,192},{192,224},{224... | collective-permute-start | bytes 1572872 | tf_op jit(solution)/shard_map/ppermute | solution.py:30
  59.0 13.3 %collective-permute-start.12 = (bf16[1024,256]{1,0:T(8,128)(2,1)S(1)}, bf16[1024,256]{1,0:T(8,128)(2,1)S(1)}, u32[]{:S(2)}, u32[]{:S(2)}) collective-permute-start(bf16[1024,256]{1,0:T(8,128)(2,1)S(1)} %collective-permute-done.11.b1), channel_id=1, source_target_pairs={{0,224},{32,0},{64,32},{96,64},{128,96},{160,128},{192,160},{224,1... | collective-permute-start | bytes 1572872 | tf_op jit(solution)/shard_map/ppermute | solution.py:30
  63.7 43.2 %collective-permute-start.1 = (bf16[16,10,16,128]{3,2,1,0:T(8,128)(2,1)S(1)}, bf16[16,10,16,128]{3,2,1,0:T(8,128)(2,1)S(1)}, u32[]{:S(2)}, u32[]{:S(2)}) collective-permute-start(bf16[16,10,16,128]{3,2,1,0:T(8,128)(2,1)S(1)} %all-to-all-done.2.near_ref), channel_id=1, source_target_pairs={{0,1},{1,0},{2,3},{3,2},{4,5},{5,4},{6,7},{7,6},{8,9},{9,8},{10,11... | collective-permute-start | bytes 1966088 | tf_op jit(solution)/shard_map/ppermute | solution.py:34
  72.3 39.7 %collective-permute-start.13 = (bf16[1024,256]{1,0:T(8,128)(2,1)S(1)}, bf16[1024,256]{1,0:T(8,128)(2,1)S(1)}, u32[]{:S(2)}, u32[]{:S(2)}) collective-permute-start(bf16[1024,256]{1,0:T(8,128)(2,1)S(1)} %collective-permute-done.6.f2), channel_id=1, source_target_pairs={{0,32},{32,64},{64,96},{96,128},{128,160},{160,192},{192,224},{224... | collective-permute-start | bytes 1572872 | tf_op jit(solution)/shard_map/ppermute | solution.py:30
  72.3 39.7 %collective-permute-start.14 = (bf16[1024,256]{1,0:T(8,128)(2,1)S(1)}, bf16[1024,256]{1,0:T(8,128)(2,1)S(1)}, u32[]{:S(2)}, u32[]{:S(2)}) collective-permute-start(bf16[1024,256]{1,0:T(8,128)(2,1)S(1)} %collective-permute-done.12.b2), channel_id=1, source_target_pairs={{0,224},{32,0},{64,32},{96,64},{128,96},{160,128},{192,160},{224,1... | collective-permute-start | bytes 1572872 | tf_op jit(solution)/shard_map/ppermute | solution.py:30
  75.5 16.9 %collective-permute-start.7 = (bf16[64,1024]{1,0:T(8,128)(2,1)S(1)}, bf16[64,1024]{1,0:T(8,128)(2,1)S(1)}, u32[]{:S(2)}, u32[]{:S(2)}) collective-permute-start(bf16[64,1024]{1,0:T(8,128)(2,1)S(1)} %get-tuple-element.16.own_ref), channel_id=1, source_target_pairs={{0,128},{32,160},{64,192},{96,224},{128,0},{160,32},{192,64},{224,... | collective-permute-start | bytes 393224 | tf_op jit(solution)/shard_map/ppermute | solution.py:30
  92.4 7.2 %collective-permute-start.10 = (bf16[64,1024]{1,0:T(8,128)(2,1)S(1)}, bf16[64,1024]{1,0:T(8,128)(2,1)S(1)}, u32[]{:S(2)}, u32[]{:S(2)}) collective-permute-start(bf16[64,1024]{1,0:T(8,128)(2,1)S(1)} %collective-permute-done.7.own_ref), channel_id=1, source_target_pairs={{0,24},{8,0},{16,8},{24,16},{1,25},{9,1},{17,9},{25,17},{2,26},{10... | collective-permute-start | bytes 393224 | tf_op jit(solution)/shard_map/ppermute | solution.py:30
  92.4 7.2 %collective-permute-start.8 = (bf16[64,1024]{1,0:T(8,128)(2,1)S(1)}, bf16[64,1024]{1,0:T(8,128)(2,1)S(1)}, u32[]{:S(2)}, u32[]{:S(2)}) collective-permute-start(bf16[64,1024]{1,0:T(8,128)(2,1)S(1)} %collective-permute-done.7.own_ref), channel_id=1, source_target_pairs={{0,8},{8,16},{16,24},{24,0},{1,9},{9,17},{17,25},{25,1},{2,10},{10... | collective-permute-start | bytes 393224 | tf_op jit(solution)/shard_map/ppermute | solution.py:30
  99.6 6.5 %collective-permute-start.9 = (bf16[64,1024]{1,0:T(8,128)(2,1)S(1)}, bf16[64,1024]{1,0:T(8,128)(2,1)S(1)}, u32[]{:S(2)}, u32[]{:S(2)}) collective-permute-start(bf16[64,1024]{1,0:T(8,128)(2,1)S(1)} %collective-permute-done.7.own_ref), channel_id=1, source_target_pairs={{0,16},{8,24},{16,0},{24,8},{1,17},{9,25},{17,1},{25,9},{2,18},{10... | collective-permute-start | bytes 393224 | tf_op jit(solution)/shard_map/ppermute | solution.py:30

commit v5 on v4

--- a/solution.py
+++ b/solution.py
@@ -109,7 +109,7 @@
         out_shape=[
             jax.ShapeDtypeStruct((tokens, half), jnp.float32),
             jax.ShapeDtypeStruct((tokens, half), jnp.bfloat16),
-            jax.ShapeDtypeStruct(weight.shape, jnp.bfloat16),
+            pltpu.VMEM(weight.shape, jnp.bfloat16),
         ],
         scratch_shapes=[
             pltpu.VMEM((tokens, values), jnp.bfloat16),
@@ -125,27 +125,31 @@
     )(place, *in_hbm(lam, first_mix, second_mix, gain, basis, weight))
 
 
-def widen_kernel(place_ref, own_ref, one_ref, two_ref, three_ref, out_ref, slots):
+def widen_kernel(place_ref, own_ref, one_hbm, two_hbm, three_hbm, out_ref, slots, sems):
     y = place_ref[1]
-    slots[y] = own_ref[...].astype(jnp.float32)
-    slots[(y + 3) % 4] = one_ref[...].astype(jnp.float32)
-    slots[(y + 2) % 4] = two_ref[...].astype(jnp.float32)
-    slots[(y + 1) % 4] = three_ref[...].astype(jnp.float32)
+    copies = []
+    for hops, source in ((1, one_hbm), (2, two_hbm), (3, three_hbm)):
+        copy = pltpu.make_async_copy(source, slots.at[(y + 4 - hops) % 4], sems.at[hops])
+        copy.start()
+        copies.append(copy)
+    slots[y] = own_ref[...]
+    for copy in copies:
+        copy.wait()
     rows = slots.shape[0] * slots.shape[1]
-    out_ref[...] = slots[...].reshape(rows, slots.shape[2]).T.astype(jnp.bfloat16)
+    out_ref[...] = slots[...].reshape(rows, slots.shape[2]).astype(jnp.float32).T.astype(jnp.bfloat16)
 
 
 def widen(place, blocks):
     rows, cols = blocks[0].shape
     return pl.pallas_call(
         widen_kernel,
-        in_specs=[SMEM] + [VMEM] * 4,
+        in_specs=[SMEM, VMEM] + [HBM] * 3,
         out_specs=VMEM,
         out_shape=jax.ShapeDtypeStruct((cols, 4 * rows), jnp.bfloat16),
-        scratch_shapes=[pltpu.VMEM((4, rows, cols), jnp.float32)],
-        compiler_params=limit(8),
+        scratch_shapes=[pltpu.VMEM((4, rows, cols), jnp.bfloat16), pltpu.SemaphoreType.DMA((4,))],
+        compiler_params=limit(6),
         name="widen",
-    )(place, *blocks)
+    )(place, blocks[0], *in_hbm(*blocks[1:]))
 
 
 def gradient_kernel(own_ref, far_ref, cot_ref, out_hbm, parts, sems):
@@ -249,13 +253,21 @@
 
 
 def finish_kernel(
-    place_ref, basis_hbm, weight_hbm, first_hbm, second_hbm, near_ref, far_ref, w0, f1, f2, w4, b2, b1,
+    place_ref, basis_hbm, weight_hbm, first_hbm, second_hbm, near_ref, far_ref, w0, w4, b1, f1_hbm, f2_hbm, b2_hbm,
     new_ref, step_ref, copy_ref, first_out, second_out, later_ref,
-    basis_ref, weight_ref, first_ref, second_ref, tiles, sems,
+    basis_ref, weight_ref, first_ref, second_ref, blocks, tiles, sems,
 ):
     fetched = []
     for slot, (source, target) in enumerate(
-        ((basis_hbm, basis_ref), (weight_hbm, weight_ref), (first_hbm, first_ref), (second_hbm, second_ref))
+        (
+            (basis_hbm, basis_ref),
+            (f1_hbm, blocks.at[0]),
+            (f2_hbm, blocks.at[1]),
+            (b2_hbm, blocks.at[2]),
+            (weight_hbm, weight_ref),
+            (first_hbm, first_ref),
+            (second_hbm, second_ref),
+        )
     ):
         copy = pltpu.make_async_copy(source, target, sems.at[6 + slot])
         copy.start()
@@ -267,8 +279,7 @@
     count = 2 * near.shape[0] * near.shape[1] * near.shape[2] * near.shape[3]
     spread = jnp.sqrt(jnp.full((1, 128), energy / count, jnp.float32))
     scale = (-1.0 / (spread + 1e-06))[:, :1]
-    for copy in fetched:
-        copy.wait()
+    fetched[0].wait()
     basis = basis_ref[...]
 
     def rows_of(close, distant):
@@ -282,7 +293,10 @@
         return dot(basis, rows_of(near_ref[:, at], far_ref[:, at]), 1, 1) * scale
 
     copies = []
-    for slot, (block, hops) in enumerate(((w0, 0), (f1, 7), (b1, 1), (f2, 6), (b2, 2), (w4, 4))):
+    near_blocks = ((w0, 0), (w4, 4), (b1, 1), (blocks.at[0], 7), (blocks.at[1], 6), (blocks.at[2], 2))
+    for slot, (block, hops) in enumerate(near_blocks):
+        if slot >= 3:
+            fetched[slot - 2].wait()
         tiles[slot] = (block[...].astype(jnp.float32) + step_of(z + hops)).astype(jnp.bfloat16)
         copy = pltpu.make_async_copy(tiles.at[slot], copy_ref.at[:, columns(z + hops)], sems.at[slot])
         copy.start()
@@ -290,6 +304,8 @@
     for slot, hops in enumerate((5, 3)):
         later_ref[slot] = step_of(z + hops)
 
+    for copy in fetched[4:]:
+        copy.wait()
     mine = pl.ds(y * 4, 4)
     step = dot(rows_of(near_ref[mine, z], far_ref[mine, z]), basis, 1, 1) * scale
     step_ref[...] = step
@@ -310,7 +326,7 @@
     like = lambda array: jax.ShapeDtypeStruct(array.shape, jnp.float32)
     return pl.pallas_call(
         finish_kernel,
-        in_specs=[SMEM] + [HBM] * 4 + [VMEM] * (2 + len(blocks)),
+        in_specs=[SMEM] + [HBM] * 4 + [VMEM] * 5 + [HBM] * 3,
         out_specs=[VMEM, VMEM, HBM, VMEM, VMEM, VMEM],
         out_shape=[
             like(weight),
@@ -325,12 +341,13 @@
             pltpu.VMEM(weight.shape, weight.dtype),
             pltpu.VMEM(first.shape, first.dtype),
             pltpu.VMEM(second.shape, second.dtype),
+            pltpu.VMEM((3, values, 256), jnp.bfloat16),
             pltpu.VMEM((6, values, 256), jnp.bfloat16),
-            pltpu.SemaphoreType.DMA((10,)),
+            pltpu.SemaphoreType.DMA((13,)),
         ],
         compiler_params=limit(16),
         name="finish",
-    )(place, *in_hbm(basis, weight, first, second), near, far, *in_vmem(*blocks))
+    )(place, *in_hbm(basis, weight, first, second), near, far, *blocks[:3], *in_hbm(*blocks[3:]))
 
 
 def last_kernel(place_ref, later_ref, f3, b3, copy_in, copy_ref, tiles, sems):
@@ -355,7 +372,7 @@
         scratch_shapes=[pltpu.VMEM((2, copy.shape[0], 256), copy.dtype), pltpu.SemaphoreType.DMA((2,))],
         compiler_params=limit(8),
         name="last",
-    )(place, *in_vmem(later, f3, b3), *in_hbm(copy))
+    )(place, *in_vmem(later), f3, b3, *in_hbm(copy))
 
 
 def exchange(array, axes):
@@ -379,7 +396,7 @@
     near = exchange(update(place, exchange(sums, "z")), ("y", "x"))
     far = swap_cores(near)
     weight_new, step_out, most, first_new, second_new, later = finish(
-        place, basis, turned, first_moment, second_moment, near, far, (w0, f1, f2, w4, b2, b1)
+        place, basis, turned, first_moment, second_moment, near, far, (w0, w4, b1, f1, f2, b2)
     )
     weight_copy = last(place, later, f3, b3, most)
     return (weight_new.T, weight_copy, step_out.T, first_new, second_new)

time: 114 us -> 119 us (1.044)
  the two profiles are of different devices: /device:TPU:28 before, /device:TPU:36 now
where the time goes in v5:
time: 119 us; the launch traced here: 118 us
  waiting for transfers between devices  45 us (38%)
  starting transfers between devices  34.7 us (29%)
  Pallas kernels  19.3 us (16%)
  blocking collectives  16.7 us (14%)
  local copies, waits for them, and re-layouts  1.47 us (1%)
    ppermute x13, waiting for transfers between devices, shift(): lax.ppermute(array, axis, [(i, (i + hops) % count) for i in range(count)])  39.5 us
    ppermute x13, starting transfers between devices, shift(): lax.ppermute(array, axis, [(i, (i + hops) % count) for i in range(count)])  19.2 us
    all_to_all x1, blocking collectives, exchange(): return lax.all_to_all(array, axes, 0, 0, tiled=True)  16.7 us
    all_to_all x2, starting transfers between devices, exchange(): return lax.all_to_all(array, axes, 0, 0, tiled=True)  15.4 us
    pallas_call x1, Pallas kernels, finish(): pl.pallas_call(finish_kernel, in_specs=[SMEM] + [HBM] * 4 + [VMEM] * 5 +...  5.55 us
    pallas_call x1, Pallas kernels, heads(): pl.pallas_call(heads_kernel, in_specs=[SMEM] + [HBM] * 6, out_specs=[VMEM...  4.14 us
    all_to_all x2, waiting for transfers between devices, exchange(): return lax.all_to_all(array, axes, 0, 0, tiled=True)  4.1 us
    pallas_call x2, Pallas kernels, widen(): pl.pallas_call(widen_kernel, in_specs=[SMEM, VMEM] + [HBM] * 3, out_specs...  3.64 us
  transfers between devices with their start and end apart: 17, of which 10 were waited for; matrix products, arithmetic and copies ran while one was open for 0% of the time, Pallas kernels for 9%

profile of v5, /device:TPU:36, one launch (start us, length us, event | category | flops | bytes accessed | tf_op | source)
XLA Modules:
  0.0 118.2 jit_solution(12616750414951500374)
XLA Ops:
  0.6 0.1 pad_add_fusion.place_ref
  0.7 4.1 %heads.1 = (f32[768,128]{1,0:T(8,128)S(1)}, bf16[768,128]{1,0:T(8,128)(2,1)S(1)}, bf16[64,1024]{1,0:T(8,128)(2,1)S(1)}) custom-call(s32[4]{0:T(128)S(1)} %pad_add_fusion.place_ref, f32[1,4]{1,0:T(1,128)} %bitcast.12, bf16[768,1024]{1,0:T(8,128)(2,1)} %first_hbm.2, bf16[768,1024]{1,0:T(8,128)(2,1)} %second_hbm.2, f32[1,256]{1,0:T(1,128)} %bitcast.11, ...), custom_call_target="tpu_custom_call" | custom-call | tf_op jit(solution)/shard_map/heads/pallas_call | solution.py:105
  4.9 0.0 copy-start.1
  4.9 0.0 copy-start.2
  4.9 0.1 collective-permute-start
  5.0 1.4 %collective-permute-done.far_ref = bf16[768,128]{1,0:T(8,128)(2,1)S(1)} collective-permute-done((bf16[768,128]{1,0:T(8,128)(2,1)S(1)}, bf16[768,128]{1,0:T(8,128)(2,1)S(1)}, u32[]{:S(2)}, u32[]{:S(2)}) %collective-permute-start) | collective-permute-done | bytes 196640 | tf_op jit(solution)/shard_map/ppermute | solution.py:34
  6.4 1.4 %gradient.1 = bf16[16,8,16,128]{3,2,1,0:T(8,128)(2,1)} custom-call(f32[768,128]{1,0:T(8,128)S(1)} %get-tuple-element.14.own_ref, bf16[768,128]{1,0:T(8,128)(2,1)S(1)} %collective-permute-done.far_ref, bf16[768,2048]{1,0:T(8,128)(2,1)S(1)} %copy-done), custom_call_target="tpu_custom_call" | custom-call | tf_op jit(solution)/shard_map/gradient/pallas_call | solution.py:174
  7.8 16.7 %all_to_all.15.parts_ref = bf16[16,8,16,128]{3,2,1,0:T(8,128)(2,1)S(1)} all-to-all(bf16[16,8,16,128]{3,2,1,0:T(8,128)(2,1)} %gradient.1), channel_id=1, replica_groups=mesh['z'=8,'y'=4,'x'=4,'tp'=2] {'y','x'}, dimensions={0} | all-to-all | bytes 1048576 | tf_op jit(solution)/shard_map/all_to_all | solution.py:379
  24.5 1.4 %fold.1 = bf16[8,10,16,128]{3,2,1,0:T(8,128)(2,1)} custom-call(s32[4]{0:T(128)S(1)} %pad_add_fusion.place_ref, bf16[16,8,16,128]{3,2,1,0:T(8,128)(2,1)S(1)} %all_to_all.15.parts_ref, f32[64,128]{1,0:T(8,128)S(1)} %copy-done.1, f32[64,128]{1,0:T(8,128)S(1)} %copy-done.2), custom_call_target="tpu_custom_call" | custom-call | tf_op jit(solution)/shard_map/fold/pallas_call | solution.py:205
  25.9 8.6 %all-to-all-start.1 = ((bf16[8,10,16,128]{3,2,1,0:T(8,128)(2,1)}), bf16[8,10,16,128]{3,2,1,0:T(8,128)(2,1)S(1)}, u32[]{:S(2)}, u32[]{:S(2)}) async-start(bf16[8,10,16,128]{3,2,1,0:T(8,128)(2,1)} %fold.1), calls=%async_computation.1 | async-start | bytes 655360 | tf_op jit(solution)/shard_map/all_to_all | solution.py:379
  34.5 0.6 collective-permute-start.2
  35.1 1.9 %collective-permute-start.3 = (bf16[64,1024]{1,0:T(8,128)(2,1)S(1)}, bf16[64,1024]{1,0:T(8,128)(2,1)S(1)}, u32[]{:S(2)}, u32[]{:S(2)}) collective-permute-start(bf16[64,1024]{1,0:T(8,128)(2,1)S(1)} %get-tuple-element.16.own_ref), channel_id=1, source_target_pairs={{0,16},{8,24},{16,0},{24,8},{1,17},{9,25},{17,1},{25,9},{2,18},{10... | collective-permute-start | bytes 393224 | tf_op jit(solution)/shard_map/ppermute | solution.py:30
  37.1 1.6 %collective-permute-start.4 = (bf16[64,1024]{1,0:T(8,128)(2,1)S(1)}, bf16[64,1024]{1,0:T(8,128)(2,1)S(1)}, u32[]{:S(2)}, u32[]{:S(2)}) collective-permute-start(bf16[64,1024]{1,0:T(8,128)(2,1)S(1)} %get-tuple-element.16.own_ref), channel_id=1, source_target_pairs={{0,24},{8,0},{16,8},{24,16},{1,25},{9,1},{17,9},{25,17},{2,26},{10... | collective-permute-start | bytes 393224 | tf_op jit(solution)/shard_map/ppermute | solution.py:30
  38.6 4.4 %collective-permute-done.2.one_hbm = bf16[64,1024]{1,0:T(8,128)(2,1)S(1)} collective-permute-done((bf16[64,1024]{1,0:T(8,128)(2,1)S(1)}, bf16[64,1024]{1,0:T(8,128)(2,1)S(1)}, u32[]{:S(2)}, u32[]{:S(2)}) %collective-permute-start.2) | collective-permute-done | bytes 131104 | tf_op jit(solution)/shard_map/ppermute | solution.py:30
  43.0 0.0 collective-permute-done.3.two_hbm
  43.0 0.6 collective-permute-done.4.three_hbm
  43.6 0.1 copy-done.7
  43.7 0.0 copy-done.9
  43.7 0.7 copy-done.10
  44.4 1.8 %widen.2.w0 = bf16[1024,256]{1,0:T(8,128)(2,1)S(1)} custom-call(s32[4]{0:T(128)S(1)} %pad_add_fusion.place_ref, bf16[64,1024]{1,0:T(8,128)(2,1)S(1)} %get-tuple-element.16.own_ref, bf16[64,1024]{1,0:T(8,128)(2,1)} %copy-done.7, bf16[64,1024]{1,0:T(8,128)(2,1)} %copy-done.9, bf16[64,1024]{1,0:T(8,128)(2,1)} %copy-done.10), custom_call_target="tpu_custom_call" | custom-call | tf_op jit(solution)/shard_map/widen/pallas_call | solution.py:144
  46.2 1.5 %collective-permute-start.10 = (bf16[1024,256]{1,0:T(8,128)(2,1)S(1)}, bf16[1024,256]{1,0:T(8,128)(2,1)S(1)}, u32[]{:S(2)}, u32[]{:S(2)}) collective-permute-start(bf16[1024,256]{1,0:T(8,128)(2,1)S(1)} %widen.2.w0), channel_id=1, source_target_pairs={{0,32},{32,64},{64,96},{96,128},{128,160},{160,192},{192,224},{224... | collective-permute-start | bytes 1572872 | tf_op jit(solution)/shard_map/ppermute | solution.py:30
  47.8 0.6 collective-permute-start.9
  48.3 0.0 all-to-all-done.1.letters_ref
  48.3 1.6 %update.1 = bf16[16,10,16,128]{3,2,1,0:T(8,128)(2,1)} custom-call(s32[4]{0:T(128)S(1)} %pad_add_fusion.place_ref, bf16[8,10,16,128]{3,2,1,0:T(8,128)(2,1)S(1)} %all-to-all-done.1.letters_ref), custom_call_target="tpu_custom_call" | custom-call | tf_op jit(solution)/shard_map/update/pallas_call | solution.py:236
  49.9 6.8 %all-to-all-start.2 = ((bf16[16,10,16,128]{3,2,1,0:T(8,128)(2,1)}), bf16[16,10,16,128]{3,2,1,0:T(8,128)(2,1)S(1)}, u32[]{:S(2)}, u32[]{:S(2)}) async-start(bf16[16,10,16,128]{3,2,1,0:T(8,128)(2,1)} %update.1), calls=%async_computation.2 | async-start | bytes 1310720 | tf_op jit(solution)/shard_map/all_to_all | solution.py:379
  56.7 2.9 %collective-permute-done.10.f1_hbm = bf16[1024,256]{1,0:T(8,128)(2,1)S(1)} collective-permute-done((bf16[1024,256]{1,0:T(8,128)(2,1)S(1)}, bf16[1024,256]{1,0:T(8,128)(2,1)S(1)}, u32[]{:S(2)}, u32[]{:S(2)}) %collective-permute-start.10) | collective-permute-done | bytes 524320 | tf_op jit(solution)/shard_map/ppermute | solution.py:30
  59.6 1.5 %collective-permute-start.11 = (bf16[1024,256]{1,0:T(8,128)(2,1)S(1)}, bf16[1024,256]{1,0:T(8,128)(2,1)S(1)}, u32[]{:S(2)}, u32[]{:S(2)}) collective-permute-start(bf16[1024,256]{1,0:T(8,128)(2,1)S(1)} %collective-permute-done.10.f1_hbm), channel_id=1, source_target_pairs={{0,32},{32,64},{64,96},{96,128},{128,160},{160,192},{192,224},{224... | collective-permute-start | bytes 1572872 | tf_op jit(solution)/shard_map/ppermute | solution.py:30
  61.1 0.0 collective-permute-done.9.b1
  61.1 0.6 collective-permute-start.12
  61.6 4.1 %all-to-all-done.2.near_ref = bf16[16,10,16,128]{3,2,1,0:T(8,128)(2,1)S(1)} async-done(((bf16[16,10,16,128]{3,2,1,0:T(8,128)(2,1)}), bf16[16,10,16,128]{3,2,1,0:T(8,128)(2,1)S(1)}, u32[]{:S(2)}, u32[]{:S(2)}) %all-to-all-start.2) | async-done | bytes 655392 | tf_op jit(solution)/shard_map/all_to_all | solution.py:379
  65.7 0.0 collective-permute-start.1
  65.7 6.3 %collective-permute-done.11.f2_hbm = bf16[1024,256]{1,0:T(8,128)(2,1)S(1)} collective-permute-done((bf16[1024,256]{1,0:T(8,128)(2,1)S(1)}, bf16[1024,256]{1,0:T(8,128)(2,1)S(1)}, u32[]{:S(2)}, u32[]{:S(2)}) %collective-permute-start.11) | collective-permute-done | bytes 524320 | tf_op jit(solution)/shard_map/ppermute | solution.py:30
  72.1 1.5 %collective-permute-start.13 = (bf16[1024,256]{1,0:T(8,128)(2,1)S(1)}, bf16[1024,256]{1,0:T(8,128)(2,1)S(1)}, u32[]{:S(2)}, u32[]{:S(2)}) collective-permute-start(bf16[1024,256]{1,0:T(8,128)(2,1)S(1)} %collective-permute-done.11.f2_hbm), channel_id=1, source_target_pairs={{0,32},{32,64},{64,96},{96,128},{128,160},{160,192},{192,224},{224... | collective-permute-start | bytes 1572872 | tf_op jit(solution)/shard_map/ppermute | solution.py:30
  73.5 0.4 collective-permute-done.12.b2_hbm
  73.9 1.0 collective-permute-start.14
  74.9 5.6 %collective-permute-start.5 = (bf16[64,1024]{1,0:T(8,128)(2,1)S(1)}, bf16[64,1024]{1,0:T(8,128)(2,1)S(1)}, u32[]{:S(2)}, u32[]{:S(2)}) collective-permute-start(bf16[64,1024]{1,0:T(8,128)(2,1)S(1)} %get-tuple-element.16.own_ref), channel_id=1, source_target_pairs={{0,128},{32,160},{64,192},{96,224},{128,0},{160,32},{192,64},{224,... | collective-permute-start | bytes 393224 | tf_op jit(solution)/shard_map/ppermute | solution.py:30
  80.5 15.2 %collective-permute-done.5.own_ref = bf16[64,1024]{1,0:T(8,128)(2,1)S(1)} collective-permute-done((bf16[64,1024]{1,0:T(8,128)(2,1)S(1)}, bf16[64,1024]{1,0:T(8,128)(2,1)S(1)}, u32[]{:S(2)}, u32[]{:S(2)}) %collective-permute-start.5) | collective-permute-done | bytes 131104 | tf_op jit(solution)/shard_map/ppermute | solution.py:30
  95.7 0.0 collective-permute-start.6
  95.7 2.8 %collective-permute-start.7 = (bf16[64,1024]{1,0:T(8,128)(2,1)S(1)}, bf16[64,1024]{1,0:T(8,128)(2,1)S(1)}, u32[]{:S(2)}, u32[]{:S(2)}) collective-permute-start(bf16[64,1024]{1,0:T(8,128)(2,1)S(1)} %collective-permute-done.5.own_ref), channel_id=1, source_target_pairs={{0,16},{8,24},{16,0},{24,8},{1,17},{9,25},{17,1},{25,9},{2,18},{10... | collective-permute-start | bytes 393224 | tf_op jit(solution)/shard_map/ppermute | solution.py:30
  98.5 4.8 %collective-permute-done.6.one_hbm = bf16[64,1024]{1,0:T(8,128)(2,1)S(1)} collective-permute-done((bf16[64,1024]{1,0:T(8,128)(2,1)S(1)}, bf16[64,1024]{1,0:T(8,128)(2,1)S(1)}, u32[]{:S(2)}, u32[]{:S(2)}) %collective-permute-start.6) | collective-permute-done | bytes 131104 | tf_op jit(solution)/shard_map/ppermute | solution.py:30
  103.3 0.0 collective-permute-start.8
  103.3 0.0 copy-start.8
  103.3 4.9 %collective-permute-done.8.three_hbm = bf16[64,1024]{1,0:T(8,128)(2,1)S(1)} collective-permute-done((bf16[64,1024]{1,0:T(8,128)(2,1)S(1)}, bf16[64,1024]{1,0:T(8,128)(2,1)S(1)}, u32[]{:S(2)}, u32[]{:S(2)}) %collective-permute-start.8) | collective-permute-done | bytes 131104 | tf_op jit(solution)/shard_map/ppermute | solution.py:30
  108.3 0.7 copy-done.11
  108.9 1.8 %widen.3.w4 = bf16[1024,256]{1,0:T(8,128)(2,1)S(1)} custom-call(s32[4]{0:T(128)S(1)} %pad_add_fusion.place_ref, bf16[64,1024]{1,0:T(8,128)(2,1)S(1)} %collective-permute-done.5.own_ref, bf16[64,1024]{1,0:T(8,128)(2,1)} %copy-done.6, bf16[64,1024]{1,0:T(8,128)(2,1)} %copy-done.8, bf16[64,1024]{1,0:T(8,128)(2,1)} %copy-done.11), custom_call_target="tpu_custom_call" | custom-call | tf_op jit(solution)/shard_map/widen/pallas_call | solution.py:144
  110.8 0.0 collective-permute-done.1.far_ref
  110.8 5.5 %finish.1 = (f32[64,1024]{1,0:T(8,128)}, f32[64,1024]{1,0:T(8,128)}, bf16[1024,2048]{1,0:T(8,128)(2,1)}, f32[64,128]{1,0:T(8,128)}, f32[64,128]{1,0:T(8,128)}, /*index=5*/f32[2,1024,256]{2,1,0:T(8,128)S(1)}) custom-call(s32[4]{0:T(128)S(1)} %pad_add_fusion.place_ref, bf16[1024,256]{1,0:T(8,128)(2,1)} %basis_hbm.3, f32[64,1024]{1,0:T(8,128)} %bitcast.10, ...), custom_call_target="tpu_custom_call" | custom-call | tf_op jit(solution)/shard_map/finish/pallas_call | solution.py:327
  116.4 1.6 %last.1 = bf16[1024,2048]{1,0:T(8,128)(2,1)} custom-call(s32[4]{0:T(128)S(1)} %pad_add_fusion.place_ref, f32[2,1024,256]{2,1,0:T(8,128)S(1)} %get-tuple-element.18.later_ref, bf16[1024,256]{1,0:T(8,128)(2,1)S(1)} %collective-permute-done.13.f3, bf16[1024,256]{1,0:T(8,128)(2,1)S(1)} %collective-permute-done.14.b3, ...), custom_call_target="tpu_custom_call", output_to_operand_aliasing={{}: (4, {})} | custom-call | tf_op jit(solution)/shard_map/last/pallas_call | solution.py:366
  (20 shorter events, 0.0 us)
Async XLA Ops:
  0.6 5.8 %copy-start = (bf16[768,2048]{1,0:T(8,128)(2,1)S(1)}, bf16[768,2048]{1,0:T(8,128)(2,1)}, u32[]{:S(2)}) copy-start(bf16[768,2048]{1,0:T(8,128)(2,1)} %cot_ref.1) | copy-start | bytes 9437188
  4.9 19.6 %copy-start.1 = (f32[64,128]{1,0:T(8,128)S(1)}, f32[64,128]{1,0:T(8,128)}, u32[]{:S(2)}) copy-start(f32[64,128]{1,0:T(8,128)} %first_hbm.3) | copy-start | bytes 98308
  4.9 19.6 %copy-start.2 = (f32[64,128]{1,0:T(8,128)S(1)}, f32[64,128]{1,0:T(8,128)}, u32[]{:S(2)}) copy-start(f32[64,128]{1,0:T(8,128)} %second_hbm.3) | copy-start | bytes 98308
  4.9 1.5 %collective-permute-start = (bf16[768,128]{1,0:T(8,128)(2,1)S(1)}, bf16[768,128]{1,0:T(8,128)(2,1)S(1)}, u32[]{:S(2)}, u32[]{:S(2)}) collective-permute-start(bf16[768,128]{1,0:T(8,128)(2,1)S(1)} %get-tuple-element.15), channel_id=1, source_target_pairs={{0,1},{1,0},{2,3},{3,2},{4,5},{5,4},{6,7},{7,6},{8,9},{9,8},{10,11... | collective-permute-start | bytes 589832 | tf_op jit(solution)/shard_map/ppermute | solution.py:34
  25.9 22.4 %all-to-all-start.1 = ((bf16[8,10,16,128]{3,2,1,0:T(8,128)(2,1)}), bf16[8,10,16,128]{3,2,1,0:T(8,128)(2,1)S(1)}, u32[]{:S(2)}, u32[]{:S(2)}) async-start(bf16[8,10,16,128]{3,2,1,0:T(8,128)(2,1)} %fold.1), calls=%async_computation.1 | async-start | bytes 655360 | tf_op jit(solution)/shard_map/all_to_all | solution.py:379
  34.5 8.5 %collective-permute-start.2 = (bf16[64,1024]{1,0:T(8,128)(2,1)S(1)}, bf16[64,1024]{1,0:T(8,128)(2,1)S(1)}, u32[]{:S(2)}, u32[]{:S(2)}) collective-permute-start(bf16[64,1024]{1,0:T(8,128)(2,1)S(1)} %get-tuple-element.16.own_ref), channel_id=1, source_target_pairs={{0,8},{8,16},{16,24},{24,0},{1,9},{9,17},{17,25},{25,1},{2,10},{10... | collective-permute-start | bytes 393224 | tf_op jit(solution)/shard_map/ppermute | solution.py:30
  35.1 7.9 %collective-permute-start.3 = (bf16[64,1024]{1,0:T(8,128)(2,1)S(1)}, bf16[64,1024]{1,0:T(8,128)(2,1)S(1)}, u32[]{:S(2)}, u32[]{:S(2)}) collective-permute-start(bf16[64,1024]{1,0:T(8,128)(2,1)S(1)} %get-tuple-element.16.own_ref), channel_id=1, source_target_pairs={{0,16},{8,24},{16,0},{24,8},{1,17},{9,25},{17,1},{25,9},{2,18},{10... | collective-permute-start | bytes 393224 | tf_op jit(solution)/shard_map/ppermute | solution.py:30
  37.1 6.5 %collective-permute-start.4 = (bf16[64,1024]{1,0:T(8,128)(2,1)S(1)}, bf16[64,1024]{1,0:T(8,128)(2,1)S(1)}, u32[]{:S(2)}, u32[]{:S(2)}) collective-permute-start(bf16[64,1024]{1,0:T(8,128)(2,1)S(1)} %get-tuple-element.16.own_ref), channel_id=1, source_target_pairs={{0,24},{8,0},{16,8},{24,16},{1,25},{9,1},{17,9},{25,17},{2,26},{10... | collective-permute-start | bytes 393224 | tf_op jit(solution)/shard_map/ppermute | solution.py:30
  43.0 0.7 copy-start.7
  43.0 0.7 copy-start.9
  43.7 0.7 copy-start.10
  46.2 13.4 %collective-permute-start.10 = (bf16[1024,256]{1,0:T(8,128)(2,1)S(1)}, bf16[1024,256]{1,0:T(8,128)(2,1)S(1)}, u32[]{:S(2)}, u32[]{:S(2)}) collective-permute-start(bf16[1024,256]{1,0:T(8,128)(2,1)S(1)} %widen.2.w0), channel_id=1, source_target_pairs={{0,32},{32,64},{64,96},{96,128},{128,160},{160,192},{192,224},{224... | collective-permute-start | bytes 1572872 | tf_op jit(solution)/shard_map/ppermute | solution.py:30
  47.8 13.3 %collective-permute-start.9 = (bf16[1024,256]{1,0:T(8,128)(2,1)S(1)}, bf16[1024,256]{1,0:T(8,128)(2,1)S(1)}, u32[]{:S(2)}, u32[]{:S(2)}) collective-permute-start(bf16[1024,256]{1,0:T(8,128)(2,1)S(1)} %widen.2.w0), channel_id=1, source_target_pairs={{0,224},{32,0},{64,32},{96,64},{128,96},{160,128},{192,160},{224,1... | collective-permute-start | bytes 1572872 | tf_op jit(solution)/shard_map/ppermute | solution.py:30
  49.9 15.8 %all-to-all-start.2 = ((bf16[16,10,16,128]{3,2,1,0:T(8,128)(2,1)}), bf16[16,10,16,128]{3,2,1,0:T(8,128)(2,1)S(1)}, u32[]{:S(2)}, u32[]{:S(2)}) async-start(bf16[16,10,16,128]{3,2,1,0:T(8,128)(2,1)} %update.1), calls=%async_computation.2 | async-start | bytes 1310720 | tf_op jit(solution)/shard_map/all_to_all | solution.py:379
  59.6 51.2 %copy-start.3 = (bf16[1024,256]{1,0:T(8,128)(2,1)}, bf16[1024,256]{1,0:T(8,128)(2,1)S(1)}, u32[]{:S(2)}) copy-start(bf16[1024,256]{1,0:T(8,128)(2,1)S(1)} %collective-permute-done.10.f1_hbm) | copy-start | bytes 1572868
  59.6 12.5 %collective-permute-start.11 = (bf16[1024,256]{1,0:T(8,128)(2,1)S(1)}, bf16[1024,256]{1,0:T(8,128)(2,1)S(1)}, u32[]{:S(2)}, u32[]{:S(2)}) collective-permute-start(bf16[1024,256]{1,0:T(8,128)(2,1)S(1)} %collective-permute-done.10.f1_hbm), channel_id=1, source_target_pairs={{0,32},{32,64},{64,96},{96,128},{128,160},{160,192},{192,224},{224... | collective-permute-start | bytes 1572872 | tf_op jit(solution)/shard_map/ppermute | solution.py:30
  61.1 12.8 %collective-permute-start.12 = (bf16[1024,256]{1,0:T(8,128)(2,1)S(1)}, bf16[1024,256]{1,0:T(8,128)(2,1)S(1)}, u32[]{:S(2)}, u32[]{:S(2)}) collective-permute-start(bf16[1024,256]{1,0:T(8,128)(2,1)S(1)} %collective-permute-done.9.b1), channel_id=1, source_target_pairs={{0,224},{32,0},{64,32},{96,64},{128,96},{160,128},{192,160},{224,1... | collective-permute-start | bytes 1572872 | tf_op jit(solution)/shard_map/ppermute | solution.py:30
  65.7 45.0 %collective-permute-start.1 = (bf16[16,10,16,128]{3,2,1,0:T(8,128)(2,1)S(1)}, bf16[16,10,16,128]{3,2,1,0:T(8,128)(2,1)S(1)}, u32[]{:S(2)}, u32[]{:S(2)}) collective-permute-start(bf16[16,10,16,128]{3,2,1,0:T(8,128)(2,1)S(1)} %all-to-all-done.2.near_ref), channel_id=1, source_target_pairs={{0,1},{1,0},{2,3},{3,2},{4,5},{5,4},{6,7},{7,6},{8,9},{9,8},{10,11... | collective-permute-start | bytes 1966088 | tf_op jit(solution)/shard_map/ppermute | solution.py:34
  72.1 38.7 %copy-start.4 = (bf16[1024,256]{1,0:T(8,128)(2,1)}, bf16[1024,256]{1,0:T(8,128)(2,1)S(1)}, u32[]{:S(2)}) copy-start(bf16[1024,256]{1,0:T(8,128)(2,1)S(1)} %collective-permute-done.11.f2_hbm) | copy-start | bytes 1572868
  72.1 44.3 %collective-permute-start.13 = (bf16[1024,256]{1,0:T(8,128)(2,1)S(1)}, bf16[1024,256]{1,0:T(8,128)(2,1)S(1)}, u32[]{:S(2)}, u32[]{:S(2)}) collective-permute-start(bf16[1024,256]{1,0:T(8,128)(2,1)S(1)} %collective-permute-done.11.f2_hbm), channel_id=1, source_target_pairs={{0,32},{32,64},{64,96},{96,128},{128,160},{160,192},{192,224},{224... | collective-permute-start | bytes 1572872 | tf_op jit(solution)/shard_map/ppermute | solution.py:30
  73.9 36.9 %copy-start.5 = (bf16[1024,256]{1,0:T(8,128)(2,1)}, bf16[1024,256]{1,0:T(8,128)(2,1)S(1)}, u32[]{:S(2)}) copy-start(bf16[1024,256]{1,0:T(8,128)(2,1)S(1)} %collective-permute-done.12.b2_hbm) | copy-start | bytes 1572868
  73.9 42.5 %collective-permute-start.14 = (bf16[1024,256]{1,0:T(8,128)(2,1)S(1)}, bf16[1024,256]{1,0:T(8,128)(2,1)S(1)}, u32[]{:S(2)}, u32[]{:S(2)}) collective-permute-start(bf16[1024,256]{1,0:T(8,128)(2,1)S(1)} %collective-permute-done.12.b2_hbm), channel_id=1, source_target_pairs={{0,224},{32,0},{64,32},{96,64},{128,96},{160,128},{192,160},{224,1... | collective-permute-start | bytes 1572872 | tf_op jit(solution)/shard_map/ppermute | solution.py:30
  74.9 20.8 %collective-permute-start.5 = (bf16[64,1024]{1,0:T(8,128)(2,1)S(1)}, bf16[64,1024]{1,0:T(8,128)(2,1)S(1)}, u32[]{:S(2)}, u32[]{:S(2)}) collective-permute-start(bf16[64,1024]{1,0:T(8,128)(2,1)S(1)} %get-tuple-element.16.own_ref), channel_id=1, source_target_pairs={{0,128},{32,160},{64,192},{96,224},{128,0},{160,32},{192,64},{224,... | collective-permute-start | bytes 393224 | tf_op jit(solution)/shard_map/ppermute | solution.py:30
  95.7 7.6 %collective-permute-start.6 = (bf16[64,1024]{1,0:T(8,128)(2,1)S(1)}, bf16[64,1024]{1,0:T(8,128)(2,1)S(1)}, u32[]{:S(2)}, u32[]{:S(2)}) collective-permute-start(bf16[64,1024]{1,0:T(8,128)(2,1)S(1)} %collective-permute-done.5.own_ref), channel_id=1, source_target_pairs={{0,8},{8,16},{16,24},{24,0},{1,9},{9,17},{17,25},{25,1},{2,10},{10... | collective-permute-start | bytes 393224 | tf_op jit(solution)/shard_map/ppermute | solution.py:30
  95.7 7.6 %collective-permute-start.7 = (bf16[64,1024]{1,0:T(8,128)(2,1)S(1)}, bf16[64,1024]{1,0:T(8,128)(2,1)S(1)}, u32[]{:S(2)}, u32[]{:S(2)}) collective-permute-start(bf16[64,1024]{1,0:T(8,128)(2,1)S(1)} %collective-permute-done.5.own_ref), channel_id=1, source_target_pairs={{0,16},{8,24},{16,0},{24,8},{1,17},{9,25},{17,1},{25,9},{2,18},{10... | collective-permute-start | bytes 393224 | tf_op jit(solution)/shard_map/ppermute | solution.py:30
  103.3 5.0 %copy-start.6 = (bf16[64,1024]{1,0:T(8,128)(2,1)}, bf16[64,1024]{1,0:T(8,128)(2,1)S(1)}, u32[]{:S(2)}) copy-start(bf16[64,1024]{1,0:T(8,128)(2,1)S(1)} %collective-permute-done.6.one_hbm) | copy-start | bytes 393220
  103.3 5.0 %collective-permute-start.8 = (bf16[64,1024]{1,0:T(8,128)(2,1)S(1)}, bf16[64,1024]{1,0:T(8,128)(2,1)S(1)}, u32[]{:S(2)}, u32[]{:S(2)}) collective-permute-start(bf16[64,1024]{1,0:T(8,128)(2,1)S(1)} %collective-permute-done.5.own_ref), channel_id=1, source_target_pairs={{0,24},{8,0},{16,8},{24,16},{1,25},{9,1},{17,9},{25,17},{2,26},{10... | collective-permute-start | bytes 393224 | tf_op jit(solution)/shard_map/ppermute | solution.py:30
  103.3 5.0 %copy-start.8 = (bf16[64,1024]{1,0:T(8,128)(2,1)}, bf16[64,1024]{1,0:T(8,128)(2,1)S(1)}, u32[]{:S(2)}) copy-start(bf16[64,1024]{1,0:T(8,128)(2,1)S(1)} %collective-permute-done.7.two_hbm) | copy-start | bytes 393220
  108.3 0.7 copy-start.11

commit v6 on v4

--- a/solution.py
+++ b/solution.py
@@ -9,8 +9,10 @@
 OUT_SCALE = 0.8
 BETA_FIRST = 0.9
 BETA_SECOND = 0.95
-FS = ("z", "y")
-FS_REP = ("z", "y", "x")
+Z = ("zh", "zl")
+FS = (*Z, "y")
+FS_REP = (*FS, "x")
+NEAR = ("zl", "y", "x")
 SMEM = pl.BlockSpec(memory_space=pltpu.SMEM)
 VMEM = pl.BlockSpec(memory_space=pltpu.VMEM)
 HBM = pl.BlockSpec(memory_space=pltpu.HBM)
@@ -109,7 +111,7 @@
         out_shape=[
             jax.ShapeDtypeStruct((tokens, half), jnp.float32),
             jax.ShapeDtypeStruct((tokens, half), jnp.bfloat16),
-            jax.ShapeDtypeStruct(weight.shape, jnp.bfloat16),
+            pltpu.VMEM(weight.shape, jnp.bfloat16),
         ],
         scratch_shapes=[
             pltpu.VMEM((tokens, values), jnp.bfloat16),
@@ -156,9 +158,8 @@
         block = dot(reduced, cot_ref[:, at * wide : (at + 1) * wide], 1, 0).T.astype(jnp.bfloat16)
         for z in range(2):
             rows = block[z * 256 : (z + 1) * 256]
-            parts[:, at * 2 + z] = rows.reshape(16, 16, rows.shape[1])
-        pair = pl.ds(at * 2, 2)
-        copy = pltpu.make_async_copy(parts.at[:, pair], out_hbm.at[:, pair], sems.at[at])
+            parts[z * 16 : (z + 1) * 16, at] = rows.reshape(16, 16, rows.shape[1])
+        copy = pltpu.make_async_copy(parts.at[:, at], out_hbm.at[:, at], sems.at[at])
         copy.start()
         copies.append(copy)
     for copy in copies:
@@ -166,7 +167,7 @@
 
 
 def gradient(own, far, cot):
-    shape = (16, 8, 16, own.shape[1])
+    shape = (32, 4, 16, own.shape[1])
     return pl.pallas_call(
         gradient_kernel,
         in_specs=[VMEM] * 3,
@@ -190,20 +191,20 @@
 
 def fold_kernel(place_ref, parts_ref, first_ref, second_ref, out_hbm, letter_ref, sems):
     rows = pl.ds(pl.multiple_of(place_ref[2] * 16, 16), 16)
-    letter_ref[:8] = jnp.sum(parts_ref[...].astype(jnp.float32), axis=0).astype(jnp.bfloat16)
-    letter_ref[8] = first_ref[rows, :].astype(jnp.bfloat16)
-    letter_ref[9] = second_ref[rows, :].astype(jnp.bfloat16)
-    send([(letter_ref, out_hbm.at[z]) for z in range(8)], sems)
+    letter_ref[:4] = jnp.sum(parts_ref[...].astype(jnp.float32), axis=0).astype(jnp.bfloat16)
+    letter_ref[4] = first_ref[rows, :].astype(jnp.bfloat16)
+    letter_ref[5] = second_ref[rows, :].astype(jnp.bfloat16)
+    send([(letter_ref, out_hbm.at[peer]) for peer in range(4)], sems)
 
 
 def fold(place, parts, first, second):
-    shape = (10, *parts.shape[2:])
+    shape = (6, *parts.shape[2:])
     return pl.pallas_call(
         fold_kernel,
         in_specs=[SMEM] + [VMEM] * 3,
         out_specs=HBM,
-        out_shape=pltpu.HBM((8, *shape), jnp.bfloat16),
-        scratch_shapes=[pltpu.VMEM(shape, jnp.bfloat16), pltpu.SemaphoreType.DMA((8,))],
+        out_shape=pltpu.HBM((4, *shape), jnp.bfloat16),
+        scratch_shapes=[pltpu.VMEM(shape, jnp.bfloat16), pltpu.SemaphoreType.DMA((4,))],
         compiler_params=limit(8),
         name="fold",
     )(place, parts, first, second)
@@ -216,15 +217,15 @@
 
 
 def update_kernel(place_ref, letters_ref, out_hbm, letter_ref, projected_ref, sems):
-    projected_ref[...] = jnp.sum(letters_ref[:, :8].astype(jnp.float32), axis=0)
-    first, second = letters_ref[:, 8].astype(jnp.float32), letters_ref[:, 9].astype(jnp.float32)
+    projected_ref[...] = jnp.sum(letters_ref[:, :4].astype(jnp.float32), axis=0)
+    first, second = letters_ref[:, 4].astype(jnp.float32), letters_ref[:, 5].astype(jnp.float32)
     first_new, second_new = moments(projected_ref[...], first, second)
-    letter_ref[:8] = (first_new / (jnp.sqrt(second_new) + 1e-08)).astype(jnp.bfloat16)
-    mine = projected_ref[place_ref[0]]
+    letter_ref[:4] = (first_new / (jnp.sqrt(second_new) + 1e-08)).astype(jnp.bfloat16)
+    mine = projected_ref[place_ref[0] // 2]
     high = mine.astype(jnp.bfloat16)
-    letter_ref[8] = high
-    letter_ref[9] = (mine - high.astype(jnp.float32)).astype(jnp.bfloat16)
-    send([(letter_ref, out_hbm.at[peer]) for peer in range(16)], sems)
+    letter_ref[4] = high
+    letter_ref[5] = (mine - high.astype(jnp.float32)).astype(jnp.bfloat16)
+    send([(letter_ref, out_hbm.at[peer]) for peer in range(32)], sems)
 
 
 def update(place, letters):
@@ -233,11 +234,11 @@
         update_kernel,
         in_specs=[SMEM, VMEM],
         out_specs=HBM,
-        out_shape=pltpu.HBM((16, *shape), jnp.bfloat16),
+        out_shape=pltpu.HBM((32, *shape), jnp.bfloat16),
         scratch_shapes=[
             pltpu.VMEM(shape, jnp.bfloat16),
-            pltpu.VMEM((8, *shape[1:]), jnp.float32),
-            pltpu.SemaphoreType.DMA((16,)),
+            pltpu.VMEM((4, *shape[1:]), jnp.float32),
+            pltpu.SemaphoreType.DMA((32,)),
         ],
         compiler_params=limit(8),
         name="update",
@@ -249,27 +250,38 @@
 
 
 def finish_kernel(
-    place_ref, basis_hbm, weight_hbm, first_hbm, second_hbm, near_ref, far_ref, w0, f1, f2, w4, b2, b1,
-    new_ref, step_ref, copy_ref, first_out, second_out, later_ref,
-    basis_ref, weight_ref, first_ref, second_ref, tiles, sems,
+    place_ref, basis_hbm, weight_hbm, first_hbm, second_hbm, near_ref, far_ref,
+    w0_hbm, b1_hbm, f1_hbm, w4_hbm, f2_hbm, b2_hbm,
+    new_ref, step_ref, copy_ref, first_out, second_out, rows_out, scale_out, basis_ref,
+    weight_ref, first_ref, second_ref, blocks, tiles, sems,
 ):
     fetched = []
     for slot, (source, target) in enumerate(
-        ((basis_hbm, basis_ref), (weight_hbm, weight_ref), (first_hbm, first_ref), (second_hbm, second_ref))
+        (
+            (basis_hbm, basis_ref),
+            (w0_hbm, blocks.at[0]),
+            (b1_hbm, blocks.at[1]),
+            (f1_hbm, blocks.at[2]),
+            (w4_hbm, blocks.at[3]),
+            (f2_hbm, blocks.at[4]),
+            (b2_hbm, blocks.at[5]),
+            (weight_hbm, weight_ref),
+            (first_hbm, first_ref),
+            (second_hbm, second_ref),
+        )
     ):
         copy = pltpu.make_async_copy(source, target, sems.at[6 + slot])
         copy.start()
         fetched.append(copy)
     z, y = place_ref[0], place_ref[1]
     is_low = place_ref[3] == 0
-    near, far = near_ref[:, :8].astype(jnp.float32), far_ref[:, :8].astype(jnp.float32)
+    near, far = near_ref[:, :4].astype(jnp.float32), far_ref[:, :4].astype(jnp.float32)
     energy = jnp.sum(near * near + far * far)
     count = 2 * near.shape[0] * near.shape[1] * near.shape[2] * near.shape[3]
     spread = jnp.sqrt(jnp.full((1, 128), energy / count, jnp.float32))
-    scale = (-1.0 / (spread + 1e-06))[:, :1]
-    for copy in fetched:
-        copy.wait()
-    basis = basis_ref[...]
+    scales = -1.0 / (spread + 1e-06)
+    scale_out[...] = scales
+    scale = scales[:, :1]
 
     def rows_of(close, distant):
         close, distant = (array.reshape(-1, array.shape[-1]) for array in (close, distant))
@@ -277,27 +289,34 @@
             [jnp.where(is_low, close, distant), jnp.where(is_low, distant, close)], axis=1
         )
 
-    def step_of(block):
-        at = block % 8
-        return dot(basis, rows_of(near_ref[:, at], far_ref[:, at]), 1, 1) * scale
-
+    def block_rows(block):
+        peers, at = pl.ds(pl.multiple_of(block % 2 * 16, 16), 16), block % 8 // 2
+        return rows_of(near_ref[peers, at], far_ref[peers, at])
+
+    fetched[0].wait()
+    basis = basis_ref[...]
     copies = []
-    for slot, (block, hops) in enumerate(((w0, 0), (f1, 7), (b1, 1), (f2, 6), (b2, 2), (w4, 4))):
-        tiles[slot] = (block[...].astype(jnp.float32) + step_of(z + hops)).astype(jnp.bfloat16)
+    for slot, hops in enumerate((0, 1, 7, 4, 6, 2)):
+        step = dot(basis, block_rows(z + hops), 1, 1) * scale
+        fetched[slot + 1].wait()
+        tiles[slot] = (blocks[slot].astype(jnp.float32) + step).astype(jnp.bfloat16)
         copy = pltpu.make_async_copy(tiles.at[slot], copy_ref.at[:, columns(z + hops)], sems.at[slot])
         copy.start()
         copies.append(copy)
     for slot, hops in enumerate((5, 3)):
-        later_ref[slot] = step_of(z + hops)
-
-    mine = pl.ds(y * 4, 4)
-    step = dot(rows_of(near_ref[mine, z], far_ref[mine, z]), basis, 1, 1) * scale
+        rows_out[slot] = block_rows(z + hops)
+
+    for copy in fetched[7:]:
+        copy.wait()
+    first_letter = z % 2 * 16 + y * 4
+    mine = pl.ds(first_letter, 4)
+    step = dot(rows_of(near_ref[mine, z // 2], far_ref[mine, z // 2]), basis, 1, 1) * scale
     step_ref[...] = step
     new_ref[...] = weight_ref[...] + step
     for source in range(4):
         rows = pl.ds(source * 16, 16)
-        letter = y * 4 + source
-        piece = near_ref[letter, 8].astype(jnp.float32) + near_ref[letter, 9].astype(jnp.float32)
+        letter = first_letter + source
+        piece = near_ref[letter, 4].astype(jnp.float32) + near_ref[letter, 5].astype(jnp.float32)
         first_new, second_new = moments(piece, first_ref[rows, :], second_ref[rows, :])
         first_out[rows, :] = first_new
         second_out[rows, :] = second_new
@@ -306,38 +325,41 @@
 
 
 def finish(place, basis, weight, first, second, near, far, blocks):
-    values = basis.shape[0]
+    values, rank = basis.shape
     like = lambda array: jax.ShapeDtypeStruct(array.shape, jnp.float32)
     return pl.pallas_call(
         finish_kernel,
-        in_specs=[SMEM] + [HBM] * 4 + [VMEM] * (2 + len(blocks)),
-        out_specs=[VMEM, VMEM, HBM, VMEM, VMEM, VMEM],
+        in_specs=[SMEM] + [HBM] * 4 + [VMEM] * 2 + [HBM] * 6,
+        out_specs=[VMEM, VMEM, HBM] + [VMEM] * 5,
         out_shape=[
             like(weight),
             like(weight),
             pltpu.HBM((values, 2048), jnp.bfloat16),
             like(first),
             like(second),
-            pltpu.VMEM((2, values, 256), jnp.float32),
+            pltpu.VMEM((2, 256, rank), jnp.bfloat16),
+            pltpu.VMEM((1, 128), jnp.float32),
+            pltpu.VMEM(basis.shape, basis.dtype),
         ],
         scratch_shapes=[
-            pltpu.VMEM(basis.shape, basis.dtype),
             pltpu.VMEM(weight.shape, weight.dtype),
             pltpu.VMEM(first.shape, first.dtype),
             pltpu.VMEM(second.shape, second.dtype),
             pltpu.VMEM((6, values, 256), jnp.bfloat16),
-            pltpu.SemaphoreType.DMA((10,)),
+            pltpu.VMEM((6, values, 256), jnp.bfloat16),
+            pltpu.SemaphoreType.DMA((16,)),
         ],
-        compiler_params=limit(16),
+        compiler_params=limit(20),
         name="finish",
-    )(place, *in_hbm(basis, weight, first, second), near, far, *in_vmem(*blocks))
-
-
-def last_kernel(place_ref, later_ref, f3, b3, copy_in, copy_ref, tiles, sems):
+    )(place, *in_hbm(basis, weight, first, second), near, far, *in_hbm(*blocks))
+
+
+def last_kernel(place_ref, rows_ref, scale_ref, basis_ref, f3, b3, copy_in, copy_ref, tiles, sems):
     z = place_ref[0]
     copies = []
     for slot, (block, hops) in enumerate(((f3, 5), (b3, 3))):
-        tiles[slot] = (block[...].astype(jnp.float32) + later_ref[slot]).astype(jnp.bfloat16)
+        step = dot(basis_ref[...], rows_ref[slot], 1, 1) * scale_ref[:, :1]
+        tiles[slot] = (block[...].astype(jnp.float32) + step).astype(jnp.bfloat16)
         copy = pltpu.make_async_copy(tiles.at[slot], copy_ref.at[:, columns(z + hops)], sems.at[slot])
         copy.start()
         copies.append(copy)
@@ -348,14 +370,14 @@
 def last(place, later, f3, b3, copy):
     return pl.pallas_call(
         last_kernel,
-        in_specs=[SMEM, VMEM, VMEM, VMEM, HBM],
+        in_specs=[SMEM] + [VMEM] * 5 + [HBM],
         out_specs=HBM,
         out_shape=pltpu.HBM(copy.shape, copy.dtype),
-        input_output_aliases={4: 0},
+        input_output_aliases={6: 0},
         scratch_shapes=[pltpu.VMEM((2, copy.shape[0], 256), copy.dtype), pltpu.SemaphoreType.DMA((2,))],
         compiler_params=limit(8),
         name="last",
-    )(place, *in_vmem(later, f3, b3), *in_hbm(copy))
+    )(place, *in_vmem(*later), f3, b3, *in_hbm(copy))
 
 
 def exchange(array, axes):
@@ -363,23 +385,23 @@
 
 
 def chain(first_mix, second_mix, lambda_head, head_gain, out_cotangent, basis, weight, first_moment, second_moment):
-    place = jnp.stack([lax.axis_index(name).astype(jnp.int32) for name in ("z", "y", "x", "tp")])
+    place = jnp.stack([lax.axis_index(name).astype(jnp.int32) for name in (Z, "y", "x", "tp")])
     turned = weight.T
     own, sent, narrow = heads(place, lambda_head, first_mix, second_mix, head_gain, basis, turned)
 
     w0 = widen(place, [narrow] + [shift(narrow, "y", hops) for hops in (1, 2, 3)])
-    opposite = shift(narrow, "z", 4)
+    opposite = shift(narrow, Z, 4)
     w4 = widen(place, [opposite] + [shift(opposite, "y", hops) for hops in (1, 2, 3)])
-    f1, b1 = shift(w0, "z", 1), shift(w0, "z", -1)
-    f2, b2 = shift(f1, "z", 1), shift(b1, "z", -1)
-    f3, b3 = shift(f2, "z", 1), shift(b2, "z", -1)
+    f1, b1 = shift(w0, Z, 1), shift(w0, Z, -1)
+    f2, b2 = shift(f1, Z, 1), shift(b1, Z, -1)
+    f3, b3 = shift(f2, Z, 1), shift(b2, Z, -1)
 
     parts = gradient(own, swap_cores(sent), out_cotangent)
-    sums = fold(place, exchange(parts, ("y", "x")), first_moment, second_moment)
-    near = exchange(update(place, exchange(sums, "z")), ("y", "x"))
+    sums = fold(place, exchange(parts, NEAR), first_moment, second_moment)
+    near = exchange(update(place, exchange(sums, "zh")), NEAR)
     far = swap_cores(near)
-    weight_new, step_out, most, first_new, second_new, later = finish(
-        place, basis, turned, first_moment, second_moment, near, far, (w0, f1, f2, w4, b2, b1)
+    weight_new, step_out, most, first_new, second_new, *later = finish(
+        place, basis, turned, first_moment, second_moment, near, far, (w0, b1, f1, w4, f2, b2)
     )
     weight_copy = last(place, later, f3, b3, most)
     return (weight_new.T, weight_copy, step_out.T, first_new, second_new)
@@ -387,8 +409,8 @@
 
 def solution(mesh):
     finer = Mesh(
-        mesh.devices.reshape(8, 4, mesh.shape["rep"], mesh.shape["tp"]),
-        ("z", "y", "x", "tp"),
+        mesh.devices.reshape(4, 2, 4, mesh.shape["rep"], mesh.shape["tp"]),
+        (*FS_REP, "tp"),
     )
     return jax.shard_map(
         chain,

time: 114 us -> 139 us (1.22)
  the two profiles are of different devices: /device:TPU:28 before, /device:TPU:24 now
where the time goes in v6:
time: 139 us
  waiting for transfers between devices  59.1 us (43%)
  blocking collectives  35.4 us (25%)
  starting transfers between devices  23 us (17%)
  Pallas kernels  19.1 us (14%)
    ppermute x13, waiting for transfers between devices, shift(): lax.ppermute(array, axis, [(i, (i + hops) % count) for i in range(count)])  57.7 us
    all_to_all x2, blocking collectives, exchange(): return lax.all_to_all(array, axes, 0, 0, tiled=True)  35.4 us
    ppermute x13, starting transfers between devices, shift(): lax.ppermute(array, axis, [(i, (i + hops) % count) for i in range(count)])  17.7 us
    pallas_call x1, Pallas kernels, finish(): pl.pallas_call(finish_kernel, in_specs=[SMEM] + [HBM] * 4 + [VMEM] * 2 +...  6.97 us
    all_to_all x1, starting transfers between devices, exchange(): return lax.all_to_all(array, axes, 0, 0, tiled=True)  5.23 us
    pallas_call x1, Pallas kernels, heads(): pl.pallas_call(heads_kernel, in_specs=[SMEM] + [HBM] * 6, out_specs=[VMEM...  4.14 us
  transfers between devices with their start and end apart: 16, of which 9 were waited for; matrix products, arithmetic and copies ran while one was open for 0% of the time, Pallas kernels for 6%

profile of v6, /device:TPU:24, one launch (start us, length us, event | category | flops | bytes accessed | tf_op | source)
XLA Modules:
  0.0 138.5 jit_solution(16605665044970252362)
XLA Ops:
  0.7 0.1 pad_add_fusion.place_ref
  0.7 4.1 %heads.1 = (f32[768,128]{1,0:T(8,128)S(1)}, bf16[768,128]{1,0:T(8,128)(2,1)S(1)}, bf16[64,1024]{1,0:T(8,128)(2,1)S(1)}) custom-call(s32[4]{0:T(128)S(1)} %pad_add_fusion.place_ref, f32[1,4]{1,0:T(1,128)} %bitcast.12, bf16[768,1024]{1,0:T(8,128)(2,1)} %first_hbm.2, bf16[768,1024]{1,0:T(8,128)(2,1)} %second_hbm.2, f32[1,256]{1,0:T(1,128)} %bitcast.11, ...), custom_call_target="tpu_custom_call" | custom-call | tf_op jit(solution)/shard_map/heads/pallas_call | solution.py:107
  4.9 0.0 copy-start.3
  4.9 0.0 copy-start.4
  4.9 0.1 collective-permute-start
  5.0 1.4 %collective-permute-done.far_ref = bf16[768,128]{1,0:T(8,128)(2,1)S(1)} collective-permute-done((bf16[768,128]{1,0:T(8,128)(2,1)S(1)}, bf16[768,128]{1,0:T(8,128)(2,1)S(1)}, u32[]{:S(2)}, u32[]{:S(2)}) %collective-permute-start) | collective-permute-done | bytes 196640 | tf_op jit(solution)/shard_map/ppermute | solution.py:36
  6.4 0.0 copy-done
  6.4 1.4 %gradient.1 = bf16[32,4,16,128]{3,2,1,0:T(8,128)(2,1)} custom-call(f32[768,128]{1,0:T(8,128)S(1)} %get-tuple-element.16.own_ref, bf16[768,128]{1,0:T(8,128)(2,1)S(1)} %collective-permute-done.far_ref, bf16[768,2048]{1,0:T(8,128)(2,1)S(1)} %copy-done), custom_call_target="tpu_custom_call" | custom-call | tf_op jit(solution)/shard_map/gradient/pallas_call | solution.py:171
  7.8 19.3 %all_to_all.15.parts_ref = bf16[32,4,16,128]{3,2,1,0:T(8,128)(2,1)S(1)} all-to-all(bf16[32,4,16,128]{3,2,1,0:T(8,128)(2,1)} %gradient.1), channel_id=1, replica_groups=mesh['zh'=4,'zl'=2,'y'=4,'x'=4,'tp'=2] {'zl','y','x'}, dimensions={0} | all-to-all | bytes 1048576 | tf_op jit(solution)/shard_map/all_to_all | solution.py:384
  27.2 1.3 fold.1
  28.5 16.0 %all_to_all.16.letters_ref = bf16[4,6,16,128]{3,2,1,0:T(8,128)(2,1)S(1)} all-to-all(bf16[4,6,16,128]{3,2,1,0:T(8,128)(2,1)} %fold.1), channel_id=1, replica_groups=mesh['zh'=4,'zl'=2,'y'=4,'x'=4,'tp'=2] {'zh'}, dimensions={0} | all-to-all | bytes 196608 | tf_op jit(solution)/shard_map/all_to_all | solution.py:384
  44.5 1.7 %update.1 = bf16[32,6,16,128]{3,2,1,0:T(8,128)(2,1)} custom-call(s32[4]{0:T(128)S(1)} %pad_add_fusion.place_ref, bf16[4,6,16,128]{3,2,1,0:T(8,128)(2,1)S(1)} %all_to_all.16.letters_ref), custom_call_target="tpu_custom_call" | custom-call | tf_op jit(solution)/shard_map/update/pallas_call | solution.py:233
  46.2 5.2 %all-to-all-start.2 = ((bf16[32,6,16,128]{3,2,1,0:T(8,128)(2,1)}), bf16[32,6,16,128]{3,2,1,0:T(8,128)(2,1)S(1)}, u32[]{:S(2)}, u32[]{:S(2)}) async-start(bf16[32,6,16,128]{3,2,1,0:T(8,128)(2,1)} %update.1), calls=%async_computation.2 | async-start | bytes 1572864 | tf_op jit(solution)/shard_map/all_to_all | solution.py:384
  51.5 0.3 collective-permute-start.2
  51.8 2.7 %collective-permute-start.3 = (bf16[64,1024]{1,0:T(8,128)(2,1)S(1)}, bf16[64,1024]{1,0:T(8,128)(2,1)S(1)}, u32[]{:S(2)}, u32[]{:S(2)}) collective-permute-start(bf16[64,1024]{1,0:T(8,128)(2,1)S(1)} %get-tuple-element.18.own_ref), channel_id=1, source_target_pairs={{0,16},{8,24},{16,0},{24,8},{1,17},{9,25},{17,1},{25,9},{2,18},{10... | collective-permute-start | bytes 393224 | tf_op jit(solution)/shard_map/ppermute | solution.py:32
  54.5 0.0 collective-permute-start.4
  54.5 8.9 %collective-permute-done.2.one_ref = bf16[64,1024]{1,0:T(8,128)(2,1)S(1)} collective-permute-done((bf16[64,1024]{1,0:T(8,128)(2,1)S(1)}, bf16[64,1024]{1,0:T(8,128)(2,1)S(1)}, u32[]{:S(2)}, u32[]{:S(2)}) %collective-permute-start.2) | collective-permute-done | bytes 131104 | tf_op jit(solution)/shard_map/ppermute | solution.py:32
  63.4 0.6 collective-permute-done.3.two_ref
  64.0 1.7 %collective-permute-done.4.three_ref = bf16[64,1024]{1,0:T(8,128)(2,1)S(1)} collective-permute-done((bf16[64,1024]{1,0:T(8,128)(2,1)S(1)}, bf16[64,1024]{1,0:T(8,128)(2,1)S(1)}, u32[]{:S(2)}, u32[]{:S(2)}) %collective-permute-start.4) | collective-permute-done | bytes 131104 | tf_op jit(solution)/shard_map/ppermute | solution.py:32
  65.7 0.8 widen.2.w0_hbm
  66.5 1.4 collective-permute-start.6
  67.9 1.9 %collective-permute-start.5 = (bf16[1024,256]{1,0:T(8,128)(2,1)S(1)}, bf16[1024,256]{1,0:T(8,128)(2,1)S(1)}, u32[]{:S(2)}, u32[]{:S(2)}) collective-permute-start(bf16[1024,256]{1,0:T(8,128)(2,1)S(1)} %widen.2.w0_hbm), channel_id=1, source_target_pairs={{0,224},{32,0},{64,32},{96,64},{128,96},{160,128},{192,160},{224,1... | collective-permute-start | bytes 1572872 | tf_op jit(solution)/shard_map/ppermute | solution.py:32
  69.8 11.7 %collective-permute-done.6.f1_hbm = bf16[1024,256]{1,0:T(8,128)(2,1)S(1)} collective-permute-done((bf16[1024,256]{1,0:T(8,128)(2,1)S(1)}, bf16[1024,256]{1,0:T(8,128)(2,1)S(1)}, u32[]{:S(2)}, u32[]{:S(2)}) %collective-permute-start.6) | collective-permute-done | bytes 524320 | tf_op jit(solution)/shard_map/ppermute | solution.py:32
  81.6 0.2 collective-permute-start.11
  81.8 0.0 collective-permute-done.5.b1_hbm
  81.8 3.0 %collective-permute-start.12 = (bf16[1024,256]{1,0:T(8,128)(2,1)S(1)}, bf16[1024,256]{1,0:T(8,128)(2,1)S(1)}, u32[]{:S(2)}, u32[]{:S(2)}) collective-permute-start(bf16[1024,256]{1,0:T(8,128)(2,1)S(1)} %collective-permute-done.5.b1_hbm), channel_id=1, source_target_pairs={{0,224},{32,0},{64,32},{96,64},{128,96},{160,128},{192,160},{224,1... | collective-permute-start | bytes 1572872 | tf_op jit(solution)/shard_map/ppermute | solution.py:32
  84.8 0.0 all-to-all-done.2.near_ref
  84.8 0.0 collective-permute-start.1
  84.8 10.9 %collective-permute-done.11.f2_hbm = bf16[1024,256]{1,0:T(8,128)(2,1)S(1)} collective-permute-done((bf16[1024,256]{1,0:T(8,128)(2,1)S(1)}, bf16[1024,256]{1,0:T(8,128)(2,1)S(1)}, u32[]{:S(2)}, u32[]{:S(2)}) %collective-permute-start.11) | collective-permute-done | bytes 524320 | tf_op jit(solution)/shard_map/ppermute | solution.py:32
  95.7 0.0 collective-permute-start.13
  95.7 0.0 collective-permute-done.12.b2_hbm
  95.7 0.0 copy-start.8
  95.7 3.2 %collective-permute-start.14 = (bf16[1024,256]{1,0:T(8,128)(2,1)S(1)}, bf16[1024,256]{1,0:T(8,128)(2,1)S(1)}, u32[]{:S(2)}, u32[]{:S(2)}) collective-permute-start(bf16[1024,256]{1,0:T(8,128)(2,1)S(1)} %collective-permute-done.12.b2_hbm), channel_id=1, source_target_pairs={{0,224},{32,0},{64,32},{96,64},{128,96},{160,128},{192,160},{224,1... | collective-permute-start | bytes 1572872 | tf_op jit(solution)/shard_map/ppermute | solution.py:32
  99.0 1.7 %collective-permute-start.7 = (bf16[64,1024]{1,0:T(8,128)(2,1)S(1)}, bf16[64,1024]{1,0:T(8,128)(2,1)S(1)}, u32[]{:S(2)}, u32[]{:S(2)}) collective-permute-start(bf16[64,1024]{1,0:T(8,128)(2,1)S(1)} %get-tuple-element.18.own_ref), channel_id=1, source_target_pairs={{0,128},{32,160},{64,192},{96,224},{128,0},{160,32},{192,64},{224,... | collective-permute-start | bytes 393224 | tf_op jit(solution)/shard_map/ppermute | solution.py:32
  100.6 13.0 %collective-permute-done.7.own_ref = bf16[64,1024]{1,0:T(8,128)(2,1)S(1)} collective-permute-done((bf16[64,1024]{1,0:T(8,128)(2,1)S(1)}, bf16[64,1024]{1,0:T(8,128)(2,1)S(1)}, u32[]{:S(2)}, u32[]{:S(2)}) %collective-permute-start.7) | collective-permute-done | bytes 131104 | tf_op jit(solution)/shard_map/ppermute | solution.py:32
  113.7 0.0 collective-permute-start.10
  113.7 3.2 %collective-permute-start.8 = (bf16[64,1024]{1,0:T(8,128)(2,1)S(1)}, bf16[64,1024]{1,0:T(8,128)(2,1)S(1)}, u32[]{:S(2)}, u32[]{:S(2)}) collective-permute-start(bf16[64,1024]{1,0:T(8,128)(2,1)S(1)} %collective-permute-done.7.own_ref), channel_id=1, source_target_pairs={{0,8},{8,16},{16,24},{24,0},{1,9},{9,17},{17,25},{25,1},{2,10},{10... | collective-permute-start | bytes 393224 | tf_op jit(solution)/shard_map/ppermute | solution.py:32
  116.9 4.3 %collective-permute-done.10.three_ref = bf16[64,1024]{1,0:T(8,128)(2,1)S(1)} collective-permute-done((bf16[64,1024]{1,0:T(8,128)(2,1)S(1)}, bf16[64,1024]{1,0:T(8,128)(2,1)S(1)}, u32[]{:S(2)}, u32[]{:S(2)}) %collective-permute-start.10) | collective-permute-done | bytes 131104 | tf_op jit(solution)/shard_map/ppermute | solution.py:32
  121.2 0.0 collective-permute-start.9
  121.2 0.0 collective-permute-done.8.one_ref
  121.2 6.5 %collective-permute-done.9.two_ref = bf16[64,1024]{1,0:T(8,128)(2,1)S(1)} collective-permute-done((bf16[64,1024]{1,0:T(8,128)(2,1)S(1)}, bf16[64,1024]{1,0:T(8,128)(2,1)S(1)}, u32[]{:S(2)}, u32[]{:S(2)}) %collective-permute-start.9) | collective-permute-done | bytes 131104 | tf_op jit(solution)/shard_map/ppermute | solution.py:32
  127.7 0.8 widen.3.w4_hbm
  128.5 0.8 copy-done.2
  129.3 0.0 collective-permute-done.1.far_ref
  129.4 7.0 %finish.1 = (f32[64,1024]{1,0:T(8,128)}, f32[64,1024]{1,0:T(8,128)}, bf16[1024,2048]{1,0:T(8,128)(2,1)}, f32[64,128]{1,0:T(8,128)}, f32[64,128]{1,0:T(8,128)}, /...) custom-call(s32[4]{0:T(128)S(1)} %pad_add_fusion.place_ref, ...), custom_call_target="tpu_custom_call" | custom-call | tf_op jit(solution)/shard_map/finish/pallas_call | solution.py:330
  136.3 0.0 collective-permute-done.13.f3
  136.3 0.0 collective-permute-done.14.b3
  136.4 2.0 %last.1 = bf16[1024,2048]{1,0:T(8,128)(2,1)} custom-call(s32[4]{0:T(128)S(1)} %pad_add_fusion.place_ref, bf16[2,256,256]{2,1,0:T(8,128)(2,1)S(1)} %get-tuple-element.20.rows_ref, f32[1,128]{1,0:T(1,128)S(1)} %get-tuple-element.21.scale_ref, bf16[1024,256]{1,0:T(8,128)(2,1)S(1)} %get-tuple-element.22.basis_ref, ...), custom_call_target="tpu_custom_call", output_to_operand_aliasing={{}: (6, {})} | custom-call | tf_op jit(solution)/shard_map/last/pallas_call | solution.py:371
  (13 shorter events, 0.0 us)
Async XLA Ops:
  0.6 5.8 %copy-start = (bf16[768,2048]{1,0:T(8,128)(2,1)S(1)}, bf16[768,2048]{1,0:T(8,128)(2,1)}, u32[]{:S(2)}) copy-start(bf16[768,2048]{1,0:T(8,128)(2,1)} %cot_ref.1) | copy-start | bytes 9437188
  4.9 22.3 %copy-start.3 = (f32[64,128]{1,0:T(8,128)S(1)}, f32[64,128]{1,0:T(8,128)}, u32[]{:S(2)}) copy-start(f32[64,128]{1,0:T(8,128)} %first_hbm.3) | copy-start | bytes 98308
  4.9 22.3 %copy-start.4 = (f32[64,128]{1,0:T(8,128)S(1)}, f32[64,128]{1,0:T(8,128)}, u32[]{:S(2)}) copy-start(f32[64,128]{1,0:T(8,128)} %second_hbm.3) | copy-start | bytes 98308
  4.9 1.5 %collective-permute-start = (bf16[768,128]{1,0:T(8,128)(2,1)S(1)}, bf16[768,128]{1,0:T(8,128)(2,1)S(1)}, u32[]{:S(2)}, u32[]{:S(2)}) collective-permute-start(bf16[768,128]{1,0:T(8,128)(2,1)S(1)} %get-tuple-element.17), channel_id=1, source_target_pairs={{0,1},{1,0},{2,3},{3,2},{4,5},{5,4},{6,7},{7,6},{8,9},{9,8},{10,11... | collective-permute-start | bytes 589832 | tf_op jit(solution)/shard_map/ppermute | solution.py:36
  46.2 38.6 %all-to-all-start.2 = ((bf16[32,6,16,128]{3,2,1,0:T(8,128)(2,1)}), bf16[32,6,16,128]{3,2,1,0:T(8,128)(2,1)S(1)}, u32[]{:S(2)}, u32[]{:S(2)}) async-start(bf16[32,6,16,128]{3,2,1,0:T(8,128)(2,1)} %update.1), calls=%async_computation.2 | async-start | bytes 1572864 | tf_op jit(solution)/shard_map/all_to_all | solution.py:384
  51.5 11.9 %collective-permute-start.2 = (bf16[64,1024]{1,0:T(8,128)(2,1)S(1)}, bf16[64,1024]{1,0:T(8,128)(2,1)S(1)}, u32[]{:S(2)}, u32[]{:S(2)}) collective-permute-start(bf16[64,1024]{1,0:T(8,128)(2,1)S(1)} %get-tuple-element.18.own_ref), channel_id=1, source_target_pairs={{0,8},{8,16},{16,24},{24,0},{1,9},{9,17},{17,25},{25,1},{2,10},{10... | collective-permute-start | bytes 393224 | tf_op jit(solution)/shard_map/ppermute | solution.py:32
  51.8 12.3 %collective-permute-start.3 = (bf16[64,1024]{1,0:T(8,128)(2,1)S(1)}, bf16[64,1024]{1,0:T(8,128)(2,1)S(1)}, u32[]{:S(2)}, u32[]{:S(2)}) collective-permute-start(bf16[64,1024]{1,0:T(8,128)(2,1)S(1)} %get-tuple-element.18.own_ref), channel_id=1, source_target_pairs={{0,16},{8,24},{16,0},{24,8},{1,17},{9,25},{17,1},{25,9},{2,18},{10... | collective-permute-start | bytes 393224 | tf_op jit(solution)/shard_map/ppermute | solution.py:32
  54.5 11.2 %collective-permute-start.4 = (bf16[64,1024]{1,0:T(8,128)(2,1)S(1)}, bf16[64,1024]{1,0:T(8,128)(2,1)S(1)}, u32[]{:S(2)}, u32[]{:S(2)}) collective-permute-start(bf16[64,1024]{1,0:T(8,128)(2,1)S(1)} %get-tuple-element.18.own_ref), channel_id=1, source_target_pairs={{0,24},{8,0},{16,8},{24,16},{1,25},{9,1},{17,9},{25,17},{2,26},{10... | collective-permute-start | bytes 393224 | tf_op jit(solution)/shard_map/ppermute | solution.py:32
  66.5 62.8 %copy-start.1 = (bf16[1024,256]{1,0:T(8,128)(2,1)}, bf16[1024,256]{1,0:T(8,128)(2,1)S(1)}, u32[]{:S(2)}) copy-start(bf16[1024,256]{1,0:T(8,128)(2,1)S(1)} %widen.2.w0_hbm) | copy-start | bytes 1572868
  66.5 15.1 %collective-permute-start.6 = (bf16[1024,256]{1,0:T(8,128)(2,1)S(1)}, bf16[1024,256]{1,0:T(8,128)(2,1)S(1)}, u32[]{:S(2)}, u32[]{:S(2)}) collective-permute-start(bf16[1024,256]{1,0:T(8,128)(2,1)S(1)} %widen.2.w0_hbm), channel_id=1, source_target_pairs={{0,32},{32,64},{64,96},{96,128},{128,160},{160,192},{192,224},{224... | collective-permute-start | bytes 1572872 | tf_op jit(solution)/shard_map/ppermute | solution.py:32
  67.9 13.9 %collective-permute-start.5 = (bf16[1024,256]{1,0:T(8,128)(2,1)S(1)}, bf16[1024,256]{1,0:T(8,128)(2,1)S(1)}, u32[]{:S(2)}, u32[]{:S(2)}) collective-permute-start(bf16[1024,256]{1,0:T(8,128)(2,1)S(1)} %widen.2.w0_hbm), channel_id=1, source_target_pairs={{0,224},{32,0},{64,32},{96,64},{128,96},{160,128},{192,160},{224,1... | collective-permute-start | bytes 1572872 | tf_op jit(solution)/shard_map/ppermute | solution.py:32
  81.6 47.7 %copy-start.5 = (bf16[1024,256]{1,0:T(8,128)(2,1)}, bf16[1024,256]{1,0:T(8,128)(2,1)S(1)}, u32[]{:S(2)}) copy-start(bf16[1024,256]{1,0:T(8,128)(2,1)S(1)} %collective-permute-done.6.f1_hbm) | copy-start | bytes 1572868
  81.6 14.1 %collective-permute-start.11 = (bf16[1024,256]{1,0:T(8,128)(2,1)S(1)}, bf16[1024,256]{1,0:T(8,128)(2,1)S(1)}, u32[]{:S(2)}, u32[]{:S(2)}) collective-permute-start(bf16[1024,256]{1,0:T(8,128)(2,1)S(1)} %collective-permute-done.6.f1_hbm), channel_id=1, source_target_pairs={{0,32},{32,64},{64,96},{96,128},{128,160},{160,192},{192,224},{224... | collective-permute-start | bytes 1572872 | tf_op jit(solution)/shard_map/ppermute | solution.py:32
  81.8 47.6 %copy-start.6 = (bf16[1024,256]{1,0:T(8,128)(2,1)}, bf16[1024,256]{1,0:T(8,128)(2,1)S(1)}, u32[]{:S(2)}) copy-start(bf16[1024,256]{1,0:T(8,128)(2,1)S(1)} %collective-permute-done.5.b1_hbm) | copy-start | bytes 1572868
  81.8 13.9 %collective-permute-start.12 = (bf16[1024,256]{1,0:T(8,128)(2,1)S(1)}, bf16[1024,256]{1,0:T(8,128)(2,1)S(1)}, u32[]{:S(2)}, u32[]{:S(2)}) collective-permute-start(bf16[1024,256]{1,0:T(8,128)(2,1)S(1)} %collective-permute-done.5.b1_hbm), channel_id=1, source_target_pairs={{0,224},{32,0},{64,32},{96,64},{128,96},{160,128},{192,160},{224,1... | collective-permute-start | bytes 1572872 | tf_op jit(solution)/shard_map/ppermute | solution.py:32
  84.8 44.5 %collective-permute-start.1 = (bf16[32,6,16,128]{3,2,1,0:T(8,128)(2,1)S(1)}, bf16[32,6,16,128]{3,2,1,0:T(8,128)(2,1)S(1)}, u32[]{:S(2)}, u32[]{:S(2)}) collective-permute-start(bf16[32,6,16,128]{3,2,1,0:T(8,128)(2,1)S(1)} %all-to-all-done.2.near_ref), channel_id=1, source_target_pairs={{0,1},{1,0},{2,3},{3,2},{4,5},{5,4},{6,7},{7,6},{8,9},{9,8},{10,11... | collective-permute-start | bytes 2359304 | tf_op jit(solution)/shard_map/ppermute | solution.py:36
  95.7 33.6 %copy-start.7 = (bf16[1024,256]{1,0:T(8,128)(2,1)}, bf16[1024,256]{1,0:T(8,128)(2,1)S(1)}, u32[]{:S(2)}) copy-start(bf16[1024,256]{1,0:T(8,128)(2,1)S(1)} %collective-permute-done.11.f2_hbm) | copy-start | bytes 1572868
  95.7 40.6 %collective-permute-start.13 = (bf16[1024,256]{1,0:T(8,128)(2,1)S(1)}, bf16[1024,256]{1,0:T(8,128)(2,1)S(1)}, u32[]{:S(2)}, u32[]{:S(2)}) collective-permute-start(bf16[1024,256]{1,0:T(8,128)(2,1)S(1)} %collective-permute-done.11.f2_hbm), channel_id=1, source_target_pairs={{0,32},{32,64},{64,96},{96,128},{128,160},{160,192},{192,224},{224... | collective-permute-start | bytes 1572872 | tf_op jit(solution)/shard_map/ppermute | solution.py:32
  95.7 33.6 %copy-start.8 = (bf16[1024,256]{1,0:T(8,128)(2,1)}, bf16[1024,256]{1,0:T(8,128)(2,1)S(1)}, u32[]{:S(2)}) copy-start(bf16[1024,256]{1,0:T(8,128)(2,1)S(1)} %collective-permute-done.12.b2_hbm) | copy-start | bytes 1572868
  95.7 40.6 %collective-permute-start.14 = (bf16[1024,256]{1,0:T(8,128)(2,1)S(1)}, bf16[1024,256]{1,0:T(8,128)(2,1)S(1)}, u32[]{:S(2)}, u32[]{:S(2)}) collective-permute-start(bf16[1024,256]{1,0:T(8,128)(2,1)S(1)} %collective-permute-done.12.b2_hbm), channel_id=1, source_target_pairs={{0,224},{32,0},{64,32},{96,64},{128,96},{160,128},{192,160},{224,1... | collective-permute-start | bytes 1572872 | tf_op jit(solution)/shard_map/ppermute | solution.py:32
  99.0 14.7 %collective-permute-start.7 = (bf16[64,1024]{1,0:T(8,128)(2,1)S(1)}, bf16[64,1024]{1,0:T(8,128)(2,1)S(1)}, u32[]{:S(2)}, u32[]{:S(2)}) collective-permute-start(bf16[64,1024]{1,0:T(8,128)(2,1)S(1)} %get-tuple-element.18.own_ref), channel_id=1, source_target_pairs={{0,128},{32,160},{64,192},{96,224},{128,0},{160,32},{192,64},{224,... | collective-permute-start | bytes 393224 | tf_op jit(solution)/shard_map/ppermute | solution.py:32
  113.7 7.6 %collective-permute-start.10 = (bf16[64,1024]{1,0:T(8,128)(2,1)S(1)}, bf16[64,1024]{1,0:T(8,128)(2,1)S(1)}, u32[]{:S(2)}, u32[]{:S(2)}) collective-permute-start(bf16[64,1024]{1,0:T(8,128)(2,1)S(1)} %collective-permute-done.7.own_ref), channel_id=1, source_target_pairs={{0,24},{8,0},{16,8},{24,16},{1,25},{9,1},{17,9},{25,17},{2,26},{10... | collective-permute-start | bytes 393224 | tf_op jit(solution)/shard_map/ppermute | solution.py:32
  113.7 7.6 %collective-permute-start.8 = (bf16[64,1024]{1,0:T(8,128)(2,1)S(1)}, bf16[64,1024]{1,0:T(8,128)(2,1)S(1)}, u32[]{:S(2)}, u32[]{:S(2)}) collective-permute-start(bf16[64,1024]{1,0:T(8,128)(2,1)S(1)} %collective-permute-done.7.own_ref), channel_id=1, source_target_pairs={{0,8},{8,16},{16,24},{24,0},{1,9},{9,17},{17,25},{25,1},{2,10},{10... | collective-permute-start | bytes 393224 | tf_op jit(solution)/shard_map/ppermute | solution.py:32
  121.2 6.5 %collective-permute-start.9 = (bf16[64,1024]{1,0:T(8,128)(2,1)S(1)}, bf16[64,1024]{1,0:T(8,128)(2,1)S(1)}, u32[]{:S(2)}, u32[]{:S(2)}) collective-permute-start(bf16[64,1024]{1,0:T(8,128)(2,1)S(1)} %collective-permute-done.7.own_ref), channel_id=1, source_target_pairs={{0,16},{8,24},{16,0},{24,8},{1,17},{9,25},{17,1},{25,9},{2,18},{10... | collective-permute-start | bytes 393224 | tf_op jit(solution)/shard_map/ppermute | solution.py:32
  128.5 0.8 copy-start.2

commit v7 on v4

--- a/solution.py
+++ b/solution.py
@@ -109,7 +109,7 @@
         out_shape=[
             jax.ShapeDtypeStruct((tokens, half), jnp.float32),
             jax.ShapeDtypeStruct((tokens, half), jnp.bfloat16),
-            jax.ShapeDtypeStruct(weight.shape, jnp.bfloat16),
+            pltpu.VMEM(weight.shape, jnp.bfloat16),
         ],
         scratch_shapes=[
             pltpu.VMEM((tokens, values), jnp.bfloat16),
@@ -249,13 +249,23 @@
 
 
 def finish_kernel(
-    place_ref, basis_hbm, weight_hbm, first_hbm, second_hbm, near_ref, far_ref, w0, f1, f2, w4, b2, b1,
-    new_ref, step_ref, copy_ref, first_out, second_out, later_ref,
-    basis_ref, weight_ref, first_ref, second_ref, tiles, sems,
+    place_ref, basis_hbm, weight_hbm, first_hbm, second_hbm, near_ref, far_ref, w4, w0_hbm, b1_hbm, f1_hbm, f2_hbm, b2_hbm,
+    new_ref, step_ref, copy_ref, first_out, second_out, later_ref, scale_out, basis_ref,
+    weight_ref, first_ref, second_ref, blocks, tiles, sems,
 ):
     fetched = []
     for slot, (source, target) in enumerate(
-        ((basis_hbm, basis_ref), (weight_hbm, weight_ref), (first_hbm, first_ref), (second_hbm, second_ref))
+        (
+            (basis_hbm, basis_ref),
+            (w0_hbm, blocks.at[0]),
+            (b1_hbm, blocks.at[1]),
+            (f1_hbm, blocks.at[2]),
+            (f2_hbm, blocks.at[3]),
+            (b2_hbm, blocks.at[4]),
+            (weight_hbm, weight_ref),
+            (first_hbm, first_ref),
+            (second_hbm, second_ref),
+        )
     ):
         copy = pltpu.make_async_copy(source, target, sems.at[6 + slot])
         copy.start()
@@ -266,9 +276,9 @@
     energy = jnp.sum(near * near + far * far)
     count = 2 * near.shape[0] * near.shape[1] * near.shape[2] * near.shape[3]
     spread = jnp.sqrt(jnp.full((1, 128), energy / count, jnp.float32))
-    scale = (-1.0 / (spread + 1e-06))[:, :1]
-    for copy in fetched:
-        copy.wait()
+    scale_out[...] = -1.0 / (spread + 1e-06)
+    scale = scale_out[:, :1]
+    fetched[0].wait()
     basis = basis_ref[...]
 
     def rows_of(close, distant):
@@ -277,19 +287,28 @@
             [jnp.where(is_low, close, distant), jnp.where(is_low, distant, close)], axis=1
         )
 
+    def rows_at(block):
+        at = block % 8
+        return rows_of(near_ref[:, at], far_ref[:, at])
+
     def step_of(block):
-        at = block % 8
-        return dot(basis, rows_of(near_ref[:, at], far_ref[:, at]), 1, 1) * scale
+        return dot(basis, rows_at(block), 1, 1) * scale
 
     copies = []
-    for slot, (block, hops) in enumerate(((w0, 0), (f1, 7), (b1, 1), (f2, 6), (b2, 2), (w4, 4))):
-        tiles[slot] = (block[...].astype(jnp.float32) + step_of(z + hops)).astype(jnp.bfloat16)
+    for slot, hops in enumerate((4, 0, 1, 7, 6, 2)):
+        step = step_of(z + hops)
+        if slot:
+            fetched[slot].wait()
+        block = blocks[slot - 1] if slot else w4[...]
+        tiles[slot] = (block.astype(jnp.float32) + step).astype(jnp.bfloat16)
         copy = pltpu.make_async_copy(tiles.at[slot], copy_ref.at[:, columns(z + hops)], sems.at[slot])
         copy.start()
         copies.append(copy)
     for slot, hops in enumerate((5, 3)):
-        later_ref[slot] = step_of(z + hops)
-
+        later_ref[slot] = rows_at(z + hops)
+
+    for copy in fetched[6:]:
+        copy.wait()
     mine = pl.ds(y * 4, 4)
     step = dot(rows_of(near_ref[mine, z], far_ref[mine, z]), basis, 1, 1) * scale
     step_ref[...] = step
@@ -310,34 +329,37 @@
     like = lambda array: jax.ShapeDtypeStruct(array.shape, jnp.float32)
     return pl.pallas_call(
         finish_kernel,
-        in_specs=[SMEM] + [HBM] * 4 + [VMEM] * (2 + len(blocks)),
-        out_specs=[VMEM, VMEM, HBM, VMEM, VMEM, VMEM],
+        in_specs=[SMEM] + [HBM] * 4 + [VMEM] * 3 + [HBM] * 5,
+        out_specs=[VMEM, VMEM, HBM] + [VMEM] * 5,
         out_shape=[
             like(weight),
             like(weight),
             pltpu.HBM((values, 2048), jnp.bfloat16),
             like(first),
             like(second),
-            pltpu.VMEM((2, values, 256), jnp.float32),
+            pltpu.VMEM((2, 256, 256), jnp.bfloat16),
+            pltpu.VMEM((1, 128), jnp.float32),
+            pltpu.VMEM(basis.shape, basis.dtype),
         ],
         scratch_shapes=[
-            pltpu.VMEM(basis.shape, basis.dtype),
             pltpu.VMEM(weight.shape, weight.dtype),
             pltpu.VMEM(first.shape, first.dtype),
             pltpu.VMEM(second.shape, second.dtype),
+            pltpu.VMEM((5, values, 256), jnp.bfloat16),
             pltpu.VMEM((6, values, 256), jnp.bfloat16),
-            pltpu.SemaphoreType.DMA((10,)),
+            pltpu.SemaphoreType.DMA((15,)),
         ],
         compiler_params=limit(16),
         name="finish",
-    )(place, *in_hbm(basis, weight, first, second), near, far, *in_vmem(*blocks))
-
-
-def last_kernel(place_ref, later_ref, f3, b3, copy_in, copy_ref, tiles, sems):
+    )(place, *in_hbm(basis, weight, first, second), near, far, blocks[0], *in_hbm(*blocks[1:]))
+
+
+def last_kernel(place_ref, rows_ref, scale_ref, basis_ref, f3, b3, copy_in, copy_ref, tiles, sems):
     z = place_ref[0]
     copies = []
     for slot, (block, hops) in enumerate(((f3, 5), (b3, 3))):
-        tiles[slot] = (block[...].astype(jnp.float32) + later_ref[slot]).astype(jnp.bfloat16)
+        step = dot(basis_ref[...], rows_ref[slot], 1, 1) * scale_ref[:, :1]
+        tiles[slot] = (block[...].astype(jnp.float32) + step).astype(jnp.bfloat16)
         copy = pltpu.make_async_copy(tiles.at[slot], copy_ref.at[:, columns(z + hops)], sems.at[slot])
         copy.start()
         copies.append(copy)
@@ -348,14 +370,14 @@
 def last(place, later, f3, b3, copy):
     return pl.pallas_call(
         last_kernel,
-        in_specs=[SMEM, VMEM, VMEM, VMEM, HBM],
+        in_specs=[SMEM] + [VMEM] * 5 + [HBM],
         out_specs=HBM,
         out_shape=pltpu.HBM(copy.shape, copy.dtype),
-        input_output_aliases={4: 0},
+        input_output_aliases={6: 0},
         scratch_shapes=[pltpu.VMEM((2, copy.shape[0], 256), copy.dtype), pltpu.SemaphoreType.DMA((2,))],
         compiler_params=limit(8),
         name="last",
-    )(place, *in_vmem(later, f3, b3), *in_hbm(copy))
+    )(place, *in_vmem(*later), f3, b3, *in_hbm(copy))
 
 
 def exchange(array, axes):
@@ -378,8 +400,8 @@
     sums = fold(place, exchange(parts, ("y", "x")), first_moment, second_moment)
     near = exchange(update(place, exchange(sums, "z")), ("y", "x"))
     far = swap_cores(near)
-    weight_new, step_out, most, first_new, second_new, later = finish(
-        place, basis, turned, first_moment, second_moment, near, far, (w0, f1, f2, w4, b2, b1)
+    weight_new, step_out, most, first_new, second_new, *later = finish(
+        place, basis, turned, first_moment, second_moment, near, far, (w4, w0, b1, f1, f2, b2)
     )
     weight_copy = last(place, later, f3, b3, most)
     return (weight_new.T, weight_copy, step_out.T, first_new, second_new)

time: 114 us -> 114 us (level)
  the two profiles are of different devices: /device:TPU:28 before, /device:TPU:32 now
where the time goes in v7:
time: 114 us; the launch traced here: 113 us
  waiting for transfers between devices  44.5 us (39%)
  starting transfers between devices  30.5 us (27%)
  blocking collectives  18.9 us (17%)
  Pallas kernels  18.5 us (16%)
    ppermute x13, waiting for transfers between devices, shift(): lax.ppermute(array, axis, [(i, (i + hops) % count) for i in range(count)])  36.6 us
    all_to_all x1, blocking collectives, exchange(): return lax.all_to_all(array, axes, 0, 0, tiled=True)  18.9 us
    ppermute x13, starting transfers between devices, shift(): lax.ppermute(array, axis, [(i, (i + hops) % count) for i in range(count)])  16.9 us
    all_to_all x2, starting transfers between devices, exchange(): return lax.all_to_all(array, axes, 0, 0, tiled=True)  13.5 us
    all_to_all x2, waiting for transfers between devices, exchange(): return lax.all_to_all(array, axes, 0, 0, tiled=True)  6.48 us
    pallas_call x1, Pallas kernels, finish(): pl.pallas_call(finish_kernel, in_specs=[SMEM] + [HBM] * 4 + [VMEM] * 3 +...  6.35 us
    pallas_call x1, Pallas kernels, heads(): pl.pallas_call(heads_kernel, in_specs=[SMEM] + [HBM] * 6, out_specs=[VMEM...  4.14 us
  transfers between devices with their start and end apart: 17, of which 9 were waited for; matrix products, arithmetic and copies ran while one was open for 0% of the time, Pallas kernels for 8%

profile of v7, /device:TPU:32, one launch (start us, length us, event | category | flops | bytes accessed | tf_op | source)
XLA Modules:
  0.0 113.5 jit_solution(4141524061709574788)
XLA Ops:
  0.6 0.1 pad_add_fusion.place_ref
  0.7 4.1 %heads.1 = (f32[768,128]{1,0:T(8,128)S(1)}, bf16[768,128]{1,0:T(8,128)(2,1)S(1)}, bf16[64,1024]{1,0:T(8,128)(2,1)S(1)}) custom-call(s32[4]{0:T(128)S(1)} %pad_add_fusion.place_ref, f32[1,4]{1,0:T(1,128)} %bitcast.12, bf16[768,1024]{1,0:T(8,128)(2,1)} %first_hbm.2, bf16[768,1024]{1,0:T(8,128)(2,1)} %second_hbm.2, f32[1,256]{1,0:T(1,128)} %bitcast.11, ...), custom_call_target="tpu_custom_call" | custom-call | tf_op jit(solution)/shard_map/heads/pallas_call | solution.py:105
  4.9 0.0 copy-start.2
  4.9 0.0 copy-start.3
  4.9 0.1 collective-permute-start
  5.0 1.4 %collective-permute-done.far_ref = bf16[768,128]{1,0:T(8,128)(2,1)S(1)} collective-permute-done((bf16[768,128]{1,0:T(8,128)(2,1)S(1)}, bf16[768,128]{1,0:T(8,128)(2,1)S(1)}, u32[]{:S(2)}, u32[]{:S(2)}) %collective-permute-start) | collective-permute-done | bytes 196640 | tf_op jit(solution)/shard_map/ppermute | solution.py:34
  6.4 1.4 %gradient.1 = bf16[16,8,16,128]{3,2,1,0:T(8,128)(2,1)} custom-call(f32[768,128]{1,0:T(8,128)S(1)} %get-tuple-element.16.own_ref, bf16[768,128]{1,0:T(8,128)(2,1)S(1)} %collective-permute-done.far_ref, bf16[768,2048]{1,0:T(8,128)(2,1)S(1)} %copy-done), custom_call_target="tpu_custom_call" | custom-call | tf_op jit(solution)/shard_map/gradient/pallas_call | solution.py:170
  7.8 18.9 %all_to_all.15.parts_ref = bf16[16,8,16,128]{3,2,1,0:T(8,128)(2,1)S(1)} all-to-all(bf16[16,8,16,128]{3,2,1,0:T(8,128)(2,1)} %gradient.1), channel_id=1, replica_groups=mesh['z'=8,'y'=4,'x'=4,'tp'=2] {'y','x'}, dimensions={0} | all-to-all | bytes 1048576 | tf_op jit(solution)/shard_map/all_to_all | solution.py:384
  26.7 1.4 %fold.1 = bf16[8,10,16,128]{3,2,1,0:T(8,128)(2,1)} custom-call(s32[4]{0:T(128)S(1)} %pad_add_fusion.place_ref, bf16[16,8,16,128]{3,2,1,0:T(8,128)(2,1)S(1)} %all_to_all.15.parts_ref, f32[64,128]{1,0:T(8,128)S(1)} %copy-done.2, f32[64,128]{1,0:T(8,128)S(1)} %copy-done.3), custom_call_target="tpu_custom_call" | custom-call | tf_op jit(solution)/shard_map/fold/pallas_call | solution.py:201
  28.1 8.6 %all-to-all-start.1 = ((bf16[8,10,16,128]{3,2,1,0:T(8,128)(2,1)}), bf16[8,10,16,128]{3,2,1,0:T(8,128)(2,1)S(1)}, u32[]{:S(2)}, u32[]{:S(2)}) async-start(bf16[8,10,16,128]{3,2,1,0:T(8,128)(2,1)} %fold.1), calls=%async_computation.1 | async-start | bytes 655360 | tf_op jit(solution)/shard_map/all_to_all | solution.py:384
  36.7 0.0 collective-permute-start.6
  36.7 2.3 %collective-permute-start.7 = (bf16[64,1024]{1,0:T(8,128)(2,1)S(1)}, bf16[64,1024]{1,0:T(8,128)(2,1)S(1)}, u32[]{:S(2)}, u32[]{:S(2)}) collective-permute-start(bf16[64,1024]{1,0:T(8,128)(2,1)S(1)} %get-tuple-element.18.own_ref), channel_id=1, source_target_pairs={{0,16},{8,24},{16,0},{24,8},{1,17},{9,25},{17,1},{25,9},{2,18},{10... | collective-permute-start | bytes 393224 | tf_op jit(solution)/shard_map/ppermute | solution.py:30
  39.0 1.2 %collective-permute-start.8 = (bf16[64,1024]{1,0:T(8,128)(2,1)S(1)}, bf16[64,1024]{1,0:T(8,128)(2,1)S(1)}, u32[]{:S(2)}, u32[]{:S(2)}) collective-permute-start(bf16[64,1024]{1,0:T(8,128)(2,1)S(1)} %get-tuple-element.18.own_ref), channel_id=1, source_target_pairs={{0,24},{8,0},{16,8},{24,16},{1,25},{9,1},{17,9},{25,17},{2,26},{10... | collective-permute-start | bytes 393224 | tf_op jit(solution)/shard_map/ppermute | solution.py:30
  40.2 4.1 %collective-permute-done.6.one_ref = bf16[64,1024]{1,0:T(8,128)(2,1)S(1)} collective-permute-done((bf16[64,1024]{1,0:T(8,128)(2,1)S(1)}, bf16[64,1024]{1,0:T(8,128)(2,1)S(1)}, u32[]{:S(2)}, u32[]{:S(2)}) %collective-permute-start.6) | collective-permute-done | bytes 131104 | tf_op jit(solution)/shard_map/ppermute | solution.py:30
  44.3 0.0 collective-permute-done.7.two_ref
  44.3 0.9 collective-permute-done.8.three_ref
  45.2 0.8 widen.3.w0_hbm
  46.0 1.5 %collective-permute-start.10 = (bf16[1024,256]{1,0:T(8,128)(2,1)S(1)}, bf16[1024,256]{1,0:T(8,128)(2,1)S(1)}, u32[]{:S(2)}, u32[]{:S(2)}) collective-permute-start(bf16[1024,256]{1,0:T(8,128)(2,1)S(1)} %widen.3.w0_hbm), channel_id=1, source_target_pairs={{0,32},{32,64},{64,96},{96,128},{128,160},{160,192},{192,224},{224... | collective-permute-start | bytes 1572872 | tf_op jit(solution)/shard_map/ppermute | solution.py:30
  47.6 0.6 collective-permute-start.9
  48.1 0.0 all-to-all-done.1.letters_ref
  48.1 1.6 %update.1 = bf16[16,10,16,128]{3,2,1,0:T(8,128)(2,1)} custom-call(s32[4]{0:T(128)S(1)} %pad_add_fusion.place_ref, bf16[8,10,16,128]{3,2,1,0:T(8,128)(2,1)S(1)} %all-to-all-done.1.letters_ref), custom_call_target="tpu_custom_call" | custom-call | tf_op jit(solution)/shard_map/update/pallas_call | solution.py:232
  49.7 4.9 %all-to-all-start.2 = ((bf16[16,10,16,128]{3,2,1,0:T(8,128)(2,1)}), bf16[16,10,16,128]{3,2,1,0:T(8,128)(2,1)S(1)}, u32[]{:S(2)}, u32[]{:S(2)}) async-start(bf16[16,10,16,128]{3,2,1,0:T(8,128)(2,1)} %update.1), calls=%async_computation.2 | async-start | bytes 1310720 | tf_op jit(solution)/shard_map/all_to_all | solution.py:384
  54.7 3.2 %collective-permute-done.10.f1_hbm = bf16[1024,256]{1,0:T(8,128)(2,1)S(1)} collective-permute-done((bf16[1024,256]{1,0:T(8,128)(2,1)S(1)}, bf16[1024,256]{1,0:T(8,128)(2,1)S(1)}, u32[]{:S(2)}, u32[]{:S(2)}) %collective-permute-start.10) | collective-permute-done | bytes 524320 | tf_op jit(solution)/shard_map/ppermute | solution.py:30
  57.8 1.8 %collective-permute-start.11 = (bf16[1024,256]{1,0:T(8,128)(2,1)S(1)}, bf16[1024,256]{1,0:T(8,128)(2,1)S(1)}, u32[]{:S(2)}, u32[]{:S(2)}) collective-permute-start(bf16[1024,256]{1,0:T(8,128)(2,1)S(1)} %collective-permute-done.10.f1_hbm), channel_id=1, source_target_pairs={{0,32},{32,64},{64,96},{96,128},{128,160},{160,192},{192,224},{224... | collective-permute-start | bytes 1572872 | tf_op jit(solution)/shard_map/ppermute | solution.py:30
  59.7 0.0 collective-permute-done.9.b1_hbm
  59.7 0.2 collective-permute-start.12
  59.9 6.5 %all-to-all-done.2.near_ref = bf16[16,10,16,128]{3,2,1,0:T(8,128)(2,1)S(1)} async-done(((bf16[16,10,16,128]{3,2,1,0:T(8,128)(2,1)}), bf16[16,10,16,128]{3,2,1,0:T(8,128)(2,1)S(1)}, u32[]{:S(2)}, u32[]{:S(2)}) %all-to-all-start.2) | async-done | bytes 655392 | tf_op jit(solution)/shard_map/all_to_all | solution.py:384
  66.3 0.0 collective-permute-start.1
  66.3 2.2 %collective-permute-done.11.f2_hbm = bf16[1024,256]{1,0:T(8,128)(2,1)S(1)} collective-permute-done((bf16[1024,256]{1,0:T(8,128)(2,1)S(1)}, bf16[1024,256]{1,0:T(8,128)(2,1)S(1)}, u32[]{:S(2)}, u32[]{:S(2)}) %collective-permute-start.11) | collective-permute-done | bytes 524320 | tf_op jit(solution)/shard_map/ppermute | solution.py:30
  68.5 1.5 %collective-permute-start.13 = (bf16[1024,256]{1,0:T(8,128)(2,1)S(1)}, bf16[1024,256]{1,0:T(8,128)(2,1)S(1)}, u32[]{:S(2)}, u32[]{:S(2)}) collective-permute-start(bf16[1024,256]{1,0:T(8,128)(2,1)S(1)} %collective-permute-done.11.f2_hbm), channel_id=1, source_target_pairs={{0,32},{32,64},{64,96},{96,128},{128,160},{160,192},{192,224},{224... | collective-permute-start | bytes 1572872 | tf_op jit(solution)/shard_map/ppermute | solution.py:30
  70.0 0.0 collective-permute-done.12.b2_hbm
  70.0 1.1 collective-permute-start.14
  71.1 4.4 %collective-permute-start.2 = (bf16[64,1024]{1,0:T(8,128)(2,1)S(1)}, bf16[64,1024]{1,0:T(8,128)(2,1)S(1)}, u32[]{:S(2)}, u32[]{:S(2)}) collective-permute-start(bf16[64,1024]{1,0:T(8,128)(2,1)S(1)} %get-tuple-element.18.own_ref), channel_id=1, source_target_pairs={{0,128},{32,160},{64,192},{96,224},{128,0},{160,32},{192,64},{224,... | collective-permute-start | bytes 393224 | tf_op jit(solution)/shard_map/ppermute | solution.py:30
  75.5 16.0 %collective-permute-done.2.own_ref = bf16[64,1024]{1,0:T(8,128)(2,1)S(1)} collective-permute-done((bf16[64,1024]{1,0:T(8,128)(2,1)S(1)}, bf16[64,1024]{1,0:T(8,128)(2,1)S(1)}, u32[]{:S(2)}, u32[]{:S(2)}) %collective-permute-start.2) | collective-permute-done | bytes 131104 | tf_op jit(solution)/shard_map/ppermute | solution.py:30
  91.5 0.0 collective-permute-start.3
  91.5 2.3 %collective-permute-start.4 = (bf16[64,1024]{1,0:T(8,128)(2,1)S(1)}, bf16[64,1024]{1,0:T(8,128)(2,1)S(1)}, u32[]{:S(2)}, u32[]{:S(2)}) collective-permute-start(bf16[64,1024]{1,0:T(8,128)(2,1)S(1)} %collective-permute-done.2.own_ref), channel_id=1, source_target_pairs={{0,16},{8,24},{16,0},{24,8},{1,17},{9,25},{17,1},{25,9},{2,18},{10... | collective-permute-start | bytes 393224 | tf_op jit(solution)/shard_map/ppermute | solution.py:30
  93.8 5.3 %collective-permute-done.3.one_ref = bf16[64,1024]{1,0:T(8,128)(2,1)S(1)} collective-permute-done((bf16[64,1024]{1,0:T(8,128)(2,1)S(1)}, bf16[64,1024]{1,0:T(8,128)(2,1)S(1)}, u32[]{:S(2)}, u32[]{:S(2)}) %collective-permute-start.3) | collective-permute-done | bytes 131104 | tf_op jit(solution)/shard_map/ppermute | solution.py:30
  99.1 0.0 collective-permute-start.5
  99.1 0.0 collective-permute-done.4.two_ref
  99.1 5.0 %collective-permute-done.5.three_ref = bf16[64,1024]{1,0:T(8,128)(2,1)S(1)} collective-permute-done((bf16[64,1024]{1,0:T(8,128)(2,1)S(1)}, bf16[64,1024]{1,0:T(8,128)(2,1)S(1)}, u32[]{:S(2)}, u32[]{:S(2)}) %collective-permute-start.5) | collective-permute-done | bytes 131104 | tf_op jit(solution)/shard_map/ppermute | solution.py:30
  104.1 0.8 widen.2.w4
  104.9 0.0 collective-permute-done.1.far_ref
  104.9 0.0 copy-done.1
  104.9 0.0 copy-done.4
  105.0 6.3 %finish.1 = (f32[64,1024]{1,0:T(8,128)}, f32[64,1024]{1,0:T(8,128)}, bf16[1024,2048]{1,0:T(8,128)(2,1)}, f32[64,128]{1,0:T(8,128)}, f32[64,128]{1,0:T(8,128)}, /...) custom-call(s32[4]{0:T(128)S(1)} %pad_add_fusion.place_ref, ...), custom_call_target="tpu_custom_call" | custom-call | tf_op jit(solution)/shard_map/finish/pallas_call | solution.py:330
  111.3 0.0 collective-permute-done.13.f3
  111.3 0.0 collective-permute-done.14.b3
  111.3 2.0 %last.1 = bf16[1024,2048]{1,0:T(8,128)(2,1)} custom-call(s32[4]{0:T(128)S(1)} %pad_add_fusion.place_ref, bf16[2,256,256]{2,1,0:T(8,128)(2,1)S(1)} %get-tuple-element.20.rows_ref, f32[1,128]{1,0:T(1,128)S(1)} %get-tuple-element.21.scale_ref, bf16[1024,256]{1,0:T(8,128)(2,1)S(1)} %get-tuple-element.22.basis_ref, ...), custom_call_target="tpu_custom_call", output_to_operand_aliasing={{}: (6, {})} | custom-call | tf_op jit(solution)/shard_map/last/pallas_call | solution.py:371
  (12 shorter events, 0.0 us)
Async XLA Ops:
  0.6 5.8 %copy-start = (bf16[768,2048]{1,0:T(8,128)(2,1)S(1)}, bf16[768,2048]{1,0:T(8,128)(2,1)}, u32[]{:S(2)}) copy-start(bf16[768,2048]{1,0:T(8,128)(2,1)} %cot_ref.1) | copy-start | bytes 9437188
  4.9 21.8 %copy-start.2 = (f32[64,128]{1,0:T(8,128)S(1)}, f32[64,128]{1,0:T(8,128)}, u32[]{:S(2)}) copy-start(f32[64,128]{1,0:T(8,128)} %first_hbm.3) | copy-start | bytes 98308
  4.9 21.8 %copy-start.3 = (f32[64,128]{1,0:T(8,128)S(1)}, f32[64,128]{1,0:T(8,128)}, u32[]{:S(2)}) copy-start(f32[64,128]{1,0:T(8,128)} %second_hbm.3) | copy-start | bytes 98308
  4.9 1.5 %collective-permute-start = (bf16[768,128]{1,0:T(8,128)(2,1)S(1)}, bf16[768,128]{1,0:T(8,128)(2,1)S(1)}, u32[]{:S(2)}, u32[]{:S(2)}) collective-permute-start(bf16[768,128]{1,0:T(8,128)(2,1)S(1)} %get-tuple-element.17), channel_id=1, source_target_pairs={{0,1},{1,0},{2,3},{3,2},{4,5},{5,4},{6,7},{7,6},{8,9},{9,8},{10,11... | collective-permute-start | bytes 589832 | tf_op jit(solution)/shard_map/ppermute | solution.py:34
  28.1 20.0 %all-to-all-start.1 = ((bf16[8,10,16,128]{3,2,1,0:T(8,128)(2,1)}), bf16[8,10,16,128]{3,2,1,0:T(8,128)(2,1)S(1)}, u32[]{:S(2)}, u32[]{:S(2)}) async-start(bf16[8,10,16,128]{3,2,1,0:T(8,128)(2,1)} %fold.1), calls=%async_computation.1 | async-start | bytes 655360 | tf_op jit(solution)/shard_map/all_to_all | solution.py:384
  36.7 7.6 %collective-permute-start.6 = (bf16[64,1024]{1,0:T(8,128)(2,1)S(1)}, bf16[64,1024]{1,0:T(8,128)(2,1)S(1)}, u32[]{:S(2)}, u32[]{:S(2)}) collective-permute-start(bf16[64,1024]{1,0:T(8,128)(2,1)S(1)} %get-tuple-element.18.own_ref), channel_id=1, source_target_pairs={{0,8},{8,16},{16,24},{24,0},{1,9},{9,17},{17,25},{25,1},{2,10},{10... | collective-permute-start | bytes 393224 | tf_op jit(solution)/shard_map/ppermute | solution.py:30
  36.7 7.6 %collective-permute-start.7 = (bf16[64,1024]{1,0:T(8,128)(2,1)S(1)}, bf16[64,1024]{1,0:T(8,128)(2,1)S(1)}, u32[]{:S(2)}, u32[]{:S(2)}) collective-permute-start(bf16[64,1024]{1,0:T(8,128)(2,1)S(1)} %get-tuple-element.18.own_ref), channel_id=1, source_target_pairs={{0,16},{8,24},{16,0},{24,8},{1,17},{9,25},{17,1},{25,9},{2,18},{10... | collective-permute-start | bytes 393224 | tf_op jit(solution)/shard_map/ppermute | solution.py:30
  39.0 6.2 %collective-permute-start.8 = (bf16[64,1024]{1,0:T(8,128)(2,1)S(1)}, bf16[64,1024]{1,0:T(8,128)(2,1)S(1)}, u32[]{:S(2)}, u32[]{:S(2)}) collective-permute-start(bf16[64,1024]{1,0:T(8,128)(2,1)S(1)} %get-tuple-element.18.own_ref), channel_id=1, source_target_pairs={{0,24},{8,0},{16,8},{24,16},{1,25},{9,1},{17,9},{25,17},{2,26},{10... | collective-permute-start | bytes 393224 | tf_op jit(solution)/shard_map/ppermute | solution.py:30
  46.0 58.9 %copy-start.1 = (bf16[1024,256]{1,0:T(8,128)(2,1)}, bf16[1024,256]{1,0:T(8,128)(2,1)S(1)}, u32[]{:S(2)}) copy-start(bf16[1024,256]{1,0:T(8,128)(2,1)S(1)} %widen.3.w0_hbm) | copy-start | bytes 1572868
  46.0 11.8 %collective-permute-start.10 = (bf16[1024,256]{1,0:T(8,128)(2,1)S(1)}, bf16[1024,256]{1,0:T(8,128)(2,1)S(1)}, u32[]{:S(2)}, u32[]{:S(2)}) collective-permute-start(bf16[1024,256]{1,0:T(8,128)(2,1)S(1)} %widen.3.w0_hbm), channel_id=1, source_target_pairs={{0,32},{32,64},{64,96},{96,128},{128,160},{160,192},{192,224},{224... | collective-permute-start | bytes 1572872 | tf_op jit(solution)/shard_map/ppermute | solution.py:30
  47.6 12.1 %collective-permute-start.9 = (bf16[1024,256]{1,0:T(8,128)(2,1)S(1)}, bf16[1024,256]{1,0:T(8,128)(2,1)S(1)}, u32[]{:S(2)}, u32[]{:S(2)}) collective-permute-start(bf16[1024,256]{1,0:T(8,128)(2,1)S(1)} %widen.3.w0_hbm), channel_id=1, source_target_pairs={{0,224},{32,0},{64,32},{96,64},{128,96},{160,128},{192,160},{224,1... | collective-permute-start | bytes 1572872 | tf_op jit(solution)/shard_map/ppermute | solution.py:30
  49.7 16.6 %all-to-all-start.2 = ((bf16[16,10,16,128]{3,2,1,0:T(8,128)(2,1)}), bf16[16,10,16,128]{3,2,1,0:T(8,128)(2,1)S(1)}, u32[]{:S(2)}, u32[]{:S(2)}) async-start(bf16[16,10,16,128]{3,2,1,0:T(8,128)(2,1)} %update.1), calls=%async_computation.2 | async-start | bytes 1310720 | tf_op jit(solution)/shard_map/all_to_all | solution.py:384
  57.8 47.1 %copy-start.4 = (bf16[1024,256]{1,0:T(8,128)(2,1)}, bf16[1024,256]{1,0:T(8,128)(2,1)S(1)}, u32[]{:S(2)}) copy-start(bf16[1024,256]{1,0:T(8,128)(2,1)S(1)} %collective-permute-done.10.f1_hbm) | copy-start | bytes 1572868
  57.8 10.7 %collective-permute-start.11 = (bf16[1024,256]{1,0:T(8,128)(2,1)S(1)}, bf16[1024,256]{1,0:T(8,128)(2,1)S(1)}, u32[]{:S(2)}, u32[]{:S(2)}) collective-permute-start(bf16[1024,256]{1,0:T(8,128)(2,1)S(1)} %collective-permute-done.10.f1_hbm), channel_id=1, source_target_pairs={{0,32},{32,64},{64,96},{96,128},{128,160},{160,192},{192,224},{224... | collective-permute-start | bytes 1572872 | tf_op jit(solution)/shard_map/ppermute | solution.py:30
  59.7 45.3 %copy-start.5 = (bf16[1024,256]{1,0:T(8,128)(2,1)}, bf16[1024,256]{1,0:T(8,128)(2,1)S(1)}, u32[]{:S(2)}) copy-start(bf16[1024,256]{1,0:T(8,128)(2,1)S(1)} %collective-permute-done.9.b1_hbm) | copy-start | bytes 1572868
  59.7 10.3 %collective-permute-start.12 = (bf16[1024,256]{1,0:T(8,128)(2,1)S(1)}, bf16[1024,256]{1,0:T(8,128)(2,1)S(1)}, u32[]{:S(2)}, u32[]{:S(2)}) collective-permute-start(bf16[1024,256]{1,0:T(8,128)(2,1)S(1)} %collective-permute-done.9.b1_hbm), channel_id=1, source_target_pairs={{0,224},{32,0},{64,32},{96,64},{128,96},{160,128},{192,160},{224,1... | collective-permute-start | bytes 1572872 | tf_op jit(solution)/shard_map/ppermute | solution.py:30
  66.3 38.6 %collective-permute-start.1 = (bf16[16,10,16,128]{3,2,1,0:T(8,128)(2,1)S(1)}, bf16[16,10,16,128]{3,2,1,0:T(8,128)(2,1)S(1)}, u32[]{:S(2)}, u32[]{:S(2)}) collective-permute-start(bf16[16,10,16,128]{3,2,1,0:T(8,128)(2,1)S(1)} %all-to-all-done.2.near_ref), channel_id=1, source_target_pairs={{0,1},{1,0},{2,3},{3,2},{4,5},{5,4},{6,7},{7,6},{8,9},{9,8},{10,11... | collective-permute-start | bytes 1966088 | tf_op jit(solution)/shard_map/ppermute | solution.py:34
  68.5 36.4 %copy-start.6 = (bf16[1024,256]{1,0:T(8,128)(2,1)}, bf16[1024,256]{1,0:T(8,128)(2,1)S(1)}, u32[]{:S(2)}) copy-start(bf16[1024,256]{1,0:T(8,128)(2,1)S(1)} %collective-permute-done.11.f2_hbm) | copy-start | bytes 1572868
  68.5 42.8 %collective-permute-start.13 = (bf16[1024,256]{1,0:T(8,128)(2,1)S(1)}, bf16[1024,256]{1,0:T(8,128)(2,1)S(1)}, u32[]{:S(2)}, u32[]{:S(2)}) collective-permute-start(bf16[1024,256]{1,0:T(8,128)(2,1)S(1)} %collective-permute-done.11.f2_hbm), channel_id=1, source_target_pairs={{0,32},{32,64},{64,96},{96,128},{128,160},{160,192},{192,224},{224... | collective-permute-start | bytes 1572872 | tf_op jit(solution)/shard_map/ppermute | solution.py:30
  70.0 34.9 %copy-start.7 = (bf16[1024,256]{1,0:T(8,128)(2,1)}, bf16[1024,256]{1,0:T(8,128)(2,1)S(1)}, u32[]{:S(2)}) copy-start(bf16[1024,256]{1,0:T(8,128)(2,1)S(1)} %collective-permute-done.12.b2_hbm) | copy-start | bytes 1572868
  70.0 41.3 %collective-permute-start.14 = (bf16[1024,256]{1,0:T(8,128)(2,1)S(1)}, bf16[1024,256]{1,0:T(8,128)(2,1)S(1)}, u32[]{:S(2)}, u32[]{:S(2)}) collective-permute-start(bf16[1024,256]{1,0:T(8,128)(2,1)S(1)} %collective-permute-done.12.b2_hbm), channel_id=1, source_target_pairs={{0,224},{32,0},{64,32},{96,64},{128,96},{160,128},{192,160},{224,1... | collective-permute-start | bytes 1572872 | tf_op jit(solution)/shard_map/ppermute | solution.py:30
  71.1 20.5 %collective-permute-start.2 = (bf16[64,1024]{1,0:T(8,128)(2,1)S(1)}, bf16[64,1024]{1,0:T(8,128)(2,1)S(1)}, u32[]{:S(2)}, u32[]{:S(2)}) collective-permute-start(bf16[64,1024]{1,0:T(8,128)(2,1)S(1)} %get-tuple-element.18.own_ref), channel_id=1, source_target_pairs={{0,128},{32,160},{64,192},{96,224},{128,0},{160,32},{192,64},{224,... | collective-permute-start | bytes 393224 | tf_op jit(solution)/shard_map/ppermute | solution.py:30
  91.5 7.6 %collective-permute-start.3 = (bf16[64,1024]{1,0:T(8,128)(2,1)S(1)}, bf16[64,1024]{1,0:T(8,128)(2,1)S(1)}, u32[]{:S(2)}, u32[]{:S(2)}) collective-permute-start(bf16[64,1024]{1,0:T(8,128)(2,1)S(1)} %collective-permute-done.2.own_ref), channel_id=1, source_target_pairs={{0,8},{8,16},{16,24},{24,0},{1,9},{9,17},{17,25},{25,1},{2,10},{10... | collective-permute-start | bytes 393224 | tf_op jit(solution)/shard_map/ppermute | solution.py:30
  91.5 7.6 %collective-permute-start.4 = (bf16[64,1024]{1,0:T(8,128)(2,1)S(1)}, bf16[64,1024]{1,0:T(8,128)(2,1)S(1)}, u32[]{:S(2)}, u32[]{:S(2)}) collective-permute-start(bf16[64,1024]{1,0:T(8,128)(2,1)S(1)} %collective-permute-done.2.own_ref), channel_id=1, source_target_pairs={{0,16},{8,24},{16,0},{24,8},{1,17},{9,25},{17,1},{25,9},{2,18},{10... | collective-permute-start | bytes 393224 | tf_op jit(solution)/shard_map/ppermute | solution.py:30
  99.1 5.0 %collective-permute-start.5 = (bf16[64,1024]{1,0:T(8,128)(2,1)S(1)}, bf16[64,1024]{1,0:T(8,128)(2,1)S(1)}, u32[]{:S(2)}, u32[]{:S(2)}) collective-permute-start(bf16[64,1024]{1,0:T(8,128)(2,1)S(1)} %collective-permute-done.2.own_ref), channel_id=1, source_target_pairs={{0,24},{8,0},{16,8},{24,16},{1,25},{9,1},{17,9},{25,17},{2,26},{10... | collective-permute-start | bytes 393224 | tf_op jit(solution)/shard_map/ppermute | solution.py:30

commit v8 on v7

--- a/solution.py
+++ b/solution.py
@@ -249,7 +249,7 @@
 
 
 def finish_kernel(
-    place_ref, basis_hbm, weight_hbm, first_hbm, second_hbm, near_ref, far_ref, w4, w0_hbm, b1_hbm, f1_hbm, f2_hbm, b2_hbm,
+    place_ref, basis_hbm, weight_hbm, first_hbm, second_hbm, near_ref, far_ref, w0, w4, b1, f1_hbm, f2_hbm, b2_hbm,
     new_ref, step_ref, copy_ref, first_out, second_out, later_ref, scale_out, basis_ref,
     weight_ref, first_ref, second_ref, blocks, tiles, sems,
 ):
@@ -257,11 +257,9 @@
     for slot, (source, target) in enumerate(
         (
             (basis_hbm, basis_ref),
-            (w0_hbm, blocks.at[0]),
-            (b1_hbm, blocks.at[1]),
-            (f1_hbm, blocks.at[2]),
-            (f2_hbm, blocks.at[3]),
-            (b2_hbm, blocks.at[4]),
+            (f1_hbm, blocks.at[0]),
+            (f2_hbm, blocks.at[1]),
+            (b2_hbm, blocks.at[2]),
             (weight_hbm, weight_ref),
             (first_hbm, first_ref),
             (second_hbm, second_ref),
@@ -295,19 +293,18 @@
         return dot(basis, rows_at(block), 1, 1) * scale
 
     copies = []
-    for slot, hops in enumerate((4, 0, 1, 7, 6, 2)):
-        step = step_of(z + hops)
-        if slot:
-            fetched[slot].wait()
-        block = blocks[slot - 1] if slot else w4[...]
-        tiles[slot] = (block.astype(jnp.float32) + step).astype(jnp.bfloat16)
+    near_blocks = ((w0, 0), (w4, 4), (b1, 1), (blocks.at[0], 7), (blocks.at[1], 6), (blocks.at[2], 2))
+    for slot, (block, hops) in enumerate(near_blocks):
+        if slot >= 3:
+            fetched[slot - 2].wait()
+        tiles[slot] = (block[...].astype(jnp.float32) + step_of(z + hops)).astype(jnp.bfloat16)
         copy = pltpu.make_async_copy(tiles.at[slot], copy_ref.at[:, columns(z + hops)], sems.at[slot])
         copy.start()
         copies.append(copy)
     for slot, hops in enumerate((5, 3)):
         later_ref[slot] = rows_at(z + hops)
 
-    for copy in fetched[6:]:
+    for copy in fetched[4:]:
         copy.wait()
     mine = pl.ds(y * 4, 4)
     step = dot(rows_of(near_ref[mine, z], far_ref[mine, z]), basis, 1, 1) * scale
@@ -329,7 +326,7 @@
     like = lambda array: jax.ShapeDtypeStruct(array.shape, jnp.float32)
     return pl.pallas_call(
         finish_kernel,
-        in_specs=[SMEM] + [HBM] * 4 + [VMEM] * 3 + [HBM] * 5,
+        in_specs=[SMEM] + [HBM] * 4 + [VMEM] * 5 + [HBM] * 3,
         out_specs=[VMEM, VMEM, HBM] + [VMEM] * 5,
         out_shape=[
             like(weight),
@@ -345,13 +342,13 @@
             pltpu.VMEM(weight.shape, weight.dtype),
             pltpu.VMEM(first.shape, first.dtype),
             pltpu.VMEM(second.shape, second.dtype),
-            pltpu.VMEM((5, values, 256), jnp.bfloat16),
+            pltpu.VMEM((3, values, 256), jnp.bfloat16),
             pltpu.VMEM((6, values, 256), jnp.bfloat16),
-            pltpu.SemaphoreType.DMA((15,)),
+            pltpu.SemaphoreType.DMA((13,)),
         ],
         compiler_params=limit(16),
         name="finish",
-    )(place, *in_hbm(basis, weight, first, second), near, far, blocks[0], *in_hbm(*blocks[1:]))
+    )(place, *in_hbm(basis, weight, first, second), near, far, *blocks[:3], *in_hbm(*blocks[3:]))
 
 
 def last_kernel(place_ref, rows_ref, scale_ref, basis_ref, f3, b3, copy_in, copy_ref, tiles, sems):
@@ -401,7 +398,7 @@
     near = exchange(update(place, exchange(sums, "z")), ("y", "x"))
     far = swap_cores(near)
     weight_new, step_out, most, first_new, second_new, *later = finish(
-        place, basis, turned, first_moment, second_moment, near, far, (w4, w0, b1, f1, f2, b2)
+        place, basis, turned, first_moment, second_moment, near, far, (w0, w4, b1, f1, f2, b2)
     )
     weight_copy = last(place, later, f3, b3, most)
     return (weight_new.T, weight_copy, step_out.T, first_new, second_new)

time: 114 us -> 113 us (level)
  no operation moved by 1% of the time
where the time goes in v8:
time: 113 us
  waiting for transfers between devices  44.6 us (39%)
  starting transfers between devices  30.5 us (27%)
  blocking collectives  18.9 us (17%)
  Pallas kernels  17.7 us (16%)
    ppermute x13, waiting for transfers between devices, shift(): lax.ppermute(array, axis, [(i, (i + hops) % count) for i in range(count)])  36.7 us
    all_to_all x1, blocking collectives, exchange(): return lax.all_to_all(array, axes, 0, 0, tiled=True)  18.9 us
    ppermute x13, starting transfers between devices, shift(): lax.ppermute(array, axis, [(i, (i + hops) % count) for i in range(count)])  16.9 us
    all_to_all x2, starting transfers between devices, exchange(): return lax.all_to_all(array, axes, 0, 0, tiled=True)  13.5 us
    all_to_all x2, waiting for transfers between devices, exchange(): return lax.all_to_all(array, axes, 0, 0, tiled=True)  6.46 us
    pallas_call x1, Pallas kernels, finish(): pl.pallas_call(finish_kernel, in_specs=[SMEM] + [HBM] * 4 + [VMEM] * 5 +...  5.54 us
    pallas_call x1, Pallas kernels, heads(): pl.pallas_call(heads_kernel, in_specs=[SMEM] + [HBM] * 6, out_specs=[VMEM...  4.14 us
  transfers between devices with their start and end apart: 17, of which 9 were waited for; matrix products, arithmetic and copies ran while one was open for 0% of the time, Pallas kernels for 8%

profile of v8, /device:TPU:32, one launch (start us, length us, event | category | flops | bytes accessed | tf_op | source)
XLA Modules:
  0.0 112.7 jit_solution(17250562164617814617)
XLA Ops:
  0.6 0.1 pad_add_fusion.place_ref
  0.7 4.1 %heads.1 = (f32[768,128]{1,0:T(8,128)S(1)}, bf16[768,128]{1,0:T(8,128)(2,1)S(1)}, bf16[64,1024]{1,0:T(8,128)(2,1)S(1)}) custom-call(s32[4]{0:T(128)S(1)} %pad_add_fusion.place_ref, f32[1,4]{1,0:T(1,128)} %bitcast.12, bf16[768,1024]{1,0:T(8,128)(2,1)} %first_hbm.2, bf16[768,1024]{1,0:T(8,128)(2,1)} %second_hbm.2, f32[1,256]{1,0:T(1,128)} %bitcast.11, ...), custom_call_target="tpu_custom_call" | custom-call | tf_op jit(solution)/shard_map/heads/pallas_call | solution.py:105
  4.9 0.0 copy-start.1
  4.9 0.0 copy-start.2
  4.9 0.1 collective-permute-start
  5.0 1.4 %collective-permute-done.far_ref = bf16[768,128]{1,0:T(8,128)(2,1)S(1)} collective-permute-done((bf16[768,128]{1,0:T(8,128)(2,1)S(1)}, bf16[768,128]{1,0:T(8,128)(2,1)S(1)}, u32[]{:S(2)}, u32[]{:S(2)}) %collective-permute-start) | collective-permute-done | bytes 196640 | tf_op jit(solution)/shard_map/ppermute | solution.py:34
  6.4 1.4 %gradient.1 = bf16[16,8,16,128]{3,2,1,0:T(8,128)(2,1)} custom-call(f32[768,128]{1,0:T(8,128)S(1)} %get-tuple-element.16.own_ref, bf16[768,128]{1,0:T(8,128)(2,1)S(1)} %collective-permute-done.far_ref, bf16[768,2048]{1,0:T(8,128)(2,1)S(1)} %copy-done), custom_call_target="tpu_custom_call" | custom-call | tf_op jit(solution)/shard_map/gradient/pallas_call | solution.py:170
  7.8 18.9 %all_to_all.15.parts_ref = bf16[16,8,16,128]{3,2,1,0:T(8,128)(2,1)S(1)} all-to-all(bf16[16,8,16,128]{3,2,1,0:T(8,128)(2,1)} %gradient.1), channel_id=1, replica_groups=mesh['z'=8,'y'=4,'x'=4,'tp'=2] {'y','x'}, dimensions={0} | all-to-all | bytes 1048576 | tf_op jit(solution)/shard_map/all_to_all | solution.py:381
  26.7 1.4 %fold.1 = bf16[8,10,16,128]{3,2,1,0:T(8,128)(2,1)} custom-call(s32[4]{0:T(128)S(1)} %pad_add_fusion.place_ref, bf16[16,8,16,128]{3,2,1,0:T(8,128)(2,1)S(1)} %all_to_all.15.parts_ref, f32[64,128]{1,0:T(8,128)S(1)} %copy-done.1, f32[64,128]{1,0:T(8,128)S(1)} %copy-done.2), custom_call_target="tpu_custom_call" | custom-call | tf_op jit(solution)/shard_map/fold/pallas_call | solution.py:201
  28.1 8.6 %all-to-all-start.1 = ((bf16[8,10,16,128]{3,2,1,0:T(8,128)(2,1)}), bf16[8,10,16,128]{3,2,1,0:T(8,128)(2,1)S(1)}, u32[]{:S(2)}, u32[]{:S(2)}) async-start(bf16[8,10,16,128]{3,2,1,0:T(8,128)(2,1)} %fold.1), calls=%async_computation.1 | async-start | bytes 655360 | tf_op jit(solution)/shard_map/all_to_all | solution.py:381
  36.7 0.0 collective-permute-start.2
  36.7 2.3 %collective-permute-start.3 = (bf16[64,1024]{1,0:T(8,128)(2,1)S(1)}, bf16[64,1024]{1,0:T(8,128)(2,1)S(1)}, u32[]{:S(2)}, u32[]{:S(2)}) collective-permute-start(bf16[64,1024]{1,0:T(8,128)(2,1)S(1)} %get-tuple-element.18.own_ref), channel_id=1, source_target_pairs={{0,16},{8,24},{16,0},{24,8},{1,17},{9,25},{17,1},{25,9},{2,18},{10... | collective-permute-start | bytes 393224 | tf_op jit(solution)/shard_map/ppermute | solution.py:30
  39.0 1.2 %collective-permute-start.4 = (bf16[64,1024]{1,0:T(8,128)(2,1)S(1)}, bf16[64,1024]{1,0:T(8,128)(2,1)S(1)}, u32[]{:S(2)}, u32[]{:S(2)}) collective-permute-start(bf16[64,1024]{1,0:T(8,128)(2,1)S(1)} %get-tuple-element.18.own_ref), channel_id=1, source_target_pairs={{0,24},{8,0},{16,8},{24,16},{1,25},{9,1},{17,9},{25,17},{2,26},{10... | collective-permute-start | bytes 393224 | tf_op jit(solution)/shard_map/ppermute | solution.py:30
  40.2 4.1 %collective-permute-done.2.one_ref = bf16[64,1024]{1,0:T(8,128)(2,1)S(1)} collective-permute-done((bf16[64,1024]{1,0:T(8,128)(2,1)S(1)}, bf16[64,1024]{1,0:T(8,128)(2,1)S(1)}, u32[]{:S(2)}, u32[]{:S(2)}) %collective-permute-start.2) | collective-permute-done | bytes 131104 | tf_op jit(solution)/shard_map/ppermute | solution.py:30
  44.3 0.0 collective-permute-done.3.two_ref
  44.3 0.9 collective-permute-done.4.three_ref
  45.2 0.8 widen.2.w0
  46.0 1.5 %collective-permute-start.10 = (bf16[1024,256]{1,0:T(8,128)(2,1)S(1)}, bf16[1024,256]{1,0:T(8,128)(2,1)S(1)}, u32[]{:S(2)}, u32[]{:S(2)}) collective-permute-start(bf16[1024,256]{1,0:T(8,128)(2,1)S(1)} %widen.2.w0), channel_id=1, source_target_pairs={{0,32},{32,64},{64,96},{96,128},{128,160},{160,192},{192,224},{224... | collective-permute-start | bytes 1572872 | tf_op jit(solution)/shard_map/ppermute | solution.py:30
  47.6 0.6 collective-permute-start.9
  48.1 0.0 all-to-all-done.1.letters_ref
  48.1 1.6 %update.1 = bf16[16,10,16,128]{3,2,1,0:T(8,128)(2,1)} custom-call(s32[4]{0:T(128)S(1)} %pad_add_fusion.place_ref, bf16[8,10,16,128]{3,2,1,0:T(8,128)(2,1)S(1)} %all-to-all-done.1.letters_ref), custom_call_target="tpu_custom_call" | custom-call | tf_op jit(solution)/shard_map/update/pallas_call | solution.py:232
  49.7 4.9 %all-to-all-start.2 = ((bf16[16,10,16,128]{3,2,1,0:T(8,128)(2,1)}), bf16[16,10,16,128]{3,2,1,0:T(8,128)(2,1)S(1)}, u32[]{:S(2)}, u32[]{:S(2)}) async-start(bf16[16,10,16,128]{3,2,1,0:T(8,128)(2,1)} %update.1), calls=%async_computation.2 | async-start | bytes 1310720 | tf_op jit(solution)/shard_map/all_to_all | solution.py:381
  54.7 3.2 %collective-permute-done.10.f1_hbm = bf16[1024,256]{1,0:T(8,128)(2,1)S(1)} collective-permute-done((bf16[1024,256]{1,0:T(8,128)(2,1)S(1)}, bf16[1024,256]{1,0:T(8,128)(2,1)S(1)}, u32[]{:S(2)}, u32[]{:S(2)}) %collective-permute-start.10) | collective-permute-done | bytes 524320 | tf_op jit(solution)/shard_map/ppermute | solution.py:30
  57.8 1.8 %collective-permute-start.11 = (bf16[1024,256]{1,0:T(8,128)(2,1)S(1)}, bf16[1024,256]{1,0:T(8,128)(2,1)S(1)}, u32[]{:S(2)}, u32[]{:S(2)}) collective-permute-start(bf16[1024,256]{1,0:T(8,128)(2,1)S(1)} %collective-permute-done.10.f1_hbm), channel_id=1, source_target_pairs={{0,32},{32,64},{64,96},{96,128},{128,160},{160,192},{192,224},{224... | collective-permute-start | bytes 1572872 | tf_op jit(solution)/shard_map/ppermute | solution.py:30
  59.6 0.0 collective-permute-done.9.b1
  59.6 0.2 collective-permute-start.12
  59.9 6.5 %all-to-all-done.2.near_ref = bf16[16,10,16,128]{3,2,1,0:T(8,128)(2,1)S(1)} async-done(((bf16[16,10,16,128]{3,2,1,0:T(8,128)(2,1)}), bf16[16,10,16,128]{3,2,1,0:T(8,128)(2,1)S(1)}, u32[]{:S(2)}, u32[]{:S(2)}) %all-to-all-start.2) | async-done | bytes 655392 | tf_op jit(solution)/shard_map/all_to_all | solution.py:381
  66.3 0.0 collective-permute-start.1
  66.3 2.2 %collective-permute-done.11.f2_hbm = bf16[1024,256]{1,0:T(8,128)(2,1)S(1)} collective-permute-done((bf16[1024,256]{1,0:T(8,128)(2,1)S(1)}, bf16[1024,256]{1,0:T(8,128)(2,1)S(1)}, u32[]{:S(2)}, u32[]{:S(2)}) %collective-permute-start.11) | collective-permute-done | bytes 524320 | tf_op jit(solution)/shard_map/ppermute | solution.py:30
  68.5 1.5 %collective-permute-start.13 = (bf16[1024,256]{1,0:T(8,128)(2,1)S(1)}, bf16[1024,256]{1,0:T(8,128)(2,1)S(1)}, u32[]{:S(2)}, u32[]{:S(2)}) collective-permute-start(bf16[1024,256]{1,0:T(8,128)(2,1)S(1)} %collective-permute-done.11.f2_hbm), channel_id=1, source_target_pairs={{0,32},{32,64},{64,96},{96,128},{128,160},{160,192},{192,224},{224... | collective-permute-start | bytes 1572872 | tf_op jit(solution)/shard_map/ppermute | solution.py:30
  70.0 0.0 collective-permute-done.12.b2_hbm
  70.0 1.0 collective-permute-start.14
  71.1 4.4 %collective-permute-start.5 = (bf16[64,1024]{1,0:T(8,128)(2,1)S(1)}, bf16[64,1024]{1,0:T(8,128)(2,1)S(1)}, u32[]{:S(2)}, u32[]{:S(2)}) collective-permute-start(bf16[64,1024]{1,0:T(8,128)(2,1)S(1)} %get-tuple-element.18.own_ref), channel_id=1, source_target_pairs={{0,128},{32,160},{64,192},{96,224},{128,0},{160,32},{192,64},{224,... | collective-permute-start | bytes 393224 | tf_op jit(solution)/shard_map/ppermute | solution.py:30
  75.5 16.0 %collective-permute-done.5.own_ref = bf16[64,1024]{1,0:T(8,128)(2,1)S(1)} collective-permute-done((bf16[64,1024]{1,0:T(8,128)(2,1)S(1)}, bf16[64,1024]{1,0:T(8,128)(2,1)S(1)}, u32[]{:S(2)}, u32[]{:S(2)}) %collective-permute-start.5) | collective-permute-done | bytes 131104 | tf_op jit(solution)/shard_map/ppermute | solution.py:30
  91.5 0.0 collective-permute-start.6
  91.5 2.3 %collective-permute-start.7 = (bf16[64,1024]{1,0:T(8,128)(2,1)S(1)}, bf16[64,1024]{1,0:T(8,128)(2,1)S(1)}, u32[]{:S(2)}, u32[]{:S(2)}) collective-permute-start(bf16[64,1024]{1,0:T(8,128)(2,1)S(1)} %collective-permute-done.5.own_ref), channel_id=1, source_target_pairs={{0,16},{8,24},{16,0},{24,8},{1,17},{9,25},{17,1},{25,9},{2,18},{10... | collective-permute-start | bytes 393224 | tf_op jit(solution)/shard_map/ppermute | solution.py:30
  93.8 5.3 %collective-permute-done.6.one_ref = bf16[64,1024]{1,0:T(8,128)(2,1)S(1)} collective-permute-done((bf16[64,1024]{1,0:T(8,128)(2,1)S(1)}, bf16[64,1024]{1,0:T(8,128)(2,1)S(1)}, u32[]{:S(2)}, u32[]{:S(2)}) %collective-permute-start.6) | collective-permute-done | bytes 131104 | tf_op jit(solution)/shard_map/ppermute | solution.py:30
  99.1 0.0 collective-permute-start.8
  99.1 0.0 collective-permute-done.7.two_ref
  99.1 5.0 %collective-permute-done.8.three_ref = bf16[64,1024]{1,0:T(8,128)(2,1)S(1)} collective-permute-done((bf16[64,1024]{1,0:T(8,128)(2,1)S(1)}, bf16[64,1024]{1,0:T(8,128)(2,1)S(1)}, u32[]{:S(2)}, u32[]{:S(2)}) %collective-permute-start.8) | collective-permute-done | bytes 131104 | tf_op jit(solution)/shard_map/ppermute | solution.py:30
  104.1 0.8 widen.3.w4
  104.9 0.0 collective-permute-done.1.far_ref
  104.9 0.0 copy-done.3
  104.9 0.0 copy-done.4
  104.9 5.5 %finish.1 = (f32[64,1024]{1,0:T(8,128)}, f32[64,1024]{1,0:T(8,128)}, bf16[1024,2048]{1,0:T(8,128)(2,1)}, f32[64,128]{1,0:T(8,128)}, f32[64,128]{1,0:T(8,128)}, /...) custom-call(s32[4]{0:T(128)S(1)} %pad_add_fusion.place_ref, ...), custom_call_target="tpu_custom_call" | custom-call | tf_op jit(solution)/shard_map/finish/pallas_call | solution.py:327
  110.5 0.0 collective-permute-done.13.f3
  110.5 0.0 collective-permute-done.14.b3
  110.5 2.0 %last.1 = bf16[1024,2048]{1,0:T(8,128)(2,1)} custom-call(s32[4]{0:T(128)S(1)} %pad_add_fusion.place_ref, bf16[2,256,256]{2,1,0:T(8,128)(2,1)S(1)} %get-tuple-element.20.rows_ref, f32[1,128]{1,0:T(1,128)S(1)} %get-tuple-element.21.scale_ref, bf16[1024,256]{1,0:T(8,128)(2,1)S(1)} %get-tuple-element.22.basis_ref, ...), custom_call_target="tpu_custom_call", output_to_operand_aliasing={{}: (6, {})} | custom-call | tf_op jit(solution)/shard_map/last/pallas_call | solution.py:368
  (8 shorter events, 0.0 us)
Async XLA Ops:
  0.6 5.8 %copy-start = (bf16[768,2048]{1,0:T(8,128)(2,1)S(1)}, bf16[768,2048]{1,0:T(8,128)(2,1)}, u32[]{:S(2)}) copy-start(bf16[768,2048]{1,0:T(8,128)(2,1)} %cot_ref.1) | copy-start | bytes 9437188
  4.9 21.8 %copy-start.1 = (f32[64,128]{1,0:T(8,128)S(1)}, f32[64,128]{1,0:T(8,128)}, u32[]{:S(2)}) copy-start(f32[64,128]{1,0:T(8,128)} %first_hbm.3) | copy-start | bytes 98308
  4.9 21.8 %copy-start.2 = (f32[64,128]{1,0:T(8,128)S(1)}, f32[64,128]{1,0:T(8,128)}, u32[]{:S(2)}) copy-start(f32[64,128]{1,0:T(8,128)} %second_hbm.3) | copy-start | bytes 98308
  4.9 1.5 %collective-permute-start = (bf16[768,128]{1,0:T(8,128)(2,1)S(1)}, bf16[768,128]{1,0:T(8,128)(2,1)S(1)}, u32[]{:S(2)}, u32[]{:S(2)}) collective-permute-start(bf16[768,128]{1,0:T(8,128)(2,1)S(1)} %get-tuple-element.17), channel_id=1, source_target_pairs={{0,1},{1,0},{2,3},{3,2},{4,5},{5,4},{6,7},{7,6},{8,9},{9,8},{10,11... | collective-permute-start | bytes 589832 | tf_op jit(solution)/shard_map/ppermute | solution.py:34
  28.1 20.0 %all-to-all-start.1 = ((bf16[8,10,16,128]{3,2,1,0:T(8,128)(2,1)}), bf16[8,10,16,128]{3,2,1,0:T(8,128)(2,1)S(1)}, u32[]{:S(2)}, u32[]{:S(2)}) async-start(bf16[8,10,16,128]{3,2,1,0:T(8,128)(2,1)} %fold.1), calls=%async_computation.1 | async-start | bytes 655360 | tf_op jit(solution)/shard_map/all_to_all | solution.py:381
  36.7 7.6 %collective-permute-start.2 = (bf16[64,1024]{1,0:T(8,128)(2,1)S(1)}, bf16[64,1024]{1,0:T(8,128)(2,1)S(1)}, u32[]{:S(2)}, u32[]{:S(2)}) collective-permute-start(bf16[64,1024]{1,0:T(8,128)(2,1)S(1)} %get-tuple-element.18.own_ref), channel_id=1, source_target_pairs={{0,8},{8,16},{16,24},{24,0},{1,9},{9,17},{17,25},{25,1},{2,10},{10... | collective-permute-start | bytes 393224 | tf_op jit(solution)/shard_map/ppermute | solution.py:30
  36.7 7.6 %collective-permute-start.3 = (bf16[64,1024]{1,0:T(8,128)(2,1)S(1)}, bf16[64,1024]{1,0:T(8,128)(2,1)S(1)}, u32[]{:S(2)}, u32[]{:S(2)}) collective-permute-start(bf16[64,1024]{1,0:T(8,128)(2,1)S(1)} %get-tuple-element.18.own_ref), channel_id=1, source_target_pairs={{0,16},{8,24},{16,0},{24,8},{1,17},{9,25},{17,1},{25,9},{2,18},{10... | collective-permute-start | bytes 393224 | tf_op jit(solution)/shard_map/ppermute | solution.py:30
  39.0 6.2 %collective-permute-start.4 = (bf16[64,1024]{1,0:T(8,128)(2,1)S(1)}, bf16[64,1024]{1,0:T(8,128)(2,1)S(1)}, u32[]{:S(2)}, u32[]{:S(2)}) collective-permute-start(bf16[64,1024]{1,0:T(8,128)(2,1)S(1)} %get-tuple-element.18.own_ref), channel_id=1, source_target_pairs={{0,24},{8,0},{16,8},{24,16},{1,25},{9,1},{17,9},{25,17},{2,26},{10... | collective-permute-start | bytes 393224 | tf_op jit(solution)/shard_map/ppermute | solution.py:30
  46.0 11.8 %collective-permute-start.10 = (bf16[1024,256]{1,0:T(8,128)(2,1)S(1)}, bf16[1024,256]{1,0:T(8,128)(2,1)S(1)}, u32[]{:S(2)}, u32[]{:S(2)}) collective-permute-start(bf16[1024,256]{1,0:T(8,128)(2,1)S(1)} %widen.2.w0), channel_id=1, source_target_pairs={{0,32},{32,64},{64,96},{96,128},{128,160},{160,192},{192,224},{224... | collective-permute-start | bytes 1572872 | tf_op jit(solution)/shard_map/ppermute | solution.py:30
  47.6 12.1 %collective-permute-start.9 = (bf16[1024,256]{1,0:T(8,128)(2,1)S(1)}, bf16[1024,256]{1,0:T(8,128)(2,1)S(1)}, u32[]{:S(2)}, u32[]{:S(2)}) collective-permute-start(bf16[1024,256]{1,0:T(8,128)(2,1)S(1)} %widen.2.w0), channel_id=1, source_target_pairs={{0,224},{32,0},{64,32},{96,64},{128,96},{160,128},{192,160},{224,1... | collective-permute-start | bytes 1572872 | tf_op jit(solution)/shard_map/ppermute | solution.py:30
  49.7 16.6 %all-to-all-start.2 = ((bf16[16,10,16,128]{3,2,1,0:T(8,128)(2,1)}), bf16[16,10,16,128]{3,2,1,0:T(8,128)(2,1)S(1)}, u32[]{:S(2)}, u32[]{:S(2)}) async-start(bf16[16,10,16,128]{3,2,1,0:T(8,128)(2,1)} %update.1), calls=%async_computation.2 | async-start | bytes 1310720 | tf_op jit(solution)/shard_map/all_to_all | solution.py:381
  57.8 47.1 %copy-start.3 = (bf16[1024,256]{1,0:T(8,128)(2,1)}, bf16[1024,256]{1,0:T(8,128)(2,1)S(1)}, u32[]{:S(2)}) copy-start(bf16[1024,256]{1,0:T(8,128)(2,1)S(1)} %collective-permute-done.10.f1_hbm) | copy-start | bytes 1572868
  57.8 10.7 %collective-permute-start.11 = (bf16[1024,256]{1,0:T(8,128)(2,1)S(1)}, bf16[1024,256]{1,0:T(8,128)(2,1)S(1)}, u32[]{:S(2)}, u32[]{:S(2)}) collective-permute-start(bf16[1024,256]{1,0:T(8,128)(2,1)S(1)} %collective-permute-done.10.f1_hbm), channel_id=1, source_target_pairs={{0,32},{32,64},{64,96},{96,128},{128,160},{160,192},{192,224},{224... | collective-permute-start | bytes 1572872 | tf_op jit(solution)/shard_map/ppermute | solution.py:30
  59.6 10.4 %collective-permute-start.12 = (bf16[1024,256]{1,0:T(8,128)(2,1)S(1)}, bf16[1024,256]{1,0:T(8,128)(2,1)S(1)}, u32[]{:S(2)}, u32[]{:S(2)}) collective-permute-start(bf16[1024,256]{1,0:T(8,128)(2,1)S(1)} %collective-permute-done.9.b1), channel_id=1, source_target_pairs={{0,224},{32,0},{64,32},{96,64},{128,96},{160,128},{192,160},{224,1... | collective-permute-start | bytes 1572872 | tf_op jit(solution)/shard_map/ppermute | solution.py:30
  66.3 38.6 %collective-permute-start.1 = (bf16[16,10,16,128]{3,2,1,0:T(8,128)(2,1)S(1)}, bf16[16,10,16,128]{3,2,1,0:T(8,128)(2,1)S(1)}, u32[]{:S(2)}, u32[]{:S(2)}) collective-permute-start(bf16[16,10,16,128]{3,2,1,0:T(8,128)(2,1)S(1)} %all-to-all-done.2.near_ref), channel_id=1, source_target_pairs={{0,1},{1,0},{2,3},{3,2},{4,5},{5,4},{6,7},{7,6},{8,9},{9,8},{10,11... | collective-permute-start | bytes 1966088 | tf_op jit(solution)/shard_map/ppermute | solution.py:34
  68.5 36.4 %copy-start.4 = (bf16[1024,256]{1,0:T(8,128)(2,1)}, bf16[1024,256]{1,0:T(8,128)(2,1)S(1)}, u32[]{:S(2)}) copy-start(bf16[1024,256]{1,0:T(8,128)(2,1)S(1)} %collective-permute-done.11.f2_hbm) | copy-start | bytes 1572868
  68.5 41.9 %collective-permute-start.13 = (bf16[1024,256]{1,0:T(8,128)(2,1)S(1)}, bf16[1024,256]{1,0:T(8,128)(2,1)S(1)}, u32[]{:S(2)}, u32[]{:S(2)}) collective-permute-start(bf16[1024,256]{1,0:T(8,128)(2,1)S(1)} %collective-permute-done.11.f2_hbm), channel_id=1, source_target_pairs={{0,32},{32,64},{64,96},{96,128},{128,160},{160,192},{192,224},{224... | collective-permute-start | bytes 1572872 | tf_op jit(solution)/shard_map/ppermute | solution.py:30
  70.0 34.9 %copy-start.5 = (bf16[1024,256]{1,0:T(8,128)(2,1)}, bf16[1024,256]{1,0:T(8,128)(2,1)S(1)}, u32[]{:S(2)}) copy-start(bf16[1024,256]{1,0:T(8,128)(2,1)S(1)} %collective-permute-done.12.b2_hbm) | copy-start | bytes 1572868
  70.0 40.5 %collective-permute-start.14 = (bf16[1024,256]{1,0:T(8,128)(2,1)S(1)}, bf16[1024,256]{1,0:T(8,128)(2,1)S(1)}, u32[]{:S(2)}, u32[]{:S(2)}) collective-permute-start(bf16[1024,256]{1,0:T(8,128)(2,1)S(1)} %collective-permute-done.12.b2_hbm), channel_id=1, source_target_pairs={{0,224},{32,0},{64,32},{96,64},{128,96},{160,128},{192,160},{224,1... | collective-permute-start | bytes 1572872 | tf_op jit(solution)/shard_map/ppermute | solution.py:30
  71.1 20.5 %collective-permute-start.5 = (bf16[64,1024]{1,0:T(8,128)(2,1)S(1)}, bf16[64,1024]{1,0:T(8,128)(2,1)S(1)}, u32[]{:S(2)}, u32[]{:S(2)}) collective-permute-start(bf16[64,1024]{1,0:T(8,128)(2,1)S(1)} %get-tuple-element.18.own_ref), channel_id=1, source_target_pairs={{0,128},{32,160},{64,192},{96,224},{128,0},{160,32},{192,64},{224,... | collective-permute-start | bytes 393224 | tf_op jit(solution)/shard_map/ppermute | solution.py:30
  91.5 7.6 %collective-permute-start.6 = (bf16[64,1024]{1,0:T(8,128)(2,1)S(1)}, bf16[64,1024]{1,0:T(8,128)(2,1)S(1)}, u32[]{:S(2)}, u32[]{:S(2)}) collective-permute-start(bf16[64,1024]{1,0:T(8,128)(2,1)S(1)} %collective-permute-done.5.own_ref), channel_id=1, source_target_pairs={{0,8},{8,16},{16,24},{24,0},{1,9},{9,17},{17,25},{25,1},{2,10},{10... | collective-permute-start | bytes 393224 | tf_op jit(solution)/shard_map/ppermute | solution.py:30
  91.5 7.6 %collective-permute-start.7 = (bf16[64,1024]{1,0:T(8,128)(2,1)S(1)}, bf16[64,1024]{1,0:T(8,128)(2,1)S(1)}, u32[]{:S(2)}, u32[]{:S(2)}) collective-permute-start(bf16[64,1024]{1,0:T(8,128)(2,1)S(1)} %collective-permute-done.5.own_ref), channel_id=1, source_target_pairs={{0,16},{8,24},{16,0},{24,8},{1,17},{9,25},{17,1},{25,9},{2,18},{10... | collective-permute-start | bytes 393224 | tf_op jit(solution)/shard_map/ppermute | solution.py:30
  99.1 5.0 %collective-permute-start.8 = (bf16[64,1024]{1,0:T(8,128)(2,1)S(1)}, bf16[64,1024]{1,0:T(8,128)(2,1)S(1)}, u32[]{:S(2)}, u32[]{:S(2)}) collective-permute-start(bf16[64,1024]{1,0:T(8,128)(2,1)S(1)} %collective-permute-done.5.own_ref), channel_id=1, source_target_pairs={{0,24},{8,0},{16,8},{24,16},{1,25},{9,1},{17,9},{25,17},{2,26},{10... | collective-permute-start | bytes 393224 | tf_op jit(solution)/shard_map/ppermute | solution.py:30

commit v9 on v8

--- a/solution.py
+++ b/solution.py
@@ -50,7 +50,8 @@
 ):
     tokens, values = first_ref.shape
     width = gain_ref.shape[1]
-    tile = tokens // 3
+    steps = 6
+    tile = tokens // steps
 
     def fetch(source, target, slot):
         copy = pltpu.make_async_copy(source, target, sems.at[slot])
@@ -59,7 +60,7 @@
 
     fixed = [fetch(lam_hbm, lam_ref, 0), fetch(gain_hbm, gain_ref, 1)]
     moving = []
-    for step in range(3):
+    for step in range(steps):
         rows = pl.ds(step * tile, tile)
         moving.append(
             [
@@ -74,7 +75,7 @@
         copy.wait()
     gain = gain_ref[...] * OUT_SCALE
     is_low = place_ref[3] == 0
-    for step in range(3):
+    for step in range(steps):
         rows = pl.ds(step * tile, tile)
         for copy in moving[step]:
             copy.wait()
@@ -118,7 +119,7 @@
             pltpu.VMEM(lam.shape, jnp.float32),
             pltpu.VMEM(gain.shape, jnp.float32),
             pltpu.VMEM(weight.shape, jnp.float32),
-            pltpu.SemaphoreType.DMA((10,)),
+            pltpu.SemaphoreType.DMA((16,)),
         ],
         compiler_params=limit(12),
         name="heads",

time: 113 us -> 114 us (level)
  no operation moved by 1% of the time
where the time goes in v9:
time: 114 us; the launch traced here: 113 us
  waiting for transfers between devices  44.6 us (39%)
  starting transfers between devices  30.5 us (27%)
  blocking collectives  18.9 us (17%)
  Pallas kernels  18.5 us (16%)
    ppermute x13, waiting for transfers between devices, shift(): lax.ppermute(array, axis, [(i, (i + hops) % count) for i in range(count)])  36.7 us
    all_to_all x1, blocking collectives, exchange(): return lax.all_to_all(array, axes, 0, 0, tiled=True)  18.9 us
    ppermute x13, starting transfers between devices, shift(): lax.ppermute(array, axis, [(i, (i + hops) % count) for i in range(count)])  16.9 us
    all_to_all x2, starting transfers between devices, exchange(): return lax.all_to_all(array, axes, 0, 0, tiled=True)  13.5 us
    all_to_all x2, waiting for transfers between devices, exchange(): return lax.all_to_all(array, axes, 0, 0, tiled=True)  6.46 us
    pallas_call x1, Pallas kernels, finish(): pl.pallas_call(finish_kernel, in_specs=[SMEM] + [HBM] * 4 + [VMEM] * 5 +...  5.55 us
    pallas_call x1, Pallas kernels, heads(): pl.pallas_call(heads_kernel, in_specs=[SMEM] + [HBM] * 6, out_specs=[VMEM...  4.93 us
  transfers between devices with their start and end apart: 17, of which 9 were waited for; matrix products, arithmetic and copies ran while one was open for 0% of the time, Pallas kernels for 8%

profile of v9, /device:TPU:32, one launch (start us, length us, event | category | flops | bytes accessed | tf_op | source)
XLA Modules:
  0.0 113.5 jit_solution(1071889861352249074)
XLA Ops:
  0.6 0.0 copy-start
  0.6 0.1 pad_add_fusion.place_ref
  0.7 4.9 %heads.1 = (f32[768,128]{1,0:T(8,128)S(1)}, bf16[768,128]{1,0:T(8,128)(2,1)S(1)}, bf16[64,1024]{1,0:T(8,128)(2,1)S(1)}) custom-call(s32[4]{0:T(128)S(1)} %pad_add_fusion.place_ref, f32[1,4]{1,0:T(1,128)} %bitcast.12, bf16[768,1024]{1,0:T(8,128)(2,1)} %first_hbm.2, bf16[768,1024]{1,0:T(8,128)(2,1)} %second_hbm.2, f32[1,256]{1,0:T(1,128)} %bitcast.11, ...), custom_call_target="tpu_custom_call" | custom-call | tf_op jit(solution)/shard_map/heads/pallas_call | solution.py:106
  5.7 0.0 copy-start.1
  5.7 0.0 copy-start.2
  5.7 0.1 collective-permute-start
  5.8 1.4 %collective-permute-done.far_ref = bf16[768,128]{1,0:T(8,128)(2,1)S(1)} collective-permute-done((bf16[768,128]{1,0:T(8,128)(2,1)S(1)}, bf16[768,128]{1,0:T(8,128)(2,1)S(1)}, u32[]{:S(2)}, u32[]{:S(2)}) %collective-permute-start) | collective-permute-done | bytes 196640 | tf_op jit(solution)/shard_map/ppermute | solution.py:34
  7.2 0.0 copy-done
  7.2 1.4 %gradient.1 = bf16[16,8,16,128]{3,2,1,0:T(8,128)(2,1)} custom-call(f32[768,128]{1,0:T(8,128)S(1)} %get-tuple-element.16.own_ref, bf16[768,128]{1,0:T(8,128)(2,1)S(1)} %collective-permute-done.far_ref, bf16[768,2048]{1,0:T(8,128)(2,1)S(1)} %copy-done), custom_call_target="tpu_custom_call" | custom-call | tf_op jit(solution)/shard_map/gradient/pallas_call | solution.py:171
  8.6 18.9 %all_to_all.15.parts_ref = bf16[16,8,16,128]{3,2,1,0:T(8,128)(2,1)S(1)} all-to-all(bf16[16,8,16,128]{3,2,1,0:T(8,128)(2,1)} %gradient.1), channel_id=1, replica_groups=mesh['z'=8,'y'=4,'x'=4,'tp'=2] {'y','x'}, dimensions={0} | all-to-all | bytes 1048576 | tf_op jit(solution)/shard_map/all_to_all | solution.py:382
  27.5 1.4 %fold.1 = bf16[8,10,16,128]{3,2,1,0:T(8,128)(2,1)} custom-call(s32[4]{0:T(128)S(1)} %pad_add_fusion.place_ref, bf16[16,8,16,128]{3,2,1,0:T(8,128)(2,1)S(1)} %all_to_all.15.parts_ref, f32[64,128]{1,0:T(8,128)S(1)} %copy-done.1, f32[64,128]{1,0:T(8,128)S(1)} %copy-done.2), custom_call_target="tpu_custom_call" | custom-call | tf_op jit(solution)/shard_map/fold/pallas_call | solution.py:202
  28.9 8.6 %all-to-all-start.1 = ((bf16[8,10,16,128]{3,2,1,0:T(8,128)(2,1)}), bf16[8,10,16,128]{3,2,1,0:T(8,128)(2,1)S(1)}, u32[]{:S(2)}, u32[]{:S(2)}) async-start(bf16[8,10,16,128]{3,2,1,0:T(8,128)(2,1)} %fold.1), calls=%async_computation.1 | async-start | bytes 655360 | tf_op jit(solution)/shard_map/all_to_all | solution.py:382
  37.5 0.0 collective-permute-start.2
  37.5 2.3 %collective-permute-start.3 = (bf16[64,1024]{1,0:T(8,128)(2,1)S(1)}, bf16[64,1024]{1,0:T(8,128)(2,1)S(1)}, u32[]{:S(2)}, u32[]{:S(2)}) collective-permute-start(bf16[64,1024]{1,0:T(8,128)(2,1)S(1)} %get-tuple-element.18.own_ref), channel_id=1, source_target_pairs={{0,16},{8,24},{16,0},{24,8},{1,17},{9,25},{17,1},{25,9},{2,18},{10... | collective-permute-start | bytes 393224 | tf_op jit(solution)/shard_map/ppermute | solution.py:30
  39.8 1.2 %collective-permute-start.4 = (bf16[64,1024]{1,0:T(8,128)(2,1)S(1)}, bf16[64,1024]{1,0:T(8,128)(2,1)S(1)}, u32[]{:S(2)}, u32[]{:S(2)}) collective-permute-start(bf16[64,1024]{1,0:T(8,128)(2,1)S(1)} %get-tuple-element.18.own_ref), channel_id=1, source_target_pairs={{0,24},{8,0},{16,8},{24,16},{1,25},{9,1},{17,9},{25,17},{2,26},{10... | collective-permute-start | bytes 393224 | tf_op jit(solution)/shard_map/ppermute | solution.py:30
  41.0 4.1 %collective-permute-done.2.one_ref = bf16[64,1024]{1,0:T(8,128)(2,1)S(1)} collective-permute-done((bf16[64,1024]{1,0:T(8,128)(2,1)S(1)}, bf16[64,1024]{1,0:T(8,128)(2,1)S(1)}, u32[]{:S(2)}, u32[]{:S(2)}) %collective-permute-start.2) | collective-permute-done | bytes 131104 | tf_op jit(solution)/shard_map/ppermute | solution.py:30
  45.1 0.0 collective-permute-done.3.two_ref
  45.1 0.9 collective-permute-done.4.three_ref
  46.0 0.8 widen.2.w0
  46.8 1.5 %collective-permute-start.10 = (bf16[1024,256]{1,0:T(8,128)(2,1)S(1)}, bf16[1024,256]{1,0:T(8,128)(2,1)S(1)}, u32[]{:S(2)}, u32[]{:S(2)}) collective-permute-start(bf16[1024,256]{1,0:T(8,128)(2,1)S(1)} %widen.2.w0), channel_id=1, source_target_pairs={{0,32},{32,64},{64,96},{96,128},{128,160},{160,192},{192,224},{224... | collective-permute-start | bytes 1572872 | tf_op jit(solution)/shard_map/ppermute | solution.py:30
  48.4 0.6 collective-permute-start.9
  48.9 0.0 all-to-all-done.1.letters_ref
  48.9 1.6 %update.1 = bf16[16,10,16,128]{3,2,1,0:T(8,128)(2,1)} custom-call(s32[4]{0:T(128)S(1)} %pad_add_fusion.place_ref, bf16[8,10,16,128]{3,2,1,0:T(8,128)(2,1)S(1)} %all-to-all-done.1.letters_ref), custom_call_target="tpu_custom_call" | custom-call | tf_op jit(solution)/shard_map/update/pallas_call | solution.py:233
  50.5 4.9 %all-to-all-start.2 = ((bf16[16,10,16,128]{3,2,1,0:T(8,128)(2,1)}), bf16[16,10,16,128]{3,2,1,0:T(8,128)(2,1)S(1)}, u32[]{:S(2)}, u32[]{:S(2)}) async-start(bf16[16,10,16,128]{3,2,1,0:T(8,128)(2,1)} %update.1), calls=%async_computation.2 | async-start | bytes 1310720 | tf_op jit(solution)/shard_map/all_to_all | solution.py:382
  55.5 3.2 %collective-permute-done.10.f1_hbm = bf16[1024,256]{1,0:T(8,128)(2,1)S(1)} collective-permute-done((bf16[1024,256]{1,0:T(8,128)(2,1)S(1)}, bf16[1024,256]{1,0:T(8,128)(2,1)S(1)}, u32[]{:S(2)}, u32[]{:S(2)}) %collective-permute-start.10) | collective-permute-done | bytes 524320 | tf_op jit(solution)/shard_map/ppermute | solution.py:30
  58.6 1.8 %collective-permute-start.11 = (bf16[1024,256]{1,0:T(8,128)(2,1)S(1)}, bf16[1024,256]{1,0:T(8,128)(2,1)S(1)}, u32[]{:S(2)}, u32[]{:S(2)}) collective-permute-start(bf16[1024,256]{1,0:T(8,128)(2,1)S(1)} %collective-permute-done.10.f1_hbm), channel_id=1, source_target_pairs={{0,32},{32,64},{64,96},{96,128},{128,160},{160,192},{192,224},{224... | collective-permute-start | bytes 1572872 | tf_op jit(solution)/shard_map/ppermute | solution.py:30
  60.4 0.0 collective-permute-done.9.b1
  60.4 0.2 collective-permute-start.12
  60.7 6.5 %all-to-all-done.2.near_ref = bf16[16,10,16,128]{3,2,1,0:T(8,128)(2,1)S(1)} async-done(((bf16[16,10,16,128]{3,2,1,0:T(8,128)(2,1)}), bf16[16,10,16,128]{3,2,1,0:T(8,128)(2,1)S(1)}, u32[]{:S(2)}, u32[]{:S(2)}) %all-to-all-start.2) | async-done | bytes 655392 | tf_op jit(solution)/shard_map/all_to_all | solution.py:382
  67.1 0.0 collective-permute-start.1
  67.1 2.2 %collective-permute-done.11.f2_hbm = bf16[1024,256]{1,0:T(8,128)(2,1)S(1)} collective-permute-done((bf16[1024,256]{1,0:T(8,128)(2,1)S(1)}, bf16[1024,256]{1,0:T(8,128)(2,1)S(1)}, u32[]{:S(2)}, u32[]{:S(2)}) %collective-permute-start.11) | collective-permute-done | bytes 524320 | tf_op jit(solution)/shard_map/ppermute | solution.py:30
  69.3 1.5 %collective-permute-start.13 = (bf16[1024,256]{1,0:T(8,128)(2,1)S(1)}, bf16[1024,256]{1,0:T(8,128)(2,1)S(1)}, u32[]{:S(2)}, u32[]{:S(2)}) collective-permute-start(bf16[1024,256]{1,0:T(8,128)(2,1)S(1)} %collective-permute-done.11.f2_hbm), channel_id=1, source_target_pairs={{0,32},{32,64},{64,96},{96,128},{128,160},{160,192},{192,224},{224... | collective-permute-start | bytes 1572872 | tf_op jit(solution)/shard_map/ppermute | solution.py:30
  70.8 0.0 collective-permute-done.12.b2_hbm
  70.8 1.0 collective-permute-start.14
  71.9 4.4 %collective-permute-start.5 = (bf16[64,1024]{1,0:T(8,128)(2,1)S(1)}, bf16[64,1024]{1,0:T(8,128)(2,1)S(1)}, u32[]{:S(2)}, u32[]{:S(2)}) collective-permute-start(bf16[64,1024]{1,0:T(8,128)(2,1)S(1)} %get-tuple-element.18.own_ref), channel_id=1, source_target_pairs={{0,128},{32,160},{64,192},{96,224},{128,0},{160,32},{192,64},{224,... | collective-permute-start | bytes 393224 | tf_op jit(solution)/shard_map/ppermute | solution.py:30
  76.3 16.0 %collective-permute-done.5.own_ref = bf16[64,1024]{1,0:T(8,128)(2,1)S(1)} collective-permute-done((bf16[64,1024]{1,0:T(8,128)(2,1)S(1)}, bf16[64,1024]{1,0:T(8,128)(2,1)S(1)}, u32[]{:S(2)}, u32[]{:S(2)}) %collective-permute-start.5) | collective-permute-done | bytes 131104 | tf_op jit(solution)/shard_map/ppermute | solution.py:30
  92.3 0.0 collective-permute-start.6
  92.3 2.3 %collective-permute-start.7 = (bf16[64,1024]{1,0:T(8,128)(2,1)S(1)}, bf16[64,1024]{1,0:T(8,128)(2,1)S(1)}, u32[]{:S(2)}, u32[]{:S(2)}) collective-permute-start(bf16[64,1024]{1,0:T(8,128)(2,1)S(1)} %collective-permute-done.5.own_ref), channel_id=1, source_target_pairs={{0,16},{8,24},{16,0},{24,8},{1,17},{9,25},{17,1},{25,9},{2,18},{10... | collective-permute-start | bytes 393224 | tf_op jit(solution)/shard_map/ppermute | solution.py:30
  94.6 5.3 %collective-permute-done.6.one_ref = bf16[64,1024]{1,0:T(8,128)(2,1)S(1)} collective-permute-done((bf16[64,1024]{1,0:T(8,128)(2,1)S(1)}, bf16[64,1024]{1,0:T(8,128)(2,1)S(1)}, u32[]{:S(2)}, u32[]{:S(2)}) %collective-permute-start.6) | collective-permute-done | bytes 131104 | tf_op jit(solution)/shard_map/ppermute | solution.py:30
  99.9 0.0 collective-permute-start.8
  99.9 0.0 collective-permute-done.7.two_ref
  99.9 5.0 %collective-permute-done.8.three_ref = bf16[64,1024]{1,0:T(8,128)(2,1)S(1)} collective-permute-done((bf16[64,1024]{1,0:T(8,128)(2,1)S(1)}, bf16[64,1024]{1,0:T(8,128)(2,1)S(1)}, u32[]{:S(2)}, u32[]{:S(2)}) %collective-permute-start.8) | collective-permute-done | bytes 131104 | tf_op jit(solution)/shard_map/ppermute | solution.py:30
  104.9 0.8 widen.3.w4
  105.7 0.0 collective-permute-done.1.far_ref
  105.7 5.5 %finish.1 = (f32[64,1024]{1,0:T(8,128)}, f32[64,1024]{1,0:T(8,128)}, bf16[1024,2048]{1,0:T(8,128)(2,1)}, f32[64,128]{1,0:T(8,128)}, f32[64,128]{1,0:T(8,128)}, /...) custom-call(s32[4]{0:T(128)S(1)} %pad_add_fusion.place_ref, ...), custom_call_target="tpu_custom_call" | custom-call | tf_op jit(solution)/shard_map/finish/pallas_call | solution.py:328
  111.3 0.0 collective-permute-done.13.f3
  111.3 0.0 collective-permute-done.14.b3
  111.3 2.0 %last.1 = bf16[1024,2048]{1,0:T(8,128)(2,1)} custom-call(s32[4]{0:T(128)S(1)} %pad_add_fusion.place_ref, bf16[2,256,256]{2,1,0:T(8,128)(2,1)S(1)} %get-tuple-element.20.rows_ref, f32[1,128]{1,0:T(1,128)S(1)} %get-tuple-element.21.scale_ref, bf16[1024,256]{1,0:T(8,128)(2,1)S(1)} %get-tuple-element.22.basis_ref, ...), custom_call_target="tpu_custom_call", output_to_operand_aliasing={{}: (6, {})} | custom-call | tf_op jit(solution)/shard_map/last/pallas_call | solution.py:369
  (8 shorter events, 0.0 us)
Async XLA Ops:
  0.6 6.6 %copy-start = (bf16[768,2048]{1,0:T(8,128)(2,1)S(1)}, bf16[768,2048]{1,0:T(8,128)(2,1)}, u32[]{:S(2)}) copy-start(bf16[768,2048]{1,0:T(8,128)(2,1)} %cot_ref.1) | copy-start | bytes 9437188
  5.7 21.8 %copy-start.1 = (f32[64,128]{1,0:T(8,128)S(1)}, f32[64,128]{1,0:T(8,128)}, u32[]{:S(2)}) copy-start(f32[64,128]{1,0:T(8,128)} %first_hbm.3) | copy-start | bytes 98308
  5.7 21.8 %copy-start.2 = (f32[64,128]{1,0:T(8,128)S(1)}, f32[64,128]{1,0:T(8,128)}, u32[]{:S(2)}) copy-start(f32[64,128]{1,0:T(8,128)} %second_hbm.3) | copy-start | bytes 98308
  5.7 1.5 %collective-permute-start = (bf16[768,128]{1,0:T(8,128)(2,1)S(1)}, bf16[768,128]{1,0:T(8,128)(2,1)S(1)}, u32[]{:S(2)}, u32[]{:S(2)}) collective-permute-start(bf16[768,128]{1,0:T(8,128)(2,1)S(1)} %get-tuple-element.17), channel_id=1, source_target_pairs={{0,1},{1,0},{2,3},{3,2},{4,5},{5,4},{6,7},{7,6},{8,9},{9,8},{10,11... | collective-permute-start | bytes 589832 | tf_op jit(solution)/shard_map/ppermute | solution.py:34
  28.9 20.0 %all-to-all-start.1 = ((bf16[8,10,16,128]{3,2,1,0:T(8,128)(2,1)}), bf16[8,10,16,128]{3,2,1,0:T(8,128)(2,1)S(1)}, u32[]{:S(2)}, u32[]{:S(2)}) async-start(bf16[8,10,16,128]{3,2,1,0:T(8,128)(2,1)} %fold.1), calls=%async_computation.1 | async-start | bytes 655360 | tf_op jit(solution)/shard_map/all_to_all | solution.py:382
  37.5 7.6 %collective-permute-start.2 = (bf16[64,1024]{1,0:T(8,128)(2,1)S(1)}, bf16[64,1024]{1,0:T(8,128)(2,1)S(1)}, u32[]{:S(2)}, u32[]{:S(2)}) collective-permute-start(bf16[64,1024]{1,0:T(8,128)(2,1)S(1)} %get-tuple-element.18.own_ref), channel_id=1, source_target_pairs={{0,8},{8,16},{16,24},{24,0},{1,9},{9,17},{17,25},{25,1},{2,10},{10... | collective-permute-start | bytes 393224 | tf_op jit(solution)/shard_map/ppermute | solution.py:30
  37.5 7.6 %collective-permute-start.3 = (bf16[64,1024]{1,0:T(8,128)(2,1)S(1)}, bf16[64,1024]{1,0:T(8,128)(2,1)S(1)}, u32[]{:S(2)}, u32[]{:S(2)}) collective-permute-start(bf16[64,1024]{1,0:T(8,128)(2,1)S(1)} %get-tuple-element.18.own_ref), channel_id=1, source_target_pairs={{0,16},{8,24},{16,0},{24,8},{1,17},{9,25},{17,1},{25,9},{2,18},{10... | collective-permute-start | bytes 393224 | tf_op jit(solution)/shard_map/ppermute | solution.py:30
  39.8 6.2 %collective-permute-start.4 = (bf16[64,1024]{1,0:T(8,128)(2,1)S(1)}, bf16[64,1024]{1,0:T(8,128)(2,1)S(1)}, u32[]{:S(2)}, u32[]{:S(2)}) collective-permute-start(bf16[64,1024]{1,0:T(8,128)(2,1)S(1)} %get-tuple-element.18.own_ref), channel_id=1, source_target_pairs={{0,24},{8,0},{16,8},{24,16},{1,25},{9,1},{17,9},{25,17},{2,26},{10... | collective-permute-start | bytes 393224 | tf_op jit(solution)/shard_map/ppermute | solution.py:30
  46.8 11.8 %collective-permute-start.10 = (bf16[1024,256]{1,0:T(8,128)(2,1)S(1)}, bf16[1024,256]{1,0:T(8,128)(2,1)S(1)}, u32[]{:S(2)}, u32[]{:S(2)}) collective-permute-start(bf16[1024,256]{1,0:T(8,128)(2,1)S(1)} %widen.2.w0), channel_id=1, source_target_pairs={{0,32},{32,64},{64,96},{96,128},{128,160},{160,192},{192,224},{224... | collective-permute-start | bytes 1572872 | tf_op jit(solution)/shard_map/ppermute | solution.py:30
  48.4 12.1 %collective-permute-start.9 = (bf16[1024,256]{1,0:T(8,128)(2,1)S(1)}, bf16[1024,256]{1,0:T(8,128)(2,1)S(1)}, u32[]{:S(2)}, u32[]{:S(2)}) collective-permute-start(bf16[1024,256]{1,0:T(8,128)(2,1)S(1)} %widen.2.w0), channel_id=1, source_target_pairs={{0,224},{32,0},{64,32},{96,64},{128,96},{160,128},{192,160},{224,1... | collective-permute-start | bytes 1572872 | tf_op jit(solution)/shard_map/ppermute | solution.py:30
  50.5 16.6 %all-to-all-start.2 = ((bf16[16,10,16,128]{3,2,1,0:T(8,128)(2,1)}), bf16[16,10,16,128]{3,2,1,0:T(8,128)(2,1)S(1)}, u32[]{:S(2)}, u32[]{:S(2)}) async-start(bf16[16,10,16,128]{3,2,1,0:T(8,128)(2,1)} %update.1), calls=%async_computation.2 | async-start | bytes 1310720 | tf_op jit(solution)/shard_map/all_to_all | solution.py:382
  58.6 47.1 %copy-start.3 = (bf16[1024,256]{1,0:T(8,128)(2,1)}, bf16[1024,256]{1,0:T(8,128)(2,1)S(1)}, u32[]{:S(2)}) copy-start(bf16[1024,256]{1,0:T(8,128)(2,1)S(1)} %collective-permute-done.10.f1_hbm) | copy-start | bytes 1572868
  58.6 10.7 %collective-permute-start.11 = (bf16[1024,256]{1,0:T(8,128)(2,1)S(1)}, bf16[1024,256]{1,0:T(8,128)(2,1)S(1)}, u32[]{:S(2)}, u32[]{:S(2)}) collective-permute-start(bf16[1024,256]{1,0:T(8,128)(2,1)S(1)} %collective-permute-done.10.f1_hbm), channel_id=1, source_target_pairs={{0,32},{32,64},{64,96},{96,128},{128,160},{160,192},{192,224},{224... | collective-permute-start | bytes 1572872 | tf_op jit(solution)/shard_map/ppermute | solution.py:30
  60.4 10.4 %collective-permute-start.12 = (bf16[1024,256]{1,0:T(8,128)(2,1)S(1)}, bf16[1024,256]{1,0:T(8,128)(2,1)S(1)}, u32[]{:S(2)}, u32[]{:S(2)}) collective-permute-start(bf16[1024,256]{1,0:T(8,128)(2,1)S(1)} %collective-permute-done.9.b1), channel_id=1, source_target_pairs={{0,224},{32,0},{64,32},{96,64},{128,96},{160,128},{192,160},{224,1... | collective-permute-start | bytes 1572872 | tf_op jit(solution)/shard_map/ppermute | solution.py:30
  67.1 38.6 %collective-permute-start.1 = (bf16[16,10,16,128]{3,2,1,0:T(8,128)(2,1)S(1)}, bf16[16,10,16,128]{3,2,1,0:T(8,128)(2,1)S(1)}, u32[]{:S(2)}, u32[]{:S(2)}) collective-permute-start(bf16[16,10,16,128]{3,2,1,0:T(8,128)(2,1)S(1)} %all-to-all-done.2.near_ref), channel_id=1, source_target_pairs={{0,1},{1,0},{2,3},{3,2},{4,5},{5,4},{6,7},{7,6},{8,9},{9,8},{10,11... | collective-permute-start | bytes 1966088 | tf_op jit(solution)/shard_map/ppermute | solution.py:34
  69.3 36.4 %copy-start.4 = (bf16[1024,256]{1,0:T(8,128)(2,1)}, bf16[1024,256]{1,0:T(8,128)(2,1)S(1)}, u32[]{:S(2)}) copy-start(bf16[1024,256]{1,0:T(8,128)(2,1)S(1)} %collective-permute-done.11.f2_hbm) | copy-start | bytes 1572868
  69.3 41.9 %collective-permute-start.13 = (bf16[1024,256]{1,0:T(8,128)(2,1)S(1)}, bf16[1024,256]{1,0:T(8,128)(2,1)S(1)}, u32[]{:S(2)}, u32[]{:S(2)}) collective-permute-start(bf16[1024,256]{1,0:T(8,128)(2,1)S(1)} %collective-permute-done.11.f2_hbm), channel_id=1, source_target_pairs={{0,32},{32,64},{64,96},{96,128},{128,160},{160,192},{192,224},{224... | collective-permute-start | bytes 1572872 | tf_op jit(solution)/shard_map/ppermute | solution.py:30
  70.8 34.9 %copy-start.5 = (bf16[1024,256]{1,0:T(8,128)(2,1)}, bf16[1024,256]{1,0:T(8,128)(2,1)S(1)}, u32[]{:S(2)}) copy-start(bf16[1024,256]{1,0:T(8,128)(2,1)S(1)} %collective-permute-done.12.b2_hbm) | copy-start | bytes 1572868
  70.8 40.5 %collective-permute-start.14 = (bf16[1024,256]{1,0:T(8,128)(2,1)S(1)}, bf16[1024,256]{1,0:T(8,128)(2,1)S(1)}, u32[]{:S(2)}, u32[]{:S(2)}) collective-permute-start(bf16[1024,256]{1,0:T(8,128)(2,1)S(1)} %collective-permute-done.12.b2_hbm), channel_id=1, source_target_pairs={{0,224},{32,0},{64,32},{96,64},{128,96},{160,128},{192,160},{224,1... | collective-permute-start | bytes 1572872 | tf_op jit(solution)/shard_map/ppermute | solution.py:30
  71.9 20.5 %collective-permute-start.5 = (bf16[64,1024]{1,0:T(8,128)(2,1)S(1)}, bf16[64,1024]{1,0:T(8,128)(2,1)S(1)}, u32[]{:S(2)}, u32[]{:S(2)}) collective-permute-start(bf16[64,1024]{1,0:T(8,128)(2,1)S(1)} %get-tuple-element.18.own_ref), channel_id=1, source_target_pairs={{0,128},{32,160},{64,192},{96,224},{128,0},{160,32},{192,64},{224,... | collective-permute-start | bytes 393224 | tf_op jit(solution)/shard_map/ppermute | solution.py:30
  92.3 7.6 %collective-permute-start.6 = (bf16[64,1024]{1,0:T(8,128)(2,1)S(1)}, bf16[64,1024]{1,0:T(8,128)(2,1)S(1)}, u32[]{:S(2)}, u32[]{:S(2)}) collective-permute-start(bf16[64,1024]{1,0:T(8,128)(2,1)S(1)} %collective-permute-done.5.own_ref), channel_id=1, source_target_pairs={{0,8},{8,16},{16,24},{24,0},{1,9},{9,17},{17,25},{25,1},{2,10},{10... | collective-permute-start | bytes 393224 | tf_op jit(solution)/shard_map/ppermute | solution.py:30
  92.3 7.6 %collective-permute-start.7 = (bf16[64,1024]{1,0:T(8,128)(2,1)S(1)}, bf16[64,1024]{1,0:T(8,128)(2,1)S(1)}, u32[]{:S(2)}, u32[]{:S(2)}) collective-permute-start(bf16[64,1024]{1,0:T(8,128)(2,1)S(1)} %collective-permute-done.5.own_ref), channel_id=1, source_target_pairs={{0,16},{8,24},{16,0},{24,8},{1,17},{9,25},{17,1},{25,9},{2,18},{10... | collective-permute-start | bytes 393224 | tf_op jit(solution)/shard_map/ppermute | solution.py:30
  99.9 5.0 %collective-permute-start.8 = (bf16[64,1024]{1,0:T(8,128)(2,1)S(1)}, bf16[64,1024]{1,0:T(8,128)(2,1)S(1)}, u32[]{:S(2)}, u32[]{:S(2)}) collective-permute-start(bf16[64,1024]{1,0:T(8,128)(2,1)S(1)} %collective-permute-done.5.own_ref), channel_id=1, source_target_pairs={{0,24},{8,0},{16,8},{24,16},{1,25},{9,1},{17,9},{25,17},{2,26},{10... | collective-permute-start | bytes 393224 | tf_op jit(solution)/shard_map/ppermute | solution.py:30

commit v10 on v9

--- a/solution.py
+++ b/solution.py
@@ -50,7 +50,7 @@
 ):
     tokens, values = first_ref.shape
     width = gain_ref.shape[1]
-    steps = 6
+    steps = 3
     tile = tokens // steps
 
     def fetch(source, target, slot):
@@ -354,13 +354,18 @@
 
 def last_kernel(place_ref, rows_ref, scale_ref, basis_ref, f3, b3, copy_in, copy_ref, tiles, sems):
     z = place_ref[0]
+    part = basis_ref.shape[0] // 2
     copies = []
     for slot, (block, hops) in enumerate(((f3, 5), (b3, 3))):
-        step = dot(basis_ref[...], rows_ref[slot], 1, 1) * scale_ref[:, :1]
-        tiles[slot] = (block[...].astype(jnp.float32) + step).astype(jnp.bfloat16)
-        copy = pltpu.make_async_copy(tiles.at[slot], copy_ref.at[:, columns(z + hops)], sems.at[slot])
-        copy.start()
-        copies.append(copy)
+        for half in range(2):
+            rows = pl.ds(half * part, part)
+            step = dot(basis_ref[rows, :], rows_ref[slot], 1, 1) * scale_ref[:, :1]
+            tiles[slot, rows] = (block[rows, :].astype(jnp.float32) + step).astype(jnp.bfloat16)
+            copy = pltpu.make_async_copy(
+                tiles.at[slot, rows], copy_ref.at[rows, columns(z + hops)], sems.at[2 * slot + half]
+            )
+            copy.start()
+            copies.append(copy)
     for copy in copies:
         copy.wait()
 
@@ -372,7 +377,7 @@
         out_specs=HBM,
         out_shape=pltpu.HBM(copy.shape, copy.dtype),
         input_output_aliases={6: 0},
-        scratch_shapes=[pltpu.VMEM((2, copy.shape[0], 256), copy.dtype), pltpu.SemaphoreType.DMA((2,))],
+        scratch_shapes=[pltpu.VMEM((2, copy.shape[0], 256), copy.dtype), pltpu.SemaphoreType.DMA((4,))],
         compiler_params=limit(8),
         name="last",
     )(place, *in_vmem(*later), f3, b3, *in_hbm(copy))

time: 114 us -> 113 us (level)
  no operation moved by 1% of the time
where the time goes in v10:
time: 113 us
  waiting for transfers between devices  44.6 us (39%)
  starting transfers between devices  30.5 us (27%)
  blocking collectives  18.9 us (17%)
  Pallas kernels  17.6 us (16%)
    ppermute x13, waiting for transfers between devices, shift(): lax.ppermute(array, axis, [(i, (i + hops) % count) for i in range(count)])  36.7 us
    all_to_all x1, blocking collectives, exchange(): return lax.all_to_all(array, axes, 0, 0, tiled=True)  18.9 us
    ppermute x13, starting transfers between devices, shift(): lax.ppermute(array, axis, [(i, (i + hops) % count) for i in range(count)])  16.9 us
    all_to_all x2, starting transfers between devices, exchange(): return lax.all_to_all(array, axes, 0, 0, tiled=True)  13.5 us
    all_to_all x2, waiting for transfers between devices, exchange(): return lax.all_to_all(array, axes, 0, 0, tiled=True)  6.46 us
    pallas_call x1, Pallas kernels, finish(): pl.pallas_call(finish_kernel, in_specs=[SMEM] + [HBM] * 4 + [VMEM] * 5 +...  5.54 us
    pallas_call x1, Pallas kernels, heads(): pl.pallas_call(heads_kernel, in_specs=[SMEM] + [HBM] * 6, out_specs=[VMEM...  4.19 us
  transfers between devices with their start and end apart: 17, of which 9 were waited for; matrix products, arithmetic and copies ran while one was open for 0% of the time, Pallas kernels for 8%

profile of v10, /device:TPU:32, one launch (start us, length us, event | category | flops | bytes accessed | tf_op | source)
XLA Modules:
  0.0 112.6 jit_solution(7734869812497329680)
XLA Ops:
  0.6 0.0 copy-start
  0.6 0.1 pad_add_fusion.place_ref
  0.7 4.2 %heads.1 = (f32[768,128]{1,0:T(8,128)S(1)}, bf16[768,128]{1,0:T(8,128)(2,1)S(1)}, bf16[64,1024]{1,0:T(8,128)(2,1)S(1)}) custom-call(s32[4]{0:T(128)S(1)} %pad_add_fusion.place_ref, f32[1,4]{1,0:T(1,128)} %bitcast.12, bf16[768,1024]{1,0:T(8,128)(2,1)} %first_hbm.2, bf16[768,1024]{1,0:T(8,128)(2,1)} %second_hbm.2, f32[1,256]{1,0:T(1,128)} %bitcast.11, ...), custom_call_target="tpu_custom_call" | custom-call | tf_op jit(solution)/shard_map/heads/pallas_call | solution.py:106
  4.9 0.0 copy-start.1
  4.9 0.0 copy-start.2
  5.0 0.1 collective-permute-start
  5.1 1.4 %collective-permute-done.far_ref = bf16[768,128]{1,0:T(8,128)(2,1)S(1)} collective-permute-done((bf16[768,128]{1,0:T(8,128)(2,1)S(1)}, bf16[768,128]{1,0:T(8,128)(2,1)S(1)}, u32[]{:S(2)}, u32[]{:S(2)}) %collective-permute-start) | collective-permute-done | bytes 196640 | tf_op jit(solution)/shard_map/ppermute | solution.py:34
  6.5 1.4 %gradient.1 = bf16[16,8,16,128]{3,2,1,0:T(8,128)(2,1)} custom-call(f32[768,128]{1,0:T(8,128)S(1)} %get-tuple-element.16.own_ref, bf16[768,128]{1,0:T(8,128)(2,1)S(1)} %collective-permute-done.far_ref, bf16[768,2048]{1,0:T(8,128)(2,1)S(1)} %copy-done), custom_call_target="tpu_custom_call" | custom-call | tf_op jit(solution)/shard_map/gradient/pallas_call | solution.py:171
  7.9 18.9 %all_to_all.15.parts_ref = bf16[16,8,16,128]{3,2,1,0:T(8,128)(2,1)S(1)} all-to-all(bf16[16,8,16,128]{3,2,1,0:T(8,128)(2,1)} %gradient.1), channel_id=1, replica_groups=mesh['z'=8,'y'=4,'x'=4,'tp'=2] {'y','x'}, dimensions={0} | all-to-all | bytes 1048576 | tf_op jit(solution)/shard_map/all_to_all | solution.py:387
  26.8 0.0 copy-done.2
  26.8 1.4 %fold.1 = bf16[8,10,16,128]{3,2,1,0:T(8,128)(2,1)} custom-call(s32[4]{0:T(128)S(1)} %pad_add_fusion.place_ref, bf16[16,8,16,128]{3,2,1,0:T(8,128)(2,1)S(1)} %all_to_all.15.parts_ref, f32[64,128]{1,0:T(8,128)S(1)} %copy-done.1, f32[64,128]{1,0:T(8,128)S(1)} %copy-done.2), custom_call_target="tpu_custom_call" | custom-call | tf_op jit(solution)/shard_map/fold/pallas_call | solution.py:202
  28.2 8.6 %all-to-all-start.1 = ((bf16[8,10,16,128]{3,2,1,0:T(8,128)(2,1)}), bf16[8,10,16,128]{3,2,1,0:T(8,128)(2,1)S(1)}, u32[]{:S(2)}, u32[]{:S(2)}) async-start(bf16[8,10,16,128]{3,2,1,0:T(8,128)(2,1)} %fold.1), calls=%async_computation.1 | async-start | bytes 655360 | tf_op jit(solution)/shard_map/all_to_all | solution.py:387
  36.8 0.0 collective-permute-start.2
  36.8 2.3 %collective-permute-start.3 = (bf16[64,1024]{1,0:T(8,128)(2,1)S(1)}, bf16[64,1024]{1,0:T(8,128)(2,1)S(1)}, u32[]{:S(2)}, u32[]{:S(2)}) collective-permute-start(bf16[64,1024]{1,0:T(8,128)(2,1)S(1)} %get-tuple-element.18.own_ref), channel_id=1, source_target_pairs={{0,16},{8,24},{16,0},{24,8},{1,17},{9,25},{17,1},{25,9},{2,18},{10... | collective-permute-start | bytes 393224 | tf_op jit(solution)/shard_map/ppermute | solution.py:30
  39.1 1.2 %collective-permute-start.4 = (bf16[64,1024]{1,0:T(8,128)(2,1)S(1)}, bf16[64,1024]{1,0:T(8,128)(2,1)S(1)}, u32[]{:S(2)}, u32[]{:S(2)}) collective-permute-start(bf16[64,1024]{1,0:T(8,128)(2,1)S(1)} %get-tuple-element.18.own_ref), channel_id=1, source_target_pairs={{0,24},{8,0},{16,8},{24,16},{1,25},{9,1},{17,9},{25,17},{2,26},{10... | collective-permute-start | bytes 393224 | tf_op jit(solution)/shard_map/ppermute | solution.py:30
  40.2 4.1 %collective-permute-done.2.one_ref = bf16[64,1024]{1,0:T(8,128)(2,1)S(1)} collective-permute-done((bf16[64,1024]{1,0:T(8,128)(2,1)S(1)}, bf16[64,1024]{1,0:T(8,128)(2,1)S(1)}, u32[]{:S(2)}, u32[]{:S(2)}) %collective-permute-start.2) | collective-permute-done | bytes 131104 | tf_op jit(solution)/shard_map/ppermute | solution.py:30
  44.4 0.0 collective-permute-done.3.two_ref
  44.4 0.9 collective-permute-done.4.three_ref
  45.3 0.8 widen.2.w0
  46.1 1.5 %collective-permute-start.10 = (bf16[1024,256]{1,0:T(8,128)(2,1)S(1)}, bf16[1024,256]{1,0:T(8,128)(2,1)S(1)}, u32[]{:S(2)}, u32[]{:S(2)}) collective-permute-start(bf16[1024,256]{1,0:T(8,128)(2,1)S(1)} %widen.2.w0), channel_id=1, source_target_pairs={{0,32},{32,64},{64,96},{96,128},{128,160},{160,192},{192,224},{224... | collective-permute-start | bytes 1572872 | tf_op jit(solution)/shard_map/ppermute | solution.py:30
  47.6 0.6 collective-permute-start.9
  48.2 0.0 all-to-all-done.1.letters_ref
  48.2 1.6 %update.1 = bf16[16,10,16,128]{3,2,1,0:T(8,128)(2,1)} custom-call(s32[4]{0:T(128)S(1)} %pad_add_fusion.place_ref, bf16[8,10,16,128]{3,2,1,0:T(8,128)(2,1)S(1)} %all-to-all-done.1.letters_ref), custom_call_target="tpu_custom_call" | custom-call | tf_op jit(solution)/shard_map/update/pallas_call | solution.py:233
  49.8 4.9 %all-to-all-start.2 = ((bf16[16,10,16,128]{3,2,1,0:T(8,128)(2,1)}), bf16[16,10,16,128]{3,2,1,0:T(8,128)(2,1)S(1)}, u32[]{:S(2)}, u32[]{:S(2)}) async-start(bf16[16,10,16,128]{3,2,1,0:T(8,128)(2,1)} %update.1), calls=%async_computation.2 | async-start | bytes 1310720 | tf_op jit(solution)/shard_map/all_to_all | solution.py:387
  54.7 3.2 %collective-permute-done.10.f1_hbm = bf16[1024,256]{1,0:T(8,128)(2,1)S(1)} collective-permute-done((bf16[1024,256]{1,0:T(8,128)(2,1)S(1)}, bf16[1024,256]{1,0:T(8,128)(2,1)S(1)}, u32[]{:S(2)}, u32[]{:S(2)}) %collective-permute-start.10) | collective-permute-done | bytes 524320 | tf_op jit(solution)/shard_map/ppermute | solution.py:30
  57.9 1.8 %collective-permute-start.11 = (bf16[1024,256]{1,0:T(8,128)(2,1)S(1)}, bf16[1024,256]{1,0:T(8,128)(2,1)S(1)}, u32[]{:S(2)}, u32[]{:S(2)}) collective-permute-start(bf16[1024,256]{1,0:T(8,128)(2,1)S(1)} %collective-permute-done.10.f1_hbm), channel_id=1, source_target_pairs={{0,32},{32,64},{64,96},{96,128},{128,160},{160,192},{192,224},{224... | collective-permute-start | bytes 1572872 | tf_op jit(solution)/shard_map/ppermute | solution.py:30
  59.7 0.0 collective-permute-done.9.b1
  59.7 0.2 collective-permute-start.12
  59.9 6.5 %all-to-all-done.2.near_ref = bf16[16,10,16,128]{3,2,1,0:T(8,128)(2,1)S(1)} async-done(((bf16[16,10,16,128]{3,2,1,0:T(8,128)(2,1)}), bf16[16,10,16,128]{3,2,1,0:T(8,128)(2,1)S(1)}, u32[]{:S(2)}, u32[]{:S(2)}) %all-to-all-start.2) | async-done | bytes 655392 | tf_op jit(solution)/shard_map/all_to_all | solution.py:387
  66.4 0.0 collective-permute-start.1
  66.4 2.2 %collective-permute-done.11.f2_hbm = bf16[1024,256]{1,0:T(8,128)(2,1)S(1)} collective-permute-done((bf16[1024,256]{1,0:T(8,128)(2,1)S(1)}, bf16[1024,256]{1,0:T(8,128)(2,1)S(1)}, u32[]{:S(2)}, u32[]{:S(2)}) %collective-permute-start.11) | collective-permute-done | bytes 524320 | tf_op jit(solution)/shard_map/ppermute | solution.py:30
  68.6 1.5 %collective-permute-start.13 = (bf16[1024,256]{1,0:T(8,128)(2,1)S(1)}, bf16[1024,256]{1,0:T(8,128)(2,1)S(1)}, u32[]{:S(2)}, u32[]{:S(2)}) collective-permute-start(bf16[1024,256]{1,0:T(8,128)(2,1)S(1)} %collective-permute-done.11.f2_hbm), channel_id=1, source_target_pairs={{0,32},{32,64},{64,96},{96,128},{128,160},{160,192},{192,224},{224... | collective-permute-start | bytes 1572872 | tf_op jit(solution)/shard_map/ppermute | solution.py:30
  70.1 0.0 collective-permute-done.12.b2_hbm
  70.1 1.0 collective-permute-start.14
  71.1 4.4 %collective-permute-start.5 = (bf16[64,1024]{1,0:T(8,128)(2,1)S(1)}, bf16[64,1024]{1,0:T(8,128)(2,1)S(1)}, u32[]{:S(2)}, u32[]{:S(2)}) collective-permute-start(bf16[64,1024]{1,0:T(8,128)(2,1)S(1)} %get-tuple-element.18.own_ref), channel_id=1, source_target_pairs={{0,128},{32,160},{64,192},{96,224},{128,0},{160,32},{192,64},{224,... | collective-permute-start | bytes 393224 | tf_op jit(solution)/shard_map/ppermute | solution.py:30
  75.5 16.0 %collective-permute-done.5.own_ref = bf16[64,1024]{1,0:T(8,128)(2,1)S(1)} collective-permute-done((bf16[64,1024]{1,0:T(8,128)(2,1)S(1)}, bf16[64,1024]{1,0:T(8,128)(2,1)S(1)}, u32[]{:S(2)}, u32[]{:S(2)}) %collective-permute-start.5) | collective-permute-done | bytes 131104 | tf_op jit(solution)/shard_map/ppermute | solution.py:30
  91.6 0.0 collective-permute-start.6
  91.6 2.3 %collective-permute-start.7 = (bf16[64,1024]{1,0:T(8,128)(2,1)S(1)}, bf16[64,1024]{1,0:T(8,128)(2,1)S(1)}, u32[]{:S(2)}, u32[]{:S(2)}) collective-permute-start(bf16[64,1024]{1,0:T(8,128)(2,1)S(1)} %collective-permute-done.5.own_ref), channel_id=1, source_target_pairs={{0,16},{8,24},{16,0},{24,8},{1,17},{9,25},{17,1},{25,9},{2,18},{10... | collective-permute-start | bytes 393224 | tf_op jit(solution)/shard_map/ppermute | solution.py:30
  93.9 5.3 %collective-permute-done.6.one_ref = bf16[64,1024]{1,0:T(8,128)(2,1)S(1)} collective-permute-done((bf16[64,1024]{1,0:T(8,128)(2,1)S(1)}, bf16[64,1024]{1,0:T(8,128)(2,1)S(1)}, u32[]{:S(2)}, u32[]{:S(2)}) %collective-permute-start.6) | collective-permute-done | bytes 131104 | tf_op jit(solution)/shard_map/ppermute | solution.py:30
  99.2 0.0 collective-permute-start.8
  99.2 0.0 collective-permute-done.7.two_ref
  99.2 5.0 %collective-permute-done.8.three_ref = bf16[64,1024]{1,0:T(8,128)(2,1)S(1)} collective-permute-done((bf16[64,1024]{1,0:T(8,128)(2,1)S(1)}, bf16[64,1024]{1,0:T(8,128)(2,1)S(1)}, u32[]{:S(2)}, u32[]{:S(2)}) %collective-permute-start.8) | collective-permute-done | bytes 131104 | tf_op jit(solution)/shard_map/ppermute | solution.py:30
  104.1 0.8 widen.3.w4
  104.9 0.0 collective-permute-done.1.far_ref
  105.0 5.5 %finish.1 = (f32[64,1024]{1,0:T(8,128)}, f32[64,1024]{1,0:T(8,128)}, bf16[1024,2048]{1,0:T(8,128)(2,1)}, f32[64,128]{1,0:T(8,128)}, f32[64,128]{1,0:T(8,128)}, /...) custom-call(s32[4]{0:T(128)S(1)} %pad_add_fusion.place_ref, ...), custom_call_target="tpu_custom_call" | custom-call | tf_op jit(solution)/shard_map/finish/pallas_call | solution.py:328
  110.5 0.0 collective-permute-done.13.f3
  110.5 0.0 collective-permute-done.14.b3
  110.6 1.9 %last.1 = bf16[1024,2048]{1,0:T(8,128)(2,1)} custom-call(s32[4]{0:T(128)S(1)} %pad_add_fusion.place_ref, bf16[2,256,256]{2,1,0:T(8,128)(2,1)S(1)} %get-tuple-element.20.rows_ref, f32[1,128]{1,0:T(1,128)S(1)} %get-tuple-element.21.scale_ref, bf16[1024,256]{1,0:T(8,128)(2,1)S(1)} %get-tuple-element.22.basis_ref, ...), custom_call_target="tpu_custom_call", output_to_operand_aliasing={{}: (6, {})} | custom-call | tf_op jit(solution)/shard_map/last/pallas_call | solution.py:374
  (8 shorter events, 0.0 us)
Async XLA Ops:
  0.6 5.9 %copy-start = (bf16[768,2048]{1,0:T(8,128)(2,1)S(1)}, bf16[768,2048]{1,0:T(8,128)(2,1)}, u32[]{:S(2)}) copy-start(bf16[768,2048]{1,0:T(8,128)(2,1)} %cot_ref.1) | copy-start | bytes 9437188
  4.9 21.9 %copy-start.1 = (f32[64,128]{1,0:T(8,128)S(1)}, f32[64,128]{1,0:T(8,128)}, u32[]{:S(2)}) copy-start(f32[64,128]{1,0:T(8,128)} %first_hbm.3) | copy-start | bytes 98308
  4.9 21.8 %copy-start.2 = (f32[64,128]{1,0:T(8,128)S(1)}, f32[64,128]{1,0:T(8,128)}, u32[]{:S(2)}) copy-start(f32[64,128]{1,0:T(8,128)} %second_hbm.3) | copy-start | bytes 98308
  5.0 1.5 %collective-permute-start = (bf16[768,128]{1,0:T(8,128)(2,1)S(1)}, bf16[768,128]{1,0:T(8,128)(2,1)S(1)}, u32[]{:S(2)}, u32[]{:S(2)}) collective-permute-start(bf16[768,128]{1,0:T(8,128)(2,1)S(1)} %get-tuple-element.17), channel_id=1, source_target_pairs={{0,1},{1,0},{2,3},{3,2},{4,5},{5,4},{6,7},{7,6},{8,9},{9,8},{10,11... | collective-permute-start | bytes 589832 | tf_op jit(solution)/shard_map/ppermute | solution.py:34
  28.2 20.0 %all-to-all-start.1 = ((bf16[8,10,16,128]{3,2,1,0:T(8,128)(2,1)}), bf16[8,10,16,128]{3,2,1,0:T(8,128)(2,1)S(1)}, u32[]{:S(2)}, u32[]{:S(2)}) async-start(bf16[8,10,16,128]{3,2,1,0:T(8,128)(2,1)} %fold.1), calls=%async_computation.1 | async-start | bytes 655360 | tf_op jit(solution)/shard_map/all_to_all | solution.py:387
  36.8 7.6 %collective-permute-start.2 = (bf16[64,1024]{1,0:T(8,128)(2,1)S(1)}, bf16[64,1024]{1,0:T(8,128)(2,1)S(1)}, u32[]{:S(2)}, u32[]{:S(2)}) collective-permute-start(bf16[64,1024]{1,0:T(8,128)(2,1)S(1)} %get-tuple-element.18.own_ref), channel_id=1, source_target_pairs={{0,8},{8,16},{16,24},{24,0},{1,9},{9,17},{17,25},{25,1},{2,10},{10... | collective-permute-start | bytes 393224 | tf_op jit(solution)/shard_map/ppermute | solution.py:30
  36.8 7.6 %collective-permute-start.3 = (bf16[64,1024]{1,0:T(8,128)(2,1)S(1)}, bf16[64,1024]{1,0:T(8,128)(2,1)S(1)}, u32[]{:S(2)}, u32[]{:S(2)}) collective-permute-start(bf16[64,1024]{1,0:T(8,128)(2,1)S(1)} %get-tuple-element.18.own_ref), channel_id=1, source_target_pairs={{0,16},{8,24},{16,0},{24,8},{1,17},{9,25},{17,1},{25,9},{2,18},{10... | collective-permute-start | bytes 393224 | tf_op jit(solution)/shard_map/ppermute | solution.py:30
  39.1 6.2 %collective-permute-start.4 = (bf16[64,1024]{1,0:T(8,128)(2,1)S(1)}, bf16[64,1024]{1,0:T(8,128)(2,1)S(1)}, u32[]{:S(2)}, u32[]{:S(2)}) collective-permute-start(bf16[64,1024]{1,0:T(8,128)(2,1)S(1)} %get-tuple-element.18.own_ref), channel_id=1, source_target_pairs={{0,24},{8,0},{16,8},{24,16},{1,25},{9,1},{17,9},{25,17},{2,26},{10... | collective-permute-start | bytes 393224 | tf_op jit(solution)/shard_map/ppermute | solution.py:30
  46.1 11.8 %collective-permute-start.10 = (bf16[1024,256]{1,0:T(8,128)(2,1)S(1)}, bf16[1024,256]{1,0:T(8,128)(2,1)S(1)}, u32[]{:S(2)}, u32[]{:S(2)}) collective-permute-start(bf16[1024,256]{1,0:T(8,128)(2,1)S(1)} %widen.2.w0), channel_id=1, source_target_pairs={{0,32},{32,64},{64,96},{96,128},{128,160},{160,192},{192,224},{224... | collective-permute-start | bytes 1572872 | tf_op jit(solution)/shard_map/ppermute | solution.py:30
  47.6 12.1 %collective-permute-start.9 = (bf16[1024,256]{1,0:T(8,128)(2,1)S(1)}, bf16[1024,256]{1,0:T(8,128)(2,1)S(1)}, u32[]{:S(2)}, u32[]{:S(2)}) collective-permute-start(bf16[1024,256]{1,0:T(8,128)(2,1)S(1)} %widen.2.w0), channel_id=1, source_target_pairs={{0,224},{32,0},{64,32},{96,64},{128,96},{160,128},{192,160},{224,1... | collective-permute-start | bytes 1572872 | tf_op jit(solution)/shard_map/ppermute | solution.py:30
  49.8 16.6 %all-to-all-start.2 = ((bf16[16,10,16,128]{3,2,1,0:T(8,128)(2,1)}), bf16[16,10,16,128]{3,2,1,0:T(8,128)(2,1)S(1)}, u32[]{:S(2)}, u32[]{:S(2)}) async-start(bf16[16,10,16,128]{3,2,1,0:T(8,128)(2,1)} %update.1), calls=%async_computation.2 | async-start | bytes 1310720 | tf_op jit(solution)/shard_map/all_to_all | solution.py:387
  57.9 47.1 %copy-start.3 = (bf16[1024,256]{1,0:T(8,128)(2,1)}, bf16[1024,256]{1,0:T(8,128)(2,1)S(1)}, u32[]{:S(2)}) copy-start(bf16[1024,256]{1,0:T(8,128)(2,1)S(1)} %collective-permute-done.10.f1_hbm) | copy-start | bytes 1572868
  57.9 10.7 %collective-permute-start.11 = (bf16[1024,256]{1,0:T(8,128)(2,1)S(1)}, bf16[1024,256]{1,0:T(8,128)(2,1)S(1)}, u32[]{:S(2)}, u32[]{:S(2)}) collective-permute-start(bf16[1024,256]{1,0:T(8,128)(2,1)S(1)} %collective-permute-done.10.f1_hbm), channel_id=1, source_target_pairs={{0,32},{32,64},{64,96},{96,128},{128,160},{160,192},{192,224},{224... | collective-permute-start | bytes 1572872 | tf_op jit(solution)/shard_map/ppermute | solution.py:30
  59.7 10.4 %collective-permute-start.12 = (bf16[1024,256]{1,0:T(8,128)(2,1)S(1)}, bf16[1024,256]{1,0:T(8,128)(2,1)S(1)}, u32[]{:S(2)}, u32[]{:S(2)}) collective-permute-start(bf16[1024,256]{1,0:T(8,128)(2,1)S(1)} %collective-permute-done.9.b1), channel_id=1, source_target_pairs={{0,224},{32,0},{64,32},{96,64},{128,96},{160,128},{192,160},{224,1... | collective-permute-start | bytes 1572872 | tf_op jit(solution)/shard_map/ppermute | solution.py:30
  66.4 38.6 %collective-permute-start.1 = (bf16[16,10,16,128]{3,2,1,0:T(8,128)(2,1)S(1)}, bf16[16,10,16,128]{3,2,1,0:T(8,128)(2,1)S(1)}, u32[]{:S(2)}, u32[]{:S(2)}) collective-permute-start(bf16[16,10,16,128]{3,2,1,0:T(8,128)(2,1)S(1)} %all-to-all-done.2.near_ref), channel_id=1, source_target_pairs={{0,1},{1,0},{2,3},{3,2},{4,5},{5,4},{6,7},{7,6},{8,9},{9,8},{10,11... | collective-permute-start | bytes 1966088 | tf_op jit(solution)/shard_map/ppermute | solution.py:34
  68.6 36.4 %copy-start.4 = (bf16[1024,256]{1,0:T(8,128)(2,1)}, bf16[1024,256]{1,0:T(8,128)(2,1)S(1)}, u32[]{:S(2)}) copy-start(bf16[1024,256]{1,0:T(8,128)(2,1)S(1)} %collective-permute-done.11.f2_hbm) | copy-start | bytes 1572868
  68.6 41.9 %collective-permute-start.13 = (bf16[1024,256]{1,0:T(8,128)(2,1)S(1)}, bf16[1024,256]{1,0:T(8,128)(2,1)S(1)}, u32[]{:S(2)}, u32[]{:S(2)}) collective-permute-start(bf16[1024,256]{1,0:T(8,128)(2,1)S(1)} %collective-permute-done.11.f2_hbm), channel_id=1, source_target_pairs={{0,32},{32,64},{64,96},{96,128},{128,160},{160,192},{192,224},{224... | collective-permute-start | bytes 1572872 | tf_op jit(solution)/shard_map/ppermute | solution.py:30
  70.1 34.9 %copy-start.5 = (bf16[1024,256]{1,0:T(8,128)(2,1)}, bf16[1024,256]{1,0:T(8,128)(2,1)S(1)}, u32[]{:S(2)}) copy-start(bf16[1024,256]{1,0:T(8,128)(2,1)S(1)} %collective-permute-done.12.b2_hbm) | copy-start | bytes 1572868
  70.1 40.5 %collective-permute-start.14 = (bf16[1024,256]{1,0:T(8,128)(2,1)S(1)}, bf16[1024,256]{1,0:T(8,128)(2,1)S(1)}, u32[]{:S(2)}, u32[]{:S(2)}) collective-permute-start(bf16[1024,256]{1,0:T(8,128)(2,1)S(1)} %collective-permute-done.12.b2_hbm), channel_id=1, source_target_pairs={{0,224},{32,0},{64,32},{96,64},{128,96},{160,128},{192,160},{224,1... | collective-permute-start | bytes 1572872 | tf_op jit(solution)/shard_map/ppermute | solution.py:30
  71.1 20.5 %collective-permute-start.5 = (bf16[64,1024]{1,0:T(8,128)(2,1)S(1)}, bf16[64,1024]{1,0:T(8,128)(2,1)S(1)}, u32[]{:S(2)}, u32[]{:S(2)}) collective-permute-start(bf16[64,1024]{1,0:T(8,128)(2,1)S(1)} %get-tuple-element.18.own_ref), channel_id=1, source_target_pairs={{0,128},{32,160},{64,192},{96,224},{128,0},{160,32},{192,64},{224,... | collective-permute-start | bytes 393224 | tf_op jit(solution)/shard_map/ppermute | solution.py:30
  91.6 7.6 %collective-permute-start.6 = (bf16[64,1024]{1,0:T(8,128)(2,1)S(1)}, bf16[64,1024]{1,0:T(8,128)(2,1)S(1)}, u32[]{:S(2)}, u32[]{:S(2)}) collective-permute-start(bf16[64,1024]{1,0:T(8,128)(2,1)S(1)} %collective-permute-done.5.own_ref), channel_id=1, source_target_pairs={{0,8},{8,16},{16,24},{24,0},{1,9},{9,17},{17,25},{25,1},{2,10},{10... | collective-permute-start | bytes 393224 | tf_op jit(solution)/shard_map/ppermute | solution.py:30
  91.6 7.6 %collective-permute-start.7 = (bf16[64,1024]{1,0:T(8,128)(2,1)S(1)}, bf16[64,1024]{1,0:T(8,128)(2,1)S(1)}, u32[]{:S(2)}, u32[]{:S(2)}) collective-permute-start(bf16[64,1024]{1,0:T(8,128)(2,1)S(1)} %collective-permute-done.5.own_ref), channel_id=1, source_target_pairs={{0,16},{8,24},{16,0},{24,8},{1,17},{9,25},{17,1},{25,9},{2,18},{10... | collective-permute-start | bytes 393224 | tf_op jit(solution)/shard_map/ppermute | solution.py:30
  99.2 5.0 %collective-permute-start.8 = (bf16[64,1024]{1,0:T(8,128)(2,1)S(1)}, bf16[64,1024]{1,0:T(8,128)(2,1)S(1)}, u32[]{:S(2)}, u32[]{:S(2)}) collective-permute-start(bf16[64,1024]{1,0:T(8,128)(2,1)S(1)} %collective-permute-done.5.own_ref), channel_id=1, source_target_pairs={{0,24},{8,0},{16,8},{24,16},{1,25},{9,1},{17,9},{25,17},{2,26},{10... | collective-permute-start | bytes 393224 | tf_op jit(solution)/shard_map/ppermute | solution.py:30

commit v11 on v10

--- a/solution.py
+++ b/solution.py
@@ -222,14 +222,12 @@
     first_new, second_new = moments(projected_ref[...], first, second)
     letter_ref[:8] = (first_new / (jnp.sqrt(second_new) + 1e-08)).astype(jnp.bfloat16)
     mine = projected_ref[place_ref[0]]
-    high = mine.astype(jnp.bfloat16)
-    letter_ref[8] = high
-    letter_ref[9] = (mine - high.astype(jnp.float32)).astype(jnp.bfloat16)
+    letter_ref[8] = mine.astype(jnp.bfloat16)
     send([(letter_ref, out_hbm.at[peer]) for peer in range(16)], sems)
 
 
 def update(place, letters):
-    shape = letters.shape[1:]
+    shape = (9, *letters.shape[2:])
     return pl.pallas_call(
         update_kernel,
         in_specs=[SMEM, VMEM],
@@ -314,7 +312,7 @@
     for source in range(4):
         rows = pl.ds(source * 16, 16)
         letter = y * 4 + source
-        piece = near_ref[letter, 8].astype(jnp.float32) + near_ref[letter, 9].astype(jnp.float32)
+        piece = near_ref[letter, 8].astype(jnp.float32)
         first_new, second_new = moments(piece, first_ref[rows, :], second_ref[rows, :])
         first_out[rows, :] = first_new
         second_out[rows, :] = second_new

time: 113 us -> 113 us (level)
  the two profiles are of different devices: /device:TPU:32 before, /device:TPU:28 now
where the time goes in v11:
time: 113 us; the launch traced here: 112 us
  waiting for transfers between devices  44.5 us (39%)
  starting transfers between devices  34.1 us (30%)
  Pallas kernels  17.6 us (16%)
  blocking collectives  14.8 us (13%)
    ppermute x13, waiting for transfers between devices, shift(): lax.ppermute(array, axis, [(i, (i + hops) % count) for i in range(count)])  42 us
    ppermute x13, starting transfers between devices, shift(): lax.ppermute(array, axis, [(i, (i + hops) % count) for i in range(count)])  18.6 us
    all_to_all x2, starting transfers between devices, exchange(): return lax.all_to_all(array, axes, 0, 0, tiled=True)  15.4 us
    all_to_all x1, blocking collectives, exchange(): return lax.all_to_all(array, axes, 0, 0, tiled=True)  14.8 us
    pallas_call x1, Pallas kernels, finish(): pl.pallas_call(finish_kernel, in_specs=[SMEM] + [HBM] * 4 + [VMEM] * 5 +...  5.54 us
    pallas_call x1, Pallas kernels, heads(): pl.pallas_call(heads_kernel, in_specs=[SMEM] + [HBM] * 6, out_specs=[VMEM...  4.19 us
  transfers between devices with their start and end apart: 17, of which 11 were waited for; matrix products, arithmetic and copies ran while one was open for 0% of the time, Pallas kernels for 8%

profile of v11, /device:TPU:28, one launch (start us, length us, event | category | flops | bytes accessed | tf_op | source)
XLA Modules:
  0.0 112.1 jit_solution(9824001373945907111)
XLA Ops:
  0.6 0.0 copy-start
  0.6 0.1 pad_add_fusion.place_ref
  0.7 4.2 %heads.1 = (f32[768,128]{1,0:T(8,128)S(1)}, bf16[768,128]{1,0:T(8,128)(2,1)S(1)}, bf16[64,1024]{1,0:T(8,128)(2,1)S(1)}) custom-call(s32[4]{0:T(128)S(1)} %pad_add_fusion.place_ref, f32[1,4]{1,0:T(1,128)} %bitcast.12, bf16[768,1024]{1,0:T(8,128)(2,1)} %first_hbm.2, bf16[768,1024]{1,0:T(8,128)(2,1)} %second_hbm.2, f32[1,256]{1,0:T(1,128)} %bitcast.11, ...), custom_call_target="tpu_custom_call" | custom-call | tf_op jit(solution)/shard_map/heads/pallas_call | solution.py:106
  4.9 0.0 copy-start.1
  4.9 0.0 copy-start.2
  5.0 0.1 collective-permute-start
  5.1 1.4 %collective-permute-done.far_ref = bf16[768,128]{1,0:T(8,128)(2,1)S(1)} collective-permute-done((bf16[768,128]{1,0:T(8,128)(2,1)S(1)}, bf16[768,128]{1,0:T(8,128)(2,1)S(1)}, u32[]{:S(2)}, u32[]{:S(2)}) %collective-permute-start) | collective-permute-done | bytes 196640 | tf_op jit(solution)/shard_map/ppermute | solution.py:34
  6.5 1.4 %gradient.1 = bf16[16,8,16,128]{3,2,1,0:T(8,128)(2,1)} custom-call(f32[768,128]{1,0:T(8,128)S(1)} %get-tuple-element.16.own_ref, bf16[768,128]{1,0:T(8,128)(2,1)S(1)} %collective-permute-done.far_ref, bf16[768,2048]{1,0:T(8,128)(2,1)S(1)} %copy-done), custom_call_target="tpu_custom_call" | custom-call | tf_op jit(solution)/shard_map/gradient/pallas_call | solution.py:171
  7.9 14.8 %all_to_all.15.parts_ref = bf16[16,8,16,128]{3,2,1,0:T(8,128)(2,1)S(1)} all-to-all(bf16[16,8,16,128]{3,2,1,0:T(8,128)(2,1)} %gradient.1), channel_id=1, replica_groups=mesh['z'=8,'y'=4,'x'=4,'tp'=2] {'y','x'}, dimensions={0} | all-to-all | bytes 1048576 | tf_op jit(solution)/shard_map/all_to_all | solution.py:385
  22.7 0.0 copy-done.1
  22.7 1.4 %fold.1 = bf16[8,10,16,128]{3,2,1,0:T(8,128)(2,1)} custom-call(s32[4]{0:T(128)S(1)} %pad_add_fusion.place_ref, bf16[16,8,16,128]{3,2,1,0:T(8,128)(2,1)S(1)} %all_to_all.15.parts_ref, f32[64,128]{1,0:T(8,128)S(1)} %copy-done.1, f32[64,128]{1,0:T(8,128)S(1)} %copy-done.2), custom_call_target="tpu_custom_call" | custom-call | tf_op jit(solution)/shard_map/fold/pallas_call | solution.py:202
  24.1 8.5 %all-to-all-start.1 = ((bf16[8,10,16,128]{3,2,1,0:T(8,128)(2,1)}), bf16[8,10,16,128]{3,2,1,0:T(8,128)(2,1)S(1)}, u32[]{:S(2)}, u32[]{:S(2)}) async-start(bf16[8,10,16,128]{3,2,1,0:T(8,128)(2,1)} %fold.1), calls=%async_computation.1 | async-start | bytes 655360 | tf_op jit(solution)/shard_map/all_to_all | solution.py:385
  32.5 2.1 %collective-permute-start.2 = (bf16[64,1024]{1,0:T(8,128)(2,1)S(1)}, bf16[64,1024]{1,0:T(8,128)(2,1)S(1)}, u32[]{:S(2)}, u32[]{:S(2)}) collective-permute-start(bf16[64,1024]{1,0:T(8,128)(2,1)S(1)} %get-tuple-element.18.own_ref), channel_id=1, source_target_pairs={{0,8},{8,16},{16,24},{24,0},{1,9},{9,17},{17,25},{25,1},{2,10},{10... | collective-permute-start | bytes 393224 | tf_op jit(solution)/shard_map/ppermute | solution.py:30
  34.7 0.9 collective-permute-start.3
  35.6 0.6 collective-permute-start.4
  36.2 3.7 %collective-permute-done.2.one_ref = bf16[64,1024]{1,0:T(8,128)(2,1)S(1)} collective-permute-done((bf16[64,1024]{1,0:T(8,128)(2,1)S(1)}, bf16[64,1024]{1,0:T(8,128)(2,1)S(1)}, u32[]{:S(2)}, u32[]{:S(2)}) %collective-permute-start.2) | collective-permute-done | bytes 131104 | tf_op jit(solution)/shard_map/ppermute | solution.py:30
  39.8 2.3 %collective-permute-done.3.two_ref = bf16[64,1024]{1,0:T(8,128)(2,1)S(1)} collective-permute-done((bf16[64,1024]{1,0:T(8,128)(2,1)S(1)}, bf16[64,1024]{1,0:T(8,128)(2,1)S(1)}, u32[]{:S(2)}, u32[]{:S(2)}) %collective-permute-start.3) | collective-permute-done | bytes 131104 | tf_op jit(solution)/shard_map/ppermute | solution.py:30
  42.1 1.4 %collective-permute-done.4.three_ref = bf16[64,1024]{1,0:T(8,128)(2,1)S(1)} collective-permute-done((bf16[64,1024]{1,0:T(8,128)(2,1)S(1)}, bf16[64,1024]{1,0:T(8,128)(2,1)S(1)}, u32[]{:S(2)}, u32[]{:S(2)}) %collective-permute-start.4) | collective-permute-done | bytes 131104 | tf_op jit(solution)/shard_map/ppermute | solution.py:30
  43.5 0.8 widen.2.w0
  44.3 1.8 %collective-permute-start.10 = (bf16[1024,256]{1,0:T(8,128)(2,1)S(1)}, bf16[1024,256]{1,0:T(8,128)(2,1)S(1)}, u32[]{:S(2)}, u32[]{:S(2)}) collective-permute-start(bf16[1024,256]{1,0:T(8,128)(2,1)S(1)} %widen.2.w0), channel_id=1, source_target_pairs={{0,32},{32,64},{64,96},{96,128},{128,160},{160,192},{192,224},{224... | collective-permute-start | bytes 1572872 | tf_op jit(solution)/shard_map/ppermute | solution.py:30
  46.1 1.5 %collective-permute-start.9 = (bf16[1024,256]{1,0:T(8,128)(2,1)S(1)}, bf16[1024,256]{1,0:T(8,128)(2,1)S(1)}, u32[]{:S(2)}, u32[]{:S(2)}) collective-permute-start(bf16[1024,256]{1,0:T(8,128)(2,1)S(1)} %widen.2.w0), channel_id=1, source_target_pairs={{0,224},{32,0},{64,32},{96,64},{128,96},{160,128},{192,160},{224,1... | collective-permute-start | bytes 1572872 | tf_op jit(solution)/shard_map/ppermute | solution.py:30
  47.6 0.0 all-to-all-done.1.letters_ref
  47.6 1.6 %update.1 = bf16[16,9,16,128]{3,2,1,0:T(8,128)(2,1)} custom-call(s32[4]{0:T(128)S(1)} %pad_add_fusion.place_ref, bf16[8,10,16,128]{3,2,1,0:T(8,128)(2,1)S(1)} %all-to-all-done.1.letters_ref), custom_call_target="tpu_custom_call" | custom-call | tf_op jit(solution)/shard_map/update/pallas_call | solution.py:231
  49.2 6.9 %all-to-all-start.2 = ((bf16[16,9,16,128]{3,2,1,0:T(8,128)(2,1)}), bf16[16,9,16,128]{3,2,1,0:T(8,128)(2,1)S(1)}, u32[]{:S(2)}, u32[]{:S(2)}) async-start(bf16[16,9,16,128]{3,2,1,0:T(8,128)(2,1)} %update.1), calls=%async_computation.2 | async-start | bytes 1179648 | tf_op jit(solution)/shard_map/all_to_all | solution.py:385
  56.2 2.6 %collective-permute-done.10.f1_hbm = bf16[1024,256]{1,0:T(8,128)(2,1)S(1)} collective-permute-done((bf16[1024,256]{1,0:T(8,128)(2,1)S(1)}, bf16[1024,256]{1,0:T(8,128)(2,1)S(1)}, u32[]{:S(2)}, u32[]{:S(2)}) %collective-permute-start.10) | collective-permute-done | bytes 524320 | tf_op jit(solution)/shard_map/ppermute | solution.py:30
  58.8 0.3 collective-permute-start.11
  59.0 0.0 collective-permute-done.9.b1
  59.0 3.0 %collective-permute-start.12 = (bf16[1024,256]{1,0:T(8,128)(2,1)S(1)}, bf16[1024,256]{1,0:T(8,128)(2,1)S(1)}, u32[]{:S(2)}, u32[]{:S(2)}) collective-permute-start(bf16[1024,256]{1,0:T(8,128)(2,1)S(1)} %collective-permute-done.9.b1), channel_id=1, source_target_pairs={{0,224},{32,0},{64,32},{96,64},{128,96},{160,128},{192,160},{224,1... | collective-permute-start | bytes 1572872 | tf_op jit(solution)/shard_map/ppermute | solution.py:30
  62.0 1.1 all-to-all-done.2.near_ref
  63.1 0.0 collective-permute-start.1
  63.1 9.2 %collective-permute-done.11.f2_hbm = bf16[1024,256]{1,0:T(8,128)(2,1)S(1)} collective-permute-done((bf16[1024,256]{1,0:T(8,128)(2,1)S(1)}, bf16[1024,256]{1,0:T(8,128)(2,1)S(1)}, u32[]{:S(2)}, u32[]{:S(2)}) %collective-permute-start.11) | collective-permute-done | bytes 524320 | tf_op jit(solution)/shard_map/ppermute | solution.py:30
  72.3 0.0 collective-permute-start.13
  72.3 0.0 collective-permute-done.12.b2_hbm
  72.4 3.2 %collective-permute-start.14 = (bf16[1024,256]{1,0:T(8,128)(2,1)S(1)}, bf16[1024,256]{1,0:T(8,128)(2,1)S(1)}, u32[]{:S(2)}, u32[]{:S(2)}) collective-permute-start(bf16[1024,256]{1,0:T(8,128)(2,1)S(1)} %collective-permute-done.12.b2_hbm), channel_id=1, source_target_pairs={{0,224},{32,0},{64,32},{96,64},{128,96},{160,128},{192,160},{224,1... | collective-permute-start | bytes 1572872 | tf_op jit(solution)/shard_map/ppermute | solution.py:30
  75.6 5.1 %collective-permute-start.5 = (bf16[64,1024]{1,0:T(8,128)(2,1)S(1)}, bf16[64,1024]{1,0:T(8,128)(2,1)S(1)}, u32[]{:S(2)}, u32[]{:S(2)}) collective-permute-start(bf16[64,1024]{1,0:T(8,128)(2,1)S(1)} %get-tuple-element.18.own_ref), channel_id=1, source_target_pairs={{0,128},{32,160},{64,192},{96,224},{128,0},{160,32},{192,64},{224,... | collective-permute-start | bytes 393224 | tf_op jit(solution)/shard_map/ppermute | solution.py:30
  80.7 11.8 %collective-permute-done.5.own_ref = bf16[64,1024]{1,0:T(8,128)(2,1)S(1)} collective-permute-done((bf16[64,1024]{1,0:T(8,128)(2,1)S(1)}, bf16[64,1024]{1,0:T(8,128)(2,1)S(1)}, u32[]{:S(2)}, u32[]{:S(2)}) %collective-permute-start.5) | collective-permute-done | bytes 131104 | tf_op jit(solution)/shard_map/ppermute | solution.py:30
  92.5 0.0 collective-permute-start.6
  92.5 0.1 collective-permute-start.7
  92.6 4.8 %collective-permute-done.6.one_ref = bf16[64,1024]{1,0:T(8,128)(2,1)S(1)} collective-permute-done((bf16[64,1024]{1,0:T(8,128)(2,1)S(1)}, bf16[64,1024]{1,0:T(8,128)(2,1)S(1)}, u32[]{:S(2)}, u32[]{:S(2)}) %collective-permute-start.6) | collective-permute-done | bytes 131104 | tf_op jit(solution)/shard_map/ppermute | solution.py:30
  97.5 0.0 collective-permute-start.8
  97.5 1.5 %collective-permute-done.7.two_ref = bf16[64,1024]{1,0:T(8,128)(2,1)S(1)} collective-permute-done((bf16[64,1024]{1,0:T(8,128)(2,1)S(1)}, bf16[64,1024]{1,0:T(8,128)(2,1)S(1)}, u32[]{:S(2)}, u32[]{:S(2)}) %collective-permute-start.7) | collective-permute-done | bytes 131104 | tf_op jit(solution)/shard_map/ppermute | solution.py:30
  99.0 4.7 %collective-permute-done.8.three_ref = bf16[64,1024]{1,0:T(8,128)(2,1)S(1)} collective-permute-done((bf16[64,1024]{1,0:T(8,128)(2,1)S(1)}, bf16[64,1024]{1,0:T(8,128)(2,1)S(1)}, u32[]{:S(2)}, u32[]{:S(2)}) %collective-permute-start.8) | collective-permute-done | bytes 131104 | tf_op jit(solution)/shard_map/ppermute | solution.py:30
  103.6 0.8 widen.3.w4
  104.5 0.0 collective-permute-done.1.far_ref
  104.5 5.5 %finish.1 = (f32[64,1024]{1,0:T(8,128)}, f32[64,1024]{1,0:T(8,128)}, bf16[1024,2048]{1,0:T(8,128)(2,1)}, f32[64,128]{1,0:T(8,128)}, f32[64,128]{1,0:T(8,128)}, /...) custom-call(s32[4]{0:T(128)S(1)} %pad_add_fusion.place_ref, ...), custom_call_target="tpu_custom_call" | custom-call | tf_op jit(solution)/shard_map/finish/pallas_call | solution.py:326
  110.1 0.0 collective-permute-done.13.f3
  110.1 0.0 collective-permute-done.14.b3
  110.1 1.9 %last.1 = bf16[1024,2048]{1,0:T(8,128)(2,1)} custom-call(s32[4]{0:T(128)S(1)} %pad_add_fusion.place_ref, bf16[2,256,256]{2,1,0:T(8,128)(2,1)S(1)} %get-tuple-element.20.rows_ref, f32[1,128]{1,0:T(1,128)S(1)} %get-tuple-element.21.scale_ref, bf16[1024,256]{1,0:T(8,128)(2,1)S(1)} %get-tuple-element.22.basis_ref, ...), custom_call_target="tpu_custom_call", output_to_operand_aliasing={{}: (6, {})} | custom-call | tf_op jit(solution)/shard_map/last/pallas_call | solution.py:372
  (8 shorter events, 0.0 us)
Async XLA Ops:
  0.6 5.9 %copy-start = (bf16[768,2048]{1,0:T(8,128)(2,1)S(1)}, bf16[768,2048]{1,0:T(8,128)(2,1)}, u32[]{:S(2)}) copy-start(bf16[768,2048]{1,0:T(8,128)(2,1)} %cot_ref.1) | copy-start | bytes 9437188
  4.9 17.7 %copy-start.1 = (f32[64,128]{1,0:T(8,128)S(1)}, f32[64,128]{1,0:T(8,128)}, u32[]{:S(2)}) copy-start(f32[64,128]{1,0:T(8,128)} %first_hbm.3) | copy-start | bytes 98308
  4.9 17.7 %copy-start.2 = (f32[64,128]{1,0:T(8,128)S(1)}, f32[64,128]{1,0:T(8,128)}, u32[]{:S(2)}) copy-start(f32[64,128]{1,0:T(8,128)} %second_hbm.3) | copy-start | bytes 98308
  5.0 1.5 %collective-permute-start = (bf16[768,128]{1,0:T(8,128)(2,1)S(1)}, bf16[768,128]{1,0:T(8,128)(2,1)S(1)}, u32[]{:S(2)}, u32[]{:S(2)}) collective-permute-start(bf16[768,128]{1,0:T(8,128)(2,1)S(1)} %get-tuple-element.17), channel_id=1, source_target_pairs={{0,1},{1,0},{2,3},{3,2},{4,5},{5,4},{6,7},{7,6},{8,9},{9,8},{10,11... | collective-permute-start | bytes 589832 | tf_op jit(solution)/shard_map/ppermute | solution.py:34
  24.1 23.6 %all-to-all-start.1 = ((bf16[8,10,16,128]{3,2,1,0:T(8,128)(2,1)}), bf16[8,10,16,128]{3,2,1,0:T(8,128)(2,1)S(1)}, u32[]{:S(2)}, u32[]{:S(2)}) async-start(bf16[8,10,16,128]{3,2,1,0:T(8,128)(2,1)} %fold.1), calls=%async_computation.1 | async-start | bytes 655360 | tf_op jit(solution)/shard_map/all_to_all | solution.py:385
  32.5 7.3 %collective-permute-start.2 = (bf16[64,1024]{1,0:T(8,128)(2,1)S(1)}, bf16[64,1024]{1,0:T(8,128)(2,1)S(1)}, u32[]{:S(2)}, u32[]{:S(2)}) collective-permute-start(bf16[64,1024]{1,0:T(8,128)(2,1)S(1)} %get-tuple-element.18.own_ref), channel_id=1, source_target_pairs={{0,8},{8,16},{16,24},{24,0},{1,9},{9,17},{17,25},{25,1},{2,10},{10... | collective-permute-start | bytes 393224 | tf_op jit(solution)/shard_map/ppermute | solution.py:30
  34.7 7.4 %collective-permute-start.3 = (bf16[64,1024]{1,0:T(8,128)(2,1)S(1)}, bf16[64,1024]{1,0:T(8,128)(2,1)S(1)}, u32[]{:S(2)}, u32[]{:S(2)}) collective-permute-start(bf16[64,1024]{1,0:T(8,128)(2,1)S(1)} %get-tuple-element.18.own_ref), channel_id=1, source_target_pairs={{0,16},{8,24},{16,0},{24,8},{1,17},{9,25},{17,1},{25,9},{2,18},{10... | collective-permute-start | bytes 393224 | tf_op jit(solution)/shard_map/ppermute | solution.py:30
  35.6 7.9 %collective-permute-start.4 = (bf16[64,1024]{1,0:T(8,128)(2,1)S(1)}, bf16[64,1024]{1,0:T(8,128)(2,1)S(1)}, u32[]{:S(2)}, u32[]{:S(2)}) collective-permute-start(bf16[64,1024]{1,0:T(8,128)(2,1)S(1)} %get-tuple-element.18.own_ref), channel_id=1, source_target_pairs={{0,24},{8,0},{16,8},{24,16},{1,25},{9,1},{17,9},{25,17},{2,26},{10... | collective-permute-start | bytes 393224 | tf_op jit(solution)/shard_map/ppermute | solution.py:30
  44.3 14.5 %collective-permute-start.10 = (bf16[1024,256]{1,0:T(8,128)(2,1)S(1)}, bf16[1024,256]{1,0:T(8,128)(2,1)S(1)}, u32[]{:S(2)}, u32[]{:S(2)}) collective-permute-start(bf16[1024,256]{1,0:T(8,128)(2,1)S(1)} %widen.2.w0), channel_id=1, source_target_pairs={{0,32},{32,64},{64,96},{96,128},{128,160},{160,192},{192,224},{224... | collective-permute-start | bytes 1572872 | tf_op jit(solution)/shard_map/ppermute | solution.py:30
  46.1 12.9 %collective-permute-start.9 = (bf16[1024,256]{1,0:T(8,128)(2,1)S(1)}, bf16[1024,256]{1,0:T(8,128)(2,1)S(1)}, u32[]{:S(2)}, u32[]{:S(2)}) collective-permute-start(bf16[1024,256]{1,0:T(8,128)(2,1)S(1)} %widen.2.w0), channel_id=1, source_target_pairs={{0,224},{32,0},{64,32},{96,64},{128,96},{160,128},{192,160},{224,1... | collective-permute-start | bytes 1572872 | tf_op jit(solution)/shard_map/ppermute | solution.py:30
  49.2 13.9 %all-to-all-start.2 = ((bf16[16,9,16,128]{3,2,1,0:T(8,128)(2,1)}), bf16[16,9,16,128]{3,2,1,0:T(8,128)(2,1)S(1)}, u32[]{:S(2)}, u32[]{:S(2)}) async-start(bf16[16,9,16,128]{3,2,1,0:T(8,128)(2,1)} %update.1), calls=%async_computation.2 | async-start | bytes 1179648 | tf_op jit(solution)/shard_map/all_to_all | solution.py:385
  58.8 45.7 %copy-start.3 = (bf16[1024,256]{1,0:T(8,128)(2,1)}, bf16[1024,256]{1,0:T(8,128)(2,1)S(1)}, u32[]{:S(2)}) copy-start(bf16[1024,256]{1,0:T(8,128)(2,1)S(1)} %collective-permute-done.10.f1_hbm) | copy-start | bytes 1572868
  58.8 13.5 %collective-permute-start.11 = (bf16[1024,256]{1,0:T(8,128)(2,1)S(1)}, bf16[1024,256]{1,0:T(8,128)(2,1)S(1)}, u32[]{:S(2)}, u32[]{:S(2)}) collective-permute-start(bf16[1024,256]{1,0:T(8,128)(2,1)S(1)} %collective-permute-done.10.f1_hbm), channel_id=1, source_target_pairs={{0,32},{32,64},{64,96},{96,128},{128,160},{160,192},{192,224},{224... | collective-permute-start | bytes 1572872 | tf_op jit(solution)/shard_map/ppermute | solution.py:30
  59.0 13.3 %collective-permute-start.12 = (bf16[1024,256]{1,0:T(8,128)(2,1)S(1)}, bf16[1024,256]{1,0:T(8,128)(2,1)S(1)}, u32[]{:S(2)}, u32[]{:S(2)}) collective-permute-start(bf16[1024,256]{1,0:T(8,128)(2,1)S(1)} %collective-permute-done.9.b1), channel_id=1, source_target_pairs={{0,224},{32,0},{64,32},{96,64},{128,96},{160,128},{192,160},{224,1... | collective-permute-start | bytes 1572872 | tf_op jit(solution)/shard_map/ppermute | solution.py:30
  63.1 41.3 %collective-permute-start.1 = (bf16[16,9,16,128]{3,2,1,0:T(8,128)(2,1)S(1)}, bf16[16,9,16,128]{3,2,1,0:T(8,128)(2,1)S(1)}, u32[]{:S(2)}, u32[]{:S(2)}) collective-permute-start(bf16[16,9,16,128]{3,2,1,0:T(8,128)(2,1)S(1)} %all-to-all-done.2.near_ref), channel_id=1, source_target_pairs={{0,1},{1,0},{2,3},{3,2},{4,5},{5,4},{6,7},{7,6},{8,9},{9,8},{10,11... | collective-permute-start | bytes 1769480 | tf_op jit(solution)/shard_map/ppermute | solution.py:34
  72.3 32.1 %copy-start.4 = (bf16[1024,256]{1,0:T(8,128)(2,1)}, bf16[1024,256]{1,0:T(8,128)(2,1)S(1)}, u32[]{:S(2)}) copy-start(bf16[1024,256]{1,0:T(8,128)(2,1)S(1)} %collective-permute-done.11.f2_hbm) | copy-start | bytes 1572868
  72.3 37.7 %collective-permute-start.13 = (bf16[1024,256]{1,0:T(8,128)(2,1)S(1)}, bf16[1024,256]{1,0:T(8,128)(2,1)S(1)}, u32[]{:S(2)}, u32[]{:S(2)}) collective-permute-start(bf16[1024,256]{1,0:T(8,128)(2,1)S(1)} %collective-permute-done.11.f2_hbm), channel_id=1, source_target_pairs={{0,32},{32,64},{64,96},{96,128},{128,160},{160,192},{192,224},{224... | collective-permute-start | bytes 1572872 | tf_op jit(solution)/shard_map/ppermute | solution.py:30
  72.3 32.1 %copy-start.5 = (bf16[1024,256]{1,0:T(8,128)(2,1)}, bf16[1024,256]{1,0:T(8,128)(2,1)S(1)}, u32[]{:S(2)}) copy-start(bf16[1024,256]{1,0:T(8,128)(2,1)S(1)} %collective-permute-done.12.b2_hbm) | copy-start | bytes 1572868
  72.4 37.7 %collective-permute-start.14 = (bf16[1024,256]{1,0:T(8,128)(2,1)S(1)}, bf16[1024,256]{1,0:T(8,128)(2,1)S(1)}, u32[]{:S(2)}, u32[]{:S(2)}) collective-permute-start(bf16[1024,256]{1,0:T(8,128)(2,1)S(1)} %collective-permute-done.12.b2_hbm), channel_id=1, source_target_pairs={{0,224},{32,0},{64,32},{96,64},{128,96},{160,128},{192,160},{224,1... | collective-permute-start | bytes 1572872 | tf_op jit(solution)/shard_map/ppermute | solution.py:30
  75.6 16.9 %collective-permute-start.5 = (bf16[64,1024]{1,0:T(8,128)(2,1)S(1)}, bf16[64,1024]{1,0:T(8,128)(2,1)S(1)}, u32[]{:S(2)}, u32[]{:S(2)}) collective-permute-start(bf16[64,1024]{1,0:T(8,128)(2,1)S(1)} %get-tuple-element.18.own_ref), channel_id=1, source_target_pairs={{0,128},{32,160},{64,192},{96,224},{128,0},{160,32},{192,64},{224,... | collective-permute-start | bytes 393224 | tf_op jit(solution)/shard_map/ppermute | solution.py:30
  92.5 5.0 %collective-permute-start.6 = (bf16[64,1024]{1,0:T(8,128)(2,1)S(1)}, bf16[64,1024]{1,0:T(8,128)(2,1)S(1)}, u32[]{:S(2)}, u32[]{:S(2)}) collective-permute-start(bf16[64,1024]{1,0:T(8,128)(2,1)S(1)} %collective-permute-done.5.own_ref), channel_id=1, source_target_pairs={{0,8},{8,16},{16,24},{24,0},{1,9},{9,17},{17,25},{25,1},{2,10},{10... | collective-permute-start | bytes 393224 | tf_op jit(solution)/shard_map/ppermute | solution.py:30
  92.5 6.5 %collective-permute-start.7 = (bf16[64,1024]{1,0:T(8,128)(2,1)S(1)}, bf16[64,1024]{1,0:T(8,128)(2,1)S(1)}, u32[]{:S(2)}, u32[]{:S(2)}) collective-permute-start(bf16[64,1024]{1,0:T(8,128)(2,1)S(1)} %collective-permute-done.5.own_ref), channel_id=1, source_target_pairs={{0,16},{8,24},{16,0},{24,8},{1,17},{9,25},{17,1},{25,9},{2,18},{10... | collective-permute-start | bytes 393224 | tf_op jit(solution)/shard_map/ppermute | solution.py:30
  97.5 6.2 %collective-permute-start.8 = (bf16[64,1024]{1,0:T(8,128)(2,1)S(1)}, bf16[64,1024]{1,0:T(8,128)(2,1)S(1)}, u32[]{:S(2)}, u32[]{:S(2)}) collective-permute-start(bf16[64,1024]{1,0:T(8,128)(2,1)S(1)} %collective-permute-done.5.own_ref), channel_id=1, source_target_pairs={{0,24},{8,0},{16,8},{24,16},{1,25},{9,1},{17,9},{25,17},{2,26},{10... | collective-permute-start | bytes 393224 | tf_op jit(solution)/shard_map/ppermute | solution.py:30
